TPU v7x, 512 devices: a whole 4x8x8 slice. The times are simulated.
512 devices in a mesh: sp: 32 (over z, x), tp: 16 (over y, core).
Axes of the slice: x: 4, y: 8, z: 8, core: 2. Of those that a mesh axis runs over, the one named last changes fastest.
Arguments:
- queries: bfloat16 [8192, 1024], P('sp', 'tp'), may hold values from -64 to 64
- keys: bfloat16 [8192, 1024], P('sp', 'tp'), may hold values from -64 to 64
- values: bfloat16 [8192, 1024], P('sp', 'tp'), may hold values from -6 to 6
- cum_gate: float32 [16, 8192], P('tp'), may hold values from -8192 to 0, as said below
- out_weight: bfloat16 [1024, 2048], P('tp'), may hold values from -0.375 to 0.375
- resid: bfloat16 [8192, 2048], P('sp'), may hold values from -6 to 6
- norm_gain: float32 [2048], replicated, may hold values from 0.1 to 1.9
- routes: int32 [8192, 2], P('sp'), may hold values from 0 to 31, all different within a row; in each aligned block of 256 rows (0 to 255, 256 to 511, ...) at most 20 rows name the same one
- route_weight: float32 [8192, 2], P('sp'), may hold values from 0.1 to 0.9
- gate_weight: bfloat16 [32, 2048, 4096], P('sp', None, 'tp'), may hold values from -0.125 to 0.125
- up_weight: bfloat16 [32, 2048, 4096], P('sp', None, 'tp'), may hold values from -0.125 to 0.125
- down_weight: bfloat16 [32, 4096, 2048], P('sp', 'tp'), may hold values from -0.09375 to 0.09375
Outputs:
- layer_out: bfloat16 [8192, 2048], P('sp', 'tp')
Inputs may be any that keep to these rules, and one draw needn't show every extreme that they name: `routes`: each token names 2 different experts. Among the rows of one index of sp, no expert is named more than 20 times, a bound that some block reaches. `cum_gate`: each head's row does not rise along the positions.
All inputs are finite; a program needn't handle non-finite values.
Results may differ from a plain program's by a relative error of at most 0.015.
Values may be sent and summed in bfloat16 or wider, within the bound.
No kernel may reach another device: no remote copies, remote signals or barrier semaphores. Data moves between devices by JAX's collectives and lax.ppermute only.
A program may use at most 64 MiB of HBM per device.

v0:
```python
import math

import jax
import jax.numpy as jnp
from jax import lax
from jax.sharding import PartitionSpec as P

HD = 64


epsilon = 1e-06


def in_one_piece(arrays, axis, dim, along):
    ends, at = ([], 0)
    for a in arrays[:-1]:
        at += a.shape[along]
        ends.append(at)
    both = jnp.concatenate(arrays, axis=along)
    return tuple(jnp.split(lax.all_gather(both, axis, axis=dim, tiled=True), ends, axis=along))


def in_blocks(x, dim, length):
    before, after = (x.shape[:dim], x.shape[dim + 1 :])
    return jnp.moveaxis(x.reshape(*before, length, -1, *after), dim, 0)


def sum_at_owner(x, axis, dim):
    tiles = in_blocks(x, dim, lax.axis_size(axis))
    arrived = lax.all_to_all(tiles, axis, split_axis=0, concat_axis=0, tiled=True)
    return arrived.astype(jnp.float32).sum(axis=0)


def from_everyone(x, axis):
    length = lax.axis_size(axis)
    return lax.all_to_all(jnp.broadcast_to(x[None], (length, *x.shape)), axis, 0, 0, tiled=True)


def of_everyone(x, axis):
    everything = from_everyone(x, axis)
    return jnp.sum(everything, axis=0)


def attend_block(
    carried, query_heads, cum_query, key_rows, value_rows, cum_keys, query_first, key_first
):
    best_score, weight_sum, value_sum = carried
    score_scale = query_heads.shape[-1] ** (-0.5)
    scores = (
        jnp.einsum("hqd,hkd->hqk", query_heads, key_rows, preferred_element_type=jnp.float32)
        * score_scale
    )
    scores = scores + cum_query[:, :, None] - cum_keys[:, None, :]
    query_pos = query_first + jnp.arange(query_heads.shape[1], dtype=jnp.int32)
    key_pos = key_first + jnp.arange(key_rows.shape[1], dtype=jnp.int32)
    permitted_mask = (key_pos[None, :] <= query_pos[:, None])[None]
    new_best = jnp.maximum(
        best_score, jnp.max(jnp.where(permitted_mask, scores, -jnp.inf), axis=-1)
    )
    weights = jnp.where(permitted_mask, jnp.exp(scores - new_best[..., None]), 0.0)
    shrink = jnp.exp(best_score - new_best)
    weight_sum = weight_sum * shrink + jnp.sum(weights, axis=-1)
    value_sum = value_sum * shrink[..., None] + jnp.einsum(
        "hqk,hkd->hqd", weights.astype(jnp.bfloat16), value_rows, preferred_element_type=jnp.float32
    )
    return (new_best, weight_sum, value_sum)


def local(
    queries,
    keys,
    values,
    cum_gate,
    out_weight,
    resid,
    norm_gain,
    routes,
    route_weight,
    gate_weight,
    up_weight,
    down_weight,
):
    rows_here = queries.shape[0]
    heads_here = queries.shape[1] // HD
    sp_count = lax.axis_size("sp")
    tp_count = lax.axis_size("tp")
    shift_amount = lax.axis_index("sp") * rows_here
    model_width = resid.shape[1]
    columns = model_width // tp_count
    column_first = lax.axis_index("tp") * columns
    query_heads = queries.reshape(rows_here, heads_here, HD).transpose(1, 0, 2)
    cum_query = lax.dynamic_slice_in_dim(cum_gate, shift_amount, rows_here, 1)
    start_state = (
        jnp.full((heads_here, rows_here), -1e30, jnp.float32),
        jnp.zeros((heads_here, rows_here), jnp.float32),
        jnp.zeros((heads_here, rows_here, HD), jnp.float32),
    )
    key_part, value_part = in_one_piece((keys, values), "sp", 0, 1)
    piece_rows = key_part.shape[0]
    key_block = math.gcd(piece_rows, 1024)

    def attend_piece(running):

        def key_step(block_index, inner_state):
            block_first = block_index * key_block
            key_rows = lax.dynamic_slice_in_dim(key_part, block_first, key_block, 0)
            key_rows = key_rows.reshape(key_block, heads_here, HD).transpose(1, 0, 2)
            value_rows = lax.dynamic_slice_in_dim(value_part, block_first, key_block, 0)
            value_rows = value_rows.reshape(key_block, heads_here, HD).transpose(1, 0, 2)
            cum_keys = lax.dynamic_slice_in_dim(cum_gate, block_first, key_block, 1)
            return attend_block(
                inner_state,
                query_heads,
                cum_query,
                key_rows,
                value_rows,
                cum_keys,
                shift_amount,
                block_first,
            )

        return lax.fori_loop(0, piece_rows // key_block, key_step, running)

    best_score, weight_sum, value_sum = lax.cond(
        jnp.int32(0) <= shift_amount + rows_here - 1,
        attend_piece,
        lambda running: running,
        start_state,
    )
    attended = (value_sum / weight_sum[..., None]).astype(jnp.bfloat16)
    attended = attended.transpose(1, 0, 2).reshape(rows_here, heads_here * HD)
    partial_value = jnp.dot(attended, out_weight, preferred_element_type=jnp.float32)
    mixed_sum = sum_at_owner(partial_value.astype(jnp.bfloat16), "tp", 1)
    stream_cols = (
        lax.dynamic_slice_in_dim(resid, column_first, columns, 1).astype(jnp.float32) + mixed_sum
    )
    square_sum = of_everyone(jnp.sum(stream_cols * stream_cols, axis=1, keepdims=True), "tp")
    gain_cols = lax.dynamic_slice_in_dim(norm_gain, column_first, columns, 0)
    normed = (stream_cols * lax.rsqrt(square_sum / model_width + epsilon) * gain_cols).astype(
        jnp.bfloat16
    )
    capacity = 5 * rows_here // (2 * sp_count)
    chosen = routes.reshape(-1)
    onehot = (chosen[:, None] == jnp.arange(sp_count, dtype=jnp.int32)[None, :]).astype(jnp.int32)
    before = jnp.cumsum(onehot, axis=0) - onehot
    rank_within = jnp.sum(before * onehot, axis=1)
    slot_index = chosen * capacity + rank_within
    source_row = (
        jnp.zeros((sp_count * capacity,), jnp.int32)
        .at[slot_index]
        .set(jnp.arange(chosen.shape[0], dtype=jnp.int32) // routes.shape[1])
    )
    filled = jnp.zeros((sp_count * capacity,), jnp.bool_).at[slot_index].set(True)
    outgoing = jnp.where(filled[:, None], normed[source_row], jnp.zeros((), jnp.bfloat16))
    outgoing = outgoing.reshape(sp_count, capacity, normed.shape[1])
    gate_here = gate_weight[0]
    up_here = up_weight[0]
    local_down_weight = down_weight[0]
    arrived = lax.all_to_all(outgoing, "sp", split_axis=0, concat_axis=0, tiled=True)
    arrived_rows = arrived.reshape(-1, columns)
    col_part = lax.all_gather(arrived_rows, "tp", axis=1, tiled=True)
    gate_sum = jnp.dot(col_part, gate_here, preferred_element_type=jnp.float32)
    up_sum = jnp.dot(col_part, up_here, preferred_element_type=jnp.float32)
    slot_shape = arrived.shape
    hidden = (jax.nn.silu(gate_sum) * up_sum).astype(jnp.bfloat16)
    partial_term = jnp.dot(hidden, local_down_weight, preferred_element_type=jnp.float32)
    expert_rows = sum_at_owner(partial_term.astype(jnp.bfloat16), "tp", 1).astype(jnp.bfloat16)
    returned = expert_rows.reshape(slot_shape[0], slot_shape[1], columns)
    returned_back = lax.all_to_all(returned, "sp", split_axis=0, concat_axis=0, tiled=True)
    returned_flat = returned_back.reshape(sp_count * capacity, columns)
    picked = (
        returned_flat[slot_index].reshape(rows_here, routes.shape[1], columns).astype(jnp.float32)
    )
    combined = jnp.sum(picked * route_weight[..., None], axis=1)
    return (stream_cols + combined).astype(jnp.bfloat16)


def solution(mesh):
    return jax.shard_map(
        local,
        mesh=mesh,
        in_specs=(
            P("sp", "tp"),
            P("sp", "tp"),
            P("sp", "tp"),
            P("tp", None),
            P("tp", None),
            P("sp", None),
            P(),
            P("sp", None),
            P("sp", None),
            P("sp", None, "tp"),
            P("sp", None, "tp"),
            P("sp", "tp", None),
        ),
        out_specs=P("sp", "tp"),
        check_vma=False,
    )
```

profile of v0, /device:TPU:1, one launch (start us, length us, event | category | flops | bytes accessed | tf_op | source)
XLA Modules:
  0.0 370.8 jit_solution(9054272636798588638)
XLA Ops:
  9.1 86.0 %all-gather.3.cloned.1.call-done = bf16[8192,128]{1,0:T(8,128)(2,1)} async-done(((bf16[256,128]{1,0:T(8,128)(2,1)}), bf16[8192,128]{1,0:T(8,128)(2,1)}) %all-gather.3.cloned.1.call-update) | async-done | bytes 2097168 | tf_op jit(solution)/shard_map/all_gather | solution.py:20
  95.1 49.2 %conditional.1 = (f32[1,256]{1,0:T(1,128)}, f32[1,256,64]{1,2,0:T(8,128)}) conditional(s32[]{:T(128)} %convert_element_type.51, () %tuple.31, (bf16[8192,128]{1,0:T(8,128)(2,1)}, bf16[256,64]{0,1:T(8,128)(2,1)}, s32[]{:T(128)}, f32[1,8192]{1,0:T(1,128)}) %tuple.32), branch_computations={%region_0.0_spmd, %region_1.6_spmd} | conditional | flops 70830592 | bytes 8277405 | solution.py:124
  95.9 5.0 %fusion.45 = (bf16[8192,64]{1,0:T(8,128)(2,1)}, bf16[8192,64]{1,0:T(8,128)(2,1)}) fusion(bf16[8192,128]{1,0:T(8,128)(2,1)} %get-tuple-element.217), kind=kLoop, calls=%fused_computation.87 | loop fusion | bytes 4194304 | tf_op jit(solution)/shard_map/split | solution.py:20
  101.0 43.3 %while.20 = (s32[]{:T(128)}, f32[1,256]{1,0:T(1,128)S(1)}, f32[1,256]{1,0:T(1,128)}, f32[1,256,64]{1,2,0:T(8,128)}, s32[]{:T(128)}, /*index=5*/bf16[8192,64]{1,0...) while((s32[]{:T(128)}, f32[1,256]{1,0:T(1,128)S(1)}, ...), condition=%wide.region_5.5_spmd.clone, body=%wide.region_2.4_spmd.clone.sunk | while | flops 70830592 | bytes 3884243 | solution.py:122
  103.9 2.0 fusion.62
  109.3 2.0 fusion.62
  112.1 1.4 fusion.58
  114.8 2.0 fusion.62
  117.6 1.4 fusion.58
  120.3 2.0 fusion.62
  125.8 2.0 fusion.62
  131.3 2.0 fusion.62
  134.0 1.4 fusion.58
  136.8 2.0 fusion.62
  142.2 2.0 fusion.62
  146.8 12.3 %all-to-all-start = ((bf16[16,256,128]{2,1,0:T(8,128)(2,1)}), bf16[16,256,128]{2,1,0:T(8,128)(2,1)S(1)}, u32[]{:S(2)}, u32[]{:S(2)}) async-start(bf16[16,256,128]{2,1,0:T(8,128)(2,1)} %bitcast.74), calls=%async_computation | async-start | bytes 2097152 | tf_op jit(solution)/shard_map/all_to_all | solution.py:30
  161.5 2.4 scatter_custom_fusion.1
  164.0 23.2 %all-to-all-done = bf16[16,256,128]{2,1,0:T(8,128)(2,1)S(1)} async-done(((bf16[16,256,128]{2,1,0:T(8,128)(2,1)}), bf16[16,256,128]{2,1,0:T(8,128)(2,1)S(1)}, u32[]{:S(2)}, u32[]{:S(2)}) %all-to-all-start) | async-done | bytes 1048608 | tf_op jit(solution)/shard_map/all_to_all | solution.py:30
  188.9 3.4 all-to-all-start.1
  193.2 2.4 scatter_custom_fusion
  195.7 3.9 %all-to-all-done.1 = f32[16,256,1]{1,2,0:T(1,128)S(1)} async-done(((f32[16,256,1]{1,2,0:T(1,128)}), f32[16,256,1]{1,2,0:T(1,128)S(1)}, u32[]{:S(2)}, u32[]{:S(2)}) %all-to-all-start.1) | async-done | bytes 16416 | tf_op jit(solution)/shard_map/all_to_all | solution.py:36
  200.7 2.0 gather_fusion
  202.9 15.5 %all_to_all.25 = bf16[32,20,128]{2,1,0:T(8,128)(2,1)S(1)} all-to-all(bf16[32,20,128]{2,1,0:T(8,128)(2,1)S(1)} %broadcast_select_fusion.2), channel_id=1, replica_groups=mesh['sp'=32,'tp'=16] {'sp'}, dimensions={0} | all-to-all | bytes 327680 | tf_op jit(solution)/shard_map/all_to_all | solution.py:159
  219.1 38.1 %all-gather.5.cloned.1.call-done = bf16[640,2048]{1,0:T(8,128)(2,1)} async-done(((bf16[640,128]{1,0:T(8,128)(2,1)}), bf16[640,2048]{1,0:T(8,128)(2,1)}) %all-gather.5.cloned.1.call-update) | async-done | bytes 2621456 | tf_op jit(solution)/shard_map/all_gather | solution.py:161
  257.2 3.4 fusion.26
  260.7 6.2 %fusion.21 = bf16[80,16,8,128]{3,2,1,0:T(8,128)(2,1)} fusion(bf16[1,256,2048]{2,1,0:T(8,128)(2,1)S(1)} %copy-done, bf16[640,2048]{1,0:T(8,128)(2,1)} %all-gather.5.cloned.1.call-done, bf16[1,2048,256]{2,1,0:T(8,128)(2,1)S(1)} %copy-done.6, f32[640,256]{1,0:T(8,128)} %fusion.26), kind=kOutput, calls=%fused_computation.40 | convolution fusion | flops 1344471040 | bytes 7995392 | tf_op jit(solution)/shard_map/dot_general | solution.py:166
  266.9 2.4 copy.43
  269.3 67.0 %all_to_all.26 = bf16[16,640,128]{2,1,0:T(8,128)(2,1)} all-to-all(bf16[16,640,128]{2,1,0:T(8,128)(2,1)S(1)} %bitcast.91), channel_id=1, replica_groups=mesh['sp'=32,'tp'=16] {'tp'}, dimensions={0} | all-to-all | bytes 5242880 | tf_op jit(solution)/shard_map/all_to_all | solution.py:30
  336.3 2.1 reduce_sum.77
  339.2 9.9 %all-to-all-start.4 = ((bf16[32,20,128]{2,1,0:T(8,128)(2,1)}), bf16[32,20,128]{2,1,0:T(8,128)(2,1)S(1)}, u32[]{:S(2)}, u32[]{:S(2)}) async-start(bf16[32,20,128]{2,1,0:T(8,128)(2,1)} %reshape.156), calls=%async_computation.4 | async-start | bytes 393216 | tf_op jit(solution)/shard_map/all_to_all | solution.py:169
  349.3 11.5 %all-to-all-done.4 = bf16[32,20,128]{2,1,0:T(8,128)(2,1)S(1)} async-done(((bf16[32,20,128]{2,1,0:T(8,128)(2,1)}), bf16[32,20,128]{2,1,0:T(8,128)(2,1)S(1)}, u32[]{:S(2)}, u32[]{:S(2)}) %all-to-all-start.4) | async-done | bytes 163872 | tf_op jit(solution)/shard_map/all_to_all | solution.py:169
  362.5 1.5 add_convert_fusion
  (123 shorter events, 38.4 us)
Async XLA Ops:
  6.5 254.1 %copy-start = (bf16[1,256,2048]{2,1,0:T(8,128)(2,1)S(1)}, bf16[1,256,2048]{2,1,0:T(8,128)(2,1)}, u32[]{:S(2)}) copy-start(bf16[1,256,2048]{2,1,0:T(8,128)(2,1)} %param.27) | copy-start | bytes 3145732
  6.5 88.6 %all-gather.3.cloned.1.call-start = ((), (), s32[]{:S(2)}) async-start(), calls=%async_computation.5 | async-start | bytes 2162688 | tf_op jit(solution)/shard_map/all_gather | solution.py:20
  95.1 49.2 %copy-start.1 = (bf16[64,2048]{1,0:T(8,128)(2,1)S(1)}, bf16[64,2048]{1,0:T(8,128)(2,1)}, u32[]{:S(2)}) copy-start(bf16[64,2048]{1,0:T(8,128)(2,1)} %param.20) | copy-start | bytes 786436
  95.9 5.0 %copy-start.2 = (bf16[256,64]{0,1:T(8,128)(2,1)S(1)}, bf16[256,64]{0,1:T(8,128)(2,1)}, u32[]{:S(2)}) copy-start(bf16[256,64]{0,1:T(8,128)(2,1)} %get-tuple-element.272) | copy-start | bytes 98308 | tf_op jit(solution)/shard_map/cond
  144.3 14.9 %copy-start.3 = (s32[256,2]{0,1:T(2,128)S(1)}, s32[256,2]{0,1:T(2,128)}, u32[]{:S(2)}) copy-start(s32[256,2]{0,1:T(2,128)} %param.23) | copy-start | bytes 6148
  146.8 40.3 %all-to-all-start = ((bf16[16,256,128]{2,1,0:T(8,128)(2,1)}), bf16[16,256,128]{2,1,0:T(8,128)(2,1)S(1)}, u32[]{:S(2)}, u32[]{:S(2)}) async-start(bf16[16,256,128]{2,1,0:T(8,128)(2,1)} %bitcast.74), calls=%async_computation | async-start | bytes 2097152 | tf_op jit(solution)/shard_map/all_to_all | solution.py:30
  161.1 96.1 %copy-start.5 = (bf16[1,2048,256]{2,1,0:T(8,128)(2,1)S(1)}, bf16[1,2048,256]{2,1,0:T(8,128)(2,1)}, u32[]{:S(2)}) copy-start(bf16[1,2048,256]{2,1,0:T(8,128)(2,1)} %param.25) | copy-start | bytes 3145732
  188.9 10.8 %all-to-all-start.1 = ((f32[16,256,1]{1,2,0:T(1,128)}), f32[16,256,1]{1,2,0:T(1,128)S(1)}, u32[]{:S(2)}, u32[]{:S(2)}) async-start(f32[16,256,1]{1,2,0:T(1,128)} %broadcast_in_dim.90), calls=%async_computation.1 | async-start | bytes 32768 | tf_op jit(solution)/shard_map/all_to_all | solution.py:36
  192.3 64.9 %all-gather.5.cloned.1.call-start = ((), (), s32[]{:S(2)}) async-start(), calls=%async_computation.6 | async-start | bytes 2785280 | tf_op jit(solution)/shard_map/all_gather | solution.py:161
  219.1 41.5 %copy-start.6 = (bf16[1,2048,256]{2,1,0:T(8,128)(2,1)S(1)}, bf16[1,2048,256]{2,1,0:T(8,128)(2,1)}, u32[]{:S(2)}) copy-start(bf16[1,2048,256]{2,1,0:T(8,128)(2,1)} %param.26) | copy-start | bytes 3145732
  336.3 12.8 %copy-start.4 = (f32[256,2]{0,1:T(2,128)S(1)}, f32[256,2]{0,1:T(2,128)}, u32[]{:S(2)}) copy-start(f32[256,2]{0,1:T(2,128)} %param.24) | copy-start | bytes 6148
  339.2 21.5 %all-to-all-start.4 = ((bf16[32,20,128]{2,1,0:T(8,128)(2,1)}), bf16[32,20,128]{2,1,0:T(8,128)(2,1)S(1)}, u32[]{:S(2)}, u32[]{:S(2)}) async-start(bf16[32,20,128]{2,1,0:T(8,128)(2,1)} %reshape.156), calls=%async_computation.4 | async-start | bytes 393216 | tf_op jit(solution)/shard_map/all_to_all | solution.py:169
Sparse Core Ops, SparseCore 0:
  10.5 84.5 all-gather.2
  219.2 37.9 all-gather.4
where the time goes:
time: 372 us; the launch traced here: 371 us
  waiting for transfers between devices  163 us (44%)
  blocking collectives  82.6 us (22%)
  matrix products  38 us (10%)
  local copies, waits for them, and re-layouts  29.2 us (8%)
  starting transfers between devices  25.7 us (7%)
  other arithmetic  19 us (5%)
  between operations  13.6 us (4%)
    all_gather x1, waiting for transfers between devices, in_one_piece(): lax.all_gather(both, axis, axis=dim, tiled=True)  86 us
    all_to_all x1, blocking collectives, sum_at_owner(): lax.all_to_all(tiles, axis, split_axis=0, concat_axis=0, tiled=True)  67 us
    all_gather x1, waiting for transfers between devices, local(): col_part = lax.all_gather(arrived_rows, 'tp', axis=1, tiled=True)  38.1 us
    all_to_all x1, waiting for transfers between devices, sum_at_owner(): lax.all_to_all(tiles, axis, split_axis=0, concat_axis=0, tiled=True)  23.2 us
    dot_general x8, matrix products, attend_block(): jnp.einsum('hqk,hkd->hqd', weights.astype(jnp.bfloat16), value_rows, pref...  16.2 us
    all_to_all x1, blocking collectives, local(): lax.all_to_all(outgoing, 'sp', split_axis=0, concat_axis=0, tiled=True)  15.5 us
    all_to_all x1, starting transfers between devices, sum_at_owner(): lax.all_to_all(tiles, axis, split_axis=0, concat_axis=0, tiled=True)  12.3 us
    all_to_all x1, waiting for transfers between devices, local(): lax.all_to_all(returned, 'sp', split_axis=0, concat_axis=0, tiled=True)  11.5 us
  transfers between devices with their start and end apart: 5, of which 5 were waited for; matrix products, arithmetic and copies ran while one was open for 2% of the time, Pallas kernels for 0%

commit v1 on v0

v1 whole, which is shorter than its diff:
```python
import jax
import jax.numpy as jnp
from jax import lax
from jax.experimental import pallas as pl
from jax.experimental.pallas import tpu as pltpu
from jax.sharding import Mesh, PartitionSpec as P

NZ, NX, NY, NC = 8, 4, 8, 2
NSP, NTP = NZ * NX, NY * NC
SP, TP = ("z", "x"), ("y", "c")
HD = 64
TOK = 256
D = 2048
COLS = D // NTP
KEYS = NX * TOK
CAP = 20
SLOT = 24
ROWS = NSP * CAP
PADROWS = NSP * SLOT
META = 16
FFL = 256
EPS = 1e-06
LOW = -1e30
bf = jnp.bfloat16
f32 = jnp.float32

INTERPRET = False


def call(body, out_shape, inputs, smem=0, scratch=()):
    specs = [pl.BlockSpec(memory_space=pltpu.SMEM)] * smem
    specs += [pl.BlockSpec(memory_space=pltpu.VMEM)] * (len(inputs) - smem)
    many = isinstance(out_shape, (tuple, list))
    vm = pl.BlockSpec(memory_space=pltpu.VMEM)
    return pl.pallas_call(
        body,
        out_shape=out_shape,
        in_specs=specs,
        out_specs=tuple([vm] * len(out_shape)) if many else vm,
        scratch_shapes=list(scratch),
        interpret=INTERPRET,
        compiler_params=pltpu.CompilerParams(vmem_limit_bytes=48 * 1024 * 1024),
    )(*inputs)


def three(v):
    hi = v.astype(bf).astype(f32)
    rest = v - hi
    mid = rest.astype(bf).astype(f32)
    return hi, mid, rest - mid


def attend(at_ref, q_ref, kv_ref, gate_ref, out_ref, keys_ref, vals_ref):
    z, x = at_ref[0], at_ref[1]
    first = gate_ref[0:1, 0:1]
    row64 = lax.broadcasted_iota(jnp.int32, (HD, TOK), 0)
    for j in range(NX):
        bias = first - gate_ref[j : j + 1, :]
        hi, mid, lo = three(bias)
        extra = jnp.where(row64 == 0, hi, jnp.where(row64 == 1, mid, jnp.where(row64 == 2, lo, 0.0)))
        both = jnp.concatenate([kv_ref[j, 0:HD, :], extra.astype(bf)], axis=0)
        keys_ref[j * TOK : (j + 1) * TOK, :] = both.T
        vals_ref[0:HD, j * TOK : (j + 1) * TOK] = kv_ref[j, HD : 2 * HD, :]
        vals_ref[HD : HD + 16, j * TOK : (j + 1) * TOK] = jnp.ones((16, TOK), bf)
    ones = jnp.where(row64 < 3, 1.0, 0.0).astype(bf)
    row16 = lax.broadcasted_iota(jnp.int32, (16, TOK), 0)

    def part(zq, masked):
        q = jnp.concatenate([q_ref[zq] * bf(HD**-0.5), ones], axis=0)
        s = jnp.dot(keys_ref[...], q, preferred_element_type=f32)
        if masked:
            ki = lax.broadcasted_iota(jnp.int32, (KEYS, TOK), 0)
            qi = lax.broadcasted_iota(jnp.int32, (KEYS, TOK), 1) + x * TOK
            s = jnp.where(ki <= qi, s, LOW)
        m = jnp.max(s, axis=0, keepdims=True)
        p = jnp.exp(s - m).astype(bf)
        o = jnp.dot(vals_ref[...], p, preferred_element_type=f32)
        total = o[HD : HD + 1, :]
        hi, mid, lo = three(m + jnp.log(total))
        stats = jnp.where(row16 == 0, hi, jnp.where(row16 == 1, mid, jnp.where(row16 == 2, lo, 0.0)))
        out_ref[zq, 0:HD, :] = (o[0:HD, :] / total).astype(bf)
        out_ref[zq, HD : HD + 16, :] = stats.astype(bf)

    part(z, True)

    def later(zq, carry):
        part(zq, False)
        return carry

    lax.fori_loop(z + 1, NZ, later, 0)

    def earlier(zq, carry):
        out_ref[zq, 0:HD, :] = jnp.zeros((HD, TOK), bf)
        out_ref[zq, HD : HD + 16, :] = jnp.where(row16 == 0, LOW, 0.0).astype(bf)
        return carry

    lax.fori_loop(0, z, earlier, 0)


def merge(part_ref, off_ref, out_ref):
    ls = []
    for i in range(NZ):
        st = part_ref[i, HD : HD + 16, :].astype(f32)
        ls.append(st[0:1] + st[1:2] + st[2:3] + off_ref[i : i + 1, :])
    m = ls[0]
    for v in ls[1:]:
        m = jnp.maximum(m, v)
    acc = jnp.zeros((HD, TOK), f32)
    total = jnp.zeros((1, TOK), f32)
    for i in range(NZ):
        w = jnp.exp(ls[i] - m)
        total = total + w
        acc = acc + w * part_ref[i, 0:HD, :].astype(f32)
    out_ref[...] = (acc / total).astype(bf)


def project(att_ref, w_ref, resid_ref, gain_ref, routes_ref, stream_ref, out_ref, slots_ref):
    mixed = lax.dot_general(att_ref[...], w_ref[...], (((0,), (0,)), ((), ())), preferred_element_type=f32)
    stream = resid_ref[...].astype(f32) + mixed
    stream_ref[...] = stream
    square = jnp.sum(stream * stream, axis=1, keepdims=True)
    hi = square.astype(bf)
    lo = (square - hi.astype(f32)).astype(bf)
    scaled = (stream * gain_ref[...]).astype(bf)
    wide = (TOK, COLS)
    rows = jnp.concatenate([scaled, jnp.broadcast_to(hi, wide), jnp.broadcast_to(lo, wide)], axis=1)
    e0, e1 = routes_ref[0:1, :], routes_ref[1:2, :]
    io = lax.broadcasted_iota(jnp.int32, (NSP, TOK), 0)
    h0, h1 = io == e0, io == e1
    hit = jnp.where(h0, 1.0, jnp.where(h1, 1.0, 0.0)).astype(bf)
    ia = lax.broadcasted_iota(jnp.int32, (TOK, TOK), 0)
    ib = lax.broadcasted_iota(jnp.int32, (TOK, TOK), 1)
    upper = jnp.where(ia < ib, 1.0, 0.0).astype(bf)
    before = jnp.dot(hit, upper, preferred_element_type=f32)
    r0 = jnp.sum(jnp.where(h0, before, 0.0), axis=0, keepdims=True).astype(jnp.int32)
    r1 = jnp.sum(jnp.where(h1, before, 0.0), axis=0, keepdims=True).astype(jnp.int32)
    s0 = e0 * SLOT + r0
    s1 = e1 * SLOT + r1
    slots_ref[...] = jnp.concatenate([s0, s1, jnp.zeros((6, TOK), jnp.int32)], axis=0)
    ir = lax.broadcasted_iota(jnp.int32, (PADROWS, TOK), 0)
    pick = jnp.where(ir == s0, 1.0, jnp.where(ir == s1, 1.0, 0.0)).astype(bf)
    sent = jnp.dot(pick, rows, preferred_element_type=f32).reshape(NSP, SLOT, 3 * COLS)
    shape = (NSP, SLOT, COLS)
    rank = lax.broadcasted_iota(jnp.int32, shape, 1)
    lane = lax.broadcasted_iota(jnp.int32, shape, 2)
    data, his, los = sent[:, :, 0:COLS], sent[:, :, COLS : 2 * COLS], sent[:, :, 2 * COLS :]
    mh = jnp.sum(jnp.where(lane == rank, his, 0.0), axis=1, keepdims=True)
    ml = jnp.sum(jnp.where(lane == rank, los, 0.0), axis=1, keepdims=True)
    data = jnp.where(rank == CAP, mh, jnp.where(rank == CAP + 1, ml, data))
    out_ref[...] = data.astype(bf)


def squeeze(in_ref, out_ref, rows_ref):
    rank = lax.broadcasted_iota(jnp.int32, (NSP, SLOT, COLS), 1)
    x = in_ref[...].astype(f32)
    part = jnp.sum(jnp.where((rank == CAP) | (rank == CAP + 1), x, 0.0), axis=1)
    lane = lax.broadcasted_iota(jnp.int32, (NSP, COLS), 1)
    part = jnp.where(lane < CAP, part, 0.0)
    packed = part[0:8]
    for g in range(1, 4):
        packed = packed + pltpu.roll(part[8 * g : 8 * g + 8], 32 * g, 1)
    hi = packed.astype(bf).astype(f32)
    for i in range(NSP):
        rows_ref[CAP * i : CAP * i + CAP, :] = in_ref[i].astype(f32)[0:CAP, :]
    rows_ref[ROWS : ROWS + 8, :] = hi
    rows_ref[ROWS + 8 : ROWS + 16, :] = packed - hi
    out_ref[...] = rows_ref[...].astype(bf)


def experts(c_ref, own_ref, other_ref, wg_ref, wu_ref, wd_ref, mine_ref, theirs_ref, g_ref, u_ref, h_ref):
    c = c_ref[0]
    total = jnp.zeros((8, COLS), f32)
    for ref in (own_ref, other_ref):
        for y in range(NY):
            meta = ref[y, ROWS : ROWS + META, :].astype(f32)
            total = total + meta[0:8] + meta[8:16]
    scale8 = lax.rsqrt(total / D + EPS)
    shape = (ROWS, COLS)
    row = lax.broadcasted_iota(jnp.int32, shape, 0).astype(f32)
    lane = lax.broadcasted_iota(jnp.int32, shape, 1).astype(f32)
    src = jnp.floor((row + 0.5) * (1.0 / CAP))
    group = jnp.floor((src + 0.5) * 0.125)
    sub = src - 8.0 * group
    target = 32.0 * group + (row - CAP * src)
    spread = jnp.zeros(shape, f32)
    for a in range(8):
        spread = jnp.where(sub == a, scale8[a : a + 1, :], spread)
    scale = jnp.sum(jnp.where(lane == target, spread, 0.0), axis=1, keepdims=True)
    for y in range(NY):
        xx = jnp.concatenate([own_ref[y, 0:ROWS, :], other_ref[y, 0:ROWS, :]], axis=1)
        first = pl.multiple_of((2 * y + c) * COLS, COLS)
        second = pl.multiple_of((2 * y + 1 - c) * COLS, COLS)
        for w_ref, acc_ref in ((wg_ref, g_ref), (wu_ref, u_ref)):
            w = jnp.concatenate([w_ref[pl.ds(first, COLS), :], w_ref[pl.ds(second, COLS), :]], axis=0)
            part = jnp.dot(xx, w, preferred_element_type=f32)
            if y == 0:
                acc_ref[...] = part
            else:
                acc_ref[...] += part
    gate = g_ref[...] * scale
    up = u_ref[...] * scale
    h_ref[...] = (gate / (1.0 + jnp.exp(-gate)) * up).astype(bf)
    even = c == 0
    for y in range(NY):
        res = jnp.dot(h_ref[...], wd_ref[:, 2 * y * COLS : (2 * y + 2) * COLS], preferred_element_type=f32)
        low, high = res[:, 0:COLS], res[:, COLS:]
        mine_ref[y] = jnp.where(even, low, high).astype(bf)
        theirs_ref[y] = jnp.where(even, high, low).astype(bf)


def gather_sum(in_ref, out_ref, rows_ref):
    acc = in_ref[0].astype(f32)
    for y in range(1, NY):
        acc = acc + in_ref[y].astype(f32)
    rows_ref[...] = acc
    pad = jnp.zeros((SLOT - CAP, COLS), f32)
    for i in range(NSP):
        out_ref[i] = jnp.concatenate([rows_ref[CAP * i : CAP * i + CAP, :], pad], axis=0).astype(bf)


def finish(ret_ref, slots_ref, rw_ref, stream_ref, out_ref):
    slots = slots_ref[...].astype(f32).T
    weight = jnp.concatenate([rw_ref[...], jnp.zeros((6, TOK), f32)], axis=0).T
    lane = lax.broadcasted_iota(jnp.int32, (TOK, PADROWS), 1).astype(f32)
    out = stream_ref[...]
    for k in range(2):
        pick = jnp.where(lane == slots[:, k : k + 1], 1.0, 0.0).astype(bf)
        got = jnp.dot(pick, ret_ref[...], preferred_element_type=f32)
        out = out + weight[:, k : k + 1] * got
    out_ref[...] = out.astype(bf)


def to_all(v, axis):
    n = lax.axis_size(axis)
    return lax.all_to_all(jnp.broadcast_to(v[None], (n, *v.shape)), axis, 0, 0, tiled=True)


def exchange(v, axis):
    return lax.all_to_all(v, axis, 0, 0, tiled=True)


def local(
    queries,
    keys,
    values,
    cum_gate,
    out_weight,
    resid,
    norm_gain,
    routes,
    route_weight,
    gate_weight,
    up_weight,
    down_weight,
):
    z, x, y, c = (lax.axis_index(a) for a in ("z", "x", "y", "c"))
    sds = jax.ShapeDtypeStruct
    col = (y * NC + c) * COLS
    w_cols = exchange(out_weight.reshape(HD, NTP, COLS).transpose(1, 0, 2), TP).reshape(NTP * HD, COLS)
    resid_cols = lax.dynamic_slice_in_dim(resid, col, COLS, 1)
    gain_cols = lax.dynamic_slice_in_dim(norm_gain, col, COLS, 0).reshape(1, COLS)
    gate_keys = lax.dynamic_slice_in_dim(cum_gate[0], z * KEYS, KEYS, 0).reshape(NX, TOK)
    firsts = cum_gate.reshape(NZ, KEYS)[:, 0:1]
    offset = lax.dynamic_slice_in_dim(cum_gate, (z * NX + x) * TOK, TOK, 1) - firsts

    kv = to_all(jnp.concatenate([keys.T, values.T], axis=0), "x")
    q = to_all(queries.T, "z")
    at = jnp.stack([z, x]).astype(jnp.int32)
    parts = call(
        attend,
        sds((NZ, HD + 16, TOK), bf),
        (at, q, kv, gate_keys),
        smem=1,
        scratch=(pltpu.VMEM((KEYS, 2 * HD), bf), pltpu.VMEM((HD + 16, KEYS), bf)),
    )
    parts = exchange(parts, "z")
    attended = call(merge, sds((HD, TOK), bf), (parts, offset))
    attended = lax.all_gather(attended, TP, axis=0, tiled=True)
    stream, outgoing, slots = call(
        project,
        (sds((TOK, COLS), f32), sds((NSP, SLOT, COLS), bf), sds((8, TOK), jnp.int32)),
        (attended, w_cols, resid_cols, gain_cols, routes.T),
    )
    arrived = exchange(outgoing, SP)
    rows = call(squeeze, sds((ROWS + META, COLS), bf), (arrived,), scratch=(pltpu.VMEM((ROWS + META, COLS), f32),))
    own = to_all(rows, "y")
    swap = [(0, 1), (1, 0)]
    other = lax.ppermute(own, "c", swap)
    big = sds((NY, ROWS, COLS), bf)
    mine, theirs = call(
        experts,
        (big, big),
        (c.reshape(1).astype(jnp.int32), own, other, gate_weight[0], up_weight[0], down_weight[0]),
        smem=1,
        scratch=(pltpu.VMEM((ROWS, FFL), f32), pltpu.VMEM((ROWS, FFL), f32), pltpu.VMEM((ROWS, FFL), bf)),
    )
    theirs = lax.ppermute(theirs, "c", swap)
    pair = (mine.astype(f32) + theirs.astype(f32)).astype(bf)
    pair = exchange(pair, "y")
    back = call(gather_sum, sds((NSP, SLOT, COLS), bf), (pair,), scratch=(pltpu.VMEM((ROWS, COLS), f32),))
    returned = exchange(back, SP).reshape(PADROWS, COLS)
    return call(finish, sds((TOK, COLS), bf), (returned, slots, route_weight.T, stream))


def solution(mesh):
    grid = Mesh(mesh.devices.reshape(NZ, NX, NY, NC), ("z", "x", "y", "c"))
    return jax.shard_map(
        local,
        mesh=grid,
        in_specs=(
            P(SP, TP),
            P(SP, TP),
            P(SP, TP),
            P(TP, None),
            P(TP, None),
            P(SP, None),
            P(),
            P(SP, None),
            P(SP, None),
            P(SP, None, TP),
            P(SP, None, TP),
            P(SP, TP, None),
        ),
        out_specs=P(SP, TP),
        check_vma=False,
    )
```

time: 372 us -> 211 us (0.57)
  waiting for transfers between devices: 163 us -> 23.8 us
  blocking collectives: 82.6 us -> 132 us
  matrix products: 38 us -> 0 us
  local copies, waits for them, and re-layouts: 29.2 us -> 5.06 us
  other arithmetic: 19 us -> 2.07 us
  Pallas kernels: 0 us -> 13.8 us
  between operations: 13.6 us -> 0.17 us
  starting transfers between devices: 25.7 us -> 33.3 us
    all_gather x2 -> x0, waiting for transfers between devices: 124 us -> none  [the longest x1 86 us: in_one_piece(): lax.all_gather(both, axis, axis=dim, tiled=True)]
    dot_general x19 -> x0, matrix products: 38 us -> none  [the longest x8 16.2 us: attend_block(): jnp.einsum('hqk,hkd->hqd', weights.astype(jnp.bfloat16), value_rows, pref...]
    all_to_all x2 -> x5, blocking collectives: 82.6 us -> 113 us  [the longest x3 65.2 us: exchange(): return lax.all_to_all(v, axis, 0, 0, tiled=True)]
    all_to_all x3, waiting for transfers between devices: 38.6 us -> 18.5 us  [the longest x1 9.32 us: to_all(): lax.all_to_all(jnp.broadcast_to(v[None], (n, *v.shape)), axis, 0, 0, tile...]
    all_gather x0 -> x1, blocking collectives: none -> 19.4 us  [local(): attended = lax.all_gather(attended, TP, axis=0, tiled=True)]
    pallas_call x0 -> x7, Pallas kernels: none -> 13.8 us  [call(): pl.pallas_call(body, out_shape=out_shape, in_specs=specs, out_specs=tuple...]
    add x24 -> x0, other arithmetic: 8.6 us -> none  [the longest x8 8.55 us: attend_block(): weight_sum = weight_sum * shrink + jnp.sum(weights, axis=-1)]
    ppermute x0 -> x2, starting transfers between devices: none -> 8.23 us  [the longest x1 5.95 us: local(): other = lax.ppermute(own, 'c', swap)]
  transfers between devices with their start and end apart: 5 -> 5, of which waited for: 5 -> 4; matrix products, arithmetic and copies ran while one was open for 2% -> 1% of each run, Pallas kernels for 0% -> 0%
where the time goes in v1:
time: 211 us; the launch traced here: 210 us
  blocking collectives  132 us (63%)
  starting transfers between devices  33.3 us (16%)
  waiting for transfers between devices  23.8 us (11%)
  Pallas kernels  13.8 us (7%)
  local copies, waits for them, and re-layouts  5.06 us (2%)
    all_to_all x3, blocking collectives, exchange(): return lax.all_to_all(v, axis, 0, 0, tiled=True)  65.2 us
    all_to_all x2, blocking collectives, to_all(): lax.all_to_all(jnp.broadcast_to(v[None], (n, *v.shape)), axis, 0, 0, tile...  47.7 us
    all_gather x1, blocking collectives, local(): attended = lax.all_gather(attended, TP, axis=0, tiled=True)  19.4 us
    all_to_all x2, starting transfers between devices, exchange(): return lax.all_to_all(v, axis, 0, 0, tiled=True)  15 us
    pallas_call x7, Pallas kernels, call(): pl.pallas_call(body, out_shape=out_shape, in_specs=specs, out_specs=tuple...  13.8 us
    all_to_all x1, starting transfers between devices, to_all(): lax.all_to_all(jnp.broadcast_to(v[None], (n, *v.shape)), axis, 0, 0, tile...  10.1 us
    all_to_all x1, waiting for transfers between devices, to_all(): lax.all_to_all(jnp.broadcast_to(v[None], (n, *v.shape)), axis, 0, 0, tile...  9.32 us
    all_to_all x2, waiting for transfers between devices, exchange(): return lax.all_to_all(v, axis, 0, 0, tiled=True)  9.14 us
  transfers between devices with their start and end apart: 5, of which 4 were waited for; matrix products, arithmetic and copies ran while one was open for 1% of the time, Pallas kernels for 0%

profile of v1, /device:TPU:1, one launch (start us, length us, event | category | flops | bytes accessed | tf_op | source)
XLA Modules:
  0.0 210.4 jit_solution(5703069391546878955)
XLA Ops:
  0.0 0.9 pad_maximum_fusion
  0.9 10.2 %all_to_all.40.kv_ref = bf16[4,128,256]{2,1,0:T(8,128)(2,1)S(1)} all-to-all(bf16[4,128,256]{2,1,0:T(8,128)(2,1)S(1)} %broadcast_in_dim.7), channel_id=1, replica_groups=mesh['z'=8,'x'=4,'y'=8,'c'=2] {'x'}, dimensions={0} | all-to-all | bytes 524288 | tf_op jit(solution)/shard_map/all_to_all | solution.py:235
  11.1 1.5 broadcast_in_dim.6
  12.6 10.1 %all-to-all-start = ((bf16[8,64,256]{2,1,0:T(8,128)(2,1)}), bf16[8,64,256]{2,1,0:T(8,128)(2,1)S(1)}, u32[]{:S(2)}, u32[]{:S(2)}) async-start(bf16[8,64,256]{2,1,0:T(8,128)(2,1)} %broadcast_in_dim.6), calls=%async_computation | async-start | bytes 524288 | tf_op jit(solution)/shard_map/all_to_all | solution.py:235
  22.8 9.3 %all-to-all-done.q_ref = bf16[8,64,256]{2,1,0:T(8,128)(2,1)S(1)} async-done(((bf16[8,64,256]{2,1,0:T(8,128)(2,1)}), bf16[8,64,256]{2,1,0:T(8,128)(2,1)S(1)}, u32[]{:S(2)}, u32[]{:S(2)}) %all-to-all-start) | async-done | bytes 262176 | tf_op jit(solution)/shard_map/all_to_all | solution.py:235
  32.1 7.1 %shard_map.118 = bf16[8,80,256]{2,1,0:T(8,128)(2,1)} custom-call(s32[2]{0:T(128)S(1)} %pad_add_fusion.at_ref, bf16[8,64,256]{2,1,0:T(8,128)(2,1)S(1)} %all-to-all-done.q_ref, bf16[4,128,256]{2,1,0:T(8,128)(2,1)S(1)} %all_to_all.40.kv_ref, f32[4,256]{1,0:T(4,128)S(1)} %reshape.27.gate_ref), custom_call_target="tpu_custom_call" | custom-call | tf_op jit(solution)/shard_map/pallas_call | solution.py:35
  39.2 3.4 %all-to-all-start.2 = ((bf16[8,80,256]{2,1,0:T(8,128)(2,1)}), bf16[8,80,256]{2,1,0:T(8,128)(2,1)S(1)}, u32[]{:S(2)}, u32[]{:S(2)}) async-start(bf16[8,80,256]{2,1,0:T(8,128)(2,1)} %shard_map.118), calls=%async_computation.2 | async-start | bytes 655360 | tf_op jit(solution)/shard_map/all_to_all | solution.py:239
  42.7 0.8 bitcast_bitcast_fusion
  43.5 9.1 %all-to-all-done.2.part_ref = bf16[8,80,256]{2,1,0:T(8,128)(2,1)S(1)} async-done(((bf16[8,80,256]{2,1,0:T(8,128)(2,1)}), bf16[8,80,256]{2,1,0:T(8,128)(2,1)S(1)}, u32[]{:S(2)}, u32[]{:S(2)}) %all-to-all-start.2) | async-done | bytes 327712 | tf_op jit(solution)/shard_map/all_to_all | solution.py:239
  52.6 11.6 %all-to-all-start.3 = ((bf16[16,64,128]{2,1,0:T(8,128)(2,1)}), bf16[16,64,128]{2,1,0:T(8,128)(2,1)S(1)}, u32[]{:S(2)}, u32[]{:S(2)}) async-start(bf16[16,64,128]{2,1,0:T(8,128)(2,1)} %bitcast_bitcast_fusion), calls=%async_computation.3 | async-start | bytes 524288 | tf_op jit(solution)/shard_map/all_to_all | solution.py:239
  64.3 0.8 dynamic-slice_bitcast_fusion.gain_ref
  65.0 0.5 broadcast.9
  65.6 0.7 reduce.7
  66.3 0.1 copy.15
  66.5 0.1 shard_map.119
  66.5 19.4 %all_gather.3.att_ref = bf16[1024,256]{1,0:T(8,128)(2,1)S(1)} all-gather(bf16[64,256]{1,0:T(8,128)(2,1)S(1)} %shard_map.119), channel_id=1, replica_groups=mesh['z'=8,'x'=4,'y'=8,'c'=2] {'y','c'}, dimensions={0}, use_global_device_ids=true | all-gather | bytes 557056 | tf_op jit(solution)/shard_map/all_gather | solution.py:278
  85.9 0.8 shard_map.120
  86.7 13.6 %all_to_all.41.in_ref = bf16[32,24,128]{2,1,0:T(8,128)(2,1)S(1)} all-to-all(bf16[32,24,128]{2,1,0:T(8,128)(2,1)S(1)} %get-tuple-element.10), channel_id=1, replica_groups=mesh['z'=8,'x'=4,'y'=8,'c'=2] {'z','x'}, dimensions={0} | all-to-all | bytes 393216 | tf_op jit(solution)/shard_map/all_to_all | solution.py:239
  100.3 0.1 shard_map.121
  100.4 0.2 broadcast_in_dim.8
  100.6 37.5 %all_to_all.42.own_ref = bf16[8,656,128]{2,1,0:T(8,128)(2,1)S(1)} all-to-all(bf16[8,656,128]{2,1,0:T(8,128)(2,1)S(1)} %broadcast_in_dim.8), channel_id=1, replica_groups=mesh['z'=8,'x'=4,'y'=8,'c'=2] {'y'}, dimensions={0} | all-to-all | bytes 2686976 | tf_op jit(solution)/shard_map/all_to_all | solution.py:235
  138.1 5.9 %collective-permute-start = (bf16[8,656,128]{2,1,0:T(8,128)(2,1)S(1)}, bf16[8,656,128]{2,1,0:T(8,128)(2,1)S(1)}, u32[]{:S(2)}, u32[]{:S(2)}) collective-permute-start(bf16[8,656,128]{2,1,0:T(8,128)(2,1)S(1)} %all_to_all.42.own_ref), channel_id=1, source_target_pairs={{0,1},{1,0},{2,3},{3,2},{4,5},{5,4},{6,7},{7,6},{8,9},{9,8},{10,11... | collective-permute-start | bytes 4030472 | tf_op jit(solution)/shard_map/ppermute | solution.py:288
  144.1 2.7 %collective-permute-done.other_ref = bf16[8,656,128]{2,1,0:T(8,128)(2,1)S(1)} collective-permute-done((bf16[8,656,128]{2,1,0:T(8,128)(2,1)S(1)}, bf16[8,656,128]{2,1,0:T(8,128)(2,1)S(1)}, u32[]{:S(2)}, u32[]{:S(2)}) %collective-permute-start) | collective-permute-done | bytes 1343520 | tf_op jit(solution)/shard_map/ppermute | solution.py:288
  146.8 1.1 copy-done.7
  147.9 4.2 %shard_map.122 = (bf16[8,640,128]{2,1,0:T(8,128)(2,1)S(1)}, bf16[8,640,128]{2,1,0:T(8,128)(2,1)S(1)}) custom-call(s32[1]{0:T(128)} %bitcast.c_ref, bf16[8,656,128]{2,1,0:T(8,128)(2,1)} %copy-done.6, bf16[8,656,128]{2,1,0:T(8,128)(2,1)} %copy-done.7, bf16[2048,256]{1,0:T(8,128)(2,1)S(1)} %bitcast.25, bf16[2048,256]{1,0:T(8,128)(2,1)S(1)} %bitcast.26, ...), custom_call_target="tpu_custom_call" | custom-call | tf_op jit(solution)/shard_map/pallas_call | solution.py:35
  152.1 2.3 %collective-permute-start.1 = (bf16[8,640,128]{2,1,0:T(8,128)(2,1)S(1)}, bf16[8,640,128]{2,1,0:T(8,128)(2,1)S(1)}, u32[]{:S(2)}, u32[]{:S(2)}) collective-permute-start(bf16[8,640,128]{2,1,0:T(8,128)(2,1)S(1)} %get-tuple-element.12), channel_id=1, source_target_pairs={{0,1},{1,0},{2,3},{3,2},{4,5},{5,4},{6,7},{7,6},{8,9},{9,8},{10,11... | collective-permute-start | bytes 3932168 | tf_op jit(solution)/shard_map/ppermute | solution.py:297
  154.4 2.6 %collective-permute-done.1 = bf16[8,640,128]{2,1,0:T(8,128)(2,1)S(1)} collective-permute-done((bf16[8,640,128]{2,1,0:T(8,128)(2,1)S(1)}, bf16[8,640,128]{2,1,0:T(8,128)(2,1)S(1)}, u32[]{:S(2)}, u32[]{:S(2)}) %collective-permute-start.1) | collective-permute-done | bytes 1310752 | tf_op jit(solution)/shard_map/ppermute | solution.py:297
  157.0 0.3 add_convert_fusion
  157.3 37.2 %all_to_all.43.in_ref = bf16[8,640,128]{2,1,0:T(8,128)(2,1)S(1)} all-to-all(bf16[8,640,128]{2,1,0:T(8,128)(2,1)S(1)} %add_convert_fusion), channel_id=1, replica_groups=mesh['z'=8,'x'=4,'y'=8,'c'=2] {'y'}, dimensions={0} | all-to-all | bytes 2621440 | tf_op jit(solution)/shard_map/all_to_all | solution.py:239
  194.6 0.2 shard_map.123
  194.8 14.4 %all_to_all.44 = bf16[32,24,128]{2,1,0:T(8,128)(2,1)S(1)} all-to-all(bf16[32,24,128]{2,1,0:T(8,128)(2,1)S(1)} %shard_map.123), channel_id=1, replica_groups=mesh['z'=8,'x'=4,'y'=8,'c'=2] {'z','x'}, dimensions={0} | all-to-all | bytes 393216 | tf_op jit(solution)/shard_map/all_to_all | solution.py:239
  209.2 1.2 shard_map.124
  (29 shorter events, 0.3 us)
Async XLA Ops:
  0.0 42.7 %copy-start = (bf16[256,2048]{1,0:T(8,128)(2,1)S(1)}, bf16[256,2048]{1,0:T(8,128)(2,1)}, u32[]{:S(2)}) copy-start(bf16[256,2048]{1,0:T(8,128)(2,1)} %param.17) | copy-start | bytes 3145732
  0.0 22.7 %copy-start.9 = (f32[1,8192]{1,0:T(1,128)S(1)}, f32[1,8192]{1,0:T(1,128)}, u32[]{:S(2)}) copy-start(f32[1,8192]{1,0:T(1,128)} %param.15) | copy-start | bytes 98308
  11.1 31.7 %copy-start.8 = (bf16[64,2048]{1,0:T(8,128)(2,1)S(1)}, bf16[64,2048]{1,0:T(8,128)(2,1)}, u32[]{:S(2)}) copy-start(bf16[64,2048]{1,0:T(8,128)(2,1)} %param.16) | copy-start | bytes 786436
  12.6 19.5 %all-to-all-start = ((bf16[8,64,256]{2,1,0:T(8,128)(2,1)}), bf16[8,64,256]{2,1,0:T(8,128)(2,1)S(1)}, u32[]{:S(2)}, u32[]{:S(2)}) async-start(bf16[8,64,256]{2,1,0:T(8,128)(2,1)} %broadcast_in_dim.6), calls=%async_computation | async-start | bytes 524288 | tf_op jit(solution)/shard_map/all_to_all | solution.py:235
  39.2 13.4 %all-to-all-start.2 = ((bf16[8,80,256]{2,1,0:T(8,128)(2,1)}), bf16[8,80,256]{2,1,0:T(8,128)(2,1)S(1)}, u32[]{:S(2)}, u32[]{:S(2)}) async-start(bf16[8,80,256]{2,1,0:T(8,128)(2,1)} %shard_map.118), calls=%async_computation.2 | async-start | bytes 655360 | tf_op jit(solution)/shard_map/all_to_all | solution.py:239
  42.6 43.3 %copy-start.4 = (s32[256,2]{0,1:T(2,128)S(1)}, s32[256,2]{0,1:T(2,128)}, u32[]{:S(2)}) copy-start(s32[256,2]{0,1:T(2,128)} %param.19) | copy-start | bytes 6148
  52.6 33.3 %all-to-all-start.3 = ((bf16[16,64,128]{2,1,0:T(8,128)(2,1)}), bf16[16,64,128]{2,1,0:T(8,128)(2,1)S(1)}, u32[]{:S(2)}, u32[]{:S(2)}) async-start(bf16[16,64,128]{2,1,0:T(8,128)(2,1)} %bitcast_bitcast_fusion), calls=%async_computation.3 | async-start | bytes 524288 | tf_op jit(solution)/shard_map/all_to_all | solution.py:239
  100.4 47.4 %copy-start.3 = (bf16[1,256,2048]{2,1,0:T(8,128)(2,1)S(1)}, bf16[1,256,2048]{2,1,0:T(8,128)(2,1)}, u32[]{:S(2)}) copy-start(bf16[1,256,2048]{2,1,0:T(8,128)(2,1)} %param.23) | copy-start | bytes 3145732
  100.6 47.2 %copy-start.1 = (bf16[1,2048,256]{2,1,0:T(8,128)(2,1)S(1)}, bf16[1,2048,256]{2,1,0:T(8,128)(2,1)}, u32[]{:S(2)}) copy-start(bf16[1,2048,256]{2,1,0:T(8,128)(2,1)} %param.21) | copy-start | bytes 3145732
  100.6 47.2 %copy-start.2 = (bf16[1,2048,256]{2,1,0:T(8,128)(2,1)S(1)}, bf16[1,2048,256]{2,1,0:T(8,128)(2,1)}, u32[]{:S(2)}) copy-start(bf16[1,2048,256]{2,1,0:T(8,128)(2,1)} %param.22) | copy-start | bytes 3145732
  138.1 8.6 %copy-start.6 = (bf16[8,656,128]{2,1,0:T(8,128)(2,1)}, bf16[8,656,128]{2,1,0:T(8,128)(2,1)S(1)}, u32[]{:S(2)}) copy-start(bf16[8,656,128]{2,1,0:T(8,128)(2,1)S(1)} %all_to_all.42.own_ref) | copy-start | bytes 4030468
  138.1 8.6 %collective-permute-start = (bf16[8,656,128]{2,1,0:T(8,128)(2,1)S(1)}, bf16[8,656,128]{2,1,0:T(8,128)(2,1)S(1)}, u32[]{:S(2)}, u32[]{:S(2)}) collective-permute-start(bf16[8,656,128]{2,1,0:T(8,128)(2,1)S(1)} %all_to_all.42.own_ref), channel_id=1, source_target_pairs={{0,1},{1,0},{2,3},{3,2},{4,5},{5,4},{6,7},{7,6},{8,9},{9,8},{10,11... | collective-permute-start | bytes 4030472 | tf_op jit(solution)/shard_map/ppermute | solution.py:288
  146.8 1.1 copy-start.7
  152.1 4.9 %collective-permute-start.1 = (bf16[8,640,128]{2,1,0:T(8,128)(2,1)S(1)}, bf16[8,640,128]{2,1,0:T(8,128)(2,1)S(1)}, u32[]{:S(2)}, u32[]{:S(2)}) collective-permute-start(bf16[8,640,128]{2,1,0:T(8,128)(2,1)S(1)} %get-tuple-element.12), channel_id=1, source_target_pairs={{0,1},{1,0},{2,3},{3,2},{4,5},{5,4},{6,7},{7,6},{8,9},{9,8},{10,11... | collective-permute-start | bytes 3932168 | tf_op jit(solution)/shard_map/ppermute | solution.py:297
  194.6 14.6 %copy-start.5 = (f32[256,2]{0,1:T(2,128)S(1)}, f32[256,2]{0,1:T(2,128)}, u32[]{:S(2)}) copy-start(f32[256,2]{0,1:T(2,128)} %param.20) | copy-start | bytes 6148

commit v2 on v1

--- a/solution.py
+++ b/solution.py
@@ -4,6 +4,7 @@
 from jax.experimental import pallas as pl
 from jax.experimental.pallas import tpu as pltpu
 from jax.sharding import Mesh, PartitionSpec as P
+
 
 NZ, NX, NY, NC = 8, 4, 8, 2
 NSP, NTP = NZ * NX, NY * NC
@@ -15,6 +16,7 @@
 KEYS = NX * TOK
 CAP = 20
 SLOT = 24
+SEND = 48
 ROWS = NSP * CAP
 PADROWS = NSP * SLOT
 META = 16
@@ -27,7 +29,7 @@
 INTERPRET = False
 
 
-def call(body, out_shape, inputs, smem=0, scratch=()):
+def call(body, out_shape, inputs, smem=0, scratch=(), limit=12):
     specs = [pl.BlockSpec(memory_space=pltpu.SMEM)] * smem
     specs += [pl.BlockSpec(memory_space=pltpu.VMEM)] * (len(inputs) - smem)
     many = isinstance(out_shape, (tuple, list))
@@ -39,7 +41,7 @@
         out_specs=tuple([vm] * len(out_shape)) if many else vm,
         scratch_shapes=list(scratch),
         interpret=INTERPRET,
-        compiler_params=pltpu.CompilerParams(vmem_limit_bytes=48 * 1024 * 1024),
+        compiler_params=pltpu.CompilerParams(vmem_limit_bytes=limit * 1024 * 1024),
     )(*inputs)
 
 
@@ -114,14 +116,20 @@
     out_ref[...] = (acc / total).astype(bf)
 
 
-def project(att_ref, w_ref, resid_ref, gain_ref, routes_ref, stream_ref, out_ref, slots_ref):
-    mixed = lax.dot_general(att_ref[...], w_ref[...], (((0,), (0,)), ((), ())), preferred_element_type=f32)
-    stream = resid_ref[...].astype(f32) + mixed
-    stream_ref[...] = stream
+def project(at_ref, att_ref, w_ref, resid_ref, gain_ref, routes_ref, stream_ref, out_ref, slots_ref):
+    c0 = pl.multiple_of(at_ref[0], COLS)
+    c1 = pl.multiple_of(at_ref[1], COLS)
+    weights = [jnp.concatenate([w_ref[t, q * HD : (q + 1) * HD, :] for t in range(NTP)], axis=0) for q in range(2)]
+    w = jnp.concatenate(weights, axis=1)
+    mixed = lax.dot_general(att_ref[...], w, (((0,), (0,)), ((), ())), preferred_element_type=f32)
+    resid = jnp.concatenate([resid_ref[:, pl.ds(c0, COLS)], resid_ref[:, pl.ds(c1, COLS)]], axis=1)
+    gain = jnp.concatenate([gain_ref[:, pl.ds(c0, COLS)], gain_ref[:, pl.ds(c1, COLS)]], axis=1)
+    stream = resid.astype(f32) + mixed
+    stream_ref[...] = jnp.where(at_ref[2] == 0, stream[:, 0:COLS], stream[:, COLS:])
     square = jnp.sum(stream * stream, axis=1, keepdims=True)
     hi = square.astype(bf)
     lo = (square - hi.astype(f32)).astype(bf)
-    scaled = (stream * gain_ref[...]).astype(bf)
+    scaled = (stream * gain).astype(bf)
     wide = (TOK, COLS)
     rows = jnp.concatenate([scaled, jnp.broadcast_to(hi, wide), jnp.broadcast_to(lo, wide)], axis=1)
     e0, e1 = routes_ref[0:1, :], routes_ref[1:2, :]
@@ -134,26 +142,28 @@
     before = jnp.dot(hit, upper, preferred_element_type=f32)
     r0 = jnp.sum(jnp.where(h0, before, 0.0), axis=0, keepdims=True).astype(jnp.int32)
     r1 = jnp.sum(jnp.where(h1, before, 0.0), axis=0, keepdims=True).astype(jnp.int32)
-    s0 = e0 * SLOT + r0
-    s1 = e1 * SLOT + r1
-    slots_ref[...] = jnp.concatenate([s0, s1, jnp.zeros((6, TOK), jnp.int32)], axis=0)
-    ir = lax.broadcasted_iota(jnp.int32, (PADROWS, TOK), 0)
-    pick = jnp.where(ir == s0, 1.0, jnp.where(ir == s1, 1.0, 0.0)).astype(bf)
-    sent = jnp.dot(pick, rows, preferred_element_type=f32).reshape(NSP, SLOT, 3 * COLS)
-    shape = (NSP, SLOT, COLS)
+    slots_ref[...] = jnp.concatenate([e0 * SLOT + r0, e1 * SLOT + r1, jnp.zeros((6, TOK), jnp.int32)], axis=0)
+    s0 = e0 * SEND + r0
+    s1 = e1 * SEND + r1
+    ir = lax.broadcasted_iota(jnp.int32, (NSP * SEND, TOK), 0)
+    hits = (ir == s0) | (ir == s1) | (ir == s0 + CAP) | (ir == s1 + CAP)
+    pick = jnp.where(hits, 1.0, 0.0).astype(bf)
+    sent = jnp.dot(pick, rows, preferred_element_type=f32).reshape(NSP, SEND, 4 * COLS)
+    shape = (NSP, SEND, COLS)
     rank = lax.broadcasted_iota(jnp.int32, shape, 1)
     lane = lax.broadcasted_iota(jnp.int32, shape, 2)
-    data, his, los = sent[:, :, 0:COLS], sent[:, :, COLS : 2 * COLS], sent[:, :, 2 * COLS :]
-    mh = jnp.sum(jnp.where(lane == rank, his, 0.0), axis=1, keepdims=True)
-    ml = jnp.sum(jnp.where(lane == rank, los, 0.0), axis=1, keepdims=True)
-    data = jnp.where(rank == CAP, mh, jnp.where(rank == CAP + 1, ml, data))
+    data = jnp.where(rank < CAP, sent[:, :, 0:COLS], sent[:, :, COLS : 2 * COLS])
+    same = (lane == rank) & (rank < CAP)
+    mh = jnp.sum(jnp.where(same, sent[:, :, 2 * COLS : 3 * COLS], 0.0), axis=1, keepdims=True)
+    ml = jnp.sum(jnp.where(same, sent[:, :, 3 * COLS :], 0.0), axis=1, keepdims=True)
+    data = jnp.where(rank == 2 * CAP, mh, jnp.where(rank == 2 * CAP + 1, ml, data))
     out_ref[...] = data.astype(bf)
 
 
-def squeeze(in_ref, out_ref, rows_ref):
-    rank = lax.broadcasted_iota(jnp.int32, (NSP, SLOT, COLS), 1)
+def squeeze(in_ref, all_ref, low_ref, high_ref, rows_ref):
+    rank = lax.broadcasted_iota(jnp.int32, (NSP, SEND, COLS), 1)
     x = in_ref[...].astype(f32)
-    part = jnp.sum(jnp.where((rank == CAP) | (rank == CAP + 1), x, 0.0), axis=1)
+    part = jnp.sum(jnp.where((rank == 2 * CAP) | (rank == 2 * CAP + 1), x, 0.0), axis=1)
     lane = lax.broadcasted_iota(jnp.int32, (NSP, COLS), 1)
     part = jnp.where(lane < CAP, part, 0.0)
     packed = part[0:8]
@@ -161,18 +171,37 @@
         packed = packed + pltpu.roll(part[8 * g : 8 * g + 8], 32 * g, 1)
     hi = packed.astype(bf).astype(f32)
     for i in range(NSP):
-        rows_ref[CAP * i : CAP * i + CAP, :] = in_ref[i].astype(f32)[0:CAP, :]
-    rows_ref[ROWS : ROWS + 8, :] = hi
-    rows_ref[ROWS + 8 : ROWS + 16, :] = packed - hi
-    out_ref[...] = rows_ref[...].astype(bf)
-
-
-def experts(c_ref, own_ref, other_ref, wg_ref, wu_ref, wd_ref, mine_ref, theirs_ref, g_ref, u_ref, h_ref):
-    c = c_ref[0]
+        x = in_ref[i].astype(f32)
+        rows_ref[ROWS + CAP * i : ROWS + CAP * i + CAP, :] = x[0:CAP, :]
+        rows_ref[CAP * i : CAP * i + CAP, :] = x[CAP : 2 * CAP, :]
+    rows_ref[2 * ROWS : 2 * ROWS + 8, :] = hi
+    rows_ref[2 * ROWS + 8 : 2 * ROWS + META, :] = packed - hi
+    all_ref[...] = rows_ref[...].astype(bf)
+    high_ref[...] = rows_ref[0:ROWS, :].astype(bf)
+    low_ref[...] = rows_ref[ROWS : 2 * ROWS + META, :].astype(bf)
+
+
+PIECES = (
+    (0, 0, 0, ROWS),
+    (0, 1, 0, 0),
+    (3, 0, 1, ROWS),
+    (3, 1, 1, 0),
+    (1, 0, 2, ROWS),
+    (1, 1, 2, 0),
+    (2, 0, 3, 0),
+    (2, 1, 4, 0),
+)
+METAS = ((0, 2 * ROWS), (1, 2 * ROWS), (2, 2 * ROWS), (3, ROWS))
+
+
+def experts(at_ref, *refs):
+    owns, others = refs[0:5], refs[5:10]
+    wg_ref, wu_ref, wd_ref, mine_ref, theirs_ref, g_ref, u_ref, h_ref = refs[10:]
+    y, c = at_ref[0], at_ref[1]
     total = jnp.zeros((8, COLS), f32)
-    for ref in (own_ref, other_ref):
-        for y in range(NY):
-            meta = ref[y, ROWS : ROWS + META, :].astype(f32)
+    for pieces in (owns, others):
+        for n, at in METAS:
+            meta = pieces[n][at : at + META, :].astype(f32)
             total = total + meta[0:8] + meta[8:16]
     scale8 = lax.rsqrt(total / D + EPS)
     shape = (ROWS, COLS)
@@ -186,14 +215,15 @@
     for a in range(8):
         spread = jnp.where(sub == a, scale8[a : a + 1, :], spread)
     scale = jnp.sum(jnp.where(lane == target, spread, 0.0), axis=1, keepdims=True)
-    for y in range(NY):
-        xx = jnp.concatenate([own_ref[y, 0:ROWS, :], other_ref[y, 0:ROWS, :]], axis=1)
-        first = pl.multiple_of((2 * y + c) * COLS, COLS)
-        second = pl.multiple_of((2 * y + 1 - c) * COLS, COLS)
+    for step, (off, upper, n, at) in enumerate(PIECES):
+        xx = jnp.concatenate([owns[n][at : at + ROWS, :], others[n][at : at + ROWS, :]], axis=1)
+        block = lax.rem(y + off, NY // 2) + upper * (NY // 2)
+        first = pl.multiple_of((2 * block + c) * COLS, COLS)
+        second = pl.multiple_of((2 * block + 1 - c) * COLS, COLS)
         for w_ref, acc_ref in ((wg_ref, g_ref), (wu_ref, u_ref)):
             w = jnp.concatenate([w_ref[pl.ds(first, COLS), :], w_ref[pl.ds(second, COLS), :]], axis=0)
             part = jnp.dot(xx, w, preferred_element_type=f32)
-            if y == 0:
+            if step == 0:
                 acc_ref[...] = part
             else:
                 acc_ref[...] += part
@@ -235,11 +265,15 @@
     return lax.all_to_all(jnp.broadcast_to(v[None], (n, *v.shape)), axis, 0, 0, tiled=True)
 
 
+def shift(v, by):
+    return lax.ppermute(v, "y", [(i, (i + by) % NY) for i in range(NY)])
+
+
 def exchange(v, axis):
     return lax.all_to_all(v, axis, 0, 0, tiled=True)
 
 
-def local(
+def layer(
     queries,
     keys,
     values,
@@ -255,17 +289,21 @@
 ):
     z, x, y, c = (lax.axis_index(a) for a in ("z", "x", "y", "c"))
     sds = jax.ShapeDtypeStruct
-    col = (y * NC + c) * COLS
-    w_cols = exchange(out_weight.reshape(HD, NTP, COLS).transpose(1, 0, 2), TP).reshape(NTP * HD, COLS)
-    resid_cols = lax.dynamic_slice_in_dim(resid, col, COLS, 1)
-    gain_cols = lax.dynamic_slice_in_dim(norm_gain, col, COLS, 0).reshape(1, COLS)
+    half = NY // 2
+    w = out_weight.reshape(HD, 2, half, NC, COLS).transpose(2, 3, 1, 0, 4).reshape(NTP // 2, 2 * HD, COLS)
+    w_cols = exchange(jnp.concatenate([w, w], axis=0), TP)
+    low = (lax.rem(y, half) * NC + c) * COLS
+    at_cols = jnp.stack([low, low + half * NC * COLS, y // half]).astype(jnp.int32)
     gate_keys = lax.dynamic_slice_in_dim(cum_gate[0], z * KEYS, KEYS, 0).reshape(NX, TOK)
     firsts = cum_gate.reshape(NZ, KEYS)[:, 0:1]
     offset = lax.dynamic_slice_in_dim(cum_gate, (z * NX + x) * TOK, TOK, 1) - firsts
 
     kv = to_all(jnp.concatenate([keys.T, values.T], axis=0), "x")
-    q = to_all(queries.T, "z")
     at = jnp.stack([z, x]).astype(jnp.int32)
+    q_send, kv, gate_keys, at, offset, at_cols = lax.optimization_barrier(
+        (jnp.broadcast_to(queries.T[None], (NZ, HD, TOK)), kv, gate_keys, at, offset, at_cols)
+    )
+    q = exchange(q_send, "z")
     parts = call(
         attend,
         sds((NZ, HD + 16, TOK), bf),
@@ -278,21 +316,33 @@
     attended = lax.all_gather(attended, TP, axis=0, tiled=True)
     stream, outgoing, slots = call(
         project,
-        (sds((TOK, COLS), f32), sds((NSP, SLOT, COLS), bf), sds((8, TOK), jnp.int32)),
-        (attended, w_cols, resid_cols, gain_cols, routes.T),
+        (sds((TOK, COLS), f32), sds((NSP, SEND, COLS), bf), sds((8, TOK), jnp.int32)),
+        (at_cols, attended, w_cols, resid, norm_gain.reshape(1, D), routes.T),
+        smem=1,
     )
     arrived = exchange(outgoing, SP)
-    rows = call(squeeze, sds((ROWS + META, COLS), bf), (arrived,), scratch=(pltpu.VMEM((ROWS + META, COLS), f32),))
-    own = to_all(rows, "y")
+    rows = 2 * ROWS + META
+    every, lower, higher = call(
+        squeeze,
+        (sds((rows, COLS), bf), sds((ROWS + META, COLS), bf), sds((ROWS, COLS), bf)),
+        (arrived,),
+        scratch=(pltpu.VMEM((rows, COLS), f32),),
+    )
     swap = [(0, 1), (1, 0)]
-    other = lax.ppermute(own, "c", swap)
+    owns = [every]
+    for v, by in ((every, 1), (every, -1), (lower, 2), (higher, -2)):
+        owns.append(shift(v, by))
+    others = []
+    for v in owns:
+        others.append(lax.ppermute(v, "c", swap))
     big = sds((NY, ROWS, COLS), bf)
     mine, theirs = call(
         experts,
         (big, big),
-        (c.reshape(1).astype(jnp.int32), own, other, gate_weight[0], up_weight[0], down_weight[0]),
+        (jnp.stack([y, c]).astype(jnp.int32), *owns, *others, gate_weight[0], up_weight[0], down_weight[0]),
         smem=1,
         scratch=(pltpu.VMEM((ROWS, FFL), f32), pltpu.VMEM((ROWS, FFL), f32), pltpu.VMEM((ROWS, FFL), bf)),
+        limit=24,
     )
     theirs = lax.ppermute(theirs, "c", swap)
     pair = (mine.astype(f32) + theirs.astype(f32)).astype(bf)
@@ -305,7 +355,7 @@
 def solution(mesh):
     grid = Mesh(mesh.devices.reshape(NZ, NX, NY, NC), ("z", "x", "y", "c"))
     return jax.shard_map(
-        local,
+        layer,
         mesh=grid,
         in_specs=(
             P(SP, TP),

time: 211 us -> 211 us (level)
  starting transfers between devices: 33.3 us -> 51.5 us
  blocking collectives: 132 us -> 116 us
  waiting for transfers between devices: 23.8 us -> 20.3 us
    all_to_all x2 -> x0, blocking collectives: 47.7 us -> none  [to_all(): lax.all_to_all(jnp.broadcast_to(v[None], (n, *v.shape)), axis, 0, 0, tile...]
    all_to_all x3 -> x4, blocking collectives: 65.2 us -> 89.2 us  [exchange(): return lax.all_to_all(v, axis, 0, 0, tiled=True)]
    ppermute x2 -> x10, starting transfers between devices: 8.23 us -> 31.6 us  [the longest x5 17.1 us: layer(): others.append(lax.ppermute(v, 'c', swap))]
    all_gather x1, blocking collectives: 19.4 us -> 27.2 us  [layer(): attended = lax.all_gather(attended, TP, axis=0, tiled=True)]
    all_to_all x1, waiting for transfers between devices: 9.32 us -> 1.74 us  [to_all(): lax.all_to_all(jnp.broadcast_to(v[None], (n, *v.shape)), axis, 0, 0, tile...]
    all_to_all x1, starting transfers between devices: 10.1 us -> 4.83 us  [to_all(): lax.all_to_all(jnp.broadcast_to(v[None], (n, *v.shape)), axis, 0, 0, tile...]
    ppermute x2 -> x10, waiting for transfers between devices: 5.33 us -> 9.68 us  [the longest x4 6.1 us: shift(): return lax.ppermute(v, 'y', [(i, (i + by) % NY) for i in range(NY)])]
  transfers between devices with their start and end apart: 5 -> 13, of which waited for: 4 -> 5; matrix products, arithmetic and copies ran while one was open for 1% -> 2% of each run, Pallas kernels for 0% -> 0%
where the time goes in v2:
time: 211 us; the launch traced here: 210 us
  blocking collectives  116 us (55%)
  starting transfers between devices  51.5 us (24%)
  waiting for transfers between devices  20.3 us (10%)
  Pallas kernels  13.8 us (7%)
  local copies, waits for them, and re-layouts  3.84 us (2%)
  other arithmetic  3.73 us (2%)
    all_to_all x4, blocking collectives, exchange(): return lax.all_to_all(v, axis, 0, 0, tiled=True)  89.2 us
    all_gather x1, blocking collectives, layer(): attended = lax.all_gather(attended, TP, axis=0, tiled=True)  27.2 us
    ppermute x5, starting transfers between devices, layer(): others.append(lax.ppermute(v, 'c', swap))  17.1 us
    all_to_all x2, starting transfers between devices, exchange(): return lax.all_to_all(v, axis, 0, 0, tiled=True)  15 us
    pallas_call x7, Pallas kernels, call(): pl.pallas_call(body, out_shape=out_shape, in_specs=specs, out_specs=tuple...  13.8 us
    ppermute x4, starting transfers between devices, shift(): return lax.ppermute(v, 'y', [(i, (i + by) % NY) for i in range(NY)])  12.2 us
    all_to_all x2, waiting for transfers between devices, exchange(): return lax.all_to_all(v, axis, 0, 0, tiled=True)  8.87 us
    ppermute x4, waiting for transfers between devices, shift(): return lax.ppermute(v, 'y', [(i, (i + by) % NY) for i in range(NY)])  6.1 us
  transfers between devices with their start and end apart: 13, of which 5 were waited for; matrix products, arithmetic and copies ran while one was open for 2% of the time, Pallas kernels for 0%

profile of v2, /device:TPU:1, one launch (start us, length us, event | category | flops | bytes accessed | tf_op | source)
XLA Modules:
  0.0 209.8 jit_solution(6645534694101687447)
XLA Ops:
  0.0 0.8 pad_maximum_fusion.1
  1.5 4.8 %all-to-all-start = ((bf16[4,128,256]{2,1,0:T(8,128)(2,1)}), bf16[4,128,256]{2,1,0:T(8,128)(2,1)S(1)}, u32[]{:S(2)}, u32[]{:S(2)}) async-start(bf16[4,128,256]{2,1,0:T(8,128)(2,1)} %broadcast_in_dim.5), calls=%async_computation | async-start | bytes 524288 | tf_op jit(solution)/shard_map/all_to_all | solution.py:265
  6.3 0.7 constant_dynamic-slice_fusion
  8.3 1.5 reduce.7
  10.1 1.7 all-to-all-done.kv_ref
  11.9 0.8 broadcast_in_dim.4
  12.6 19.3 %all_to_all.35.q_ref = bf16[8,64,256]{2,1,0:T(8,128)(2,1)S(1)} all-to-all(bf16[8,64,256]{2,1,0:T(8,128)(2,1)S(1)} %broadcast_in_dim.4), channel_id=1, replica_groups=mesh['z'=8,'x'=4,'y'=8,'c'=2] {'z'}, dimensions={0} | all-to-all | bytes 524288 | tf_op jit(solution)/shard_map/all_to_all | solution.py:273
  31.9 7.1 %shard_map.118 = bf16[8,80,256]{2,1,0:T(8,128)(2,1)} custom-call(s32[2]{0:T(128)S(1)} %pad_add_fusion.1.at_ref, bf16[8,64,256]{2,1,0:T(8,128)(2,1)S(1)} %all_to_all.35.q_ref, bf16[4,128,256]{2,1,0:T(8,128)(2,1)S(1)} %all-to-all-done.kv_ref, f32[4,256]{1,0:T(4,128)S(1)} %reshape.22.gate_ref), custom_call_target="tpu_custom_call" | custom-call | tf_op jit(solution)/shard_map/pallas_call | solution.py:37
  39.0 3.4 %all-to-all-start.2 = ((bf16[8,80,256]{2,1,0:T(8,128)(2,1)}), bf16[8,80,256]{2,1,0:T(8,128)(2,1)S(1)}, u32[]{:S(2)}, u32[]{:S(2)}) async-start(bf16[8,80,256]{2,1,0:T(8,128)(2,1)} %shard_map.118), calls=%async_computation.2 | async-start | bytes 655360 | tf_op jit(solution)/shard_map/all_to_all | solution.py:273
  42.8 0.8 pad_maximum_fusion
  43.6 8.9 %all-to-all-done.2.part_ref = bf16[8,80,256]{2,1,0:T(8,128)(2,1)S(1)} async-done(((bf16[8,80,256]{2,1,0:T(8,128)(2,1)}), bf16[8,80,256]{2,1,0:T(8,128)(2,1)S(1)}, u32[]{:S(2)}, u32[]{:S(2)}) %all-to-all-start.2) | async-done | bytes 327712 | tf_op jit(solution)/shard_map/all_to_all | solution.py:273
  52.5 11.6 %all-to-all-start.3 = ((bf16[16,128,128]{2,1,0:T(8,128)(2,1)}), bf16[16,128,128]{2,1,0:T(8,128)(2,1)S(1)}, u32[]{:S(2)}, u32[]{:S(2)}) async-start(bf16[16,128,128]{2,1,0:T(8,128)(2,1)} %pad_maximum_fusion), calls=%async_computation.3 | async-start | bytes 1048576 | tf_op jit(solution)/shard_map/all_to_all | solution.py:273
  64.2 27.2 %all_gather.3.att_ref = bf16[1024,256]{1,0:T(8,128)(2,1)S(1)} all-gather(bf16[64,256]{1,0:T(8,128)(2,1)S(1)} %shard_map.119), channel_id=1, replica_groups=mesh['z'=8,'x'=4,'y'=8,'c'=2] {'y','c'}, dimensions={0}, use_global_device_ids=true | all-gather | bytes 557056 | tf_op jit(solution)/shard_map/all_gather | solution.py:316
  91.4 2.0 shard_map.120
  93.4 17.5 %all_to_all.36.in_ref = bf16[32,48,128]{2,1,0:T(8,128)(2,1)S(1)} all-to-all(bf16[32,48,128]{2,1,0:T(8,128)(2,1)S(1)} %get-tuple-element.25), channel_id=1, replica_groups=mesh['z'=8,'x'=4,'y'=8,'c'=2] {'z','x'}, dimensions={0} | all-to-all | bytes 786432 | tf_op jit(solution)/shard_map/all_to_all | solution.py:273
  111.0 2.0 collective-permute-start.1
  113.0 3.3 %collective-permute-start = (bf16[1296,128]{1,0:T(8,128)(2,1)S(1)}, bf16[1296,128]{1,0:T(8,128)(2,1)S(1)}, u32[]{:S(2)}, u32[]{:S(2)}) collective-permute-start(bf16[1296,128]{1,0:T(8,128)(2,1)S(1)} %get-tuple-element.26.refs_0_), channel_id=1, source_target_pairs={{0,2},{2,4},{4,6},{6,8},{8,10},{10,12},{12,14},{14,0},{1,3},{3,5},... | collective-permute-start | bytes 995336 | tf_op jit(solution)/shard_map/ppermute | solution.py:269
  116.3 2.9 %collective-permute-start.2 = (bf16[656,128]{1,0:T(8,128)(2,1)S(1)}, bf16[656,128]{1,0:T(8,128)(2,1)S(1)}, u32[]{:S(2)}, u32[]{:S(2)}) collective-permute-start(bf16[656,128]{1,0:T(8,128)(2,1)S(1)} %get-tuple-element.27), channel_id=1, source_target_pairs={{0,4},{2,6},{4,8},{6,10},{8,12},{10,14},{12,0},{14,2},{1,5},{3,7},... | collective-permute-start | bytes 503816 | tf_op jit(solution)/shard_map/ppermute | solution.py:269
  119.2 4.7 %collective-permute-start.4 = (bf16[1296,128]{1,0:T(8,128)(2,1)S(1)}, bf16[1296,128]{1,0:T(8,128)(2,1)S(1)}, u32[]{:S(2)}, u32[]{:S(2)}) collective-permute-start(bf16[1296,128]{1,0:T(8,128)(2,1)S(1)} %get-tuple-element.26.refs_0_), channel_id=1, source_target_pairs={{0,1},{1,0},{2,3},{3,2},{4,5},{5,4},{6,7},{7,6},{8,9},{9,8},{10,11... | collective-permute-start | bytes 995336 | tf_op jit(solution)/shard_map/ppermute | solution.py:337
  123.9 1.9 collective-permute-start.6
  125.9 6.0 %collective-permute-start.5 = (bf16[1296,128]{1,0:T(8,128)(2,1)S(1)}, bf16[1296,128]{1,0:T(8,128)(2,1)S(1)}, u32[]{:S(2)}, u32[]{:S(2)}) collective-permute-start(bf16[1296,128]{1,0:T(8,128)(2,1)S(1)} %collective-permute-done.refs_1_), channel_id=1, source_target_pairs={{0,1},{1,0},{2,3},{3,2},{4,5},{5,4},{6,7},{7,6},{8,9},{9,8},{10,11... | collective-permute-start | bytes 995336 | tf_op jit(solution)/shard_map/ppermute | solution.py:337
  131.8 4.0 %collective-permute-start.3 = (bf16[640,128]{1,0:T(8,128)(2,1)S(1)}, bf16[640,128]{1,0:T(8,128)(2,1)S(1)}, u32[]{:S(2)}, u32[]{:S(2)}) collective-permute-start(bf16[640,128]{1,0:T(8,128)(2,1)S(1)} %get-tuple-element.28), channel_id=1, source_target_pairs={{0,12},{2,14},{4,0},{6,2},{8,4},{10,6},{12,8},{14,10},{1,13},{3,15... | collective-permute-start | bytes 491528 | tf_op jit(solution)/shard_map/ppermute | solution.py:269
  135.9 2.2 %collective-permute-start.7 = (bf16[656,128]{1,0:T(8,128)(2,1)S(1)}, bf16[656,128]{1,0:T(8,128)(2,1)S(1)}, u32[]{:S(2)}, u32[]{:S(2)}) collective-permute-start(bf16[656,128]{1,0:T(8,128)(2,1)S(1)} %collective-permute-done.2.refs_3_), channel_id=1, source_target_pairs={{0,1},{1,0},{2,3},{3,2},{4,5},{5,4},{6,7},{7,6},{8,9},{9,8},{10,11... | collective-permute-start | bytes 503816 | tf_op jit(solution)/shard_map/ppermute | solution.py:337
  138.1 6.1 %collective-permute-done.3.refs_4_ = bf16[640,128]{1,0:T(8,128)(2,1)S(1)} collective-permute-done((bf16[640,128]{1,0:T(8,128)(2,1)S(1)}, bf16[640,128]{1,0:T(8,128)(2,1)S(1)}, u32[]{:S(2)}, u32[]{:S(2)}) %collective-permute-start.3) | collective-permute-done | bytes 163872 | tf_op jit(solution)/shard_map/ppermute | solution.py:269
  144.2 2.3 %collective-permute-start.8 = (bf16[640,128]{1,0:T(8,128)(2,1)S(1)}, bf16[640,128]{1,0:T(8,128)(2,1)S(1)}, u32[]{:S(2)}, u32[]{:S(2)}) collective-permute-start(bf16[640,128]{1,0:T(8,128)(2,1)S(1)} %collective-permute-done.3.refs_4_), channel_id=1, source_target_pairs={{0,1},{1,0},{2,3},{3,2},{4,5},{5,4},{6,7},{7,6},{8,9},{9,8},{10,11... | collective-permute-start | bytes 491528 | tf_op jit(solution)/shard_map/ppermute | solution.py:337
  146.6 0.9 collective-permute-done.8.refs_9_
  147.6 3.0 %shard_map.122 = (bf16[8,640,128]{2,1,0:T(8,128)(2,1)S(1)}, bf16[8,640,128]{2,1,0:T(8,128)(2,1)S(1)}) custom-call(s32[2]{0:T(128)S(1)} %pad_add_fusion.at_ref, bf16[1296,128]{1,0:T(8,128)(2,1)S(1)} %get-tuple-element.26.refs_0_, bf16[1296,128]{1,0:T(8,128)(2,1)S(1)} %collective-permute-done.refs_1_, bf16[1296,128]{1,0:T(8,128)(2,1)S(1)} %collective-permute-done.1.refs_2_, ...), custom_call_target="tpu_custom_call" | custom-call | tf_op jit(solution)/shard_map/pallas_call | solution.py:37
  150.6 2.3 %collective-permute-start.9 = (bf16[8,640,128]{2,1,0:T(8,128)(2,1)S(1)}, bf16[8,640,128]{2,1,0:T(8,128)(2,1)S(1)}, u32[]{:S(2)}, u32[]{:S(2)}) collective-permute-start(bf16[8,640,128]{2,1,0:T(8,128)(2,1)S(1)} %get-tuple-element.30), channel_id=1, source_target_pairs={{0,1},{1,0},{2,3},{3,2},{4,5},{5,4},{6,7},{7,6},{8,9},{9,8},{10,11... | collective-permute-start | bytes 3932168 | tf_op jit(solution)/shard_map/ppermute | solution.py:347
  152.9 2.6 %collective-permute-done.9 = bf16[8,640,128]{2,1,0:T(8,128)(2,1)S(1)} collective-permute-done((bf16[8,640,128]{2,1,0:T(8,128)(2,1)S(1)}, bf16[8,640,128]{2,1,0:T(8,128)(2,1)S(1)}, u32[]{:S(2)}, u32[]{:S(2)}) %collective-permute-start.9) | collective-permute-done | bytes 1310752 | tf_op jit(solution)/shard_map/ppermute | solution.py:347
  155.9 38.8 %all_to_all.37.in_ref = bf16[8,640,128]{2,1,0:T(8,128)(2,1)S(1)} all-to-all(bf16[8,640,128]{2,1,0:T(8,128)(2,1)S(1)} %add_convert_fusion), channel_id=1, replica_groups=mesh['z'=8,'x'=4,'y'=8,'c'=2] {'y'}, dimensions={0} | all-to-all | bytes 2621440 | tf_op jit(solution)/shard_map/all_to_all | solution.py:273
  194.9 13.7 %all_to_all.38 = bf16[32,24,128]{2,1,0:T(8,128)(2,1)S(1)} all-to-all(bf16[32,24,128]{2,1,0:T(8,128)(2,1)S(1)} %shard_map.123), channel_id=1, replica_groups=mesh['z'=8,'x'=4,'y'=8,'c'=2] {'z','x'}, dimensions={0} | all-to-all | bytes 393216 | tf_op jit(solution)/shard_map/all_to_all | solution.py:273
  208.6 1.2 shard_map.124
  (41 shorter events, 3.5 us)
Async XLA Ops:
  1.5 10.4 %all-to-all-start = ((bf16[4,128,256]{2,1,0:T(8,128)(2,1)}), bf16[4,128,256]{2,1,0:T(8,128)(2,1)S(1)}, u32[]{:S(2)}, u32[]{:S(2)}) async-start(bf16[4,128,256]{2,1,0:T(8,128)(2,1)} %broadcast_in_dim.5), calls=%async_computation | async-start | bytes 524288 | tf_op jit(solution)/shard_map/all_to_all | solution.py:265
  6.3 36.2 %copy-start.7 = (bf16[64,2048]{1,0:T(8,128)(2,1)S(1)}, bf16[64,2048]{1,0:T(8,128)(2,1)}, u32[]{:S(2)}) copy-start(bf16[64,2048]{1,0:T(8,128)(2,1)} %param.16) | copy-start | bytes 786436
  39.0 13.4 %all-to-all-start.2 = ((bf16[8,80,256]{2,1,0:T(8,128)(2,1)}), bf16[8,80,256]{2,1,0:T(8,128)(2,1)S(1)}, u32[]{:S(2)}, u32[]{:S(2)}) async-start(bf16[8,80,256]{2,1,0:T(8,128)(2,1)} %shard_map.118), calls=%async_computation.2 | async-start | bytes 655360 | tf_op jit(solution)/shard_map/all_to_all | solution.py:273
  42.7 48.6 %copy-start = (bf16[256,2048]{1,0:T(8,128)(2,1)S(1)}, bf16[256,2048]{1,0:T(8,128)(2,1)}, u32[]{:S(2)}) copy-start(bf16[256,2048]{1,0:T(8,128)(2,1)} %resid_ref.1) | copy-start | bytes 3145732
  42.8 48.6 %copy-start.4 = (f32[2048]{0:T(1024)S(1)}, f32[2048]{0:T(1024)}, u32[]{:S(2)}) copy-start(f32[2048]{0:T(1024)} %param.18) | copy-start | bytes 24580
  42.8 48.6 %copy-start.6 = (s32[256,2]{0,1:T(2,128)S(1)}, s32[256,2]{0,1:T(2,128)}, u32[]{:S(2)}) copy-start(s32[256,2]{0,1:T(2,128)} %param.19) | copy-start | bytes 6148
  52.5 38.9 %all-to-all-start.3 = ((bf16[16,128,128]{2,1,0:T(8,128)(2,1)}), bf16[16,128,128]{2,1,0:T(8,128)(2,1)S(1)}, u32[]{:S(2)}, u32[]{:S(2)}) async-start(bf16[16,128,128]{2,1,0:T(8,128)(2,1)} %pad_maximum_fusion), calls=%async_computation.3 | async-start | bytes 1048576 | tf_op jit(solution)/shard_map/all_to_all | solution.py:273
  91.4 56.2 %copy-start.1 = (bf16[1,2048,256]{2,1,0:T(8,128)(2,1)S(1)}, bf16[1,2048,256]{2,1,0:T(8,128)(2,1)}, u32[]{:S(2)}) copy-start(bf16[1,2048,256]{2,1,0:T(8,128)(2,1)} %param.21) | copy-start | bytes 3145732
  91.4 56.2 %copy-start.2 = (bf16[1,2048,256]{2,1,0:T(8,128)(2,1)S(1)}, bf16[1,2048,256]{2,1,0:T(8,128)(2,1)}, u32[]{:S(2)}) copy-start(bf16[1,2048,256]{2,1,0:T(8,128)(2,1)} %param.22) | copy-start | bytes 3145732
  91.4 56.2 %copy-start.3 = (bf16[1,256,2048]{2,1,0:T(8,128)(2,1)S(1)}, bf16[1,256,2048]{2,1,0:T(8,128)(2,1)}, u32[]{:S(2)}) copy-start(bf16[1,256,2048]{2,1,0:T(8,128)(2,1)} %param.23) | copy-start | bytes 3145732
  111.0 12.9 %collective-permute-start.1 = (bf16[1296,128]{1,0:T(8,128)(2,1)S(1)}, bf16[1296,128]{1,0:T(8,128)(2,1)S(1)}, u32[]{:S(2)}, u32[]{:S(2)}) collective-permute-start(bf16[1296,128]{1,0:T(8,128)(2,1)S(1)} %get-tuple-element.26.refs_0_), channel_id=1, source_target_pairs={{0,14},{2,0},{4,2},{6,4},{8,6},{10,8},{12,10},{14,12},{1,15},{3,1}... | collective-permute-start | bytes 995336 | tf_op jit(solution)/shard_map/ppermute | solution.py:269
  113.0 12.8 %collective-permute-start = (bf16[1296,128]{1,0:T(8,128)(2,1)S(1)}, bf16[1296,128]{1,0:T(8,128)(2,1)S(1)}, u32[]{:S(2)}, u32[]{:S(2)}) collective-permute-start(bf16[1296,128]{1,0:T(8,128)(2,1)S(1)} %get-tuple-element.26.refs_0_), channel_id=1, source_target_pairs={{0,2},{2,4},{4,6},{6,8},{8,10},{10,12},{12,14},{14,0},{1,3},{3,5},... | collective-permute-start | bytes 995336 | tf_op jit(solution)/shard_map/ppermute | solution.py:269
  116.3 19.6 %collective-permute-start.2 = (bf16[656,128]{1,0:T(8,128)(2,1)S(1)}, bf16[656,128]{1,0:T(8,128)(2,1)S(1)}, u32[]{:S(2)}, u32[]{:S(2)}) collective-permute-start(bf16[656,128]{1,0:T(8,128)(2,1)S(1)} %get-tuple-element.27), channel_id=1, source_target_pairs={{0,4},{2,6},{4,8},{6,10},{8,12},{10,14},{12,0},{14,2},{1,5},{3,7},... | collective-permute-start | bytes 503816 | tf_op jit(solution)/shard_map/ppermute | solution.py:269
  119.2 28.3 %collective-permute-start.4 = (bf16[1296,128]{1,0:T(8,128)(2,1)S(1)}, bf16[1296,128]{1,0:T(8,128)(2,1)S(1)}, u32[]{:S(2)}, u32[]{:S(2)}) collective-permute-start(bf16[1296,128]{1,0:T(8,128)(2,1)S(1)} %get-tuple-element.26.refs_0_), channel_id=1, source_target_pairs={{0,1},{1,0},{2,3},{3,2},{4,5},{5,4},{6,7},{7,6},{8,9},{9,8},{10,11... | collective-permute-start | bytes 995336 | tf_op jit(solution)/shard_map/ppermute | solution.py:337
  123.9 23.6 %collective-permute-start.6 = (bf16[1296,128]{1,0:T(8,128)(2,1)S(1)}, bf16[1296,128]{1,0:T(8,128)(2,1)S(1)}, u32[]{:S(2)}, u32[]{:S(2)}) collective-permute-start(bf16[1296,128]{1,0:T(8,128)(2,1)S(1)} %collective-permute-done.1.refs_2_), channel_id=1, source_target_pairs={{0,1},{1,0},{2,3},{3,2},{4,5},{5,4},{6,7},{7,6},{8,9},{9,8},{10,11... | collective-permute-start | bytes 995336 | tf_op jit(solution)/shard_map/ppermute | solution.py:337
  125.9 21.7 %collective-permute-start.5 = (bf16[1296,128]{1,0:T(8,128)(2,1)S(1)}, bf16[1296,128]{1,0:T(8,128)(2,1)S(1)}, u32[]{:S(2)}, u32[]{:S(2)}) collective-permute-start(bf16[1296,128]{1,0:T(8,128)(2,1)S(1)} %collective-permute-done.refs_1_), channel_id=1, source_target_pairs={{0,1},{1,0},{2,3},{3,2},{4,5},{5,4},{6,7},{7,6},{8,9},{9,8},{10,11... | collective-permute-start | bytes 995336 | tf_op jit(solution)/shard_map/ppermute | solution.py:337
  131.8 12.3 %collective-permute-start.3 = (bf16[640,128]{1,0:T(8,128)(2,1)S(1)}, bf16[640,128]{1,0:T(8,128)(2,1)S(1)}, u32[]{:S(2)}, u32[]{:S(2)}) collective-permute-start(bf16[640,128]{1,0:T(8,128)(2,1)S(1)} %get-tuple-element.28), channel_id=1, source_target_pairs={{0,12},{2,14},{4,0},{6,2},{8,4},{10,6},{12,8},{14,10},{1,13},{3,15... | collective-permute-start | bytes 491528 | tf_op jit(solution)/shard_map/ppermute | solution.py:269
  135.9 11.7 %collective-permute-start.7 = (bf16[656,128]{1,0:T(8,128)(2,1)S(1)}, bf16[656,128]{1,0:T(8,128)(2,1)S(1)}, u32[]{:S(2)}, u32[]{:S(2)}) collective-permute-start(bf16[656,128]{1,0:T(8,128)(2,1)S(1)} %collective-permute-done.2.refs_3_), channel_id=1, source_target_pairs={{0,1},{1,0},{2,3},{3,2},{4,5},{5,4},{6,7},{7,6},{8,9},{9,8},{10,11... | collective-permute-start | bytes 503816 | tf_op jit(solution)/shard_map/ppermute | solution.py:337
  144.2 3.4 %collective-permute-start.8 = (bf16[640,128]{1,0:T(8,128)(2,1)S(1)}, bf16[640,128]{1,0:T(8,128)(2,1)S(1)}, u32[]{:S(2)}, u32[]{:S(2)}) collective-permute-start(bf16[640,128]{1,0:T(8,128)(2,1)S(1)} %collective-permute-done.3.refs_4_), channel_id=1, source_target_pairs={{0,1},{1,0},{2,3},{3,2},{4,5},{5,4},{6,7},{7,6},{8,9},{9,8},{10,11... | collective-permute-start | bytes 491528 | tf_op jit(solution)/shard_map/ppermute | solution.py:337
  150.6 4.9 %collective-permute-start.9 = (bf16[8,640,128]{2,1,0:T(8,128)(2,1)S(1)}, bf16[8,640,128]{2,1,0:T(8,128)(2,1)S(1)}, u32[]{:S(2)}, u32[]{:S(2)}) collective-permute-start(bf16[8,640,128]{2,1,0:T(8,128)(2,1)S(1)} %get-tuple-element.30), channel_id=1, source_target_pairs={{0,1},{1,0},{2,3},{3,2},{4,5},{5,4},{6,7},{7,6},{8,9},{9,8},{10,11... | collective-permute-start | bytes 3932168 | tf_op jit(solution)/shard_map/ppermute | solution.py:347
  194.7 13.9 %copy-start.5 = (f32[256,2]{0,1:T(2,128)S(1)}, f32[256,2]{0,1:T(2,128)}, u32[]{:S(2)}) copy-start(f32[256,2]{0,1:T(2,128)} %param.20) | copy-start | bytes 6148

commit v3 on v2

--- a/solution.py
+++ b/solution.py
@@ -52,18 +52,20 @@
     return hi, mid, rest - mid
 
 
-def attend(at_ref, q_ref, kv_ref, gate_ref, out_ref, keys_ref, vals_ref):
+def attend(at_ref, q_ref, kv0_ref, kv1_ref, kv2_ref, kv3_ref, gate_ref, out_ref, keys_ref, vals_ref):
     z, x = at_ref[0], at_ref[1]
-    first = gate_ref[0:1, 0:1]
+    first = gate_ref[:, pl.ds(pl.multiple_of(z * KEYS, KEYS), TOK)][:, 0:1]
     row64 = lax.broadcasted_iota(jnp.int32, (HD, TOK), 0)
-    for j in range(NX):
-        bias = first - gate_ref[j : j + 1, :]
+    for j, kv_ref in enumerate((kv0_ref, kv1_ref, kv2_ref, kv3_ref)):
+        where = lax.rem(x + NX - j, NX)
+        place = pl.multiple_of(where * TOK, TOK)
+        bias = first - gate_ref[:, pl.ds(pl.multiple_of(z * KEYS + where * TOK, TOK), TOK)]
         hi, mid, lo = three(bias)
         extra = jnp.where(row64 == 0, hi, jnp.where(row64 == 1, mid, jnp.where(row64 == 2, lo, 0.0)))
-        both = jnp.concatenate([kv_ref[j, 0:HD, :], extra.astype(bf)], axis=0)
-        keys_ref[j * TOK : (j + 1) * TOK, :] = both.T
-        vals_ref[0:HD, j * TOK : (j + 1) * TOK] = kv_ref[j, HD : 2 * HD, :]
-        vals_ref[HD : HD + 16, j * TOK : (j + 1) * TOK] = jnp.ones((16, TOK), bf)
+        both = jnp.concatenate([kv_ref[0:HD, :], extra.astype(bf)], axis=0)
+        keys_ref[pl.ds(place, TOK), :] = both.T
+        vals_ref[0:HD, pl.ds(place, TOK)] = kv_ref[HD : 2 * HD, :]
+        vals_ref[HD : HD + 16, pl.ds(place, TOK)] = jnp.ones((16, TOK), bf)
     ones = jnp.where(row64 < 3, 1.0, 0.0).astype(bf)
     row16 = lax.broadcasted_iota(jnp.int32, (16, TOK), 0)
 
@@ -99,11 +101,13 @@
     lax.fori_loop(0, z, earlier, 0)
 
 
-def merge(part_ref, off_ref, out_ref):
+def merge(at_ref, part_ref, gate_ref, out_ref):
     ls = []
+    place = pl.multiple_of(at_ref[0] * KEYS + at_ref[1] * TOK, TOK)
+    mine = gate_ref[:, pl.ds(place, TOK)]
     for i in range(NZ):
         st = part_ref[i, HD : HD + 16, :].astype(f32)
-        ls.append(st[0:1] + st[1:2] + st[2:3] + off_ref[i : i + 1, :])
+        ls.append(st[0:1] + st[1:2] + st[2:3] + (mine - gate_ref[:, i * KEYS : i * KEYS + 1]))
     m = ls[0]
     for v in ls[1:]:
         m = jnp.maximum(m, v)
@@ -114,6 +118,14 @@
         total = total + w
         acc = acc + w * part_ref[i, 0:HD, :].astype(f32)
     out_ref[...] = (acc / total).astype(bf)
+
+
+def spread_weight(w_ref, out_ref):
+    for y in range(NY):
+        for c in range(NC):
+            for q in range(2):
+                block = (y % (NY // 2) + q * (NY // 2)) * NC + c
+                out_ref[y * NC + c, q * HD : (q + 1) * HD, :] = w_ref[:, block * COLS : (block + 1) * COLS]
 
 
 def project(at_ref, att_ref, w_ref, resid_ref, gain_ref, routes_ref, stream_ref, out_ref, slots_ref):
@@ -195,8 +207,11 @@
 
 
 def experts(at_ref, *refs):
-    owns, others = refs[0:5], refs[5:10]
-    wg_ref, wu_ref, wd_ref, mine_ref, theirs_ref, g_ref, u_ref, h_ref = refs[10:]
+    every, near, far = refs[5:8]
+    rows = 2 * ROWS + META
+    owns = refs[0:5]
+    others = (every, near.at[0:rows], near.at[rows:], far.at[0 : ROWS + META], far.at[ROWS + META :])
+    wg_ref, wu_ref, wd_ref, mine_ref, theirs_ref, g_ref, u_ref, h_ref = refs[8:]
     y, c = at_ref[0], at_ref[1]
     total = jnp.zeros((8, COLS), f32)
     for pieces in (owns, others):
@@ -290,29 +305,25 @@
     z, x, y, c = (lax.axis_index(a) for a in ("z", "x", "y", "c"))
     sds = jax.ShapeDtypeStruct
     half = NY // 2
-    w = out_weight.reshape(HD, 2, half, NC, COLS).transpose(2, 3, 1, 0, 4).reshape(NTP // 2, 2 * HD, COLS)
-    w_cols = exchange(jnp.concatenate([w, w], axis=0), TP)
     low = (lax.rem(y, half) * NC + c) * COLS
     at_cols = jnp.stack([low, low + half * NC * COLS, y // half]).astype(jnp.int32)
-    gate_keys = lax.dynamic_slice_in_dim(cum_gate[0], z * KEYS, KEYS, 0).reshape(NX, TOK)
-    firsts = cum_gate.reshape(NZ, KEYS)[:, 0:1]
-    offset = lax.dynamic_slice_in_dim(cum_gate, (z * NX + x) * TOK, TOK, 1) - firsts
-
-    kv = to_all(jnp.concatenate([keys.T, values.T], axis=0), "x")
     at = jnp.stack([z, x]).astype(jnp.int32)
-    q_send, kv, gate_keys, at, offset, at_cols = lax.optimization_barrier(
-        (jnp.broadcast_to(queries.T[None], (NZ, HD, TOK)), kv, gate_keys, at, offset, at_cols)
-    )
-    q = exchange(q_send, "z")
+    q = to_all(queries.T, "z")
+    w_send = call(spread_weight, sds((NTP, 2 * HD, COLS), bf), (out_weight,))
+    w_cols = exchange(w_send, TP)
+    kv = [jnp.concatenate([keys.T, values.T], axis=0)]
+    for n in range(1, NX):
+        kv.append(lax.ppermute(kv[0], "x", [(i, (i + n) % NX) for i in range(NX)]))
     parts = call(
         attend,
         sds((NZ, HD + 16, TOK), bf),
-        (at, q, kv, gate_keys),
+        (at, q, *kv, cum_gate),
         smem=1,
         scratch=(pltpu.VMEM((KEYS, 2 * HD), bf), pltpu.VMEM((HD + 16, KEYS), bf)),
     )
+    parts, w_cols = lax.optimization_barrier((parts, w_cols))
     parts = exchange(parts, "z")
-    attended = call(merge, sds((HD, TOK), bf), (parts, offset))
+    attended = call(merge, sds((HD, TOK), bf), (at, parts, cum_gate), smem=1)
     attended = lax.all_gather(attended, TP, axis=0, tiled=True)
     stream, outgoing, slots = call(
         project,
@@ -333,7 +344,7 @@
     for v, by in ((every, 1), (every, -1), (lower, 2), (higher, -2)):
         owns.append(shift(v, by))
     others = []
-    for v in owns:
+    for v in (every, jnp.concatenate(owns[1:3], axis=0), jnp.concatenate(owns[3:5], axis=0)):
         others.append(lax.ppermute(v, "c", swap))
     big = sds((NY, ROWS, COLS), bf)
     mine, theirs = call(

time: 211 us -> 201 us (0.953)
  blocking collectives: 116 us -> 93.9 us
  waiting for transfers between devices: 20.3 us -> 29 us
  starting transfers between devices: 51.5 us -> 57.3 us
  other arithmetic: 3.73 us -> 0.65 us
    all_to_all x4 -> x3, blocking collectives: 89.2 us -> 72.9 us  [exchange(): return lax.all_to_all(v, axis, 0, 0, tiled=True)]
    ppermute x0 -> x3, starting transfers between devices: none -> 9.46 us  [layer(): kv.append(lax.ppermute(kv[0], 'x', [(i, (i + n) % NX) for i in range(NX)]))]
    ppermute x5 -> x3, starting transfers between devices: 17.1 us -> 10.1 us  [layer(): others.append(lax.ppermute(v, 'c', swap))]
    all_to_all x1, waiting for transfers between devices: 1.74 us -> 8.65 us  [to_all(): lax.all_to_all(jnp.broadcast_to(v[None], (n, *v.shape)), axis, 0, 0, tile...]
    all_gather x1, blocking collectives: 27.2 us -> 20.9 us  [layer(): attended = lax.all_gather(attended, TP, axis=0, tiled=True)]
    all_to_all x1, starting transfers between devices: 4.83 us -> 11 us  [to_all(): lax.all_to_all(jnp.broadcast_to(v[None], (n, *v.shape)), axis, 0, 0, tile...]
    ppermute x4, waiting for transfers between devices: 6.1 us -> 1.53 us  [shift(): return lax.ppermute(v, 'y', [(i, (i + by) % NY) for i in range(NY)])]
    ppermute x0 -> x3, waiting for transfers between devices: none -> 3.91 us  [layer(): kv.append(lax.ppermute(kv[0], 'x', [(i, (i + n) % NX) for i in range(NX)]))]
  transfers between devices with their start and end apart: 13 -> 14, of which waited for: 5 -> 7; matrix products, arithmetic and copies ran while one was open for 2% -> 0% of each run, Pallas kernels for 0% -> 4%
where the time goes in v3:
time: 201 us; the launch traced here: 199 us
  blocking collectives  93.9 us (47%)
  starting transfers between devices  57.3 us (29%)
  waiting for transfers between devices  29 us (14%)
  Pallas kernels  15.4 us (8%)
  local copies, waits for them, and re-layouts  2.5 us (1%)
    all_to_all x3, blocking collectives, exchange(): return lax.all_to_all(v, axis, 0, 0, tiled=True)  72.9 us
    all_gather x1, blocking collectives, layer(): attended = lax.all_gather(attended, TP, axis=0, tiled=True)  20.9 us
    pallas_call x8, Pallas kernels, call(): pl.pallas_call(body, out_shape=out_shape, in_specs=specs, out_specs=tuple...  15.4 us
    all_to_all x2, starting transfers between devices, exchange(): return lax.all_to_all(v, axis, 0, 0, tiled=True)  12.9 us
    ppermute x4, starting transfers between devices, shift(): return lax.ppermute(v, 'y', [(i, (i + by) % NY) for i in range(NY)])  11.6 us
    all_to_all x2, waiting for transfers between devices, exchange(): return lax.all_to_all(v, axis, 0, 0, tiled=True)  11.1 us
    all_to_all x1, starting transfers between devices, to_all(): lax.all_to_all(jnp.broadcast_to(v[None], (n, *v.shape)), axis, 0, 0, tile...  11 us
    ppermute x3, starting transfers between devices, layer(): others.append(lax.ppermute(v, 'c', swap))  10.1 us
  transfers between devices with their start and end apart: 14, of which 7 were waited for; matrix products, arithmetic and copies ran while one was open for 0% of the time, Pallas kernels for 4%

profile of v3, /device:TPU:1, one launch (start us, length us, event | category | flops | bytes accessed | tf_op | source)
XLA Modules:
  0.0 198.9 jit_solution(969794671322773849)
XLA Ops:
  0.0 1.5 broadcast_in_dim.2
  1.5 11.0 %all-to-all-start = ((bf16[8,64,256]{2,1,0:T(8,128)(2,1)}), bf16[8,64,256]{2,1,0:T(8,128)(2,1)S(1)}, u32[]{:S(2)}, u32[]{:S(2)}) async-start(bf16[8,64,256]{2,1,0:T(8,128)(2,1)} %broadcast_in_dim.2), calls=%async_computation | async-start | bytes 524288 | tf_op jit(solution)/shard_map/all_to_all | solution.py:280
  12.5 0.9 copy-done.4
  13.4 0.9 shard_map.119
  14.3 8.7 %all-to-all-done.q_ref = bf16[8,64,256]{2,1,0:T(8,128)(2,1)S(1)} async-done(((bf16[8,64,256]{2,1,0:T(8,128)(2,1)}), bf16[8,64,256]{2,1,0:T(8,128)(2,1)S(1)}, u32[]{:S(2)}, u32[]{:S(2)}) %all-to-all-start) | async-done | bytes 262176 | tf_op jit(solution)/shard_map/all_to_all | solution.py:280
  23.0 9.4 %all-to-all-start.1 = ((bf16[16,128,128]{2,1,0:T(8,128)(2,1)}), bf16[16,128,128]{2,1,0:T(8,128)(2,1)S(1)}, u32[]{:S(2)}, u32[]{:S(2)}) async-start(bf16[16,128,128]{2,1,0:T(8,128)(2,1)} %shard_map.119), calls=%async_computation.1 | async-start | bytes 1048576 | tf_op jit(solution)/shard_map/all_to_all | solution.py:288
  32.5 4.5 %collective-permute-start.2 = (bf16[128,256]{1,0:T(8,128)(2,1)S(1)}, bf16[128,256]{1,0:T(8,128)(2,1)S(1)}, u32[]{:S(2)}, u32[]{:S(2)}) collective-permute-start(bf16[128,256]{1,0:T(8,128)(2,1)S(1)} %pad_maximum_fusion.2.kv0_ref), channel_id=1, source_target_pairs={{0,48},{16,0},{32,16},{48,32},{1,49},{17,1},{33,17},{49,33},{2,50}... | collective-permute-start | bytes 196616 | tf_op jit(solution)/shard_map/ppermute | solution.py:316
  37.0 2.4 %collective-permute-start.1 = (bf16[128,256]{1,0:T(8,128)(2,1)S(1)}, bf16[128,256]{1,0:T(8,128)(2,1)S(1)}, u32[]{:S(2)}, u32[]{:S(2)}) collective-permute-start(bf16[128,256]{1,0:T(8,128)(2,1)S(1)} %pad_maximum_fusion.2.kv0_ref), channel_id=1, source_target_pairs={{0,32},{16,48},{32,0},{48,16},{1,33},{17,49},{33,1},{49,17},{2,34}... | collective-permute-start | bytes 196616 | tf_op jit(solution)/shard_map/ppermute | solution.py:316
  39.5 2.5 %collective-permute-start = (bf16[128,256]{1,0:T(8,128)(2,1)S(1)}, bf16[128,256]{1,0:T(8,128)(2,1)S(1)}, u32[]{:S(2)}, u32[]{:S(2)}) collective-permute-start(bf16[128,256]{1,0:T(8,128)(2,1)S(1)} %pad_maximum_fusion.2.kv0_ref), channel_id=1, source_target_pairs={{0,16},{16,32},{32,48},{48,0},{1,17},{17,33},{33,49},{49,1},{2,18}... | collective-permute-start | bytes 196616 | tf_op jit(solution)/shard_map/ppermute | solution.py:316
  42.1 1.8 collective-permute-done.1.kv2_ref
  43.8 2.1 %collective-permute-done.kv1_ref = bf16[128,256]{1,0:T(8,128)(2,1)S(1)} collective-permute-done((bf16[128,256]{1,0:T(8,128)(2,1)S(1)}, bf16[128,256]{1,0:T(8,128)(2,1)S(1)}, u32[]{:S(2)}, u32[]{:S(2)}) %collective-permute-start) | collective-permute-done | bytes 65568 | tf_op jit(solution)/shard_map/ppermute | solution.py:316
  46.0 7.2 %shard_map.118 = bf16[8,80,256]{2,1,0:T(8,128)(2,1)} custom-call(s32[2]{0:T(128)S(1)} %pad_add_fusion.2.at_ref, bf16[8,64,256]{2,1,0:T(8,128)(2,1)S(1)} %all-to-all-done.q_ref, bf16[128,256]{1,0:T(8,128)(2,1)S(1)} %pad_maximum_fusion.2.kv0_ref, bf16[128,256]{1,0:T(8,128)(2,1)S(1)} %collective-permute-done.kv1_ref, ...), custom_call_target="tpu_custom_call" | custom-call | tf_op jit(solution)/shard_map/pallas_call | solution.py:37
  53.2 3.4 %all-to-all-start.2 = ((bf16[8,80,256]{2,1,0:T(8,128)(2,1)}), bf16[8,80,256]{2,1,0:T(8,128)(2,1)S(1)}, u32[]{:S(2)}, u32[]{:S(2)}) async-start(bf16[8,80,256]{2,1,0:T(8,128)(2,1)} %shard_map.118), calls=%async_computation.2 | async-start | bytes 655360 | tf_op jit(solution)/shard_map/all_to_all | solution.py:288
  56.7 11.1 %all-to-all-done.2.part_ref = bf16[8,80,256]{2,1,0:T(8,128)(2,1)S(1)} async-done(((bf16[8,80,256]{2,1,0:T(8,128)(2,1)}), bf16[8,80,256]{2,1,0:T(8,128)(2,1)S(1)}, u32[]{:S(2)}, u32[]{:S(2)}) %all-to-all-start.2) | async-done | bytes 327712 | tf_op jit(solution)/shard_map/all_to_all | solution.py:288
  68.4 20.9 %all_gather.3.att_ref = bf16[1024,256]{1,0:T(8,128)(2,1)S(1)} all-gather(bf16[64,256]{1,0:T(8,128)(2,1)S(1)} %shard_map.120), channel_id=1, replica_groups=mesh['z'=8,'x'=4,'y'=8,'c'=2] {'y','c'}, dimensions={0}, use_global_device_ids=true | all-gather | bytes 557056 | tf_op jit(solution)/shard_map/all_gather | solution.py:327
  89.4 2.0 shard_map.121
  91.4 17.5 %all_to_all.30.in_ref = bf16[32,48,128]{2,1,0:T(8,128)(2,1)S(1)} all-to-all(bf16[32,48,128]{2,1,0:T(8,128)(2,1)S(1)} %get-tuple-element.17), channel_id=1, replica_groups=mesh['z'=8,'x'=4,'y'=8,'c'=2] {'z','x'}, dimensions={0} | all-to-all | bytes 786432 | tf_op jit(solution)/shard_map/all_to_all | solution.py:288
  109.1 2.9 %collective-permute-start.4 = (bf16[1296,128]{1,0:T(8,128)(2,1)S(1)}, bf16[1296,128]{1,0:T(8,128)(2,1)S(1)}, u32[]{:S(2)}, u32[]{:S(2)}) collective-permute-start(bf16[1296,128]{1,0:T(8,128)(2,1)S(1)} %get-tuple-element.18.refs_0_), channel_id=1, source_target_pairs={{0,14},{2,0},{4,2},{6,4},{8,6},{10,8},{12,10},{14,12},{1,15},{3,1}... | collective-permute-start | bytes 995336 | tf_op jit(solution)/shard_map/ppermute | solution.py:284
  112.0 2.5 %collective-permute-start.3 = (bf16[1296,128]{1,0:T(8,128)(2,1)S(1)}, bf16[1296,128]{1,0:T(8,128)(2,1)S(1)}, u32[]{:S(2)}, u32[]{:S(2)}) collective-permute-start(bf16[1296,128]{1,0:T(8,128)(2,1)S(1)} %get-tuple-element.18.refs_0_), channel_id=1, source_target_pairs={{0,2},{2,4},{4,6},{6,8},{8,10},{10,12},{12,14},{14,0},{1,3},{3,5},... | collective-permute-start | bytes 995336 | tf_op jit(solution)/shard_map/ppermute | solution.py:284
  114.5 3.7 %collective-permute-start.6 = (bf16[640,128]{1,0:T(8,128)(2,1)S(1)}, bf16[640,128]{1,0:T(8,128)(2,1)S(1)}, u32[]{:S(2)}, u32[]{:S(2)}) collective-permute-start(bf16[640,128]{1,0:T(8,128)(2,1)S(1)} %get-tuple-element.20), channel_id=1, source_target_pairs={{0,12},{2,14},{4,0},{6,2},{8,4},{10,6},{12,8},{14,10},{1,13},{3,15... | collective-permute-start | bytes 491528 | tf_op jit(solution)/shard_map/ppermute | solution.py:284
  118.2 2.5 %collective-permute-start.5 = (bf16[656,128]{1,0:T(8,128)(2,1)S(1)}, bf16[656,128]{1,0:T(8,128)(2,1)S(1)}, u32[]{:S(2)}, u32[]{:S(2)}) collective-permute-start(bf16[656,128]{1,0:T(8,128)(2,1)S(1)} %get-tuple-element.19), channel_id=1, source_target_pairs={{0,4},{2,6},{4,8},{6,10},{8,12},{10,14},{12,0},{14,2},{1,5},{3,7},... | collective-permute-start | bytes 503816 | tf_op jit(solution)/shard_map/ppermute | solution.py:284
  120.7 1.5 collective-permute-done.3.refs_1_
  122.3 5.0 %collective-permute-start.8 = (bf16[2592,128]{1,0:T(8,128)(2,1)S(1)}, bf16[2592,128]{1,0:T(8,128)(2,1)S(1)}, u32[]{:S(2)}, u32[]{:S(2)}) collective-permute-start(bf16[2592,128]{1,0:T(8,128)(2,1)S(1)} %pad_maximum_fusion), channel_id=1, source_target_pairs={{0,1},{1,0},{2,3},{3,2},{4,5},{5,4},{6,7},{7,6},{8,9},{9,8},{10,11... | collective-permute-start | bytes 1990664 | tf_op jit(solution)/shard_map/ppermute | solution.py:348
  127.3 1.9 collective-permute-start.7
  129.2 3.2 %collective-permute-start.9 = (bf16[1296,128]{1,0:T(8,128)(2,1)S(1)}, bf16[1296,128]{1,0:T(8,128)(2,1)S(1)}, u32[]{:S(2)}, u32[]{:S(2)}) collective-permute-start(bf16[1296,128]{1,0:T(8,128)(2,1)S(1)} %pad_maximum_fusion.1), channel_id=1, source_target_pairs={{0,1},{1,0},{2,3},{3,2},{4,5},{5,4},{6,7},{7,6},{8,9},{9,8},{10,11... | collective-permute-start | bytes 995336 | tf_op jit(solution)/shard_map/ppermute | solution.py:348
  132.5 1.2 collective-permute-done.9.refs_7_
  133.7 3.0 %shard_map.123 = (bf16[8,640,128]{2,1,0:T(8,128)(2,1)S(1)}, bf16[8,640,128]{2,1,0:T(8,128)(2,1)S(1)}) custom-call(s32[2]{0:T(128)S(1)} %pad_add_fusion.at_ref, bf16[1296,128]{1,0:T(8,128)(2,1)S(1)} %get-tuple-element.18.refs_0_, bf16[1296,128]{1,0:T(8,128)(2,1)S(1)} %collective-permute-done.3.refs_1_, bf16[1296,128]{1,0:T(8,128)(2,1)S(1)} %collective-permute-done.4.refs_2_, ...), custom_call_target="tpu_custom_call" | custom-call | tf_op jit(solution)/shard_map/pallas_call | solution.py:37
  136.7 2.3 %collective-permute-start.10 = (bf16[8,640,128]{2,1,0:T(8,128)(2,1)S(1)}, bf16[8,640,128]{2,1,0:T(8,128)(2,1)S(1)}, u32[]{:S(2)}, u32[]{:S(2)}) collective-permute-start(bf16[8,640,128]{2,1,0:T(8,128)(2,1)S(1)} %get-tuple-element.22), channel_id=1, source_target_pairs={{0,1},{1,0},{2,3},{3,2},{4,5},{5,4},{6,7},{7,6},{8,9},{9,8},{10,11... | collective-permute-start | bytes 3932168 | tf_op jit(solution)/shard_map/ppermute | solution.py:358
  139.0 2.6 %collective-permute-done.10 = bf16[8,640,128]{2,1,0:T(8,128)(2,1)S(1)} collective-permute-done((bf16[8,640,128]{2,1,0:T(8,128)(2,1)S(1)}, bf16[8,640,128]{2,1,0:T(8,128)(2,1)S(1)}, u32[]{:S(2)}, u32[]{:S(2)}) %collective-permute-start.10) | collective-permute-done | bytes 1310752 | tf_op jit(solution)/shard_map/ppermute | solution.py:358
  142.0 40.8 %all_to_all.31.in_ref = bf16[8,640,128]{2,1,0:T(8,128)(2,1)S(1)} all-to-all(bf16[8,640,128]{2,1,0:T(8,128)(2,1)S(1)} %add_convert_fusion), channel_id=1, replica_groups=mesh['z'=8,'x'=4,'y'=8,'c'=2] {'y'}, dimensions={0} | all-to-all | bytes 2621440 | tf_op jit(solution)/shard_map/all_to_all | solution.py:288
  183.1 14.6 %all_to_all.32 = bf16[32,24,128]{2,1,0:T(8,128)(2,1)S(1)} all-to-all(bf16[32,24,128]{2,1,0:T(8,128)(2,1)S(1)} %shard_map.124), channel_id=1, replica_groups=mesh['z'=8,'x'=4,'y'=8,'c'=2] {'z','x'}, dimensions={0} | all-to-all | bytes 393216 | tf_op jit(solution)/shard_map/all_to_all | solution.py:288
  197.7 1.2 shard_map.125
  (38 shorter events, 1.8 us)
Async XLA Ops:
  0.0 32.4 %copy-start.9 = (bf16[256,64]{0,1:T(8,128)(2,1)S(1)}, bf16[256,64]{0,1:T(8,128)(2,1)}, u32[]{:S(2)}) copy-start(bf16[256,64]{0,1:T(8,128)(2,1)} %param.14) | copy-start | bytes 98308
  0.0 32.4 %copy-start.10 = (bf16[256,64]{0,1:T(8,128)(2,1)S(1)}, bf16[256,64]{0,1:T(8,128)(2,1)}, u32[]{:S(2)}) copy-start(bf16[256,64]{0,1:T(8,128)(2,1)} %param.13) | copy-start | bytes 98308
  1.5 44.5 %copy-start.5 = (f32[1,8192]{1,0:T(1,128)S(1)}, f32[1,8192]{1,0:T(1,128)}, u32[]{:S(2)}) copy-start(f32[1,8192]{1,0:T(1,128)} %gate_ref.3) | copy-start | bytes 98308
  1.5 21.5 %all-to-all-start = ((bf16[8,64,256]{2,1,0:T(8,128)(2,1)}), bf16[8,64,256]{2,1,0:T(8,128)(2,1)S(1)}, u32[]{:S(2)}, u32[]{:S(2)}) async-start(bf16[8,64,256]{2,1,0:T(8,128)(2,1)} %broadcast_in_dim.2), calls=%async_computation | async-start | bytes 524288 | tf_op jit(solution)/shard_map/all_to_all | solution.py:280
  12.5 0.9 copy-start.4
  23.0 30.2 %all-to-all-start.1 = ((bf16[16,128,128]{2,1,0:T(8,128)(2,1)}), bf16[16,128,128]{2,1,0:T(8,128)(2,1)S(1)}, u32[]{:S(2)}, u32[]{:S(2)}) async-start(bf16[16,128,128]{2,1,0:T(8,128)(2,1)} %shard_map.119), calls=%async_computation.1 | async-start | bytes 1048576 | tf_op jit(solution)/shard_map/all_to_all | solution.py:288
  32.5 56.9 %copy-start = (bf16[256,2048]{1,0:T(8,128)(2,1)S(1)}, bf16[256,2048]{1,0:T(8,128)(2,1)}, u32[]{:S(2)}) copy-start(bf16[256,2048]{1,0:T(8,128)(2,1)} %resid_ref.1) | copy-start | bytes 3145732
  32.5 56.9 %copy-start.6 = (f32[2048]{0:T(1024)S(1)}, f32[2048]{0:T(1024)}, u32[]{:S(2)}) copy-start(f32[2048]{0:T(1024)} %param.18) | copy-start | bytes 24580
  32.5 56.9 %copy-start.8 = (s32[256,2]{0,1:T(2,128)S(1)}, s32[256,2]{0,1:T(2,128)}, u32[]{:S(2)}) copy-start(s32[256,2]{0,1:T(2,128)} %param.19) | copy-start | bytes 6148
  32.5 9.6 %collective-permute-start.2 = (bf16[128,256]{1,0:T(8,128)(2,1)S(1)}, bf16[128,256]{1,0:T(8,128)(2,1)S(1)}, u32[]{:S(2)}, u32[]{:S(2)}) collective-permute-start(bf16[128,256]{1,0:T(8,128)(2,1)S(1)} %pad_maximum_fusion.2.kv0_ref), channel_id=1, source_target_pairs={{0,48},{16,0},{32,16},{48,32},{1,49},{17,1},{33,17},{49,33},{2,50}... | collective-permute-start | bytes 196616 | tf_op jit(solution)/shard_map/ppermute | solution.py:316
  37.0 6.8 %collective-permute-start.1 = (bf16[128,256]{1,0:T(8,128)(2,1)S(1)}, bf16[128,256]{1,0:T(8,128)(2,1)S(1)}, u32[]{:S(2)}, u32[]{:S(2)}) collective-permute-start(bf16[128,256]{1,0:T(8,128)(2,1)S(1)} %pad_maximum_fusion.2.kv0_ref), channel_id=1, source_target_pairs={{0,32},{16,48},{32,0},{48,16},{1,33},{17,49},{33,1},{49,17},{2,34}... | collective-permute-start | bytes 196616 | tf_op jit(solution)/shard_map/ppermute | solution.py:316
  39.5 6.5 %collective-permute-start = (bf16[128,256]{1,0:T(8,128)(2,1)S(1)}, bf16[128,256]{1,0:T(8,128)(2,1)S(1)}, u32[]{:S(2)}, u32[]{:S(2)}) collective-permute-start(bf16[128,256]{1,0:T(8,128)(2,1)S(1)} %pad_maximum_fusion.2.kv0_ref), channel_id=1, source_target_pairs={{0,16},{16,32},{32,48},{48,0},{1,17},{17,33},{33,49},{49,1},{2,18}... | collective-permute-start | bytes 196616 | tf_op jit(solution)/shard_map/ppermute | solution.py:316
  53.2 14.6 %all-to-all-start.2 = ((bf16[8,80,256]{2,1,0:T(8,128)(2,1)}), bf16[8,80,256]{2,1,0:T(8,128)(2,1)S(1)}, u32[]{:S(2)}, u32[]{:S(2)}) async-start(bf16[8,80,256]{2,1,0:T(8,128)(2,1)} %shard_map.118), calls=%async_computation.2 | async-start | bytes 655360 | tf_op jit(solution)/shard_map/all_to_all | solution.py:288
  91.4 42.3 %copy-start.3 = (bf16[1,256,2048]{2,1,0:T(8,128)(2,1)S(1)}, bf16[1,256,2048]{2,1,0:T(8,128)(2,1)}, u32[]{:S(2)}) copy-start(bf16[1,256,2048]{2,1,0:T(8,128)(2,1)} %param.23) | copy-start | bytes 3145732
  108.9 24.8 %copy-start.1 = (bf16[1,2048,256]{2,1,0:T(8,128)(2,1)S(1)}, bf16[1,2048,256]{2,1,0:T(8,128)(2,1)}, u32[]{:S(2)}) copy-start(bf16[1,2048,256]{2,1,0:T(8,128)(2,1)} %param.21) | copy-start | bytes 3145732
  108.9 24.8 %copy-start.2 = (bf16[1,2048,256]{2,1,0:T(8,128)(2,1)S(1)}, bf16[1,2048,256]{2,1,0:T(8,128)(2,1)}, u32[]{:S(2)}) copy-start(bf16[1,2048,256]{2,1,0:T(8,128)(2,1)} %param.22) | copy-start | bytes 3145732
  109.1 11.6 %collective-permute-start.4 = (bf16[1296,128]{1,0:T(8,128)(2,1)S(1)}, bf16[1296,128]{1,0:T(8,128)(2,1)S(1)}, u32[]{:S(2)}, u32[]{:S(2)}) collective-permute-start(bf16[1296,128]{1,0:T(8,128)(2,1)S(1)} %get-tuple-element.18.refs_0_), channel_id=1, source_target_pairs={{0,14},{2,0},{4,2},{6,4},{8,6},{10,8},{12,10},{14,12},{1,15},{3,1}... | collective-permute-start | bytes 995336 | tf_op jit(solution)/shard_map/ppermute | solution.py:284
  112.0 10.2 %collective-permute-start.3 = (bf16[1296,128]{1,0:T(8,128)(2,1)S(1)}, bf16[1296,128]{1,0:T(8,128)(2,1)S(1)}, u32[]{:S(2)}, u32[]{:S(2)}) collective-permute-start(bf16[1296,128]{1,0:T(8,128)(2,1)S(1)} %get-tuple-element.18.refs_0_), channel_id=1, source_target_pairs={{0,2},{2,4},{4,6},{6,8},{8,10},{10,12},{12,14},{14,0},{1,3},{3,5},... | collective-permute-start | bytes 995336 | tf_op jit(solution)/shard_map/ppermute | solution.py:284
  114.5 14.7 %collective-permute-start.6 = (bf16[640,128]{1,0:T(8,128)(2,1)S(1)}, bf16[640,128]{1,0:T(8,128)(2,1)S(1)}, u32[]{:S(2)}, u32[]{:S(2)}) collective-permute-start(bf16[640,128]{1,0:T(8,128)(2,1)S(1)} %get-tuple-element.20), channel_id=1, source_target_pairs={{0,12},{2,14},{4,0},{6,2},{8,4},{10,6},{12,8},{14,10},{1,13},{3,15... | collective-permute-start | bytes 491528 | tf_op jit(solution)/shard_map/ppermute | solution.py:284
  118.2 11.0 %collective-permute-start.5 = (bf16[656,128]{1,0:T(8,128)(2,1)S(1)}, bf16[656,128]{1,0:T(8,128)(2,1)S(1)}, u32[]{:S(2)}, u32[]{:S(2)}) collective-permute-start(bf16[656,128]{1,0:T(8,128)(2,1)S(1)} %get-tuple-element.19), channel_id=1, source_target_pairs={{0,4},{2,6},{4,8},{6,10},{8,12},{10,14},{12,0},{14,2},{1,5},{3,7},... | collective-permute-start | bytes 503816 | tf_op jit(solution)/shard_map/ppermute | solution.py:284
  122.3 11.4 %collective-permute-start.8 = (bf16[2592,128]{1,0:T(8,128)(2,1)S(1)}, bf16[2592,128]{1,0:T(8,128)(2,1)S(1)}, u32[]{:S(2)}, u32[]{:S(2)}) collective-permute-start(bf16[2592,128]{1,0:T(8,128)(2,1)S(1)} %pad_maximum_fusion), channel_id=1, source_target_pairs={{0,1},{1,0},{2,3},{3,2},{4,5},{5,4},{6,7},{7,6},{8,9},{9,8},{10,11... | collective-permute-start | bytes 1990664 | tf_op jit(solution)/shard_map/ppermute | solution.py:348
  127.3 5.2 %collective-permute-start.7 = (bf16[1296,128]{1,0:T(8,128)(2,1)S(1)}, bf16[1296,128]{1,0:T(8,128)(2,1)S(1)}, u32[]{:S(2)}, u32[]{:S(2)}) collective-permute-start(bf16[1296,128]{1,0:T(8,128)(2,1)S(1)} %get-tuple-element.18.refs_0_), channel_id=1, source_target_pairs={{0,1},{1,0},{2,3},{3,2},{4,5},{5,4},{6,7},{7,6},{8,9},{9,8},{10,11... | collective-permute-start | bytes 995336 | tf_op jit(solution)/shard_map/ppermute | solution.py:348
  129.2 4.4 %collective-permute-start.9 = (bf16[1296,128]{1,0:T(8,128)(2,1)S(1)}, bf16[1296,128]{1,0:T(8,128)(2,1)S(1)}, u32[]{:S(2)}, u32[]{:S(2)}) collective-permute-start(bf16[1296,128]{1,0:T(8,128)(2,1)S(1)} %pad_maximum_fusion.1), channel_id=1, source_target_pairs={{0,1},{1,0},{2,3},{3,2},{4,5},{5,4},{6,7},{7,6},{8,9},{9,8},{10,11... | collective-permute-start | bytes 995336 | tf_op jit(solution)/shard_map/ppermute | solution.py:348
  136.7 4.9 %collective-permute-start.10 = (bf16[8,640,128]{2,1,0:T(8,128)(2,1)S(1)}, bf16[8,640,128]{2,1,0:T(8,128)(2,1)S(1)}, u32[]{:S(2)}, u32[]{:S(2)}) collective-permute-start(bf16[8,640,128]{2,1,0:T(8,128)(2,1)S(1)} %get-tuple-element.22), channel_id=1, source_target_pairs={{0,1},{1,0},{2,3},{3,2},{4,5},{5,4},{6,7},{7,6},{8,9},{9,8},{10,11... | collective-permute-start | bytes 3932168 | tf_op jit(solution)/shard_map/ppermute | solution.py:358
  182.8 14.9 %copy-start.7 = (f32[256,2]{0,1:T(2,128)S(1)}, f32[256,2]{0,1:T(2,128)}, u32[]{:S(2)}) copy-start(f32[256,2]{0,1:T(2,128)} %param.20) | copy-start | bytes 6148

commit v4 on v3

--- a/solution.py
+++ b/solution.py
@@ -13,7 +13,7 @@
 TOK = 256
 D = 2048
 COLS = D // NTP
-KEYS = NX * TOK
+ROW = NX * TOK
 CAP = 20
 SLOT = 24
 SEND = 48
@@ -52,68 +52,68 @@
     return hi, mid, rest - mid
 
 
-def attend(at_ref, q_ref, kv0_ref, kv1_ref, kv2_ref, kv3_ref, gate_ref, out_ref, keys_ref, vals_ref):
+def attend(at_ref, q0_ref, q1_ref, q2_ref, q3_ref, kv_ref, gate_ref, out_ref, qs_ref, s_ref, m_ref, acc_ref):
     z, x = at_ref[0], at_ref[1]
-    first = gate_ref[:, pl.ds(pl.multiple_of(z * KEYS, KEYS), TOK)][:, 0:1]
+    first = gate_ref[:, pl.ds(pl.multiple_of(z * ROW, ROW), TOK)][:, 0:1]
     row64 = lax.broadcasted_iota(jnp.int32, (HD, TOK), 0)
-    for j, kv_ref in enumerate((kv0_ref, kv1_ref, kv2_ref, kv3_ref)):
-        where = lax.rem(x + NX - j, NX)
-        place = pl.multiple_of(where * TOK, TOK)
-        bias = first - gate_ref[:, pl.ds(pl.multiple_of(z * KEYS + where * TOK, TOK), TOK)]
-        hi, mid, lo = three(bias)
+    ones = jnp.where(row64 < 3, 1.0, 0.0).astype(bf)
+    for j, q_ref in enumerate((q0_ref, q1_ref, q2_ref, q3_ref)):
+        place = pl.multiple_of(lax.rem(x + NX - j, NX) * TOK, TOK)
+        qs_ref[0:HD, pl.ds(place, TOK)] = q_ref[...] * bf(HD**-0.5)
+        qs_ref[HD : 2 * HD, pl.ds(place, TOK)] = ones
+
+    def scores(zk):
+        place = pl.multiple_of(zk * ROW + x * TOK, TOK)
+        hi, mid, lo = three(first - gate_ref[:, pl.ds(place, TOK)])
         extra = jnp.where(row64 == 0, hi, jnp.where(row64 == 1, mid, jnp.where(row64 == 2, lo, 0.0)))
-        both = jnp.concatenate([kv_ref[0:HD, :], extra.astype(bf)], axis=0)
-        keys_ref[pl.ds(place, TOK), :] = both.T
-        vals_ref[0:HD, pl.ds(place, TOK)] = kv_ref[HD : 2 * HD, :]
-        vals_ref[HD : HD + 16, pl.ds(place, TOK)] = jnp.ones((16, TOK), bf)
-    ones = jnp.where(row64 < 3, 1.0, 0.0).astype(bf)
-    row16 = lax.broadcasted_iota(jnp.int32, (16, TOK), 0)
-
-    def part(zq, masked):
-        q = jnp.concatenate([q_ref[zq] * bf(HD**-0.5), ones], axis=0)
-        s = jnp.dot(keys_ref[...], q, preferred_element_type=f32)
-        if masked:
-            ki = lax.broadcasted_iota(jnp.int32, (KEYS, TOK), 0)
-            qi = lax.broadcasted_iota(jnp.int32, (KEYS, TOK), 1) + x * TOK
-            s = jnp.where(ki <= qi, s, LOW)
-        m = jnp.max(s, axis=0, keepdims=True)
-        p = jnp.exp(s - m).astype(bf)
-        o = jnp.dot(vals_ref[...], p, preferred_element_type=f32)
-        total = o[HD : HD + 1, :]
-        hi, mid, lo = three(m + jnp.log(total))
-        stats = jnp.where(row16 == 0, hi, jnp.where(row16 == 1, mid, jnp.where(row16 == 2, lo, 0.0)))
-        out_ref[zq, 0:HD, :] = (o[0:HD, :] / total).astype(bf)
-        out_ref[zq, HD : HD + 16, :] = stats.astype(bf)
-
-    part(z, True)
-
-    def later(zq, carry):
-        part(zq, False)
+        both = jnp.concatenate([kv_ref[zk, 0:HD, :], extra.astype(bf)], axis=0)
+        return jnp.dot(both.T, qs_ref[...], preferred_element_type=f32)
+
+    s = scores(z)
+    ki = lax.broadcasted_iota(jnp.int32, (TOK, ROW), 0) + x * TOK
+    qi = lax.broadcasted_iota(jnp.int32, (TOK, ROW), 1)
+    s = jnp.where(ki <= qi, s, LOW)
+    s_ref[z] = s
+    m_ref[...] = jnp.broadcast_to(jnp.max(s, axis=0, keepdims=True), (8, ROW))
+
+    def look(zk, carry):
+        s = scores(zk)
+        s_ref[zk] = s
+        m_ref[...] = jnp.maximum(m_ref[...], jnp.max(s, axis=0, keepdims=True))
         return carry
 
-    lax.fori_loop(z + 1, NZ, later, 0)
-
-    def earlier(zq, carry):
-        out_ref[zq, 0:HD, :] = jnp.zeros((HD, TOK), bf)
-        out_ref[zq, HD : HD + 16, :] = jnp.where(row16 == 0, LOW, 0.0).astype(bf)
+    lax.fori_loop(0, z, look, 0)
+    m = m_ref[0:1, :]
+    acc_ref[...] = jnp.zeros((HD + 16, ROW), f32)
+
+    def weigh(zk, carry):
+        p = jnp.exp(s_ref[zk] - m).astype(bf)
+        v = jnp.concatenate([kv_ref[zk, HD : 2 * HD, :], jnp.ones((16, TOK), bf)], axis=0)
+        acc_ref[...] += jnp.dot(v, p, preferred_element_type=f32)
         return carry
 
-    lax.fori_loop(0, z, earlier, 0)
-
-
-def merge(at_ref, part_ref, gate_ref, out_ref):
+    lax.fori_loop(0, z + 1, weigh, 0)
+    row16 = lax.broadcasted_iota(jnp.int32, (16, ROW), 0)
+    total = acc_ref[HD : HD + 1, :]
+    hi, mid, lo = three(m + jnp.log(total))
+    stats = jnp.where(row16 == 0, hi, jnp.where(row16 == 1, mid, jnp.where(row16 == 2, lo, 0.0))).astype(bf)
+    o = (acc_ref[0:HD, :] / total).astype(bf)
+    for j in range(NX):
+        out_ref[j, 0:HD, :] = o[:, j * TOK : (j + 1) * TOK]
+        out_ref[j, HD : HD + 16, :] = stats[:, j * TOK : (j + 1) * TOK]
+
+
+def merge(part_ref, out_ref):
     ls = []
-    place = pl.multiple_of(at_ref[0] * KEYS + at_ref[1] * TOK, TOK)
-    mine = gate_ref[:, pl.ds(place, TOK)]
-    for i in range(NZ):
+    for i in range(NX):
         st = part_ref[i, HD : HD + 16, :].astype(f32)
-        ls.append(st[0:1] + st[1:2] + st[2:3] + (mine - gate_ref[:, i * KEYS : i * KEYS + 1]))
+        ls.append(st[0:1] + st[1:2] + st[2:3])
     m = ls[0]
     for v in ls[1:]:
         m = jnp.maximum(m, v)
     acc = jnp.zeros((HD, TOK), f32)
     total = jnp.zeros((1, TOK), f32)
-    for i in range(NZ):
+    for i in range(NX):
         w = jnp.exp(ls[i] - m)
         total = total + w
         acc = acc + w * part_ref[i, 0:HD, :].astype(f32)
@@ -275,11 +275,6 @@
     out_ref[...] = out.astype(bf)
 
 
-def to_all(v, axis):
-    n = lax.axis_size(axis)
-    return lax.all_to_all(jnp.broadcast_to(v[None], (n, *v.shape)), axis, 0, 0, tiled=True)
-
-
 def shift(v, by):
     return lax.ppermute(v, "y", [(i, (i + by) % NY) for i in range(NY)])
 
@@ -308,22 +303,32 @@
     low = (lax.rem(y, half) * NC + c) * COLS
     at_cols = jnp.stack([low, low + half * NC * COLS, y // half]).astype(jnp.int32)
     at = jnp.stack([z, x]).astype(jnp.int32)
-    q = to_all(queries.T, "z")
     w_send = call(spread_weight, sds((NTP, 2 * HD, COLS), bf), (out_weight,))
+    kv = jnp.concatenate([keys.T, values.T], axis=0)
+    kv, w_send, at, at_cols = lax.optimization_barrier(
+        (jnp.broadcast_to(kv[None], (NZ, 2 * HD, TOK)), w_send, at, at_cols)
+    )
+    kv = exchange(kv, "z")
     w_cols = exchange(w_send, TP)
-    kv = [jnp.concatenate([keys.T, values.T], axis=0)]
+    q = [queries.T]
     for n in range(1, NX):
-        kv.append(lax.ppermute(kv[0], "x", [(i, (i + n) % NX) for i in range(NX)]))
+        q.append(lax.ppermute(q[0], "x", [(i, (i + n) % NX) for i in range(NX)]))
     parts = call(
         attend,
-        sds((NZ, HD + 16, TOK), bf),
-        (at, q, *kv, cum_gate),
+        sds((NX, HD + 16, TOK), bf),
+        (at, *q, kv, cum_gate),
         smem=1,
-        scratch=(pltpu.VMEM((KEYS, 2 * HD), bf), pltpu.VMEM((HD + 16, KEYS), bf)),
+        scratch=(
+            pltpu.VMEM((2 * HD, ROW), bf),
+            pltpu.VMEM((NZ, TOK, ROW), f32),
+            pltpu.VMEM((8, ROW), f32),
+            pltpu.VMEM((HD + 16, ROW), f32),
+        ),
+        limit=24,
     )
     parts, w_cols = lax.optimization_barrier((parts, w_cols))
-    parts = exchange(parts, "z")
-    attended = call(merge, sds((HD, TOK), bf), (at, parts, cum_gate), smem=1)
+    parts = exchange(parts, "x")
+    attended = call(merge, sds((HD, TOK), bf), (parts,))
     attended = lax.all_gather(attended, TP, axis=0, tiled=True)
     stream, outgoing, slots = call(
         project,

time: 201 us -> 195 us (0.970)
  blocking collectives: 93.9 us -> 128 us
  waiting for transfers between devices: 29 us -> 11.8 us
  starting transfers between devices: 57.3 us -> 42.7 us
  Pallas kernels: 15.4 us -> 8.87 us
    all_to_all x3 -> x5, blocking collectives: 72.9 us -> 111 us  [exchange(): return lax.all_to_all(v, axis, 0, 0, tiled=True)]
    all_to_all x1 -> x0, starting transfers between devices: 11 us -> none  [to_all(): lax.all_to_all(jnp.broadcast_to(v[None], (n, *v.shape)), axis, 0, 0, tile...]
    all_to_all x1 -> x0, waiting for transfers between devices: 8.65 us -> none  [to_all(): lax.all_to_all(jnp.broadcast_to(v[None], (n, *v.shape)), axis, 0, 0, tile...]
    all_to_all x2 -> x1, waiting for transfers between devices: 11.1 us -> 3.17 us  [exchange(): return lax.all_to_all(v, axis, 0, 0, tiled=True)]
    pallas_call x8, Pallas kernels: 15.4 us -> 8.87 us  [call(): pl.pallas_call(body, out_shape=out_shape, in_specs=specs, out_specs=tuple...]
    all_gather x1, blocking collectives: 20.9 us -> 16.7 us  [layer(): attended = lax.all_gather(attended, TP, axis=0, tiled=True)]
    all_to_all x2 -> x1, starting transfers between devices: 12.9 us -> 9.58 us  [exchange(): return lax.all_to_all(v, axis, 0, 0, tiled=True)]
  transfers between devices with their start and end apart: 14 -> 12, of which waited for: 7 -> 6; matrix products, arithmetic and copies ran while one was open for 0% -> 0% of each run, Pallas kernels for 4% -> 1%
where the time goes in v4:
time: 195 us; the launch traced here: 194 us
  blocking collectives  128 us (66%)
  starting transfers between devices  42.7 us (22%)
  waiting for transfers between devices  11.8 us (6%)
  Pallas kernels  8.87 us (5%)
    all_to_all x5, blocking collectives, exchange(): return lax.all_to_all(v, axis, 0, 0, tiled=True)  111 us
    all_gather x1, blocking collectives, layer(): attended = lax.all_gather(attended, TP, axis=0, tiled=True)  16.7 us
    ppermute x4, starting transfers between devices, shift(): return lax.ppermute(v, 'y', [(i, (i + by) % NY) for i in range(NY)])  11.6 us
    ppermute x3, starting transfers between devices, layer(): others.append(lax.ppermute(v, 'c', swap))  9.93 us
    all_to_all x1, starting transfers between devices, exchange(): return lax.all_to_all(v, axis, 0, 0, tiled=True)  9.58 us
    ppermute x3, starting transfers between devices, layer(): q.append(lax.ppermute(q[0], 'x', [(i, (i + n) % NX) for i in range(NX)]))  9.33 us
    pallas_call x8, Pallas kernels, call(): pl.pallas_call(body, out_shape=out_shape, in_specs=specs, out_specs=tuple...  8.87 us
  transfers between devices with their start and end apart: 12, of which 6 were waited for; matrix products, arithmetic and copies ran while one was open for 0% of the time, Pallas kernels for 1%

profile of v4, /device:TPU:1, one launch (start us, length us, event | category | flops | bytes accessed | tf_op | source)
XLA Modules:
  0.0 193.9 jit_solution(14867268944794904828)
XLA Ops:
  0.0 0.9 copy-done.4
  1.0 0.9 shard_map.118
  1.9 0.8 pad_maximum_fusion.2
  2.8 26.8 %all_to_all.30.kv_ref = bf16[8,128,256]{2,1,0:T(8,128)(2,1)S(1)} all-to-all(bf16[8,128,256]{2,1,0:T(8,128)(2,1)S(1)} %broadcast_in_dim.2), channel_id=1, replica_groups=mesh['z'=8,'x'=4,'y'=8,'c'=2] {'z'}, dimensions={0} | all-to-all | bytes 1048576 | tf_op jit(solution)/shard_map/all_to_all | solution.py:283
  29.6 9.6 %all-to-all-start.1 = ((bf16[16,128,128]{2,1,0:T(8,128)(2,1)}), bf16[16,128,128]{2,1,0:T(8,128)(2,1)S(1)}, u32[]{:S(2)}, u32[]{:S(2)}) async-start(bf16[16,128,128]{2,1,0:T(8,128)(2,1)} %shard_map.118), calls=%async_computation.1 | async-start | bytes 1048576 | tf_op jit(solution)/shard_map/all_to_all | solution.py:283
  39.2 4.4 %collective-permute-start.2 = (bf16[64,256]{1,0:T(8,128)(2,1)S(1)}, bf16[64,256]{1,0:T(8,128)(2,1)S(1)}, u32[]{:S(2)}, u32[]{:S(2)}) collective-permute-start(bf16[64,256]{1,0:T(8,128)(2,1)S(1)} %bitcast.21), channel_id=1, source_target_pairs={{0,48},{16,0},{32,16},{48,32},{1,49},{17,1},{33,17},{49,33},{2,50}... | collective-permute-start | bytes 98312 | tf_op jit(solution)/shard_map/ppermute | solution.py:315
  43.6 2.4 %collective-permute-start.1 = (bf16[64,256]{1,0:T(8,128)(2,1)S(1)}, bf16[64,256]{1,0:T(8,128)(2,1)S(1)}, u32[]{:S(2)}, u32[]{:S(2)}) collective-permute-start(bf16[64,256]{1,0:T(8,128)(2,1)S(1)} %bitcast.22), channel_id=1, source_target_pairs={{0,32},{16,48},{32,0},{48,16},{1,33},{17,49},{33,1},{49,17},{2,34}... | collective-permute-start | bytes 98312 | tf_op jit(solution)/shard_map/ppermute | solution.py:315
  46.0 2.5 %collective-permute-start = (bf16[64,256]{1,0:T(8,128)(2,1)S(1)}, bf16[64,256]{1,0:T(8,128)(2,1)S(1)}, u32[]{:S(2)}, u32[]{:S(2)}) collective-permute-start(bf16[64,256]{1,0:T(8,128)(2,1)S(1)} %bitcast.23), channel_id=1, source_target_pairs={{0,16},{16,32},{32,48},{48,0},{1,17},{17,33},{33,49},{49,1},{2,18}... | collective-permute-start | bytes 98312 | tf_op jit(solution)/shard_map/ppermute | solution.py:315
  48.5 1.5 collective-permute-done.1.q2_ref
  50.0 1.8 collective-permute-done.q1_ref
  51.9 1.3 shard_map.119
  53.2 3.2 %all-to-all-done.1.w_ref = bf16[16,128,128]{2,1,0:T(8,128)(2,1)S(1)} async-done(((bf16[16,128,128]{2,1,0:T(8,128)(2,1)}), bf16[16,128,128]{2,1,0:T(8,128)(2,1)S(1)}, u32[]{:S(2)}, u32[]{:S(2)}) %all-to-all-start.1) | async-done | bytes 524320 | tf_op jit(solution)/shard_map/all_to_all | solution.py:283
  56.4 9.3 %all_to_all.31.part_ref = bf16[4,80,256]{2,1,0:T(8,128)(2,1)S(1)} all-to-all(bf16[4,80,256]{2,1,0:T(8,128)(2,1)S(1)} %shard_map.119), channel_id=1, replica_groups=mesh['z'=8,'x'=4,'y'=8,'c'=2] {'x'}, dimensions={0} | all-to-all | bytes 327680 | tf_op jit(solution)/shard_map/all_to_all | solution.py:283
  65.7 16.7 %all_gather.3.att_ref = bf16[1024,256]{1,0:T(8,128)(2,1)S(1)} all-gather(bf16[64,256]{1,0:T(8,128)(2,1)S(1)} %shard_map.120), channel_id=1, replica_groups=mesh['z'=8,'x'=4,'y'=8,'c'=2] {'y','c'}, dimensions={0}, use_global_device_ids=true | all-gather | bytes 557056 | tf_op jit(solution)/shard_map/all_gather | solution.py:332
  82.3 2.0 %shard_map.121 = (f32[256,128]{1,0:T(8,128)S(1)}, bf16[32,48,128]{2,1,0:T(8,128)(2,1)S(1)}, s32[8,256]{1,0:T(8,128)S(1)}) custom-call(s32[3]{0:T(128)S(1)} %pad_add_fusion.2.at_ref, bf16[1024,256]{1,0:T(8,128)(2,1)S(1)} %all_gather.3.att_ref, bf16[16,128,128]{2,1,0:T(8,128)(2,1)S(1)} %all-to-all-done.1.w_ref, bf16[256,2048]{1,0:T(8,128)(2,1)S(1)} %copy-done, ...), custom_call_target="tpu_custom_call" | custom-call | tf_op jit(solution)/shard_map/pallas_call | solution.py:37
  84.3 20.5 %all_to_all.32.in_ref = bf16[32,48,128]{2,1,0:T(8,128)(2,1)S(1)} all-to-all(bf16[32,48,128]{2,1,0:T(8,128)(2,1)S(1)} %get-tuple-element.25), channel_id=1, replica_groups=mesh['z'=8,'x'=4,'y'=8,'c'=2] {'z','x'}, dimensions={0} | all-to-all | bytes 786432 | tf_op jit(solution)/shard_map/all_to_all | solution.py:283
  105.0 2.9 %collective-permute-start.4 = (bf16[1296,128]{1,0:T(8,128)(2,1)S(1)}, bf16[1296,128]{1,0:T(8,128)(2,1)S(1)}, u32[]{:S(2)}, u32[]{:S(2)}) collective-permute-start(bf16[1296,128]{1,0:T(8,128)(2,1)S(1)} %get-tuple-element.26.refs_0_), channel_id=1, source_target_pairs={{0,14},{2,0},{4,2},{6,4},{8,6},{10,8},{12,10},{14,12},{1,15},{3,1}... | collective-permute-start | bytes 995336 | tf_op jit(solution)/shard_map/ppermute | solution.py:279
  107.9 2.5 %collective-permute-start.3 = (bf16[1296,128]{1,0:T(8,128)(2,1)S(1)}, bf16[1296,128]{1,0:T(8,128)(2,1)S(1)}, u32[]{:S(2)}, u32[]{:S(2)}) collective-permute-start(bf16[1296,128]{1,0:T(8,128)(2,1)S(1)} %get-tuple-element.26.refs_0_), channel_id=1, source_target_pairs={{0,2},{2,4},{4,6},{6,8},{8,10},{10,12},{12,14},{14,0},{1,3},{3,5},... | collective-permute-start | bytes 995336 | tf_op jit(solution)/shard_map/ppermute | solution.py:279
  110.4 3.7 %collective-permute-start.6 = (bf16[640,128]{1,0:T(8,128)(2,1)S(1)}, bf16[640,128]{1,0:T(8,128)(2,1)S(1)}, u32[]{:S(2)}, u32[]{:S(2)}) collective-permute-start(bf16[640,128]{1,0:T(8,128)(2,1)S(1)} %get-tuple-element.28), channel_id=1, source_target_pairs={{0,12},{2,14},{4,0},{6,2},{8,4},{10,6},{12,8},{14,10},{1,13},{3,15... | collective-permute-start | bytes 491528 | tf_op jit(solution)/shard_map/ppermute | solution.py:279
  114.1 2.5 %collective-permute-start.5 = (bf16[656,128]{1,0:T(8,128)(2,1)S(1)}, bf16[656,128]{1,0:T(8,128)(2,1)S(1)}, u32[]{:S(2)}, u32[]{:S(2)}) collective-permute-start(bf16[656,128]{1,0:T(8,128)(2,1)S(1)} %get-tuple-element.27), channel_id=1, source_target_pairs={{0,4},{2,6},{4,8},{6,10},{8,12},{10,14},{12,0},{14,2},{1,5},{3,7},... | collective-permute-start | bytes 503816 | tf_op jit(solution)/shard_map/ppermute | solution.py:279
  116.6 1.5 collective-permute-done.3.refs_1_
  118.1 5.0 %collective-permute-start.8 = (bf16[2592,128]{1,0:T(8,128)(2,1)S(1)}, bf16[2592,128]{1,0:T(8,128)(2,1)S(1)}, u32[]{:S(2)}, u32[]{:S(2)}) collective-permute-start(bf16[2592,128]{1,0:T(8,128)(2,1)S(1)} %pad_maximum_fusion), channel_id=1, source_target_pairs={{0,1},{1,0},{2,3},{3,2},{4,5},{5,4},{6,7},{7,6},{8,9},{9,8},{10,11... | collective-permute-start | bytes 1990664 | tf_op jit(solution)/shard_map/ppermute | solution.py:353
  123.1 1.9 collective-permute-start.7
  125.1 3.0 %collective-permute-start.9 = (bf16[1296,128]{1,0:T(8,128)(2,1)S(1)}, bf16[1296,128]{1,0:T(8,128)(2,1)S(1)}, u32[]{:S(2)}, u32[]{:S(2)}) collective-permute-start(bf16[1296,128]{1,0:T(8,128)(2,1)S(1)} %pad_maximum_fusion.1), channel_id=1, source_target_pairs={{0,1},{1,0},{2,3},{3,2},{4,5},{5,4},{6,7},{7,6},{8,9},{9,8},{10,11... | collective-permute-start | bytes 995336 | tf_op jit(solution)/shard_map/ppermute | solution.py:353
  128.2 1.2 collective-permute-done.9.refs_7_
  129.4 3.0 %shard_map.123 = (bf16[8,640,128]{2,1,0:T(8,128)(2,1)S(1)}, bf16[8,640,128]{2,1,0:T(8,128)(2,1)S(1)}) custom-call(s32[2]{0:T(128)S(1)} %pad_add_fusion.at_ref, bf16[1296,128]{1,0:T(8,128)(2,1)S(1)} %get-tuple-element.26.refs_0_, bf16[1296,128]{1,0:T(8,128)(2,1)S(1)} %collective-permute-done.3.refs_1_, bf16[1296,128]{1,0:T(8,128)(2,1)S(1)} %collective-permute-done.4.refs_2_, ...), custom_call_target="tpu_custom_call" | custom-call | tf_op jit(solution)/shard_map/pallas_call | solution.py:37
  132.4 2.3 %collective-permute-start.10 = (bf16[8,640,128]{2,1,0:T(8,128)(2,1)S(1)}, bf16[8,640,128]{2,1,0:T(8,128)(2,1)S(1)}, u32[]{:S(2)}, u32[]{:S(2)}) collective-permute-start(bf16[8,640,128]{2,1,0:T(8,128)(2,1)S(1)} %get-tuple-element.30), channel_id=1, source_target_pairs={{0,1},{1,0},{2,3},{3,2},{4,5},{5,4},{6,7},{7,6},{8,9},{9,8},{10,11... | collective-permute-start | bytes 3932168 | tf_op jit(solution)/shard_map/ppermute | solution.py:363
  134.7 2.6 %collective-permute-done.10 = bf16[8,640,128]{2,1,0:T(8,128)(2,1)S(1)} collective-permute-done((bf16[8,640,128]{2,1,0:T(8,128)(2,1)S(1)}, bf16[8,640,128]{2,1,0:T(8,128)(2,1)S(1)}, u32[]{:S(2)}, u32[]{:S(2)}) %collective-permute-start.10) | collective-permute-done | bytes 1310752 | tf_op jit(solution)/shard_map/ppermute | solution.py:363
  137.4 0.3 add_convert_fusion
  137.7 40.1 %all_to_all.33.in_ref = bf16[8,640,128]{2,1,0:T(8,128)(2,1)S(1)} all-to-all(bf16[8,640,128]{2,1,0:T(8,128)(2,1)S(1)} %add_convert_fusion), channel_id=1, replica_groups=mesh['z'=8,'x'=4,'y'=8,'c'=2] {'y'}, dimensions={0} | all-to-all | bytes 2621440 | tf_op jit(solution)/shard_map/all_to_all | solution.py:283
  178.1 14.6 %all_to_all.34 = bf16[32,24,128]{2,1,0:T(8,128)(2,1)S(1)} all-to-all(bf16[32,24,128]{2,1,0:T(8,128)(2,1)S(1)} %shard_map.124), channel_id=1, replica_groups=mesh['z'=8,'x'=4,'y'=8,'c'=2] {'z','x'}, dimensions={0} | all-to-all | bytes 393216 | tf_op jit(solution)/shard_map/all_to_all | solution.py:283
  192.7 1.2 shard_map.125
  (34 shorter events, 0.8 us)
Async XLA Ops:
  0.0 0.9 copy-start.4
  2.8 36.4 %copy-start.5 = (bf16[256,64]{0,1:T(8,128)(2,1)S(1)}, bf16[256,64]{0,1:T(8,128)(2,1)}, u32[]{:S(2)}) copy-start(bf16[256,64]{0,1:T(8,128)(2,1)} %param.12) | copy-start | bytes 98308
  2.8 49.1 %copy-start.6 = (f32[1,8192]{1,0:T(1,128)S(1)}, f32[1,8192]{1,0:T(1,128)}, u32[]{:S(2)}) copy-start(f32[1,8192]{1,0:T(1,128)} %gate_ref.1) | copy-start | bytes 98308
  29.6 52.8 %copy-start = (bf16[256,2048]{1,0:T(8,128)(2,1)S(1)}, bf16[256,2048]{1,0:T(8,128)(2,1)}, u32[]{:S(2)}) copy-start(bf16[256,2048]{1,0:T(8,128)(2,1)} %resid_ref.1) | copy-start | bytes 3145732
  29.6 52.8 %copy-start.7 = (f32[2048]{0:T(1024)S(1)}, f32[2048]{0:T(1024)}, u32[]{:S(2)}) copy-start(f32[2048]{0:T(1024)} %param.18) | copy-start | bytes 24580
  29.6 52.8 %copy-start.9 = (s32[256,2]{0,1:T(2,128)S(1)}, s32[256,2]{0,1:T(2,128)}, u32[]{:S(2)}) copy-start(s32[256,2]{0,1:T(2,128)} %param.19) | copy-start | bytes 6148
  29.6 26.8 %all-to-all-start.1 = ((bf16[16,128,128]{2,1,0:T(8,128)(2,1)}), bf16[16,128,128]{2,1,0:T(8,128)(2,1)S(1)}, u32[]{:S(2)}, u32[]{:S(2)}) async-start(bf16[16,128,128]{2,1,0:T(8,128)(2,1)} %shard_map.118), calls=%async_computation.1 | async-start | bytes 1048576 | tf_op jit(solution)/shard_map/all_to_all | solution.py:283
  39.2 9.4 %collective-permute-start.2 = (bf16[64,256]{1,0:T(8,128)(2,1)S(1)}, bf16[64,256]{1,0:T(8,128)(2,1)S(1)}, u32[]{:S(2)}, u32[]{:S(2)}) collective-permute-start(bf16[64,256]{1,0:T(8,128)(2,1)S(1)} %bitcast.21), channel_id=1, source_target_pairs={{0,48},{16,0},{32,16},{48,32},{1,49},{17,1},{33,17},{49,33},{2,50}... | collective-permute-start | bytes 98312 | tf_op jit(solution)/shard_map/ppermute | solution.py:315
  43.6 6.5 %collective-permute-start.1 = (bf16[64,256]{1,0:T(8,128)(2,1)S(1)}, bf16[64,256]{1,0:T(8,128)(2,1)S(1)}, u32[]{:S(2)}, u32[]{:S(2)}) collective-permute-start(bf16[64,256]{1,0:T(8,128)(2,1)S(1)} %bitcast.22), channel_id=1, source_target_pairs={{0,32},{16,48},{32,0},{48,16},{1,33},{17,49},{33,1},{49,17},{2,34}... | collective-permute-start | bytes 98312 | tf_op jit(solution)/shard_map/ppermute | solution.py:315
  46.0 5.9 %collective-permute-start = (bf16[64,256]{1,0:T(8,128)(2,1)S(1)}, bf16[64,256]{1,0:T(8,128)(2,1)S(1)}, u32[]{:S(2)}, u32[]{:S(2)}) collective-permute-start(bf16[64,256]{1,0:T(8,128)(2,1)S(1)} %bitcast.23), channel_id=1, source_target_pairs={{0,16},{16,32},{32,48},{48,0},{1,17},{17,33},{33,49},{49,1},{2,18}... | collective-permute-start | bytes 98312 | tf_op jit(solution)/shard_map/ppermute | solution.py:315
  84.3 45.1 %copy-start.3 = (bf16[1,256,2048]{2,1,0:T(8,128)(2,1)S(1)}, bf16[1,256,2048]{2,1,0:T(8,128)(2,1)}, u32[]{:S(2)}) copy-start(bf16[1,256,2048]{2,1,0:T(8,128)(2,1)} %param.23) | copy-start | bytes 3145732
  104.8 24.6 %copy-start.1 = (bf16[1,2048,256]{2,1,0:T(8,128)(2,1)S(1)}, bf16[1,2048,256]{2,1,0:T(8,128)(2,1)}, u32[]{:S(2)}) copy-start(bf16[1,2048,256]{2,1,0:T(8,128)(2,1)} %param.21) | copy-start | bytes 3145732
  104.8 24.6 %copy-start.2 = (bf16[1,2048,256]{2,1,0:T(8,128)(2,1)S(1)}, bf16[1,2048,256]{2,1,0:T(8,128)(2,1)}, u32[]{:S(2)}) copy-start(bf16[1,2048,256]{2,1,0:T(8,128)(2,1)} %param.22) | copy-start | bytes 3145732
  105.0 11.6 %collective-permute-start.4 = (bf16[1296,128]{1,0:T(8,128)(2,1)S(1)}, bf16[1296,128]{1,0:T(8,128)(2,1)S(1)}, u32[]{:S(2)}, u32[]{:S(2)}) collective-permute-start(bf16[1296,128]{1,0:T(8,128)(2,1)S(1)} %get-tuple-element.26.refs_0_), channel_id=1, source_target_pairs={{0,14},{2,0},{4,2},{6,4},{8,6},{10,8},{12,10},{14,12},{1,15},{3,1}... | collective-permute-start | bytes 995336 | tf_op jit(solution)/shard_map/ppermute | solution.py:279
  107.9 10.2 %collective-permute-start.3 = (bf16[1296,128]{1,0:T(8,128)(2,1)S(1)}, bf16[1296,128]{1,0:T(8,128)(2,1)S(1)}, u32[]{:S(2)}, u32[]{:S(2)}) collective-permute-start(bf16[1296,128]{1,0:T(8,128)(2,1)S(1)} %get-tuple-element.26.refs_0_), channel_id=1, source_target_pairs={{0,2},{2,4},{4,6},{6,8},{8,10},{10,12},{12,14},{14,0},{1,3},{3,5},... | collective-permute-start | bytes 995336 | tf_op jit(solution)/shard_map/ppermute | solution.py:279
  110.4 14.7 %collective-permute-start.6 = (bf16[640,128]{1,0:T(8,128)(2,1)S(1)}, bf16[640,128]{1,0:T(8,128)(2,1)S(1)}, u32[]{:S(2)}, u32[]{:S(2)}) collective-permute-start(bf16[640,128]{1,0:T(8,128)(2,1)S(1)} %get-tuple-element.28), channel_id=1, source_target_pairs={{0,12},{2,14},{4,0},{6,2},{8,4},{10,6},{12,8},{14,10},{1,13},{3,15... | collective-permute-start | bytes 491528 | tf_op jit(solution)/shard_map/ppermute | solution.py:279
  114.1 11.0 %collective-permute-start.5 = (bf16[656,128]{1,0:T(8,128)(2,1)S(1)}, bf16[656,128]{1,0:T(8,128)(2,1)S(1)}, u32[]{:S(2)}, u32[]{:S(2)}) collective-permute-start(bf16[656,128]{1,0:T(8,128)(2,1)S(1)} %get-tuple-element.27), channel_id=1, source_target_pairs={{0,4},{2,6},{4,8},{6,10},{8,12},{10,14},{12,0},{14,2},{1,5},{3,7},... | collective-permute-start | bytes 503816 | tf_op jit(solution)/shard_map/ppermute | solution.py:279
  118.1 11.2 %collective-permute-start.8 = (bf16[2592,128]{1,0:T(8,128)(2,1)S(1)}, bf16[2592,128]{1,0:T(8,128)(2,1)S(1)}, u32[]{:S(2)}, u32[]{:S(2)}) collective-permute-start(bf16[2592,128]{1,0:T(8,128)(2,1)S(1)} %pad_maximum_fusion), channel_id=1, source_target_pairs={{0,1},{1,0},{2,3},{3,2},{4,5},{5,4},{6,7},{7,6},{8,9},{9,8},{10,11... | collective-permute-start | bytes 1990664 | tf_op jit(solution)/shard_map/ppermute | solution.py:353
  123.1 5.1 %collective-permute-start.7 = (bf16[1296,128]{1,0:T(8,128)(2,1)S(1)}, bf16[1296,128]{1,0:T(8,128)(2,1)S(1)}, u32[]{:S(2)}, u32[]{:S(2)}) collective-permute-start(bf16[1296,128]{1,0:T(8,128)(2,1)S(1)} %get-tuple-element.26.refs_0_), channel_id=1, source_target_pairs={{0,1},{1,0},{2,3},{3,2},{4,5},{5,4},{6,7},{7,6},{8,9},{9,8},{10,11... | collective-permute-start | bytes 995336 | tf_op jit(solution)/shard_map/ppermute | solution.py:353
  125.1 4.3 %collective-permute-start.9 = (bf16[1296,128]{1,0:T(8,128)(2,1)S(1)}, bf16[1296,128]{1,0:T(8,128)(2,1)S(1)}, u32[]{:S(2)}, u32[]{:S(2)}) collective-permute-start(bf16[1296,128]{1,0:T(8,128)(2,1)S(1)} %pad_maximum_fusion.1), channel_id=1, source_target_pairs={{0,1},{1,0},{2,3},{3,2},{4,5},{5,4},{6,7},{7,6},{8,9},{9,8},{10,11... | collective-permute-start | bytes 995336 | tf_op jit(solution)/shard_map/ppermute | solution.py:353
  132.4 4.9 %collective-permute-start.10 = (bf16[8,640,128]{2,1,0:T(8,128)(2,1)S(1)}, bf16[8,640,128]{2,1,0:T(8,128)(2,1)S(1)}, u32[]{:S(2)}, u32[]{:S(2)}) collective-permute-start(bf16[8,640,128]{2,1,0:T(8,128)(2,1)S(1)} %get-tuple-element.30), channel_id=1, source_target_pairs={{0,1},{1,0},{2,3},{3,2},{4,5},{5,4},{6,7},{7,6},{8,9},{9,8},{10,11... | collective-permute-start | bytes 3932168 | tf_op jit(solution)/shard_map/ppermute | solution.py:363
  177.8 14.8 %copy-start.8 = (f32[256,2]{0,1:T(2,128)S(1)}, f32[256,2]{0,1:T(2,128)}, u32[]{:S(2)}) copy-start(f32[256,2]{0,1:T(2,128)} %param.20) | copy-start | bytes 6148

commit v5 on v4

--- a/solution.py
+++ b/solution.py
@@ -8,7 +8,9 @@
 
 NZ, NX, NY, NC = 8, 4, 8, 2
 NSP, NTP = NZ * NX, NY * NC
-SP, TP = ("z", "x"), ("y", "c")
+Y = ("yh", "yl")
+SP, TP = ("z", "x"), ("yh", "yl", "c")
+HALF = NY // 2
 HD = 64
 TOK = 256
 D = 2048
@@ -154,7 +156,7 @@
     before = jnp.dot(hit, upper, preferred_element_type=f32)
     r0 = jnp.sum(jnp.where(h0, before, 0.0), axis=0, keepdims=True).astype(jnp.int32)
     r1 = jnp.sum(jnp.where(h1, before, 0.0), axis=0, keepdims=True).astype(jnp.int32)
-    slots_ref[...] = jnp.concatenate([e0 * SLOT + r0, e1 * SLOT + r1, jnp.zeros((6, TOK), jnp.int32)], axis=0)
+    slots_ref[...] = jnp.concatenate([2 * SLOT * e0 + r0, 2 * SLOT * e1 + r1, jnp.zeros((6, TOK), jnp.int32)], axis=0)
     s0 = e0 * SEND + r0
     s1 = e1 * SEND + r1
     ir = lax.broadcasted_iota(jnp.int32, (NSP * SEND, TOK), 0)
@@ -206,12 +208,26 @@
 METAS = ((0, 2 * ROWS), (1, 2 * ROWS), (2, 2 * ROWS), (3, ROWS))
 
 
+SENDS = (
+    (0, 0, 2, 0),
+    (0, ROWS, 2, 1),
+    (1, 0, 1, 0),
+    (1, ROWS, 1, 1),
+    (1, 2 * ROWS, 3, 0),
+    (1, 3 * ROWS, 3, 1),
+    (1, 4 * ROWS, 0, 0),
+    (1, 5 * ROWS, 0, 1),
+)
+
+
 def experts(at_ref, *refs):
     every, near, far = refs[5:8]
     rows = 2 * ROWS + META
     owns = refs[0:5]
     others = (every, near.at[0:rows], near.at[rows:], far.at[0 : ROWS + META], far.at[ROWS + META :])
-    wg_ref, wu_ref, wd_ref, mine_ref, theirs_ref, g_ref, u_ref, h_ref = refs[8:]
+    wg_ref, wu_ref, wd_ref = refs[8:11]
+    outs = refs[11:15]
+    g_ref, u_ref, h_ref = refs[15:]
     y, c = at_ref[0], at_ref[1]
     total = jnp.zeros((8, COLS), f32)
     for pieces in (owns, others):
@@ -246,37 +262,43 @@
     up = u_ref[...] * scale
     h_ref[...] = (gate / (1.0 + jnp.exp(-gate)) * up).astype(bf)
     even = c == 0
-    for y in range(NY):
-        res = jnp.dot(h_ref[...], wd_ref[:, 2 * y * COLS : (2 * y + 2) * COLS], preferred_element_type=f32)
+    for ref, at, off, upper in SENDS:
+        block = lax.rem(y + off, HALF) + upper * HALF
+        place = pl.multiple_of(2 * block * COLS, 2 * COLS)
+        res = jnp.dot(h_ref[...], wd_ref[:, pl.ds(place, 2 * COLS)], preferred_element_type=f32)
         low, high = res[:, 0:COLS], res[:, COLS:]
-        mine_ref[y] = jnp.where(even, low, high).astype(bf)
-        theirs_ref[y] = jnp.where(even, high, low).astype(bf)
-
-
-def gather_sum(in_ref, out_ref, rows_ref):
-    acc = in_ref[0].astype(f32)
-    for y in range(1, NY):
-        acc = acc + in_ref[y].astype(f32)
-    rows_ref[...] = acc
+        outs[ref][at : at + ROWS, :] = jnp.where(even, low, high).astype(bf)
+        outs[ref + 2][at : at + ROWS, :] = jnp.where(even, high, low).astype(bf)
+
+
+def gather_sum(mine_ref, theirs_ref, n0_ref, n1_ref, f0_ref, f1_ref, out_ref, rows_ref):
+    base = 4 * ROWS
     pad = jnp.zeros((SLOT - CAP, COLS), f32)
-    for i in range(NSP):
-        out_ref[i] = jnp.concatenate([rows_ref[CAP * i : CAP * i + CAP, :], pad], axis=0).astype(bf)
+    for q, far_ref in enumerate((f0_ref, f1_ref)):
+        at = slice(q * ROWS, (q + 1) * ROWS)
+        kept = slice(base + q * ROWS, base + (q + 1) * ROWS)
+        acc = mine_ref[kept, :].astype(f32) + theirs_ref[kept, :].astype(f32)
+        acc = acc + n0_ref[at, :].astype(f32) + n1_ref[at, :].astype(f32)
+        rows_ref[...] = acc + far_ref[...].astype(f32)
+        for i in range(NSP):
+            out_ref[2 * i + q] = jnp.concatenate([rows_ref[CAP * i : CAP * i + CAP, :], pad], axis=0).astype(bf)
 
 
 def finish(ret_ref, slots_ref, rw_ref, stream_ref, out_ref):
     slots = slots_ref[...].astype(f32).T
     weight = jnp.concatenate([rw_ref[...], jnp.zeros((6, TOK), f32)], axis=0).T
-    lane = lax.broadcasted_iota(jnp.int32, (TOK, PADROWS), 1).astype(f32)
+    lane = lax.broadcasted_iota(jnp.int32, (TOK, 2 * PADROWS), 1).astype(f32)
     out = stream_ref[...]
     for k in range(2):
-        pick = jnp.where(lane == slots[:, k : k + 1], 1.0, 0.0).astype(bf)
+        slot = slots[:, k : k + 1]
+        pick = jnp.where((lane == slot) | (lane == slot + SLOT), 1.0, 0.0).astype(bf)
         got = jnp.dot(pick, ret_ref[...], preferred_element_type=f32)
         out = out + weight[:, k : k + 1] * got
     out_ref[...] = out.astype(bf)
 
 
 def shift(v, by):
-    return lax.ppermute(v, "y", [(i, (i + by) % NY) for i in range(NY)])
+    return lax.ppermute(v, Y, [(i, (i + by) % NY) for i in range(NY)])
 
 
 def exchange(v, axis):
@@ -297,7 +319,7 @@
     up_weight,
     down_weight,
 ):
-    z, x, y, c = (lax.axis_index(a) for a in ("z", "x", "y", "c"))
+    z, x, y, c = (lax.axis_index(a) for a in ("z", "x", Y, "c"))
     sds = jax.ShapeDtypeStruct
     half = NY // 2
     low = (lax.rem(y, half) * NC + c) * COLS
@@ -351,25 +373,42 @@
     others = []
     for v in (every, jnp.concatenate(owns[1:3], axis=0), jnp.concatenate(owns[3:5], axis=0)):
         others.append(lax.ppermute(v, "c", swap))
-    big = sds((NY, ROWS, COLS), bf)
-    mine, theirs = call(
+    far_out, near_out = sds((2 * ROWS, COLS), bf), sds((6 * ROWS, COLS), bf)
+    far_mine, near_mine, far_theirs, near_theirs = call(
         experts,
-        (big, big),
+        (far_out, near_out, far_out, near_out),
         (jnp.stack([y, c]).astype(jnp.int32), *owns, *others, gate_weight[0], up_weight[0], down_weight[0]),
         smem=1,
         scratch=(pltpu.VMEM((ROWS, FFL), f32), pltpu.VMEM((ROWS, FFL), f32), pltpu.VMEM((ROWS, FFL), bf)),
         limit=24,
     )
-    theirs = lax.ppermute(theirs, "c", swap)
-    pair = (mine.astype(f32) + theirs.astype(f32)).astype(bf)
-    pair = exchange(pair, "y")
-    back = call(gather_sum, sds((NSP, SLOT, COLS), bf), (pair,), scratch=(pltpu.VMEM((ROWS, COLS), f32),))
-    returned = exchange(back, SP).reshape(PADROWS, COLS)
+    far_theirs = lax.ppermute(far_theirs, "c", swap)
+    near_theirs = lax.ppermute(near_theirs, "c", swap)
+
+    def pair(a, b, first, count):
+        part = slice(first * ROWS, (first + count) * ROWS)
+        return (a[part].astype(f32) + b[part].astype(f32)).astype(bf)
+
+    got = []
+    for a, b, first, count, by in (
+        (far_mine, far_theirs, 0, 1, 2),
+        (far_mine, far_theirs, 1, 1, -2),
+        (near_mine, near_theirs, 0, 2, 1),
+        (near_mine, near_theirs, 2, 2, -1),
+    ):
+        got.append(shift(pair(a, b, first, count), by))
+    back = call(
+        gather_sum,
+        sds((2 * NSP, SLOT, COLS), bf),
+        (near_mine, near_theirs, got[2], got[3], got[0], got[1]),
+        scratch=(pltpu.VMEM((ROWS, COLS), f32),),
+    )
+    returned = exchange(back, ("z", "x", "yh")).reshape(2 * PADROWS, COLS)
     return call(finish, sds((TOK, COLS), bf), (returned, slots, route_weight.T, stream))
 
 
 def solution(mesh):
-    grid = Mesh(mesh.devices.reshape(NZ, NX, NY, NC), ("z", "x", "y", "c"))
+    grid = Mesh(mesh.devices.reshape(NZ, NX, 2, HALF, NC), ("z", "x", "yh", "yl", "c"))
     return jax.shard_map(
         layer,
         mesh=grid,

time: 195 us -> 192 us (0.985)
  the two profiles are of different devices: /device:TPU:1 before, /device:TPU:8 now
where the time goes in v5:
time: 192 us; the launch traced here: 191 us
  blocking collectives  103 us (54%)
  starting transfers between devices  54.4 us (28%)
  waiting for transfers between devices  21.5 us (11%)
  Pallas kernels  9.36 us (5%)
    all_to_all x4, blocking collectives, exchange(): return lax.all_to_all(v, axis, 0, 0, tiled=True)  85.3 us
    ppermute x8, starting transfers between devices, shift(): return lax.ppermute(v, Y, [(i, (i + by) % NY) for i in range(NY)])  26 us
    all_gather x1, blocking collectives, layer(): attended = lax.all_gather(attended, TP, axis=0, tiled=True)  17.6 us
    ppermute x8, waiting for transfers between devices, shift(): return lax.ppermute(v, Y, [(i, (i + by) % NY) for i in range(NY)])  15.6 us
    ppermute x3, starting transfers between devices, layer(): q.append(lax.ppermute(q[0], 'x', [(i, (i + n) % NX) for i in range(NX)]))  10.3 us
    pallas_call x8, Pallas kernels, call(): pl.pallas_call(body, out_shape=out_shape, in_specs=specs, out_specs=tuple...  9.36 us
    all_to_all x1, starting transfers between devices, exchange(): return lax.all_to_all(v, axis, 0, 0, tiled=True)  7.56 us
    ppermute x3, starting transfers between devices, layer(): others.append(lax.ppermute(v, 'c', swap))  6.25 us
  transfers between devices with their start and end apart: 17, of which 8 were waited for; matrix products, arithmetic and copies ran while one was open for 0% of the time, Pallas kernels for 1%

profile of v5, /device:TPU:8, one launch (start us, length us, event | category | flops | bytes accessed | tf_op | source)
XLA Modules:
  0.0 190.9 jit_solution(11797842734510088283)
XLA Ops:
  2.8 27.6 %all_to_all.25.kv_ref = bf16[8,128,256]{2,1,0:T(8,128)(2,1)S(1)} all-to-all(bf16[8,128,256]{2,1,0:T(8,128)(2,1)S(1)} %broadcast_in_dim.2), channel_id=1, replica_groups=mesh['z'=8,'x'=4,'yh'=2,'yl'=4,'c'=2] {'z'}, dimensions={0} | all-to-all | bytes 1048576 | tf_op jit(solution)/shard_map/all_to_all | solution.py:305
  30.4 7.6 %all-to-all-start.1 = ((bf16[16,128,128]{2,1,0:T(8,128)(2,1)}), bf16[16,128,128]{2,1,0:T(8,128)(2,1)S(1)}, u32[]{:S(2)}, u32[]{:S(2)}) async-start(bf16[16,128,128]{2,1,0:T(8,128)(2,1)} %shard_map.118), calls=%async_computation.1 | async-start | bytes 1048576 | tf_op jit(solution)/shard_map/all_to_all | solution.py:305
  38.0 4.8 %collective-permute-start.2 = (bf16[64,256]{1,0:T(8,128)(2,1)S(1)}, bf16[64,256]{1,0:T(8,128)(2,1)S(1)}, u32[]{:S(2)}, u32[]{:S(2)}) collective-permute-start(bf16[64,256]{1,0:T(8,128)(2,1)S(1)} %bitcast.21), channel_id=1, source_target_pairs={{0,48},{16,0},{32,16},{48,32},{1,49},{17,1},{33,17},{49,33},{2,50}... | collective-permute-start | bytes 98312 | tf_op jit(solution)/shard_map/ppermute | solution.py:337
  42.8 2.7 %collective-permute-start.1 = (bf16[64,256]{1,0:T(8,128)(2,1)S(1)}, bf16[64,256]{1,0:T(8,128)(2,1)S(1)}, u32[]{:S(2)}, u32[]{:S(2)}) collective-permute-start(bf16[64,256]{1,0:T(8,128)(2,1)S(1)} %bitcast.22), channel_id=1, source_target_pairs={{0,32},{16,48},{32,0},{48,16},{1,33},{17,49},{33,1},{49,17},{2,34}... | collective-permute-start | bytes 98312 | tf_op jit(solution)/shard_map/ppermute | solution.py:337
  45.6 2.8 %collective-permute-start = (bf16[64,256]{1,0:T(8,128)(2,1)S(1)}, bf16[64,256]{1,0:T(8,128)(2,1)S(1)}, u32[]{:S(2)}, u32[]{:S(2)}) collective-permute-start(bf16[64,256]{1,0:T(8,128)(2,1)S(1)} %bitcast.23), channel_id=1, source_target_pairs={{0,16},{16,32},{32,48},{48,0},{1,17},{17,33},{33,49},{49,1},{2,18}... | collective-permute-start | bytes 98312 | tf_op jit(solution)/shard_map/ppermute | solution.py:337
  48.4 1.8 collective-permute-done.1.q2_ref
  50.2 2.4 %collective-permute-done.q1_ref = bf16[64,256]{1,0:T(8,128)(2,1)S(1)} collective-permute-done((bf16[64,256]{1,0:T(8,128)(2,1)S(1)}, bf16[64,256]{1,0:T(8,128)(2,1)S(1)}, u32[]{:S(2)}, u32[]{:S(2)}) %collective-permute-start) | collective-permute-done | bytes 32800 | tf_op jit(solution)/shard_map/ppermute | solution.py:337
  52.6 1.3 shard_map.119
  53.9 8.7 %all_to_all.26.part_ref = bf16[4,80,256]{2,1,0:T(8,128)(2,1)S(1)} all-to-all(bf16[4,80,256]{2,1,0:T(8,128)(2,1)S(1)} %shard_map.119), channel_id=1, replica_groups=mesh['z'=8,'x'=4,'yh'=2,'yl'=4,'c'=2] {'x'}, dimensions={0} | all-to-all | bytes 327680 | tf_op jit(solution)/shard_map/all_to_all | solution.py:305
  62.7 17.6 %all_gather.3.att_ref = bf16[1024,256]{1,0:T(8,128)(2,1)S(1)} all-gather(bf16[64,256]{1,0:T(8,128)(2,1)S(1)} %shard_map.120), channel_id=1, replica_groups=mesh['z'=8,'x'=4,'yh'=2,'yl'=4,'c'=2] {'yh','yl','c'}, dimensions={0}, use_global_device_ids=true | all-gather | bytes 557056 | tf_op jit(solution)/shard_map/all_gather | solution.py:354
  80.3 2.0 %shard_map.121 = (f32[256,128]{1,0:T(8,128)S(1)}, bf16[32,48,128]{2,1,0:T(8,128)(2,1)S(1)}, s32[8,256]{1,0:T(8,128)S(1)}) custom-call(s32[3]{0:T(128)S(1)} %pad_add_fusion.2.at_ref, bf16[1024,256]{1,0:T(8,128)(2,1)S(1)} %all_gather.3.att_ref, bf16[16,128,128]{2,1,0:T(8,128)(2,1)S(1)} %all-to-all-done.1.w_ref, bf16[256,2048]{1,0:T(8,128)(2,1)S(1)} %copy-done, ...), custom_call_target="tpu_custom_call" | custom-call | tf_op jit(solution)/shard_map/pallas_call | solution.py:39
  82.3 21.7 %all_to_all.27.in_ref = bf16[32,48,128]{2,1,0:T(8,128)(2,1)S(1)} all-to-all(bf16[32,48,128]{2,1,0:T(8,128)(2,1)S(1)} %get-tuple-element.27), channel_id=1, replica_groups=mesh['z'=8,'x'=4,'yh'=2,'yl'=4,'c'=2] {'z','x'}, dimensions={0} | all-to-all | bytes 786432 | tf_op jit(solution)/shard_map/all_to_all | solution.py:305
  104.1 3.8 %collective-permute-start.4 = (bf16[1296,128]{1,0:T(8,128)(2,1)S(1)}, bf16[1296,128]{1,0:T(8,128)(2,1)S(1)}, u32[]{:S(2)}, u32[]{:S(2)}) collective-permute-start(bf16[1296,128]{1,0:T(8,128)(2,1)S(1)} %get-tuple-element.28.refs_0_), channel_id=1, source_target_pairs={{0,14},{2,0},{4,2},{6,4},{8,6},{10,8},{12,10},{14,12},{1,15},{3,1}... | collective-permute-start | bytes 995336 | tf_op jit(solution)/shard_map/ppermute | solution.py:301
  108.0 2.2 %collective-permute-start.3 = (bf16[1296,128]{1,0:T(8,128)(2,1)S(1)}, bf16[1296,128]{1,0:T(8,128)(2,1)S(1)}, u32[]{:S(2)}, u32[]{:S(2)}) collective-permute-start(bf16[1296,128]{1,0:T(8,128)(2,1)S(1)} %get-tuple-element.28.refs_0_), channel_id=1, source_target_pairs={{0,2},{2,4},{4,6},{6,8},{8,10},{10,12},{12,14},{14,0},{1,3},{3,5},... | collective-permute-start | bytes 995336 | tf_op jit(solution)/shard_map/ppermute | solution.py:301
  110.1 5.5 %collective-permute-start.6 = (bf16[640,128]{1,0:T(8,128)(2,1)S(1)}, bf16[640,128]{1,0:T(8,128)(2,1)S(1)}, u32[]{:S(2)}, u32[]{:S(2)}) collective-permute-start(bf16[640,128]{1,0:T(8,128)(2,1)S(1)} %get-tuple-element.30), channel_id=1, source_target_pairs={{0,12},{2,14},{4,0},{6,2},{8,4},{10,6},{12,8},{14,10},{1,13},{3,15... | collective-permute-start | bytes 491528 | tf_op jit(solution)/shard_map/ppermute | solution.py:301
  115.6 1.9 %collective-permute-start.5 = (bf16[656,128]{1,0:T(8,128)(2,1)S(1)}, bf16[656,128]{1,0:T(8,128)(2,1)S(1)}, u32[]{:S(2)}, u32[]{:S(2)}) collective-permute-start(bf16[656,128]{1,0:T(8,128)(2,1)S(1)} %get-tuple-element.29), channel_id=1, source_target_pairs={{0,4},{2,6},{4,8},{6,10},{8,12},{10,14},{12,0},{14,2},{1,5},{3,7},... | collective-permute-start | bytes 503816 | tf_op jit(solution)/shard_map/ppermute | solution.py:301
  118.8 1.9 %collective-permute-start.8 = (bf16[2592,128]{1,0:T(8,128)(2,1)S(1)}, bf16[2592,128]{1,0:T(8,128)(2,1)S(1)}, u32[]{:S(2)}, u32[]{:S(2)}) collective-permute-start(bf16[2592,128]{1,0:T(8,128)(2,1)S(1)} %pad_maximum_fusion), channel_id=1, source_target_pairs={{0,1},{1,0},{2,3},{3,2},{4,5},{5,4},{6,7},{7,6},{8,9},{9,8},{10,11... | collective-permute-start | bytes 1990664 | tf_op jit(solution)/shard_map/ppermute | solution.py:375
  120.7 2.4 %collective-permute-start.7 = (bf16[1296,128]{1,0:T(8,128)(2,1)S(1)}, bf16[1296,128]{1,0:T(8,128)(2,1)S(1)}, u32[]{:S(2)}, u32[]{:S(2)}) collective-permute-start(bf16[1296,128]{1,0:T(8,128)(2,1)S(1)} %get-tuple-element.28.refs_0_), channel_id=1, source_target_pairs={{0,1},{1,0},{2,3},{3,2},{4,5},{5,4},{6,7},{7,6},{8,9},{9,8},{10,11... | collective-permute-start | bytes 995336 | tf_op jit(solution)/shard_map/ppermute | solution.py:375
  123.2 3.8 %collective-permute-done.5.refs_3_ = bf16[656,128]{1,0:T(8,128)(2,1)S(1)} collective-permute-done((bf16[656,128]{1,0:T(8,128)(2,1)S(1)}, bf16[656,128]{1,0:T(8,128)(2,1)S(1)}, u32[]{:S(2)}, u32[]{:S(2)}) %collective-permute-start.5) | collective-permute-done | bytes 167968 | tf_op jit(solution)/shard_map/ppermute | solution.py:301
  127.0 1.9 %collective-permute-start.9 = (bf16[1296,128]{1,0:T(8,128)(2,1)S(1)}, bf16[1296,128]{1,0:T(8,128)(2,1)S(1)}, u32[]{:S(2)}, u32[]{:S(2)}) collective-permute-start(bf16[1296,128]{1,0:T(8,128)(2,1)S(1)} %pad_maximum_fusion.1), channel_id=1, source_target_pairs={{0,1},{1,0},{2,3},{3,2},{4,5},{5,4},{6,7},{7,6},{8,9},{9,8},{10,11... | collective-permute-start | bytes 995336 | tf_op jit(solution)/shard_map/ppermute | solution.py:375
  129.0 1.5 collective-permute-done.9.refs_7_
  130.5 3.0 %shard_map.123 = (bf16[1280,128]{1,0:T(8,128)(2,1)S(1)}, bf16[3840,128]{1,0:T(8,128)(2,1)S(1)}, bf16[1280,128]{1,0:T(8,128)(2,1)S(1)}, bf16[3840,128]{1,0:T(8,128)(2,1)S(1)}) custom-call(s32[2]{0:T(128)S(1)} %pad_add_fusion.at_ref, bf16[1296,128]{1,0:T(8,128)(2,1)S(1)} %get-tuple-element.28.refs_0_, bf16[1296,128]{1,0:T(8,128)(2,1)S(1)} %collective-permute-done.3.refs_1_, ...), custom_call_target="tpu_custom_call" | custom-call | tf_op jit(solution)/shard_map/pallas_call | solution.py:39
  133.6 2.0 %collective-permute-start.10 = (bf16[3840,128]{1,0:T(8,128)(2,1)S(1)}, bf16[3840,128]{1,0:T(8,128)(2,1)S(1)}, u32[]{:S(2)}, u32[]{:S(2)}) collective-permute-start(bf16[3840,128]{1,0:T(8,128)(2,1)S(1)} %get-tuple-element.32), channel_id=1, source_target_pairs={{0,1},{1,0},{2,3},{3,2},{4,5},{5,4},{6,7},{7,6},{8,9},{9,8},{10,11... | collective-permute-start | bytes 2949128 | tf_op jit(solution)/shard_map/ppermute | solution.py:386
  135.6 2.3 %collective-permute-start.13 = (bf16[1280,128]{1,0:T(8,128)(2,1)S(1)}, bf16[1280,128]{1,0:T(8,128)(2,1)S(1)}, u32[]{:S(2)}, u32[]{:S(2)}) collective-permute-start(bf16[1280,128]{1,0:T(8,128)(2,1)S(1)} %get-tuple-element.34), channel_id=1, source_target_pairs={{0,1},{1,0},{2,3},{3,2},{4,5},{5,4},{6,7},{7,6},{8,9},{9,8},{10,11... | collective-permute-start | bytes 983048 | tf_op jit(solution)/shard_map/ppermute | solution.py:385
  138.2 1.9 %collective-permute-start.12 = (bf16[1280,128]{1,0:T(8,128)(2,1)S(1)}, bf16[1280,128]{1,0:T(8,128)(2,1)S(1)}, u32[]{:S(2)}, u32[]{:S(2)}) collective-permute-start(bf16[1280,128]{1,0:T(8,128)(2,1)S(1)} %get-tuple-element.37), channel_id=1, source_target_pairs={{0,14},{2,0},{4,2},{6,4},{8,6},{10,8},{12,10},{14,12},{1,15},{3,1}... | collective-permute-start | bytes 983048 | tf_op jit(solution)/shard_map/ppermute | solution.py:301
  140.1 3.9 %collective-permute-start.11 = (bf16[1280,128]{1,0:T(8,128)(2,1)S(1)}, bf16[1280,128]{1,0:T(8,128)(2,1)S(1)}, u32[]{:S(2)}, u32[]{:S(2)}) collective-permute-start(bf16[1280,128]{1,0:T(8,128)(2,1)S(1)} %get-tuple-element.38), channel_id=1, source_target_pairs={{0,2},{2,4},{4,6},{6,8},{8,10},{10,12},{12,14},{14,0},{1,3},{3,5},... | collective-permute-start | bytes 983048 | tf_op jit(solution)/shard_map/ppermute | solution.py:301
  144.2 4.5 %collective-permute-start.15 = (bf16[640,128]{1,0:T(8,128)(2,1)S(1)}, bf16[640,128]{1,0:T(8,128)(2,1)S(1)}, u32[]{:S(2)}, u32[]{:S(2)}) collective-permute-start(bf16[640,128]{1,0:T(8,128)(2,1)S(1)} %get-tuple-element.39), channel_id=1, source_target_pairs={{0,12},{2,14},{4,0},{6,2},{8,4},{10,6},{12,8},{14,10},{1,13},{3,15... | collective-permute-start | bytes 491528 | tf_op jit(solution)/shard_map/ppermute | solution.py:301
  148.7 2.3 %collective-permute-start.14 = (bf16[640,128]{1,0:T(8,128)(2,1)S(1)}, bf16[640,128]{1,0:T(8,128)(2,1)S(1)}, u32[]{:S(2)}, u32[]{:S(2)}) collective-permute-start(bf16[640,128]{1,0:T(8,128)(2,1)S(1)} %get-tuple-element.40), channel_id=1, source_target_pairs={{0,4},{2,6},{4,8},{6,10},{8,12},{10,14},{12,0},{14,2},{1,5},{3,7},... | collective-permute-start | bytes 491528 | tf_op jit(solution)/shard_map/ppermute | solution.py:301
  150.9 4.3 %collective-permute-done.15.f1_ref = bf16[640,128]{1,0:T(8,128)(2,1)S(1)} collective-permute-done((bf16[640,128]{1,0:T(8,128)(2,1)S(1)}, bf16[640,128]{1,0:T(8,128)(2,1)S(1)}, u32[]{:S(2)}, u32[]{:S(2)}) %collective-permute-start.15) | collective-permute-done | bytes 163872 | tf_op jit(solution)/shard_map/ppermute | solution.py:301
  155.2 6.4 %collective-permute-done.14.f0_ref = bf16[640,128]{1,0:T(8,128)(2,1)S(1)} collective-permute-done((bf16[640,128]{1,0:T(8,128)(2,1)S(1)}, bf16[640,128]{1,0:T(8,128)(2,1)S(1)}, u32[]{:S(2)}, u32[]{:S(2)}) %collective-permute-start.14) | collective-permute-done | bytes 163872 | tf_op jit(solution)/shard_map/ppermute | solution.py:301
  161.9 27.3 %all_to_all.28 = bf16[64,24,128]{2,1,0:T(8,128)(2,1)S(1)} all-to-all(bf16[64,24,128]{2,1,0:T(8,128)(2,1)S(1)} %shard_map.124), channel_id=1, replica_groups=mesh['z'=8,'x'=4,'yh'=2,'yl'=4,'c'=2] {'z','x','yh'}, dimensions={0} | all-to-all | bytes 786432 | tf_op jit(solution)/shard_map/all_to_all | solution.py:305
  189.2 1.6 shard_map.125
  (44 shorter events, 5.1 us)
Async XLA Ops:
  0.0 0.9 copy-start.4
  2.8 35.2 %copy-start.5 = (bf16[256,64]{0,1:T(8,128)(2,1)S(1)}, bf16[256,64]{0,1:T(8,128)(2,1)}, u32[]{:S(2)}) copy-start(bf16[256,64]{0,1:T(8,128)(2,1)} %param.12) | copy-start | bytes 98308
  2.8 49.8 %copy-start.6 = (f32[1,8192]{1,0:T(1,128)S(1)}, f32[1,8192]{1,0:T(1,128)}, u32[]{:S(2)}) copy-start(f32[1,8192]{1,0:T(1,128)} %gate_ref.1) | copy-start | bytes 98308
  30.4 23.5 %all-to-all-start.1 = ((bf16[16,128,128]{2,1,0:T(8,128)(2,1)}), bf16[16,128,128]{2,1,0:T(8,128)(2,1)S(1)}, u32[]{:S(2)}, u32[]{:S(2)}) async-start(bf16[16,128,128]{2,1,0:T(8,128)(2,1)} %shard_map.118), calls=%async_computation.1 | async-start | bytes 1048576 | tf_op jit(solution)/shard_map/all_to_all | solution.py:305
  38.0 42.3 %copy-start = (bf16[256,2048]{1,0:T(8,128)(2,1)S(1)}, bf16[256,2048]{1,0:T(8,128)(2,1)}, u32[]{:S(2)}) copy-start(bf16[256,2048]{1,0:T(8,128)(2,1)} %resid_ref.1) | copy-start | bytes 3145732
  38.0 42.3 %copy-start.7 = (f32[2048]{0:T(1024)S(1)}, f32[2048]{0:T(1024)}, u32[]{:S(2)}) copy-start(f32[2048]{0:T(1024)} %param.18) | copy-start | bytes 24580
  38.0 42.3 %copy-start.9 = (s32[256,2]{0,1:T(2,128)S(1)}, s32[256,2]{0,1:T(2,128)}, u32[]{:S(2)}) copy-start(s32[256,2]{0,1:T(2,128)} %param.19) | copy-start | bytes 6148
  38.0 10.3 %collective-permute-start.2 = (bf16[64,256]{1,0:T(8,128)(2,1)S(1)}, bf16[64,256]{1,0:T(8,128)(2,1)S(1)}, u32[]{:S(2)}, u32[]{:S(2)}) collective-permute-start(bf16[64,256]{1,0:T(8,128)(2,1)S(1)} %bitcast.21), channel_id=1, source_target_pairs={{0,48},{16,0},{32,16},{48,32},{1,49},{17,1},{33,17},{49,33},{2,50}... | collective-permute-start | bytes 98312 | tf_op jit(solution)/shard_map/ppermute | solution.py:337
  42.8 7.3 %collective-permute-start.1 = (bf16[64,256]{1,0:T(8,128)(2,1)S(1)}, bf16[64,256]{1,0:T(8,128)(2,1)S(1)}, u32[]{:S(2)}, u32[]{:S(2)}) collective-permute-start(bf16[64,256]{1,0:T(8,128)(2,1)S(1)} %bitcast.22), channel_id=1, source_target_pairs={{0,32},{16,48},{32,0},{48,16},{1,33},{17,49},{33,1},{49,17},{2,34}... | collective-permute-start | bytes 98312 | tf_op jit(solution)/shard_map/ppermute | solution.py:337
  45.6 7.0 %collective-permute-start = (bf16[64,256]{1,0:T(8,128)(2,1)S(1)}, bf16[64,256]{1,0:T(8,128)(2,1)S(1)}, u32[]{:S(2)}, u32[]{:S(2)}) collective-permute-start(bf16[64,256]{1,0:T(8,128)(2,1)S(1)} %bitcast.23), channel_id=1, source_target_pairs={{0,16},{16,32},{32,48},{48,0},{1,17},{17,33},{33,49},{49,1},{2,18}... | collective-permute-start | bytes 98312 | tf_op jit(solution)/shard_map/ppermute | solution.py:337
  82.3 48.2 %copy-start.3 = (bf16[1,256,2048]{2,1,0:T(8,128)(2,1)S(1)}, bf16[1,256,2048]{2,1,0:T(8,128)(2,1)}, u32[]{:S(2)}) copy-start(bf16[1,256,2048]{2,1,0:T(8,128)(2,1)} %param.23) | copy-start | bytes 3145732
  104.0 26.5 %copy-start.2 = (bf16[1,2048,256]{2,1,0:T(8,128)(2,1)S(1)}, bf16[1,2048,256]{2,1,0:T(8,128)(2,1)}, u32[]{:S(2)}) copy-start(bf16[1,2048,256]{2,1,0:T(8,128)(2,1)} %param.22) | copy-start | bytes 3145732
  104.1 26.4 %copy-start.1 = (bf16[1,2048,256]{2,1,0:T(8,128)(2,1)S(1)}, bf16[1,2048,256]{2,1,0:T(8,128)(2,1)}, u32[]{:S(2)}) copy-start(bf16[1,2048,256]{2,1,0:T(8,128)(2,1)} %param.21) | copy-start | bytes 3145732
  104.1 13.4 %collective-permute-start.4 = (bf16[1296,128]{1,0:T(8,128)(2,1)S(1)}, bf16[1296,128]{1,0:T(8,128)(2,1)S(1)}, u32[]{:S(2)}, u32[]{:S(2)}) collective-permute-start(bf16[1296,128]{1,0:T(8,128)(2,1)S(1)} %get-tuple-element.28.refs_0_), channel_id=1, source_target_pairs={{0,14},{2,0},{4,2},{6,4},{8,6},{10,8},{12,10},{14,12},{1,15},{3,1}... | collective-permute-start | bytes 995336 | tf_op jit(solution)/shard_map/ppermute | solution.py:301
  108.0 10.8 %collective-permute-start.3 = (bf16[1296,128]{1,0:T(8,128)(2,1)S(1)}, bf16[1296,128]{1,0:T(8,128)(2,1)S(1)}, u32[]{:S(2)}, u32[]{:S(2)}) collective-permute-start(bf16[1296,128]{1,0:T(8,128)(2,1)S(1)} %get-tuple-element.28.refs_0_), channel_id=1, source_target_pairs={{0,2},{2,4},{4,6},{6,8},{8,10},{10,12},{12,14},{14,0},{1,3},{3,5},... | collective-permute-start | bytes 995336 | tf_op jit(solution)/shard_map/ppermute | solution.py:301
  110.1 13.0 %collective-permute-start.6 = (bf16[640,128]{1,0:T(8,128)(2,1)S(1)}, bf16[640,128]{1,0:T(8,128)(2,1)S(1)}, u32[]{:S(2)}, u32[]{:S(2)}) collective-permute-start(bf16[640,128]{1,0:T(8,128)(2,1)S(1)} %get-tuple-element.30), channel_id=1, source_target_pairs={{0,12},{2,14},{4,0},{6,2},{8,4},{10,6},{12,8},{14,10},{1,13},{3,15... | collective-permute-start | bytes 491528 | tf_op jit(solution)/shard_map/ppermute | solution.py:301
  115.6 11.3 %collective-permute-start.5 = (bf16[656,128]{1,0:T(8,128)(2,1)S(1)}, bf16[656,128]{1,0:T(8,128)(2,1)S(1)}, u32[]{:S(2)}, u32[]{:S(2)}) collective-permute-start(bf16[656,128]{1,0:T(8,128)(2,1)S(1)} %get-tuple-element.29), channel_id=1, source_target_pairs={{0,4},{2,6},{4,8},{6,10},{8,12},{10,14},{12,0},{14,2},{1,5},{3,7},... | collective-permute-start | bytes 503816 | tf_op jit(solution)/shard_map/ppermute | solution.py:301
  118.8 11.7 %collective-permute-start.8 = (bf16[2592,128]{1,0:T(8,128)(2,1)S(1)}, bf16[2592,128]{1,0:T(8,128)(2,1)S(1)}, u32[]{:S(2)}, u32[]{:S(2)}) collective-permute-start(bf16[2592,128]{1,0:T(8,128)(2,1)S(1)} %pad_maximum_fusion), channel_id=1, source_target_pairs={{0,1},{1,0},{2,3},{3,2},{4,5},{5,4},{6,7},{7,6},{8,9},{9,8},{10,11... | collective-permute-start | bytes 1990664 | tf_op jit(solution)/shard_map/ppermute | solution.py:375
  120.7 8.2 %collective-permute-start.7 = (bf16[1296,128]{1,0:T(8,128)(2,1)S(1)}, bf16[1296,128]{1,0:T(8,128)(2,1)S(1)}, u32[]{:S(2)}, u32[]{:S(2)}) collective-permute-start(bf16[1296,128]{1,0:T(8,128)(2,1)S(1)} %get-tuple-element.28.refs_0_), channel_id=1, source_target_pairs={{0,1},{1,0},{2,3},{3,2},{4,5},{5,4},{6,7},{7,6},{8,9},{9,8},{10,11... | collective-permute-start | bytes 995336 | tf_op jit(solution)/shard_map/ppermute | solution.py:375
  127.0 3.5 %collective-permute-start.9 = (bf16[1296,128]{1,0:T(8,128)(2,1)S(1)}, bf16[1296,128]{1,0:T(8,128)(2,1)S(1)}, u32[]{:S(2)}, u32[]{:S(2)}) collective-permute-start(bf16[1296,128]{1,0:T(8,128)(2,1)S(1)} %pad_maximum_fusion.1), channel_id=1, source_target_pairs={{0,1},{1,0},{2,3},{3,2},{4,5},{5,4},{6,7},{7,6},{8,9},{9,8},{10,11... | collective-permute-start | bytes 995336 | tf_op jit(solution)/shard_map/ppermute | solution.py:375
  133.6 4.5 %collective-permute-start.10 = (bf16[3840,128]{1,0:T(8,128)(2,1)S(1)}, bf16[3840,128]{1,0:T(8,128)(2,1)S(1)}, u32[]{:S(2)}, u32[]{:S(2)}) collective-permute-start(bf16[3840,128]{1,0:T(8,128)(2,1)S(1)} %get-tuple-element.32), channel_id=1, source_target_pairs={{0,1},{1,0},{2,3},{3,2},{4,5},{5,4},{6,7},{7,6},{8,9},{9,8},{10,11... | collective-permute-start | bytes 2949128 | tf_op jit(solution)/shard_map/ppermute | solution.py:386
  135.6 8.5 %collective-permute-start.13 = (bf16[1280,128]{1,0:T(8,128)(2,1)S(1)}, bf16[1280,128]{1,0:T(8,128)(2,1)S(1)}, u32[]{:S(2)}, u32[]{:S(2)}) collective-permute-start(bf16[1280,128]{1,0:T(8,128)(2,1)S(1)} %get-tuple-element.34), channel_id=1, source_target_pairs={{0,1},{1,0},{2,3},{3,2},{4,5},{5,4},{6,7},{7,6},{8,9},{9,8},{10,11... | collective-permute-start | bytes 983048 | tf_op jit(solution)/shard_map/ppermute | solution.py:385
  138.2 23.4 %collective-permute-start.12 = (bf16[1280,128]{1,0:T(8,128)(2,1)S(1)}, bf16[1280,128]{1,0:T(8,128)(2,1)S(1)}, u32[]{:S(2)}, u32[]{:S(2)}) collective-permute-start(bf16[1280,128]{1,0:T(8,128)(2,1)S(1)} %get-tuple-element.37), channel_id=1, source_target_pairs={{0,14},{2,0},{4,2},{6,4},{8,6},{10,8},{12,10},{14,12},{1,15},{3,1}... | collective-permute-start | bytes 983048 | tf_op jit(solution)/shard_map/ppermute | solution.py:301
  140.1 21.5 %collective-permute-start.11 = (bf16[1280,128]{1,0:T(8,128)(2,1)S(1)}, bf16[1280,128]{1,0:T(8,128)(2,1)S(1)}, u32[]{:S(2)}, u32[]{:S(2)}) collective-permute-start(bf16[1280,128]{1,0:T(8,128)(2,1)S(1)} %get-tuple-element.38), channel_id=1, source_target_pairs={{0,2},{2,4},{4,6},{6,8},{8,10},{10,12},{12,14},{14,0},{1,3},{3,5},... | collective-permute-start | bytes 983048 | tf_op jit(solution)/shard_map/ppermute | solution.py:301
  144.2 11.1 %collective-permute-start.15 = (bf16[640,128]{1,0:T(8,128)(2,1)S(1)}, bf16[640,128]{1,0:T(8,128)(2,1)S(1)}, u32[]{:S(2)}, u32[]{:S(2)}) collective-permute-start(bf16[640,128]{1,0:T(8,128)(2,1)S(1)} %get-tuple-element.39), channel_id=1, source_target_pairs={{0,12},{2,14},{4,0},{6,2},{8,4},{10,6},{12,8},{14,10},{1,13},{3,15... | collective-permute-start | bytes 491528 | tf_op jit(solution)/shard_map/ppermute | solution.py:301
  148.7 40.6 %copy-start.8 = (f32[256,2]{0,1:T(2,128)S(1)}, f32[256,2]{0,1:T(2,128)}, u32[]{:S(2)}) copy-start(f32[256,2]{0,1:T(2,128)} %param.20) | copy-start | bytes 6148
  148.7 12.9 %collective-permute-start.14 = (bf16[640,128]{1,0:T(8,128)(2,1)S(1)}, bf16[640,128]{1,0:T(8,128)(2,1)S(1)}, u32[]{:S(2)}, u32[]{:S(2)}) collective-permute-start(bf16[640,128]{1,0:T(8,128)(2,1)S(1)} %get-tuple-element.40), channel_id=1, source_target_pairs={{0,4},{2,6},{4,8},{6,10},{8,12},{10,14},{12,0},{14,2},{1,5},{3,7},... | collective-permute-start | bytes 491528 | tf_op jit(solution)/shard_map/ppermute | solution.py:301

commit v6 on v5

--- a/solution.py
+++ b/solution.py
@@ -54,15 +54,14 @@
     return hi, mid, rest - mid
 
 
-def attend(at_ref, q0_ref, q1_ref, q2_ref, q3_ref, kv_ref, gate_ref, out_ref, qs_ref, s_ref, m_ref, acc_ref):
+def attend(at_ref, q_ref, kv_ref, gate_ref, out0_ref, out1_ref, out2_ref, out3_ref, qs_ref, s_ref, m_ref, acc_ref, o_ref):
     z, x = at_ref[0], at_ref[1]
     first = gate_ref[:, pl.ds(pl.multiple_of(z * ROW, ROW), TOK)][:, 0:1]
     row64 = lax.broadcasted_iota(jnp.int32, (HD, TOK), 0)
     ones = jnp.where(row64 < 3, 1.0, 0.0).astype(bf)
-    for j, q_ref in enumerate((q0_ref, q1_ref, q2_ref, q3_ref)):
-        place = pl.multiple_of(lax.rem(x + NX - j, NX) * TOK, TOK)
-        qs_ref[0:HD, pl.ds(place, TOK)] = q_ref[...] * bf(HD**-0.5)
-        qs_ref[HD : 2 * HD, pl.ds(place, TOK)] = ones
+    for j in range(NX):
+        qs_ref[0:HD, j * TOK : (j + 1) * TOK] = q_ref[j] * bf(HD**-0.5)
+        qs_ref[HD : 2 * HD, j * TOK : (j + 1) * TOK] = ones
 
     def scores(zk):
         place = pl.multiple_of(zk * ROW + x * TOK, TOK)
@@ -99,16 +98,17 @@
     total = acc_ref[HD : HD + 1, :]
     hi, mid, lo = three(m + jnp.log(total))
     stats = jnp.where(row16 == 0, hi, jnp.where(row16 == 1, mid, jnp.where(row16 == 2, lo, 0.0))).astype(bf)
-    o = (acc_ref[0:HD, :] / total).astype(bf)
-    for j in range(NX):
-        out_ref[j, 0:HD, :] = o[:, j * TOK : (j + 1) * TOK]
-        out_ref[j, HD : HD + 16, :] = stats[:, j * TOK : (j + 1) * TOK]
-
-
-def merge(part_ref, out_ref):
+    o_ref[0:HD, :] = (acc_ref[0:HD, :] / total).astype(bf)
+    o_ref[HD : HD + 16, :] = stats
+    for j, out_ref in enumerate((out0_ref, out1_ref, out2_ref, out3_ref)):
+        out_ref[...] = o_ref[:, pl.ds(pl.multiple_of(lax.rem(x + j, NX) * TOK, TOK), TOK)]
+
+
+def merge(*refs):
+    parts, out_ref = refs[0:NX], refs[NX]
     ls = []
     for i in range(NX):
-        st = part_ref[i, HD : HD + 16, :].astype(f32)
+        st = parts[i][HD : HD + 16, :].astype(f32)
         ls.append(st[0:1] + st[1:2] + st[2:3])
     m = ls[0]
     for v in ls[1:]:
@@ -118,11 +118,14 @@
     for i in range(NX):
         w = jnp.exp(ls[i] - m)
         total = total + w
-        acc = acc + w * part_ref[i, 0:HD, :].astype(f32)
+        acc = acc + w * parts[i][0:HD, :].astype(f32)
     out_ref[...] = (acc / total).astype(bf)
 
 
-def spread_weight(w_ref, out_ref):
+def prepare(k_ref, v_ref, w_ref, kv_ref, out_ref):
+    for z in range(NZ):
+        kv_ref[z, 0:HD, :] = k_ref[...]
+        kv_ref[z, HD : 2 * HD, :] = v_ref[...]
     for y in range(NY):
         for c in range(NC):
             for q in range(2):
@@ -130,7 +133,26 @@
                 out_ref[y * NC + c, q * HD : (q + 1) * HD, :] = w_ref[:, block * COLS : (block + 1) * COLS]
 
 
-def project(at_ref, att_ref, w_ref, resid_ref, gain_ref, routes_ref, stream_ref, out_ref, slots_ref):
+def route(routes_ref, pick_ref, slots_ref):
+    e0, e1 = routes_ref[0:1, :], routes_ref[1:2, :]
+    io = lax.broadcasted_iota(jnp.int32, (NSP, TOK), 0)
+    h0, h1 = io == e0, io == e1
+    hit = jnp.where(h0, 1.0, jnp.where(h1, 1.0, 0.0)).astype(bf)
+    ia = lax.broadcasted_iota(jnp.int32, (TOK, TOK), 0)
+    ib = lax.broadcasted_iota(jnp.int32, (TOK, TOK), 1)
+    upper = jnp.where(ia < ib, 1.0, 0.0).astype(bf)
+    before = jnp.dot(hit, upper, preferred_element_type=f32)
+    r0 = jnp.sum(jnp.where(h0, before, 0.0), axis=0, keepdims=True).astype(jnp.int32)
+    r1 = jnp.sum(jnp.where(h1, before, 0.0), axis=0, keepdims=True).astype(jnp.int32)
+    slots_ref[...] = jnp.concatenate([2 * SLOT * e0 + r0, 2 * SLOT * e1 + r1, jnp.zeros((6, TOK), jnp.int32)], axis=0)
+    s0 = e0 * SEND + r0
+    s1 = e1 * SEND + r1
+    ir = lax.broadcasted_iota(jnp.int32, (NSP * SEND, TOK), 0)
+    hits = (ir == s0) | (ir == s1) | (ir == s0 + CAP) | (ir == s1 + CAP)
+    pick_ref[...] = jnp.where(hits, 1.0, 0.0).astype(bf)
+
+
+def project(at_ref, att_ref, w_ref, resid_ref, gain_ref, pick_ref, stream_ref, out_ref):
     c0 = pl.multiple_of(at_ref[0], COLS)
     c1 = pl.multiple_of(at_ref[1], COLS)
     weights = [jnp.concatenate([w_ref[t, q * HD : (q + 1) * HD, :] for t in range(NTP)], axis=0) for q in range(2)]
@@ -146,23 +168,7 @@
     scaled = (stream * gain).astype(bf)
     wide = (TOK, COLS)
     rows = jnp.concatenate([scaled, jnp.broadcast_to(hi, wide), jnp.broadcast_to(lo, wide)], axis=1)
-    e0, e1 = routes_ref[0:1, :], routes_ref[1:2, :]
-    io = lax.broadcasted_iota(jnp.int32, (NSP, TOK), 0)
-    h0, h1 = io == e0, io == e1
-    hit = jnp.where(h0, 1.0, jnp.where(h1, 1.0, 0.0)).astype(bf)
-    ia = lax.broadcasted_iota(jnp.int32, (TOK, TOK), 0)
-    ib = lax.broadcasted_iota(jnp.int32, (TOK, TOK), 1)
-    upper = jnp.where(ia < ib, 1.0, 0.0).astype(bf)
-    before = jnp.dot(hit, upper, preferred_element_type=f32)
-    r0 = jnp.sum(jnp.where(h0, before, 0.0), axis=0, keepdims=True).astype(jnp.int32)
-    r1 = jnp.sum(jnp.where(h1, before, 0.0), axis=0, keepdims=True).astype(jnp.int32)
-    slots_ref[...] = jnp.concatenate([2 * SLOT * e0 + r0, 2 * SLOT * e1 + r1, jnp.zeros((6, TOK), jnp.int32)], axis=0)
-    s0 = e0 * SEND + r0
-    s1 = e1 * SEND + r1
-    ir = lax.broadcasted_iota(jnp.int32, (NSP * SEND, TOK), 0)
-    hits = (ir == s0) | (ir == s1) | (ir == s0 + CAP) | (ir == s1 + CAP)
-    pick = jnp.where(hits, 1.0, 0.0).astype(bf)
-    sent = jnp.dot(pick, rows, preferred_element_type=f32).reshape(NSP, SEND, 4 * COLS)
+    sent = jnp.dot(pick_ref[...], rows, preferred_element_type=f32).reshape(NSP, SEND, 4 * COLS)
     shape = (NSP, SEND, COLS)
     rank = lax.broadcasted_iota(jnp.int32, shape, 1)
     lane = lax.broadcasted_iota(jnp.int32, shape, 2)
@@ -325,37 +331,42 @@
     low = (lax.rem(y, half) * NC + c) * COLS
     at_cols = jnp.stack([low, low + half * NC * COLS, y // half]).astype(jnp.int32)
     at = jnp.stack([z, x]).astype(jnp.int32)
-    w_send = call(spread_weight, sds((NTP, 2 * HD, COLS), bf), (out_weight,))
-    kv = jnp.concatenate([keys.T, values.T], axis=0)
-    kv, w_send, at, at_cols = lax.optimization_barrier(
-        (jnp.broadcast_to(kv[None], (NZ, 2 * HD, TOK)), w_send, at, at_cols)
-    )
-    kv = exchange(kv, "z")
+    kv_send, w_send = call(
+        prepare,
+        (sds((NZ, 2 * HD, TOK), bf), sds((NTP, 2 * HD, COLS), bf)),
+        (keys.T, values.T, out_weight),
+    )
+    kv_send, w_send, at, at_cols = lax.optimization_barrier((kv_send, w_send, at, at_cols))
+    kv = exchange(kv_send, "z")
+    q_send, kv = lax.optimization_barrier((jnp.broadcast_to(queries.T[None], (NX, HD, TOK)), kv))
+    q = exchange(q_send, "x")
     w_cols = exchange(w_send, TP)
-    q = [queries.T]
-    for n in range(1, NX):
-        q.append(lax.ppermute(q[0], "x", [(i, (i + n) % NX) for i in range(NX)]))
-    parts = call(
+    sent = call(
         attend,
-        sds((NX, HD + 16, TOK), bf),
-        (at, *q, kv, cum_gate),
+        (sds((HD + 16, TOK), bf),) * NX,
+        (at, q, kv, cum_gate),
         smem=1,
         scratch=(
             pltpu.VMEM((2 * HD, ROW), bf),
             pltpu.VMEM((NZ, TOK, ROW), f32),
             pltpu.VMEM((8, ROW), f32),
             pltpu.VMEM((HD + 16, ROW), f32),
+            pltpu.VMEM((HD + 16, ROW), bf),
         ),
         limit=24,
     )
-    parts, w_cols = lax.optimization_barrier((parts, w_cols))
-    parts = exchange(parts, "x")
-    attended = call(merge, sds((HD, TOK), bf), (parts,))
+    parts = [sent[0]]
+    for n in range(1, NX):
+        parts.append(lax.ppermute(sent[n], "x", [(i, (i + n) % NX) for i in range(NX)]))
+    pick, slots = call(
+        route, (sds((NSP * SEND, TOK), bf), sds((8, TOK), jnp.int32)), (routes.T,)
+    )
+    attended = call(merge, sds((HD, TOK), bf), tuple(parts))
     attended = lax.all_gather(attended, TP, axis=0, tiled=True)
-    stream, outgoing, slots = call(
+    stream, outgoing = call(
         project,
-        (sds((TOK, COLS), f32), sds((NSP, SEND, COLS), bf), sds((8, TOK), jnp.int32)),
-        (at_cols, attended, w_cols, resid, norm_gain.reshape(1, D), routes.T),
+        (sds((TOK, COLS), f32), sds((NSP, SEND, COLS), bf)),
+        (at_cols, attended, w_cols, resid, norm_gain.reshape(1, D), pick),
         smem=1,
     )
     arrived = exchange(outgoing, SP)

time: 192 us -> 193 us (level)
  waiting for transfers between devices: 21.5 us -> 19 us
  blocking collectives: 103 us -> 105 us
    all_to_all x4, blocking collectives: 85.3 us -> 88.2 us  [exchange(): return lax.all_to_all(v, axis, 0, 0, tiled=True)]
    ppermute x3, waiting for transfers between devices: 4.21 us -> 1.69 us  [layer(): lax.ppermute(sent[n], 'x', [(i, (i + n) % NX) for i in range(NX)])]
    pallas_call x8 -> x9, Pallas kernels: 9.36 us -> 10.5 us  [call(): pl.pallas_call(body, out_shape=out_shape, in_specs=specs, out_specs=tuple...]
  transfers between devices with their start and end apart: 17 -> 17, of which waited for: 8 -> 7; matrix products, arithmetic and copies ran while one was open for 0% -> 0% of each run, Pallas kernels for 1% -> 1%
where the time goes in v6:
time: 193 us; the launch traced here: 192 us
  blocking collectives  105 us (54%)
  starting transfers between devices  53.4 us (28%)
  waiting for transfers between devices  19 us (10%)
  Pallas kernels  10.5 us (5%)
  local copies, waits for them, and re-layouts  2.52 us (1%)
    all_to_all x4, blocking collectives, exchange(): return lax.all_to_all(v, axis, 0, 0, tiled=True)  88.2 us
    ppermute x8, starting transfers between devices, shift(): return lax.ppermute(v, Y, [(i, (i + by) % NY) for i in range(NY)])  26 us
    all_gather x1, blocking collectives, layer(): attended = lax.all_gather(attended, TP, axis=0, tiled=True)  17 us
    ppermute x8, waiting for transfers between devices, shift(): return lax.ppermute(v, Y, [(i, (i + by) % NY) for i in range(NY)])  15.6 us
    pallas_call x9, Pallas kernels, call(): pl.pallas_call(body, out_shape=out_shape, in_specs=specs, out_specs=tuple...  10.5 us
    ppermute x3, starting transfers between devices, layer(): lax.ppermute(sent[n], 'x', [(i, (i + n) % NX) for i in range(NX)])  9.18 us
    all_to_all x1, starting transfers between devices, exchange(): return lax.all_to_all(v, axis, 0, 0, tiled=True)  7.69 us
    ppermute x3, starting transfers between devices, layer(): others.append(lax.ppermute(v, 'c', swap))  6.25 us
  transfers between devices with their start and end apart: 17, of which 7 were waited for; matrix products, arithmetic and copies ran while one was open for 0% of the time, Pallas kernels for 1%

profile of v6, /device:TPU:8, one launch (start us, length us, event | category | flops | bytes accessed | tf_op | source)
XLA Modules:
  0.0 191.5 jit_solution(11262483612850973645)
XLA Ops:
  3.5 27.7 %all_to_all.25.kv_ref = bf16[8,128,256]{2,1,0:T(8,128)(2,1)S(1)} all-to-all(bf16[8,128,256]{2,1,0:T(8,128)(2,1)S(1)} %get-tuple-element.32), channel_id=1, replica_groups=mesh['z'=8,'x'=4,'yh'=2,'yl'=4,'c'=2] {'z'}, dimensions={0} | all-to-all | bytes 1048576 | tf_op jit(solution)/shard_map/all_to_all | solution.py:311
  31.3 10.1 %all_to_all.26.q_ref = bf16[4,64,256]{2,1,0:T(8,128)(2,1)S(1)} all-to-all(bf16[4,64,256]{2,1,0:T(8,128)(2,1)S(1)} %broadcast_in_dim.2), channel_id=1, replica_groups=mesh['z'=8,'x'=4,'yh'=2,'yl'=4,'c'=2] {'x'}, dimensions={0} | all-to-all | bytes 262144 | tf_op jit(solution)/shard_map/all_to_all | solution.py:311
  41.3 7.7 %all-to-all-start.2 = ((bf16[16,128,128]{2,1,0:T(8,128)(2,1)}), bf16[16,128,128]{2,1,0:T(8,128)(2,1)S(1)}, u32[]{:S(2)}, u32[]{:S(2)}) async-start(bf16[16,128,128]{2,1,0:T(8,128)(2,1)} %get-tuple-element.39), calls=%async_computation.2 | async-start | bytes 1048576 | tf_op jit(solution)/shard_map/all_to_all | solution.py:311
  49.0 1.3 shard_map.119
  50.4 2.5 %collective-permute-start = (bf16[80,256]{1,0:T(8,128)(2,1)S(1)}, bf16[80,256]{1,0:T(8,128)(2,1)S(1)}, u32[]{:S(2)}, u32[]{:S(2)}) collective-permute-start(bf16[80,256]{1,0:T(8,128)(2,1)S(1)} %get-tuple-element.36), channel_id=1, source_target_pairs={{0,16},{16,32},{32,48},{48,0},{1,17},{17,33},{33,49},{49,1},{2,18}... | collective-permute-start | bytes 122888 | tf_op jit(solution)/shard_map/ppermute | solution.py:360
  52.9 4.0 %collective-permute-start.1 = (bf16[80,256]{1,0:T(8,128)(2,1)S(1)}, bf16[80,256]{1,0:T(8,128)(2,1)S(1)}, u32[]{:S(2)}, u32[]{:S(2)}) collective-permute-start(bf16[80,256]{1,0:T(8,128)(2,1)S(1)} %get-tuple-element.37), channel_id=1, source_target_pairs={{0,32},{16,48},{32,0},{48,16},{1,33},{17,49},{33,1},{49,17},{2,34}... | collective-permute-start | bytes 122888 | tf_op jit(solution)/shard_map/ppermute | solution.py:360
  56.9 2.7 %collective-permute-start.2 = (bf16[80,256]{1,0:T(8,128)(2,1)S(1)}, bf16[80,256]{1,0:T(8,128)(2,1)S(1)}, u32[]{:S(2)}, u32[]{:S(2)}) collective-permute-start(bf16[80,256]{1,0:T(8,128)(2,1)S(1)} %get-tuple-element.38), channel_id=1, source_target_pairs={{0,48},{16,0},{32,16},{48,32},{1,49},{17,1},{33,17},{49,33},{2,50}... | collective-permute-start | bytes 122888 | tf_op jit(solution)/shard_map/ppermute | solution.py:360
  59.6 1.4 shard_map.121
  61.1 1.7 collective-permute-done.2.refs_3_
  62.8 17.0 %all_gather.3.att_ref = bf16[1024,256]{1,0:T(8,128)(2,1)S(1)} all-gather(bf16[64,256]{1,0:T(8,128)(2,1)S(1)} %shard_map.120), channel_id=1, replica_groups=mesh['z'=8,'x'=4,'yh'=2,'yl'=4,'c'=2] {'yh','yl','c'}, dimensions={0}, use_global_device_ids=true | all-gather | bytes 557056 | tf_op jit(solution)/shard_map/all_gather | solution.py:365
  79.8 1.6 shard_map.122
  81.5 23.1 %all_to_all.27.in_ref = bf16[32,48,128]{2,1,0:T(8,128)(2,1)S(1)} all-to-all(bf16[32,48,128]{2,1,0:T(8,128)(2,1)S(1)} %get-tuple-element.41), channel_id=1, replica_groups=mesh['z'=8,'x'=4,'yh'=2,'yl'=4,'c'=2] {'z','x'}, dimensions={0} | all-to-all | bytes 786432 | tf_op jit(solution)/shard_map/all_to_all | solution.py:311
  104.8 3.8 %collective-permute-start.4 = (bf16[1296,128]{1,0:T(8,128)(2,1)S(1)}, bf16[1296,128]{1,0:T(8,128)(2,1)S(1)}, u32[]{:S(2)}, u32[]{:S(2)}) collective-permute-start(bf16[1296,128]{1,0:T(8,128)(2,1)S(1)} %get-tuple-element.42.refs_0_), channel_id=1, source_target_pairs={{0,14},{2,0},{4,2},{6,4},{8,6},{10,8},{12,10},{14,12},{1,15},{3,1}... | collective-permute-start | bytes 995336 | tf_op jit(solution)/shard_map/ppermute | solution.py:307
  108.6 2.2 %collective-permute-start.3 = (bf16[1296,128]{1,0:T(8,128)(2,1)S(1)}, bf16[1296,128]{1,0:T(8,128)(2,1)S(1)}, u32[]{:S(2)}, u32[]{:S(2)}) collective-permute-start(bf16[1296,128]{1,0:T(8,128)(2,1)S(1)} %get-tuple-element.42.refs_0_), channel_id=1, source_target_pairs={{0,2},{2,4},{4,6},{6,8},{8,10},{10,12},{12,14},{14,0},{1,3},{3,5},... | collective-permute-start | bytes 995336 | tf_op jit(solution)/shard_map/ppermute | solution.py:307
  110.8 5.5 %collective-permute-start.6 = (bf16[640,128]{1,0:T(8,128)(2,1)S(1)}, bf16[640,128]{1,0:T(8,128)(2,1)S(1)}, u32[]{:S(2)}, u32[]{:S(2)}) collective-permute-start(bf16[640,128]{1,0:T(8,128)(2,1)S(1)} %get-tuple-element.44), channel_id=1, source_target_pairs={{0,12},{2,14},{4,0},{6,2},{8,4},{10,6},{12,8},{14,10},{1,13},{3,15... | collective-permute-start | bytes 491528 | tf_op jit(solution)/shard_map/ppermute | solution.py:307
  116.3 1.9 %collective-permute-start.5 = (bf16[656,128]{1,0:T(8,128)(2,1)S(1)}, bf16[656,128]{1,0:T(8,128)(2,1)S(1)}, u32[]{:S(2)}, u32[]{:S(2)}) collective-permute-start(bf16[656,128]{1,0:T(8,128)(2,1)S(1)} %get-tuple-element.43), channel_id=1, source_target_pairs={{0,4},{2,6},{4,8},{6,10},{8,12},{10,14},{12,0},{14,2},{1,5},{3,7},... | collective-permute-start | bytes 503816 | tf_op jit(solution)/shard_map/ppermute | solution.py:307
  119.4 1.9 %collective-permute-start.8 = (bf16[2592,128]{1,0:T(8,128)(2,1)S(1)}, bf16[2592,128]{1,0:T(8,128)(2,1)S(1)}, u32[]{:S(2)}, u32[]{:S(2)}) collective-permute-start(bf16[2592,128]{1,0:T(8,128)(2,1)S(1)} %pad_maximum_fusion), channel_id=1, source_target_pairs={{0,1},{1,0},{2,3},{3,2},{4,5},{5,4},{6,7},{7,6},{8,9},{9,8},{10,11... | collective-permute-start | bytes 1990664 | tf_op jit(solution)/shard_map/ppermute | solution.py:386
  121.4 2.4 %collective-permute-start.7 = (bf16[1296,128]{1,0:T(8,128)(2,1)S(1)}, bf16[1296,128]{1,0:T(8,128)(2,1)S(1)}, u32[]{:S(2)}, u32[]{:S(2)}) collective-permute-start(bf16[1296,128]{1,0:T(8,128)(2,1)S(1)} %get-tuple-element.42.refs_0_), channel_id=1, source_target_pairs={{0,1},{1,0},{2,3},{3,2},{4,5},{5,4},{6,7},{7,6},{8,9},{9,8},{10,11... | collective-permute-start | bytes 995336 | tf_op jit(solution)/shard_map/ppermute | solution.py:386
  123.8 3.8 %collective-permute-done.5.refs_3_ = bf16[656,128]{1,0:T(8,128)(2,1)S(1)} collective-permute-done((bf16[656,128]{1,0:T(8,128)(2,1)S(1)}, bf16[656,128]{1,0:T(8,128)(2,1)S(1)}, u32[]{:S(2)}, u32[]{:S(2)}) %collective-permute-start.5) | collective-permute-done | bytes 167968 | tf_op jit(solution)/shard_map/ppermute | solution.py:307
  127.6 1.9 %collective-permute-start.9 = (bf16[1296,128]{1,0:T(8,128)(2,1)S(1)}, bf16[1296,128]{1,0:T(8,128)(2,1)S(1)}, u32[]{:S(2)}, u32[]{:S(2)}) collective-permute-start(bf16[1296,128]{1,0:T(8,128)(2,1)S(1)} %pad_maximum_fusion.1), channel_id=1, source_target_pairs={{0,1},{1,0},{2,3},{3,2},{4,5},{5,4},{6,7},{7,6},{8,9},{9,8},{10,11... | collective-permute-start | bytes 995336 | tf_op jit(solution)/shard_map/ppermute | solution.py:386
  129.6 1.5 collective-permute-done.9.refs_7_
  131.1 3.0 %shard_map.124 = (bf16[1280,128]{1,0:T(8,128)(2,1)S(1)}, bf16[3840,128]{1,0:T(8,128)(2,1)S(1)}, bf16[1280,128]{1,0:T(8,128)(2,1)S(1)}, bf16[3840,128]{1,0:T(8,128)(2,1)S(1)}) custom-call(s32[2]{0:T(128)S(1)} %pad_add_fusion.at_ref, bf16[1296,128]{1,0:T(8,128)(2,1)S(1)} %get-tuple-element.42.refs_0_, bf16[1296,128]{1,0:T(8,128)(2,1)S(1)} %collective-permute-done.3.refs_1_, ...), custom_call_target="tpu_custom_call" | custom-call | tf_op jit(solution)/shard_map/pallas_call | solution.py:39
  134.2 2.0 %collective-permute-start.10 = (bf16[3840,128]{1,0:T(8,128)(2,1)S(1)}, bf16[3840,128]{1,0:T(8,128)(2,1)S(1)}, u32[]{:S(2)}, u32[]{:S(2)}) collective-permute-start(bf16[3840,128]{1,0:T(8,128)(2,1)S(1)} %get-tuple-element.46), channel_id=1, source_target_pairs={{0,1},{1,0},{2,3},{3,2},{4,5},{5,4},{6,7},{7,6},{8,9},{9,8},{10,11... | collective-permute-start | bytes 2949128 | tf_op jit(solution)/shard_map/ppermute | solution.py:397
  136.2 2.3 %collective-permute-start.13 = (bf16[1280,128]{1,0:T(8,128)(2,1)S(1)}, bf16[1280,128]{1,0:T(8,128)(2,1)S(1)}, u32[]{:S(2)}, u32[]{:S(2)}) collective-permute-start(bf16[1280,128]{1,0:T(8,128)(2,1)S(1)} %get-tuple-element.48), channel_id=1, source_target_pairs={{0,1},{1,0},{2,3},{3,2},{4,5},{5,4},{6,7},{7,6},{8,9},{9,8},{10,11... | collective-permute-start | bytes 983048 | tf_op jit(solution)/shard_map/ppermute | solution.py:396
  138.8 1.9 %collective-permute-start.12 = (bf16[1280,128]{1,0:T(8,128)(2,1)S(1)}, bf16[1280,128]{1,0:T(8,128)(2,1)S(1)}, u32[]{:S(2)}, u32[]{:S(2)}) collective-permute-start(bf16[1280,128]{1,0:T(8,128)(2,1)S(1)} %get-tuple-element.51), channel_id=1, source_target_pairs={{0,14},{2,0},{4,2},{6,4},{8,6},{10,8},{12,10},{14,12},{1,15},{3,1}... | collective-permute-start | bytes 983048 | tf_op jit(solution)/shard_map/ppermute | solution.py:307
  140.8 3.9 %collective-permute-start.11 = (bf16[1280,128]{1,0:T(8,128)(2,1)S(1)}, bf16[1280,128]{1,0:T(8,128)(2,1)S(1)}, u32[]{:S(2)}, u32[]{:S(2)}) collective-permute-start(bf16[1280,128]{1,0:T(8,128)(2,1)S(1)} %get-tuple-element.52), channel_id=1, source_target_pairs={{0,2},{2,4},{4,6},{6,8},{8,10},{10,12},{12,14},{14,0},{1,3},{3,5},... | collective-permute-start | bytes 983048 | tf_op jit(solution)/shard_map/ppermute | solution.py:307
  144.8 4.5 %collective-permute-start.15 = (bf16[640,128]{1,0:T(8,128)(2,1)S(1)}, bf16[640,128]{1,0:T(8,128)(2,1)S(1)}, u32[]{:S(2)}, u32[]{:S(2)}) collective-permute-start(bf16[640,128]{1,0:T(8,128)(2,1)S(1)} %get-tuple-element.53), channel_id=1, source_target_pairs={{0,12},{2,14},{4,0},{6,2},{8,4},{10,6},{12,8},{14,10},{1,13},{3,15... | collective-permute-start | bytes 491528 | tf_op jit(solution)/shard_map/ppermute | solution.py:307
  149.3 2.3 %collective-permute-start.14 = (bf16[640,128]{1,0:T(8,128)(2,1)S(1)}, bf16[640,128]{1,0:T(8,128)(2,1)S(1)}, u32[]{:S(2)}, u32[]{:S(2)}) collective-permute-start(bf16[640,128]{1,0:T(8,128)(2,1)S(1)} %get-tuple-element.54), channel_id=1, source_target_pairs={{0,4},{2,6},{4,8},{6,10},{8,12},{10,14},{12,0},{14,2},{1,5},{3,7},... | collective-permute-start | bytes 491528 | tf_op jit(solution)/shard_map/ppermute | solution.py:307
  151.6 4.3 %collective-permute-done.15.f1_ref = bf16[640,128]{1,0:T(8,128)(2,1)S(1)} collective-permute-done((bf16[640,128]{1,0:T(8,128)(2,1)S(1)}, bf16[640,128]{1,0:T(8,128)(2,1)S(1)}, u32[]{:S(2)}, u32[]{:S(2)}) %collective-permute-start.15) | collective-permute-done | bytes 163872 | tf_op jit(solution)/shard_map/ppermute | solution.py:307
  155.8 6.4 %collective-permute-done.14.f0_ref = bf16[640,128]{1,0:T(8,128)(2,1)S(1)} collective-permute-done((bf16[640,128]{1,0:T(8,128)(2,1)S(1)}, bf16[640,128]{1,0:T(8,128)(2,1)S(1)}, u32[]{:S(2)}, u32[]{:S(2)}) %collective-permute-start.14) | collective-permute-done | bytes 163872 | tf_op jit(solution)/shard_map/ppermute | solution.py:307
  162.5 27.3 %all_to_all.28 = bf16[64,24,128]{2,1,0:T(8,128)(2,1)S(1)} all-to-all(bf16[64,24,128]{2,1,0:T(8,128)(2,1)S(1)} %shard_map.125), channel_id=1, replica_groups=mesh['z'=8,'x'=4,'yh'=2,'yl'=4,'c'=2] {'z','x','yh'}, dimensions={0} | all-to-all | bytes 786432 | tf_op jit(solution)/shard_map/all_to_all | solution.py:311
  189.9 1.6 shard_map.126
  (48 shorter events, 5.8 us)
Async XLA Ops:
  0.0 31.2 %copy-start.11 = (bf16[256,64]{0,1:T(8,128)(2,1)S(1)}, bf16[256,64]{0,1:T(8,128)(2,1)}, u32[]{:S(2)}) copy-start(bf16[256,64]{0,1:T(8,128)(2,1)} %param.12) | copy-start | bytes 98308
  0.2 1.0 copy-start.4
  1.1 0.8 copy-start.5
  1.9 0.8 copy-start.6
  3.5 45.5 %copy-start.7 = (f32[1,8192]{1,0:T(1,128)S(1)}, f32[1,8192]{1,0:T(1,128)}, u32[]{:S(2)}) copy-start(f32[1,8192]{1,0:T(1,128)} %gate_ref.1) | copy-start | bytes 98308
  31.2 28.4 %copy-start.10 = (s32[256,2]{0,1:T(2,128)S(1)}, s32[256,2]{0,1:T(2,128)}, u32[]{:S(2)}) copy-start(s32[256,2]{0,1:T(2,128)} %param.19) | copy-start | bytes 6148
  41.3 38.5 %copy-start = (bf16[256,2048]{1,0:T(8,128)(2,1)S(1)}, bf16[256,2048]{1,0:T(8,128)(2,1)}, u32[]{:S(2)}) copy-start(bf16[256,2048]{1,0:T(8,128)(2,1)} %resid_ref.1) | copy-start | bytes 3145732
  41.3 38.5 %copy-start.8 = (f32[2048]{0:T(1024)S(1)}, f32[2048]{0:T(1024)}, u32[]{:S(2)}) copy-start(f32[2048]{0:T(1024)} %param.18) | copy-start | bytes 24580
  41.3 38.5 %all-to-all-start.2 = ((bf16[16,128,128]{2,1,0:T(8,128)(2,1)}), bf16[16,128,128]{2,1,0:T(8,128)(2,1)S(1)}, u32[]{:S(2)}, u32[]{:S(2)}) async-start(bf16[16,128,128]{2,1,0:T(8,128)(2,1)} %get-tuple-element.39), calls=%async_computation.2 | async-start | bytes 1048576 | tf_op jit(solution)/shard_map/all_to_all | solution.py:311
  50.4 10.7 %collective-permute-start = (bf16[80,256]{1,0:T(8,128)(2,1)S(1)}, bf16[80,256]{1,0:T(8,128)(2,1)S(1)}, u32[]{:S(2)}, u32[]{:S(2)}) collective-permute-start(bf16[80,256]{1,0:T(8,128)(2,1)S(1)} %get-tuple-element.36), channel_id=1, source_target_pairs={{0,16},{16,32},{32,48},{48,0},{1,17},{17,33},{33,49},{49,1},{2,18}... | collective-permute-start | bytes 122888 | tf_op jit(solution)/shard_map/ppermute | solution.py:360
  52.9 8.2 %collective-permute-start.1 = (bf16[80,256]{1,0:T(8,128)(2,1)S(1)}, bf16[80,256]{1,0:T(8,128)(2,1)S(1)}, u32[]{:S(2)}, u32[]{:S(2)}) collective-permute-start(bf16[80,256]{1,0:T(8,128)(2,1)S(1)} %get-tuple-element.37), channel_id=1, source_target_pairs={{0,32},{16,48},{32,0},{48,16},{1,33},{17,49},{33,1},{49,17},{2,34}... | collective-permute-start | bytes 122888 | tf_op jit(solution)/shard_map/ppermute | solution.py:360
  56.9 5.9 %collective-permute-start.2 = (bf16[80,256]{1,0:T(8,128)(2,1)S(1)}, bf16[80,256]{1,0:T(8,128)(2,1)S(1)}, u32[]{:S(2)}, u32[]{:S(2)}) collective-permute-start(bf16[80,256]{1,0:T(8,128)(2,1)S(1)} %get-tuple-element.38), channel_id=1, source_target_pairs={{0,48},{16,0},{32,16},{48,32},{1,49},{17,1},{33,17},{49,33},{2,50}... | collective-permute-start | bytes 122888 | tf_op jit(solution)/shard_map/ppermute | solution.py:360
  81.5 49.6 %copy-start.3 = (bf16[1,256,2048]{2,1,0:T(8,128)(2,1)S(1)}, bf16[1,256,2048]{2,1,0:T(8,128)(2,1)}, u32[]{:S(2)}) copy-start(bf16[1,256,2048]{2,1,0:T(8,128)(2,1)} %param.23) | copy-start | bytes 3145732
  104.6 26.5 %copy-start.2 = (bf16[1,2048,256]{2,1,0:T(8,128)(2,1)S(1)}, bf16[1,2048,256]{2,1,0:T(8,128)(2,1)}, u32[]{:S(2)}) copy-start(bf16[1,2048,256]{2,1,0:T(8,128)(2,1)} %param.22) | copy-start | bytes 3145732
  104.8 26.4 %copy-start.1 = (bf16[1,2048,256]{2,1,0:T(8,128)(2,1)S(1)}, bf16[1,2048,256]{2,1,0:T(8,128)(2,1)}, u32[]{:S(2)}) copy-start(bf16[1,2048,256]{2,1,0:T(8,128)(2,1)} %param.21) | copy-start | bytes 3145732
  104.8 13.4 %collective-permute-start.4 = (bf16[1296,128]{1,0:T(8,128)(2,1)S(1)}, bf16[1296,128]{1,0:T(8,128)(2,1)S(1)}, u32[]{:S(2)}, u32[]{:S(2)}) collective-permute-start(bf16[1296,128]{1,0:T(8,128)(2,1)S(1)} %get-tuple-element.42.refs_0_), channel_id=1, source_target_pairs={{0,14},{2,0},{4,2},{6,4},{8,6},{10,8},{12,10},{14,12},{1,15},{3,1}... | collective-permute-start | bytes 995336 | tf_op jit(solution)/shard_map/ppermute | solution.py:307
  108.6 10.8 %collective-permute-start.3 = (bf16[1296,128]{1,0:T(8,128)(2,1)S(1)}, bf16[1296,128]{1,0:T(8,128)(2,1)S(1)}, u32[]{:S(2)}, u32[]{:S(2)}) collective-permute-start(bf16[1296,128]{1,0:T(8,128)(2,1)S(1)} %get-tuple-element.42.refs_0_), channel_id=1, source_target_pairs={{0,2},{2,4},{4,6},{6,8},{8,10},{10,12},{12,14},{14,0},{1,3},{3,5},... | collective-permute-start | bytes 995336 | tf_op jit(solution)/shard_map/ppermute | solution.py:307
  110.8 13.0 %collective-permute-start.6 = (bf16[640,128]{1,0:T(8,128)(2,1)S(1)}, bf16[640,128]{1,0:T(8,128)(2,1)S(1)}, u32[]{:S(2)}, u32[]{:S(2)}) collective-permute-start(bf16[640,128]{1,0:T(8,128)(2,1)S(1)} %get-tuple-element.44), channel_id=1, source_target_pairs={{0,12},{2,14},{4,0},{6,2},{8,4},{10,6},{12,8},{14,10},{1,13},{3,15... | collective-permute-start | bytes 491528 | tf_op jit(solution)/shard_map/ppermute | solution.py:307
  116.3 11.3 %collective-permute-start.5 = (bf16[656,128]{1,0:T(8,128)(2,1)S(1)}, bf16[656,128]{1,0:T(8,128)(2,1)S(1)}, u32[]{:S(2)}, u32[]{:S(2)}) collective-permute-start(bf16[656,128]{1,0:T(8,128)(2,1)S(1)} %get-tuple-element.43), channel_id=1, source_target_pairs={{0,4},{2,6},{4,8},{6,10},{8,12},{10,14},{12,0},{14,2},{1,5},{3,7},... | collective-permute-start | bytes 503816 | tf_op jit(solution)/shard_map/ppermute | solution.py:307
  119.4 11.7 %collective-permute-start.8 = (bf16[2592,128]{1,0:T(8,128)(2,1)S(1)}, bf16[2592,128]{1,0:T(8,128)(2,1)S(1)}, u32[]{:S(2)}, u32[]{:S(2)}) collective-permute-start(bf16[2592,128]{1,0:T(8,128)(2,1)S(1)} %pad_maximum_fusion), channel_id=1, source_target_pairs={{0,1},{1,0},{2,3},{3,2},{4,5},{5,4},{6,7},{7,6},{8,9},{9,8},{10,11... | collective-permute-start | bytes 1990664 | tf_op jit(solution)/shard_map/ppermute | solution.py:386
  121.4 8.2 %collective-permute-start.7 = (bf16[1296,128]{1,0:T(8,128)(2,1)S(1)}, bf16[1296,128]{1,0:T(8,128)(2,1)S(1)}, u32[]{:S(2)}, u32[]{:S(2)}) collective-permute-start(bf16[1296,128]{1,0:T(8,128)(2,1)S(1)} %get-tuple-element.42.refs_0_), channel_id=1, source_target_pairs={{0,1},{1,0},{2,3},{3,2},{4,5},{5,4},{6,7},{7,6},{8,9},{9,8},{10,11... | collective-permute-start | bytes 995336 | tf_op jit(solution)/shard_map/ppermute | solution.py:386
  127.6 3.5 %collective-permute-start.9 = (bf16[1296,128]{1,0:T(8,128)(2,1)S(1)}, bf16[1296,128]{1,0:T(8,128)(2,1)S(1)}, u32[]{:S(2)}, u32[]{:S(2)}) collective-permute-start(bf16[1296,128]{1,0:T(8,128)(2,1)S(1)} %pad_maximum_fusion.1), channel_id=1, source_target_pairs={{0,1},{1,0},{2,3},{3,2},{4,5},{5,4},{6,7},{7,6},{8,9},{9,8},{10,11... | collective-permute-start | bytes 995336 | tf_op jit(solution)/shard_map/ppermute | solution.py:386
  134.2 4.5 %collective-permute-start.10 = (bf16[3840,128]{1,0:T(8,128)(2,1)S(1)}, bf16[3840,128]{1,0:T(8,128)(2,1)S(1)}, u32[]{:S(2)}, u32[]{:S(2)}) collective-permute-start(bf16[3840,128]{1,0:T(8,128)(2,1)S(1)} %get-tuple-element.46), channel_id=1, source_target_pairs={{0,1},{1,0},{2,3},{3,2},{4,5},{5,4},{6,7},{7,6},{8,9},{9,8},{10,11... | collective-permute-start | bytes 2949128 | tf_op jit(solution)/shard_map/ppermute | solution.py:397
  136.2 8.4 %collective-permute-start.13 = (bf16[1280,128]{1,0:T(8,128)(2,1)S(1)}, bf16[1280,128]{1,0:T(8,128)(2,1)S(1)}, u32[]{:S(2)}, u32[]{:S(2)}) collective-permute-start(bf16[1280,128]{1,0:T(8,128)(2,1)S(1)} %get-tuple-element.48), channel_id=1, source_target_pairs={{0,1},{1,0},{2,3},{3,2},{4,5},{5,4},{6,7},{7,6},{8,9},{9,8},{10,11... | collective-permute-start | bytes 983048 | tf_op jit(solution)/shard_map/ppermute | solution.py:396
  138.8 23.4 %collective-permute-start.12 = (bf16[1280,128]{1,0:T(8,128)(2,1)S(1)}, bf16[1280,128]{1,0:T(8,128)(2,1)S(1)}, u32[]{:S(2)}, u32[]{:S(2)}) collective-permute-start(bf16[1280,128]{1,0:T(8,128)(2,1)S(1)} %get-tuple-element.51), channel_id=1, source_target_pairs={{0,14},{2,0},{4,2},{6,4},{8,6},{10,8},{12,10},{14,12},{1,15},{3,1}... | collective-permute-start | bytes 983048 | tf_op jit(solution)/shard_map/ppermute | solution.py:307
  140.8 21.5 %collective-permute-start.11 = (bf16[1280,128]{1,0:T(8,128)(2,1)S(1)}, bf16[1280,128]{1,0:T(8,128)(2,1)S(1)}, u32[]{:S(2)}, u32[]{:S(2)}) collective-permute-start(bf16[1280,128]{1,0:T(8,128)(2,1)S(1)} %get-tuple-element.52), channel_id=1, source_target_pairs={{0,2},{2,4},{4,6},{6,8},{8,10},{10,12},{12,14},{14,0},{1,3},{3,5},... | collective-permute-start | bytes 983048 | tf_op jit(solution)/shard_map/ppermute | solution.py:307
  144.8 11.0 %collective-permute-start.15 = (bf16[640,128]{1,0:T(8,128)(2,1)S(1)}, bf16[640,128]{1,0:T(8,128)(2,1)S(1)}, u32[]{:S(2)}, u32[]{:S(2)}) collective-permute-start(bf16[640,128]{1,0:T(8,128)(2,1)S(1)} %get-tuple-element.53), channel_id=1, source_target_pairs={{0,12},{2,14},{4,0},{6,2},{8,4},{10,6},{12,8},{14,10},{1,13},{3,15... | collective-permute-start | bytes 491528 | tf_op jit(solution)/shard_map/ppermute | solution.py:307
  149.3 40.6 %copy-start.9 = (f32[256,2]{0,1:T(2,128)S(1)}, f32[256,2]{0,1:T(2,128)}, u32[]{:S(2)}) copy-start(f32[256,2]{0,1:T(2,128)} %param.20) | copy-start | bytes 6148
  149.3 12.9 %collective-permute-start.14 = (bf16[640,128]{1,0:T(8,128)(2,1)S(1)}, bf16[640,128]{1,0:T(8,128)(2,1)S(1)}, u32[]{:S(2)}, u32[]{:S(2)}) collective-permute-start(bf16[640,128]{1,0:T(8,128)(2,1)S(1)} %get-tuple-element.54), channel_id=1, source_target_pairs={{0,4},{2,6},{4,8},{6,10},{8,12},{10,14},{12,0},{14,2},{1,5},{3,7},... | collective-permute-start | bytes 491528 | tf_op jit(solution)/shard_map/ppermute | solution.py:307

commit v7 on v6

--- a/solution.py
+++ b/solution.py
@@ -18,10 +18,9 @@
 ROW = NX * TOK
 CAP = 20
 SLOT = 24
-SEND = 48
+SEND = 2 * CAP
 ROWS = NSP * CAP
 PADROWS = NSP * SLOT
-META = 16
 FFL = 256
 EPS = 1e-06
 LOW = -1e30
@@ -31,9 +30,9 @@
 INTERPRET = False
 
 
-def call(body, out_shape, inputs, smem=0, scratch=(), limit=12):
+def call(body, out_shape, inputs, smem=0, scratch=(), limit=12, space=pltpu.VMEM):
     specs = [pl.BlockSpec(memory_space=pltpu.SMEM)] * smem
-    specs += [pl.BlockSpec(memory_space=pltpu.VMEM)] * (len(inputs) - smem)
+    specs += [pl.BlockSpec(memory_space=space)] * (len(inputs) - smem)
     many = isinstance(out_shape, (tuple, list))
     vm = pl.BlockSpec(memory_space=pltpu.VMEM)
     return pl.pallas_call(
@@ -83,7 +82,16 @@
         m_ref[...] = jnp.maximum(m_ref[...], jnp.max(s, axis=0, keepdims=True))
         return carry
 
-    lax.fori_loop(0, z, look, 0)
+    def look_two(i, carry):
+        one, two = scores(2 * i), scores(2 * i + 1)
+        s_ref[2 * i] = one
+        s_ref[2 * i + 1] = two
+        top = jnp.max(jnp.maximum(one, two), axis=0, keepdims=True)
+        m_ref[...] = jnp.maximum(m_ref[...], top)
+        return carry
+
+    lax.fori_loop(0, z // 2, look_two, 0)
+    lax.fori_loop(z // 2 * 2, z, look, 0)
     m = m_ref[0:1, :]
     acc_ref[...] = jnp.zeros((HD + 16, ROW), f32)
 
@@ -93,7 +101,16 @@
         acc_ref[...] += jnp.dot(v, p, preferred_element_type=f32)
         return carry
 
-    lax.fori_loop(0, z + 1, weigh, 0)
+    def weigh_two(i, carry):
+        zk = 2 * i
+        p = jnp.exp(s_ref[pl.ds(zk, 2)].reshape(2 * TOK, ROW) - m).astype(bf)
+        v = jnp.concatenate([kv_ref[zk, HD : 2 * HD, :], kv_ref[zk + 1, HD : 2 * HD, :]], axis=1)
+        v = jnp.concatenate([v, jnp.ones((16, 2 * TOK), bf)], axis=0)
+        acc_ref[...] += jnp.dot(v, p, preferred_element_type=f32)
+        return carry
+
+    lax.fori_loop(0, (z + 1) // 2, weigh_two, 0)
+    lax.fori_loop((z + 1) // 2 * 2, z + 1, weigh, 0)
     row16 = lax.broadcasted_iota(jnp.int32, (16, ROW), 0)
     total = acc_ref[HD : HD + 1, :]
     hi, mid, lo = three(m + jnp.log(total))
@@ -122,15 +139,24 @@
     out_ref[...] = (acc / total).astype(bf)
 
 
-def prepare(k_ref, v_ref, w_ref, kv_ref, out_ref):
+def prepare(k_ref, v_ref, q_ref, w_ref, kv_ref, qs_ref, out_ref, kb_ref, vb_ref, qb_ref, wb_ref, sems):
+    pairs = ((k_ref, kb_ref), (v_ref, vb_ref), (q_ref, qb_ref), (w_ref, wb_ref))
+    copies = [pltpu.make_async_copy(a, b, sems.at[i]) for i, (a, b) in enumerate(pairs)]
+    for copy in copies:
+        copy.start()
+    for copy in copies[0:3]:
+        copy.wait()
     for z in range(NZ):
-        kv_ref[z, 0:HD, :] = k_ref[...]
-        kv_ref[z, HD : 2 * HD, :] = v_ref[...]
+        kv_ref[z, 0:HD, :] = kb_ref[...]
+        kv_ref[z, HD : 2 * HD, :] = vb_ref[...]
+    for x in range(NX):
+        qs_ref[x] = qb_ref[...]
+    copies[3].wait()
     for y in range(NY):
         for c in range(NC):
             for q in range(2):
-                block = (y % (NY // 2) + q * (NY // 2)) * NC + c
-                out_ref[y * NC + c, q * HD : (q + 1) * HD, :] = w_ref[:, block * COLS : (block + 1) * COLS]
+                block = (y % HALF + q * HALF) * NC + c
+                out_ref[y * NC + c, q * HD : (q + 1) * HD, :] = wb_ref[:, block * COLS : (block + 1) * COLS]
 
 
 def route(routes_ref, pick_ref, slots_ref):
@@ -162,58 +188,24 @@
     gain = jnp.concatenate([gain_ref[:, pl.ds(c0, COLS)], gain_ref[:, pl.ds(c1, COLS)]], axis=1)
     stream = resid.astype(f32) + mixed
     stream_ref[...] = jnp.where(at_ref[2] == 0, stream[:, 0:COLS], stream[:, COLS:])
-    square = jnp.sum(stream * stream, axis=1, keepdims=True)
-    hi = square.astype(bf)
-    lo = (square - hi.astype(f32)).astype(bf)
     scaled = (stream * gain).astype(bf)
-    wide = (TOK, COLS)
-    rows = jnp.concatenate([scaled, jnp.broadcast_to(hi, wide), jnp.broadcast_to(lo, wide)], axis=1)
-    sent = jnp.dot(pick_ref[...], rows, preferred_element_type=f32).reshape(NSP, SEND, 4 * COLS)
-    shape = (NSP, SEND, COLS)
-    rank = lax.broadcasted_iota(jnp.int32, shape, 1)
-    lane = lax.broadcasted_iota(jnp.int32, shape, 2)
-    data = jnp.where(rank < CAP, sent[:, :, 0:COLS], sent[:, :, COLS : 2 * COLS])
-    same = (lane == rank) & (rank < CAP)
-    mh = jnp.sum(jnp.where(same, sent[:, :, 2 * COLS : 3 * COLS], 0.0), axis=1, keepdims=True)
-    ml = jnp.sum(jnp.where(same, sent[:, :, 3 * COLS :], 0.0), axis=1, keepdims=True)
-    data = jnp.where(rank == 2 * CAP, mh, jnp.where(rank == 2 * CAP + 1, ml, data))
-    out_ref[...] = data.astype(bf)
+    sent = jnp.dot(pick_ref[...], scaled, preferred_element_type=f32).reshape(NSP, SEND, 2 * COLS)
+    rank = lax.broadcasted_iota(jnp.int32, (NSP, SEND, COLS), 1)
+    out_ref[...] = jnp.where(rank < CAP, sent[:, :, 0:COLS], sent[:, :, COLS:]).astype(bf)
 
 
 def squeeze(in_ref, all_ref, low_ref, high_ref, rows_ref):
-    rank = lax.broadcasted_iota(jnp.int32, (NSP, SEND, COLS), 1)
-    x = in_ref[...].astype(f32)
-    part = jnp.sum(jnp.where((rank == 2 * CAP) | (rank == 2 * CAP + 1), x, 0.0), axis=1)
-    lane = lax.broadcasted_iota(jnp.int32, (NSP, COLS), 1)
-    part = jnp.where(lane < CAP, part, 0.0)
-    packed = part[0:8]
-    for g in range(1, 4):
-        packed = packed + pltpu.roll(part[8 * g : 8 * g + 8], 32 * g, 1)
-    hi = packed.astype(bf).astype(f32)
     for i in range(NSP):
         x = in_ref[i].astype(f32)
         rows_ref[ROWS + CAP * i : ROWS + CAP * i + CAP, :] = x[0:CAP, :]
         rows_ref[CAP * i : CAP * i + CAP, :] = x[CAP : 2 * CAP, :]
-    rows_ref[2 * ROWS : 2 * ROWS + 8, :] = hi
-    rows_ref[2 * ROWS + 8 : 2 * ROWS + META, :] = packed - hi
     all_ref[...] = rows_ref[...].astype(bf)
     high_ref[...] = rows_ref[0:ROWS, :].astype(bf)
-    low_ref[...] = rows_ref[ROWS : 2 * ROWS + META, :].astype(bf)
-
-
-PIECES = (
-    (0, 0, 0, ROWS),
-    (0, 1, 0, 0),
-    (3, 0, 1, ROWS),
-    (3, 1, 1, 0),
-    (1, 0, 2, ROWS),
-    (1, 1, 2, 0),
-    (2, 0, 3, 0),
-    (2, 1, 4, 0),
-)
-METAS = ((0, 2 * ROWS), (1, 2 * ROWS), (2, 2 * ROWS), (3, ROWS))
-
-
+    low_ref[...] = rows_ref[ROWS:, :].astype(bf)
+
+
+NEAR = ((0, 0, 0, ROWS), (0, 1, 0, 0), (3, 0, 1, ROWS), (3, 1, 1, 0), (1, 0, 2, ROWS), (1, 1, 2, 0))
+FAR = ((2, 0, 0, 0), (2, 1, 1, 0))
 SENDS = (
     (0, 0, 2, 0),
     (0, ROWS, 2, 1),
@@ -226,44 +218,40 @@
 )
 
 
-def experts(at_ref, *refs):
-    every, near, far = refs[5:8]
-    rows = 2 * ROWS + META
-    owns = refs[0:5]
-    others = (every, near.at[0:rows], near.at[rows:], far.at[0 : ROWS + META], far.at[ROWS + META :])
-    wg_ref, wu_ref, wd_ref = refs[8:11]
-    outs = refs[11:15]
-    g_ref, u_ref, h_ref = refs[15:]
-    y, c = at_ref[0], at_ref[1]
-    total = jnp.zeros((8, COLS), f32)
-    for pieces in (owns, others):
-        for n, at in METAS:
-            meta = pieces[n][at : at + META, :].astype(f32)
-            total = total + meta[0:8] + meta[8:16]
-    scale8 = lax.rsqrt(total / D + EPS)
-    shape = (ROWS, COLS)
-    row = lax.broadcasted_iota(jnp.int32, shape, 0).astype(f32)
-    lane = lax.broadcasted_iota(jnp.int32, shape, 1).astype(f32)
-    src = jnp.floor((row + 0.5) * (1.0 / CAP))
-    group = jnp.floor((src + 0.5) * 0.125)
-    sub = src - 8.0 * group
-    target = 32.0 * group + (row - CAP * src)
-    spread = jnp.zeros(shape, f32)
-    for a in range(8):
-        spread = jnp.where(sub == a, scale8[a : a + 1, :], spread)
-    scale = jnp.sum(jnp.where(lane == target, spread, 0.0), axis=1, keepdims=True)
-    for step, (off, upper, n, at) in enumerate(PIECES):
-        xx = jnp.concatenate([owns[n][at : at + ROWS, :], others[n][at : at + ROWS, :]], axis=1)
-        block = lax.rem(y + off, NY // 2) + upper * (NY // 2)
+def accumulate(y, c, pieces, owns, others, wg_ref, wu_ref, gain_ref, g_ref, u_ref, sq_ref, fresh):
+    for off, upper, n, at in pieces:
+        mine, theirs = owns[n][at : at + ROWS, :], others[n][at : at + ROWS, :]
+        block = lax.rem(y + off, HALF) + upper * HALF
         first = pl.multiple_of((2 * block + c) * COLS, COLS)
         second = pl.multiple_of((2 * block + 1 - c) * COLS, COLS)
+        xx = jnp.concatenate([mine, theirs], axis=1)
         for w_ref, acc_ref in ((wg_ref, g_ref), (wu_ref, u_ref)):
             w = jnp.concatenate([w_ref[pl.ds(first, COLS), :], w_ref[pl.ds(second, COLS), :]], axis=0)
             part = jnp.dot(xx, w, preferred_element_type=f32)
-            if step == 0:
-                acc_ref[...] = part
-            else:
-                acc_ref[...] += part
+            acc_ref[...] = part if fresh else acc_ref[...] + part
+        a = mine.astype(f32) * (1.0 / gain_ref[:, pl.ds(first, COLS)])
+        b = theirs.astype(f32) * (1.0 / gain_ref[:, pl.ds(second, COLS)])
+        part = a * a + b * b
+        sq_ref[...] = part if fresh else sq_ref[...] + part
+        fresh = False
+
+
+def experts_near(at_ref, every_ref, n0_ref, n1_ref, swap_ref, near_ref, wg_ref, wu_ref, gain_ref, g_ref, u_ref, sq_ref):
+    owns = (every_ref, n0_ref, n1_ref)
+    others = (swap_ref, near_ref.at[0 : 2 * ROWS], near_ref.at[2 * ROWS :])
+    accumulate(at_ref[0], at_ref[1], NEAR, owns, others, wg_ref, wu_ref, gain_ref, g_ref, u_ref, sq_ref, True)
+
+
+def experts(at_ref, f0_ref, f1_ref, far_ref, g_in, u_in, sq_in, wg_ref, wu_ref, wd_ref, gain_ref, *refs):
+    outs = refs[0:4]
+    g_ref, u_ref, sq_ref, h_ref = refs[4:]
+    y, c = at_ref[0], at_ref[1]
+    others = (far_ref.at[0:ROWS], far_ref.at[ROWS:])
+    g_ref[...] = g_in[...]
+    u_ref[...] = u_in[...]
+    sq_ref[...] = sq_in[...]
+    accumulate(y, c, FAR, (f0_ref, f1_ref), others, wg_ref, wu_ref, gain_ref, g_ref, u_ref, sq_ref, False)
+    scale = lax.rsqrt(jnp.sum(sq_ref[...], axis=1, keepdims=True) / D + EPS)
     gate = g_ref[...] * scale
     up = u_ref[...] * scale
     h_ref[...] = (gate / (1.0 + jnp.exp(-gate)) * up).astype(bf)
@@ -331,14 +319,17 @@
     low = (lax.rem(y, half) * NC + c) * COLS
     at_cols = jnp.stack([low, low + half * NC * COLS, y // half]).astype(jnp.int32)
     at = jnp.stack([z, x]).astype(jnp.int32)
-    kv_send, w_send = call(
+    small = pltpu.VMEM((HD, TOK), bf)
+    kv_send, q_send, w_send = call(
         prepare,
-        (sds((NZ, 2 * HD, TOK), bf), sds((NTP, 2 * HD, COLS), bf)),
-        (keys.T, values.T, out_weight),
+        (sds((NZ, 2 * HD, TOK), bf), sds((NX, HD, TOK), bf), sds((NTP, 2 * HD, COLS), bf)),
+        (keys.T, values.T, queries.T, out_weight),
+        scratch=(small, small, small, pltpu.VMEM((HD, D), bf), pltpu.SemaphoreType.DMA((4,))),
+        space=pl.ANY,
     )
     kv_send, w_send, at, at_cols = lax.optimization_barrier((kv_send, w_send, at, at_cols))
     kv = exchange(kv_send, "z")
-    q_send, kv = lax.optimization_barrier((jnp.broadcast_to(queries.T[None], (NX, HD, TOK)), kv))
+    q_send, kv = lax.optimization_barrier((q_send, kv))
     q = exchange(q_send, "x")
     w_cols = exchange(w_send, TP)
     sent = call(
@@ -370,12 +361,11 @@
         smem=1,
     )
     arrived = exchange(outgoing, SP)
-    rows = 2 * ROWS + META
     every, lower, higher = call(
         squeeze,
-        (sds((rows, COLS), bf), sds((ROWS + META, COLS), bf), sds((ROWS, COLS), bf)),
+        (sds((2 * ROWS, COLS), bf), sds((ROWS, COLS), bf), sds((ROWS, COLS), bf)),
         (arrived,),
-        scratch=(pltpu.VMEM((rows, COLS), f32),),
+        scratch=(pltpu.VMEM((2 * ROWS, COLS), f32),),
     )
     swap = [(0, 1), (1, 0)]
     owns = [every]
@@ -384,14 +374,17 @@
     others = []
     for v in (every, jnp.concatenate(owns[1:3], axis=0), jnp.concatenate(owns[3:5], axis=0)):
         others.append(lax.ppermute(v, "c", swap))
+    gain = norm_gain.reshape(1, D)
+    at_yc = jnp.stack([y, c]).astype(jnp.int32)
+    sums = (sds((ROWS, FFL), f32), sds((ROWS, FFL), f32), sds((ROWS, COLS), f32))
+    partial = call(experts_near, sums, (at_yc, *owns[0:3], *others[0:2], gate_weight[0], up_weight[0], gain), smem=1)
     far_out, near_out = sds((2 * ROWS, COLS), bf), sds((6 * ROWS, COLS), bf)
     far_mine, near_mine, far_theirs, near_theirs = call(
         experts,
         (far_out, near_out, far_out, near_out),
-        (jnp.stack([y, c]).astype(jnp.int32), *owns, *others, gate_weight[0], up_weight[0], down_weight[0]),
+        (at_yc, *owns[3:5], others[2], *partial, gate_weight[0], up_weight[0], down_weight[0], gain),
         smem=1,
-        scratch=(pltpu.VMEM((ROWS, FFL), f32), pltpu.VMEM((ROWS, FFL), f32), pltpu.VMEM((ROWS, FFL), bf)),
-        limit=24,
+        scratch=[pltpu.VMEM(v.shape, f32) for v in sums] + [pltpu.VMEM((ROWS, FFL), bf)],
     )
     far_theirs = lax.ppermute(far_theirs, "c", swap)
     near_theirs = lax.ppermute(near_theirs, "c", swap)

time: 193 us -> 191 us (0.990)
  waiting for transfers between devices: 19 us -> 16.7 us
  blocking collectives: 105 us -> 103 us
    pallas_call x9 -> x10, Pallas kernels: 10.5 us -> 10.8 us  [call(): pl.pallas_call(body, out_shape=out_shape, in_specs=specs, out_specs=tuple...]
  transfers between devices with their start and end apart: 17 -> 17, of which waited for: 7 -> 6; matrix products, arithmetic and copies ran while one was open for 0% -> 0% of each run, Pallas kernels for 1% -> 2%
where the time goes in v7:
time: 191 us; the launch traced here: 190 us
  blocking collectives  103 us (54%)
  starting transfers between devices  55.1 us (29%)
  waiting for transfers between devices  16.7 us (9%)
  Pallas kernels  10.8 us (6%)
  local copies, waits for them, and re-layouts  3.26 us (2%)
    all_to_all x4, blocking collectives, exchange(): return lax.all_to_all(v, axis, 0, 0, tiled=True)  86.4 us
    ppermute x8, starting transfers between devices, shift(): return lax.ppermute(v, Y, [(i, (i + by) % NY) for i in range(NY)])  27.7 us
    all_gather x1, blocking collectives, layer(): attended = lax.all_gather(attended, TP, axis=0, tiled=True)  17 us
    ppermute x8, waiting for transfers between devices, shift(): return lax.ppermute(v, Y, [(i, (i + by) % NY) for i in range(NY)])  14.6 us
    pallas_call x10, Pallas kernels, call(): pl.pallas_call(body, out_shape=out_shape, in_specs=specs, out_specs=tuple...  10.8 us
    ppermute x3, starting transfers between devices, layer(): lax.ppermute(sent[n], 'x', [(i, (i + n) % NX) for i in range(NX)])  9.17 us
    all_to_all x1, starting transfers between devices, exchange(): return lax.all_to_all(v, axis, 0, 0, tiled=True)  7.69 us
    ppermute x3, starting transfers between devices, layer(): others.append(lax.ppermute(v, 'c', swap))  6.25 us
  transfers between devices with their start and end apart: 17, of which 6 were waited for; matrix products, arithmetic and copies ran while one was open for 0% of the time, Pallas kernels for 2%

profile of v7, /device:TPU:8, one launch (start us, length us, event | category | flops | bytes accessed | tf_op | source)
XLA Modules:
  0.0 190.2 jit_solution(4889667601575168819)
XLA Ops:
  4.5 27.6 %all_to_all.25.kv_ref = bf16[8,128,256]{2,1,0:T(8,128)(2,1)S(1)} all-to-all(bf16[8,128,256]{2,1,0:T(8,128)(2,1)S(1)} %get-tuple-element.37), channel_id=1, replica_groups=mesh['z'=8,'x'=4,'yh'=2,'yl'=4,'c'=2] {'z'}, dimensions={0} | all-to-all | bytes 1048576 | tf_op jit(solution)/shard_map/all_to_all | solution.py:299
  32.1 10.2 %all_to_all.26.q_ref = bf16[4,64,256]{2,1,0:T(8,128)(2,1)S(1)} all-to-all(bf16[4,64,256]{2,1,0:T(8,128)(2,1)S(1)} %get-tuple-element.38), channel_id=1, replica_groups=mesh['z'=8,'x'=4,'yh'=2,'yl'=4,'c'=2] {'x'}, dimensions={0} | all-to-all | bytes 262144 | tf_op jit(solution)/shard_map/all_to_all | solution.py:299
  42.3 7.7 %all-to-all-start.2 = ((bf16[16,128,128]{2,1,0:T(8,128)(2,1)}), bf16[16,128,128]{2,1,0:T(8,128)(2,1)S(1)}, u32[]{:S(2)}, u32[]{:S(2)}) async-start(bf16[16,128,128]{2,1,0:T(8,128)(2,1)} %get-tuple-element.44), calls=%async_computation.2 | async-start | bytes 1048576 | tf_op jit(solution)/shard_map/all_to_all | solution.py:299
  50.0 1.4 shard_map.119
  51.3 2.5 %collective-permute-start = (bf16[80,256]{1,0:T(8,128)(2,1)S(1)}, bf16[80,256]{1,0:T(8,128)(2,1)S(1)}, u32[]{:S(2)}, u32[]{:S(2)}) collective-permute-start(bf16[80,256]{1,0:T(8,128)(2,1)S(1)} %get-tuple-element.41), channel_id=1, source_target_pairs={{0,16},{16,32},{32,48},{48,0},{1,17},{17,33},{33,49},{49,1},{2,18}... | collective-permute-start | bytes 122888 | tf_op jit(solution)/shard_map/ppermute | solution.py:351
  53.8 4.0 %collective-permute-start.1 = (bf16[80,256]{1,0:T(8,128)(2,1)S(1)}, bf16[80,256]{1,0:T(8,128)(2,1)S(1)}, u32[]{:S(2)}, u32[]{:S(2)}) collective-permute-start(bf16[80,256]{1,0:T(8,128)(2,1)S(1)} %get-tuple-element.42), channel_id=1, source_target_pairs={{0,32},{16,48},{32,0},{48,16},{1,33},{17,49},{33,1},{49,17},{2,34}... | collective-permute-start | bytes 122888 | tf_op jit(solution)/shard_map/ppermute | solution.py:351
  57.8 2.7 %collective-permute-start.2 = (bf16[80,256]{1,0:T(8,128)(2,1)S(1)}, bf16[80,256]{1,0:T(8,128)(2,1)S(1)}, u32[]{:S(2)}, u32[]{:S(2)}) collective-permute-start(bf16[80,256]{1,0:T(8,128)(2,1)S(1)} %get-tuple-element.43), channel_id=1, source_target_pairs={{0,48},{16,0},{32,16},{48,32},{1,49},{17,1},{33,17},{49,33},{2,50}... | collective-permute-start | bytes 122888 | tf_op jit(solution)/shard_map/ppermute | solution.py:351
  61.8 1.9 %collective-permute-done.2.refs_3_ = bf16[80,256]{1,0:T(8,128)(2,1)S(1)} collective-permute-done((bf16[80,256]{1,0:T(8,128)(2,1)S(1)}, bf16[80,256]{1,0:T(8,128)(2,1)S(1)}, u32[]{:S(2)}, u32[]{:S(2)}) %collective-permute-start.2) | collective-permute-done | bytes 40992 | tf_op jit(solution)/shard_map/ppermute | solution.py:351
  63.7 17.0 %all_gather.3.att_ref = bf16[1024,256]{1,0:T(8,128)(2,1)S(1)} all-gather(bf16[64,256]{1,0:T(8,128)(2,1)S(1)} %shard_map.120), channel_id=1, replica_groups=mesh['z'=8,'x'=4,'yh'=2,'yl'=4,'c'=2] {'yh','yl','c'}, dimensions={0}, use_global_device_ids=true | all-gather | bytes 557056 | tf_op jit(solution)/shard_map/all_gather | solution.py:356
  80.8 1.4 shard_map.122
  82.2 20.8 %all_to_all.27.in_ref = bf16[32,40,128]{2,1,0:T(8,128)(2,1)S(1)} all-to-all(bf16[32,40,128]{2,1,0:T(8,128)(2,1)S(1)} %get-tuple-element.46), channel_id=1, replica_groups=mesh['z'=8,'x'=4,'yh'=2,'yl'=4,'c'=2] {'z','x'}, dimensions={0} | all-to-all | bytes 655360 | tf_op jit(solution)/shard_map/all_to_all | solution.py:299
  103.1 3.8 %collective-permute-start.7 = (bf16[1280,128]{1,0:T(8,128)(2,1)S(1)}, bf16[1280,128]{1,0:T(8,128)(2,1)S(1)}, u32[]{:S(2)}, u32[]{:S(2)}) collective-permute-start(bf16[1280,128]{1,0:T(8,128)(2,1)S(1)} %get-tuple-element.49.every_ref), channel_id=1, source_target_pairs={{0,14},{2,0},{4,2},{6,4},{8,6},{10,8},{12,10},{14,12},{1,15},{3,1}... | collective-permute-start | bytes 983048 | tf_op jit(solution)/shard_map/ppermute | solution.py:295
  107.0 2.2 %collective-permute-start.6 = (bf16[1280,128]{1,0:T(8,128)(2,1)S(1)}, bf16[1280,128]{1,0:T(8,128)(2,1)S(1)}, u32[]{:S(2)}, u32[]{:S(2)}) collective-permute-start(bf16[1280,128]{1,0:T(8,128)(2,1)S(1)} %get-tuple-element.49.every_ref), channel_id=1, source_target_pairs={{0,2},{2,4},{4,6},{6,8},{8,10},{10,12},{12,14},{14,0},{1,3},{3,5},... | collective-permute-start | bytes 983048 | tf_op jit(solution)/shard_map/ppermute | solution.py:295
  109.1 5.5 %collective-permute-start.3 = (bf16[640,128]{1,0:T(8,128)(2,1)S(1)}, bf16[640,128]{1,0:T(8,128)(2,1)S(1)}, u32[]{:S(2)}, u32[]{:S(2)}) collective-permute-start(bf16[640,128]{1,0:T(8,128)(2,1)S(1)} %get-tuple-element.47), channel_id=1, source_target_pairs={{0,4},{2,6},{4,8},{6,10},{8,12},{10,14},{12,0},{14,2},{1,5},{3,7},... | collective-permute-start | bytes 491528 | tf_op jit(solution)/shard_map/ppermute | solution.py:295
  114.6 2.5 %collective-permute-start.4 = (bf16[640,128]{1,0:T(8,128)(2,1)S(1)}, bf16[640,128]{1,0:T(8,128)(2,1)S(1)}, u32[]{:S(2)}, u32[]{:S(2)}) collective-permute-start(bf16[640,128]{1,0:T(8,128)(2,1)S(1)} %get-tuple-element.48), channel_id=1, source_target_pairs={{0,12},{2,14},{4,0},{6,2},{8,4},{10,6},{12,8},{14,10},{1,13},{3,15... | collective-permute-start | bytes 491528 | tf_op jit(solution)/shard_map/ppermute | solution.py:295
  117.1 2.4 %collective-permute-done.6.n0_ref = bf16[1280,128]{1,0:T(8,128)(2,1)S(1)} collective-permute-done((bf16[1280,128]{1,0:T(8,128)(2,1)S(1)}, bf16[1280,128]{1,0:T(8,128)(2,1)S(1)}, u32[]{:S(2)}, u32[]{:S(2)}) %collective-permute-start.6) | collective-permute-done | bytes 327712 | tf_op jit(solution)/shard_map/ppermute | solution.py:295
  119.5 1.9 %collective-permute-start.9 = (bf16[2560,128]{1,0:T(8,128)(2,1)S(1)}, bf16[2560,128]{1,0:T(8,128)(2,1)S(1)}, u32[]{:S(2)}, u32[]{:S(2)}) collective-permute-start(bf16[2560,128]{1,0:T(8,128)(2,1)S(1)} %pad_maximum_fusion), channel_id=1, source_target_pairs={{0,1},{1,0},{2,3},{3,2},{4,5},{5,4},{6,7},{7,6},{8,9},{9,8},{10,11... | collective-permute-start | bytes 1966088 | tf_op jit(solution)/shard_map/ppermute | solution.py:376
  121.4 2.4 %collective-permute-start.8 = (bf16[1280,128]{1,0:T(8,128)(2,1)S(1)}, bf16[1280,128]{1,0:T(8,128)(2,1)S(1)}, u32[]{:S(2)}, u32[]{:S(2)}) collective-permute-start(bf16[1280,128]{1,0:T(8,128)(2,1)S(1)} %get-tuple-element.49.every_ref), channel_id=1, source_target_pairs={{0,1},{1,0},{2,3},{3,2},{4,5},{5,4},{6,7},{7,6},{8,9},{9,8},{10,11... | collective-permute-start | bytes 983048 | tf_op jit(solution)/shard_map/ppermute | solution.py:376
  123.8 1.4 collective-permute-done.3.f0_ref
  125.2 1.9 %collective-permute-start.5 = (bf16[1280,128]{1,0:T(8,128)(2,1)S(1)}, bf16[1280,128]{1,0:T(8,128)(2,1)S(1)}, u32[]{:S(2)}, u32[]{:S(2)}) collective-permute-start(bf16[1280,128]{1,0:T(8,128)(2,1)S(1)} %pad_maximum_fusion.1), channel_id=1, source_target_pairs={{0,1},{1,0},{2,3},{3,2},{4,5},{5,4},{6,7},{7,6},{8,9},{9,8},{10,11... | collective-permute-start | bytes 983048 | tf_op jit(solution)/shard_map/ppermute | solution.py:376
  127.3 1.7 shard_map.124
  129.0 1.9 %shard_map.125 = (bf16[1280,128]{1,0:T(8,128)(2,1)S(1)}, bf16[3840,128]{1,0:T(8,128)(2,1)S(1)}, bf16[1280,128]{1,0:T(8,128)(2,1)S(1)}, bf16[3840,128]{1,0:T(8,128)(2,1)S(1)}) custom-call(s32[2]{0:T(128)S(1)} %pad_add_fusion.at_ref, bf16[640,128]{1,0:T(8,128)(2,1)S(1)} %collective-permute-done.3.f0_ref, bf16[640,128]{1,0:T(8,128)(2,1)S(1)} %collective-permute-done.4.f1_ref, ...), custom_call_target="tpu_custom_call" | custom-call | tf_op jit(solution)/shard_map/pallas_call | solution.py:38
  131.0 2.4 %collective-permute-start.10 = (bf16[3840,128]{1,0:T(8,128)(2,1)S(1)}, bf16[3840,128]{1,0:T(8,128)(2,1)S(1)}, u32[]{:S(2)}, u32[]{:S(2)}) collective-permute-start(bf16[3840,128]{1,0:T(8,128)(2,1)S(1)} %get-tuple-element.54), channel_id=1, source_target_pairs={{0,1},{1,0},{2,3},{3,2},{4,5},{5,4},{6,7},{7,6},{8,9},{9,8},{10,11... | collective-permute-start | bytes 2949128 | tf_op jit(solution)/shard_map/ppermute | solution.py:390
  133.4 1.9 %collective-permute-start.13 = (bf16[1280,128]{1,0:T(8,128)(2,1)S(1)}, bf16[1280,128]{1,0:T(8,128)(2,1)S(1)}, u32[]{:S(2)}, u32[]{:S(2)}) collective-permute-start(bf16[1280,128]{1,0:T(8,128)(2,1)S(1)} %get-tuple-element.56), channel_id=1, source_target_pairs={{0,1},{1,0},{2,3},{3,2},{4,5},{5,4},{6,7},{7,6},{8,9},{9,8},{10,11... | collective-permute-start | bytes 983048 | tf_op jit(solution)/shard_map/ppermute | solution.py:389
  135.8 5.1 %collective-permute-start.12 = (bf16[1280,128]{1,0:T(8,128)(2,1)S(1)}, bf16[1280,128]{1,0:T(8,128)(2,1)S(1)}, u32[]{:S(2)}, u32[]{:S(2)}) collective-permute-start(bf16[1280,128]{1,0:T(8,128)(2,1)S(1)} %get-tuple-element.59), channel_id=1, source_target_pairs={{0,14},{2,0},{4,2},{6,4},{8,6},{10,8},{12,10},{14,12},{1,15},{3,1}... | collective-permute-start | bytes 983048 | tf_op jit(solution)/shard_map/ppermute | solution.py:295
  140.9 1.9 %collective-permute-start.11 = (bf16[1280,128]{1,0:T(8,128)(2,1)S(1)}, bf16[1280,128]{1,0:T(8,128)(2,1)S(1)}, u32[]{:S(2)}, u32[]{:S(2)}) collective-permute-start(bf16[1280,128]{1,0:T(8,128)(2,1)S(1)} %get-tuple-element.60), channel_id=1, source_target_pairs={{0,2},{2,4},{4,6},{6,8},{8,10},{10,12},{12,14},{14,0},{1,3},{3,5},... | collective-permute-start | bytes 983048 | tf_op jit(solution)/shard_map/ppermute | solution.py:295
  142.9 4.6 %collective-permute-start.15 = (bf16[640,128]{1,0:T(8,128)(2,1)S(1)}, bf16[640,128]{1,0:T(8,128)(2,1)S(1)}, u32[]{:S(2)}, u32[]{:S(2)}) collective-permute-start(bf16[640,128]{1,0:T(8,128)(2,1)S(1)} %get-tuple-element.61), channel_id=1, source_target_pairs={{0,12},{2,14},{4,0},{6,2},{8,4},{10,6},{12,8},{14,10},{1,13},{3,15... | collective-permute-start | bytes 491528 | tf_op jit(solution)/shard_map/ppermute | solution.py:295
  147.5 2.2 %collective-permute-start.14 = (bf16[640,128]{1,0:T(8,128)(2,1)S(1)}, bf16[640,128]{1,0:T(8,128)(2,1)S(1)}, u32[]{:S(2)}, u32[]{:S(2)}) collective-permute-start(bf16[640,128]{1,0:T(8,128)(2,1)S(1)} %get-tuple-element.62), channel_id=1, source_target_pairs={{0,4},{2,6},{4,8},{6,10},{8,12},{10,14},{12,0},{14,2},{1,5},{3,7},... | collective-permute-start | bytes 491528 | tf_op jit(solution)/shard_map/ppermute | solution.py:295
  149.7 5.7 %collective-permute-done.15.f1_ref = bf16[640,128]{1,0:T(8,128)(2,1)S(1)} collective-permute-done((bf16[640,128]{1,0:T(8,128)(2,1)S(1)}, bf16[640,128]{1,0:T(8,128)(2,1)S(1)}, u32[]{:S(2)}, u32[]{:S(2)}) %collective-permute-start.15) | collective-permute-done | bytes 163872 | tf_op jit(solution)/shard_map/ppermute | solution.py:295
  155.4 5.1 %collective-permute-done.14.f0_ref = bf16[640,128]{1,0:T(8,128)(2,1)S(1)} collective-permute-done((bf16[640,128]{1,0:T(8,128)(2,1)S(1)}, bf16[640,128]{1,0:T(8,128)(2,1)S(1)}, u32[]{:S(2)}, u32[]{:S(2)}) %collective-permute-start.14) | collective-permute-done | bytes 163872 | tf_op jit(solution)/shard_map/ppermute | solution.py:295
  160.8 27.7 %all_to_all.28 = bf16[64,24,128]{2,1,0:T(8,128)(2,1)S(1)} all-to-all(bf16[64,24,128]{2,1,0:T(8,128)(2,1)S(1)} %shard_map.126), channel_id=1, replica_groups=mesh['z'=8,'x'=4,'yh'=2,'yl'=4,'c'=2] {'z','x','yh'}, dimensions={0} | all-to-all | bytes 786432 | tf_op jit(solution)/shard_map/all_to_all | solution.py:299
  188.5 1.6 shard_map.127
  (48 shorter events, 6.8 us)
Async XLA Ops:
  0.2 1.0 copy-start.4
  1.1 0.8 copy-start.7
  1.9 0.8 copy-start.8
  2.6 0.8 copy-start.9
  4.4 45.5 %copy-start.6 = (f32[1,8192]{1,0:T(1,128)S(1)}, f32[1,8192]{1,0:T(1,128)}, u32[]{:S(2)}) copy-start(f32[1,8192]{1,0:T(1,128)} %gate_ref.1) | copy-start | bytes 98308
  32.1 28.5 %copy-start.11 = (s32[256,2]{0,1:T(2,128)S(1)}, s32[256,2]{0,1:T(2,128)}, u32[]{:S(2)}) copy-start(s32[256,2]{0,1:T(2,128)} %param.19) | copy-start | bytes 6148
  42.3 38.5 %copy-start.2 = (bf16[256,2048]{1,0:T(8,128)(2,1)S(1)}, bf16[256,2048]{1,0:T(8,128)(2,1)}, u32[]{:S(2)}) copy-start(bf16[256,2048]{1,0:T(8,128)(2,1)} %resid_ref.1) | copy-start | bytes 3145732
  42.3 38.5 %copy-start.5 = (f32[2048]{0:T(1024)S(1)}, f32[2048]{0:T(1024)}, u32[]{:S(2)}) copy-start(f32[2048]{0:T(1024)} %param.18) | copy-start | bytes 24580
  42.3 38.5 %all-to-all-start.2 = ((bf16[16,128,128]{2,1,0:T(8,128)(2,1)}), bf16[16,128,128]{2,1,0:T(8,128)(2,1)S(1)}, u32[]{:S(2)}, u32[]{:S(2)}) async-start(bf16[16,128,128]{2,1,0:T(8,128)(2,1)} %get-tuple-element.44), calls=%async_computation.2 | async-start | bytes 1048576 | tf_op jit(solution)/shard_map/all_to_all | solution.py:299
  51.3 10.4 %collective-permute-start = (bf16[80,256]{1,0:T(8,128)(2,1)S(1)}, bf16[80,256]{1,0:T(8,128)(2,1)S(1)}, u32[]{:S(2)}, u32[]{:S(2)}) collective-permute-start(bf16[80,256]{1,0:T(8,128)(2,1)S(1)} %get-tuple-element.41), channel_id=1, source_target_pairs={{0,16},{16,32},{32,48},{48,0},{1,17},{17,33},{33,49},{49,1},{2,18}... | collective-permute-start | bytes 122888 | tf_op jit(solution)/shard_map/ppermute | solution.py:351
  53.8 8.0 %collective-permute-start.1 = (bf16[80,256]{1,0:T(8,128)(2,1)S(1)}, bf16[80,256]{1,0:T(8,128)(2,1)S(1)}, u32[]{:S(2)}, u32[]{:S(2)}) collective-permute-start(bf16[80,256]{1,0:T(8,128)(2,1)S(1)} %get-tuple-element.42), channel_id=1, source_target_pairs={{0,32},{16,48},{32,0},{48,16},{1,33},{17,49},{33,1},{49,17},{2,34}... | collective-permute-start | bytes 122888 | tf_op jit(solution)/shard_map/ppermute | solution.py:351
  57.8 5.9 %collective-permute-start.2 = (bf16[80,256]{1,0:T(8,128)(2,1)S(1)}, bf16[80,256]{1,0:T(8,128)(2,1)S(1)}, u32[]{:S(2)}, u32[]{:S(2)}) collective-permute-start(bf16[80,256]{1,0:T(8,128)(2,1)S(1)} %get-tuple-element.43), channel_id=1, source_target_pairs={{0,48},{16,0},{32,16},{48,32},{1,49},{17,1},{33,17},{49,33},{2,50}... | collective-permute-start | bytes 122888 | tf_op jit(solution)/shard_map/ppermute | solution.py:351
  103.0 24.2 %copy-start.1 = (bf16[1,2048,256]{2,1,0:T(8,128)(2,1)S(1)}, bf16[1,2048,256]{2,1,0:T(8,128)(2,1)}, u32[]{:S(2)}) copy-start(bf16[1,2048,256]{2,1,0:T(8,128)(2,1)} %param.22) | copy-start | bytes 3145732
  103.1 24.1 %copy-start = (bf16[1,2048,256]{2,1,0:T(8,128)(2,1)S(1)}, bf16[1,2048,256]{2,1,0:T(8,128)(2,1)}, u32[]{:S(2)}) copy-start(bf16[1,2048,256]{2,1,0:T(8,128)(2,1)} %param.21) | copy-start | bytes 3145732
  103.1 14.0 %collective-permute-start.7 = (bf16[1280,128]{1,0:T(8,128)(2,1)S(1)}, bf16[1280,128]{1,0:T(8,128)(2,1)S(1)}, u32[]{:S(2)}, u32[]{:S(2)}) collective-permute-start(bf16[1280,128]{1,0:T(8,128)(2,1)S(1)} %get-tuple-element.49.every_ref), channel_id=1, source_target_pairs={{0,14},{2,0},{4,2},{6,4},{8,6},{10,8},{12,10},{14,12},{1,15},{3,1}... | collective-permute-start | bytes 983048 | tf_op jit(solution)/shard_map/ppermute | solution.py:295
  107.0 12.5 %collective-permute-start.6 = (bf16[1280,128]{1,0:T(8,128)(2,1)S(1)}, bf16[1280,128]{1,0:T(8,128)(2,1)S(1)}, u32[]{:S(2)}, u32[]{:S(2)}) collective-permute-start(bf16[1280,128]{1,0:T(8,128)(2,1)S(1)} %get-tuple-element.49.every_ref), channel_id=1, source_target_pairs={{0,2},{2,4},{4,6},{6,8},{8,10},{10,12},{12,14},{14,0},{1,3},{3,5},... | collective-permute-start | bytes 983048 | tf_op jit(solution)/shard_map/ppermute | solution.py:295
  109.1 16.1 %collective-permute-start.3 = (bf16[640,128]{1,0:T(8,128)(2,1)S(1)}, bf16[640,128]{1,0:T(8,128)(2,1)S(1)}, u32[]{:S(2)}, u32[]{:S(2)}) collective-permute-start(bf16[640,128]{1,0:T(8,128)(2,1)S(1)} %get-tuple-element.47), channel_id=1, source_target_pairs={{0,4},{2,6},{4,8},{6,10},{8,12},{10,14},{12,0},{14,2},{1,5},{3,7},... | collective-permute-start | bytes 491528 | tf_op jit(solution)/shard_map/ppermute | solution.py:295
  114.6 10.6 %collective-permute-start.4 = (bf16[640,128]{1,0:T(8,128)(2,1)S(1)}, bf16[640,128]{1,0:T(8,128)(2,1)S(1)}, u32[]{:S(2)}, u32[]{:S(2)}) collective-permute-start(bf16[640,128]{1,0:T(8,128)(2,1)S(1)} %get-tuple-element.48), channel_id=1, source_target_pairs={{0,12},{2,14},{4,0},{6,2},{8,4},{10,6},{12,8},{14,10},{1,13},{3,15... | collective-permute-start | bytes 491528 | tf_op jit(solution)/shard_map/ppermute | solution.py:295
  119.5 7.8 %collective-permute-start.9 = (bf16[2560,128]{1,0:T(8,128)(2,1)S(1)}, bf16[2560,128]{1,0:T(8,128)(2,1)S(1)}, u32[]{:S(2)}, u32[]{:S(2)}) collective-permute-start(bf16[2560,128]{1,0:T(8,128)(2,1)S(1)} %pad_maximum_fusion), channel_id=1, source_target_pairs={{0,1},{1,0},{2,3},{3,2},{4,5},{5,4},{6,7},{7,6},{8,9},{9,8},{10,11... | collective-permute-start | bytes 1966088 | tf_op jit(solution)/shard_map/ppermute | solution.py:376
  121.4 5.8 %collective-permute-start.8 = (bf16[1280,128]{1,0:T(8,128)(2,1)S(1)}, bf16[1280,128]{1,0:T(8,128)(2,1)S(1)}, u32[]{:S(2)}, u32[]{:S(2)}) collective-permute-start(bf16[1280,128]{1,0:T(8,128)(2,1)S(1)} %get-tuple-element.49.every_ref), channel_id=1, source_target_pairs={{0,1},{1,0},{2,3},{3,2},{4,5},{5,4},{6,7},{7,6},{8,9},{9,8},{10,11... | collective-permute-start | bytes 983048 | tf_op jit(solution)/shard_map/ppermute | solution.py:376
  125.2 3.8 %collective-permute-start.5 = (bf16[1280,128]{1,0:T(8,128)(2,1)S(1)}, bf16[1280,128]{1,0:T(8,128)(2,1)S(1)}, u32[]{:S(2)}, u32[]{:S(2)}) collective-permute-start(bf16[1280,128]{1,0:T(8,128)(2,1)S(1)} %pad_maximum_fusion.1), channel_id=1, source_target_pairs={{0,1},{1,0},{2,3},{3,2},{4,5},{5,4},{6,7},{7,6},{8,9},{9,8},{10,11... | collective-permute-start | bytes 983048 | tf_op jit(solution)/shard_map/ppermute | solution.py:376
  127.3 1.8 copy-start.3
  131.0 4.6 %collective-permute-start.10 = (bf16[3840,128]{1,0:T(8,128)(2,1)S(1)}, bf16[3840,128]{1,0:T(8,128)(2,1)S(1)}, u32[]{:S(2)}, u32[]{:S(2)}) collective-permute-start(bf16[3840,128]{1,0:T(8,128)(2,1)S(1)} %get-tuple-element.54), channel_id=1, source_target_pairs={{0,1},{1,0},{2,3},{3,2},{4,5},{5,4},{6,7},{7,6},{8,9},{9,8},{10,11... | collective-permute-start | bytes 2949128 | tf_op jit(solution)/shard_map/ppermute | solution.py:390
  133.4 9.4 %collective-permute-start.13 = (bf16[1280,128]{1,0:T(8,128)(2,1)S(1)}, bf16[1280,128]{1,0:T(8,128)(2,1)S(1)}, u32[]{:S(2)}, u32[]{:S(2)}) collective-permute-start(bf16[1280,128]{1,0:T(8,128)(2,1)S(1)} %get-tuple-element.56), channel_id=1, source_target_pairs={{0,1},{1,0},{2,3},{3,2},{4,5},{5,4},{6,7},{7,6},{8,9},{9,8},{10,11... | collective-permute-start | bytes 983048 | tf_op jit(solution)/shard_map/ppermute | solution.py:389
  135.8 24.8 %collective-permute-start.12 = (bf16[1280,128]{1,0:T(8,128)(2,1)S(1)}, bf16[1280,128]{1,0:T(8,128)(2,1)S(1)}, u32[]{:S(2)}, u32[]{:S(2)}) collective-permute-start(bf16[1280,128]{1,0:T(8,128)(2,1)S(1)} %get-tuple-element.59), channel_id=1, source_target_pairs={{0,14},{2,0},{4,2},{6,4},{8,6},{10,8},{12,10},{14,12},{1,15},{3,1}... | collective-permute-start | bytes 983048 | tf_op jit(solution)/shard_map/ppermute | solution.py:295
  140.9 19.6 %collective-permute-start.11 = (bf16[1280,128]{1,0:T(8,128)(2,1)S(1)}, bf16[1280,128]{1,0:T(8,128)(2,1)S(1)}, u32[]{:S(2)}, u32[]{:S(2)}) collective-permute-start(bf16[1280,128]{1,0:T(8,128)(2,1)S(1)} %get-tuple-element.60), channel_id=1, source_target_pairs={{0,2},{2,4},{4,6},{6,8},{8,10},{10,12},{12,14},{14,0},{1,3},{3,5},... | collective-permute-start | bytes 983048 | tf_op jit(solution)/shard_map/ppermute | solution.py:295
  142.9 12.5 %collective-permute-start.15 = (bf16[640,128]{1,0:T(8,128)(2,1)S(1)}, bf16[640,128]{1,0:T(8,128)(2,1)S(1)}, u32[]{:S(2)}, u32[]{:S(2)}) collective-permute-start(bf16[640,128]{1,0:T(8,128)(2,1)S(1)} %get-tuple-element.61), channel_id=1, source_target_pairs={{0,12},{2,14},{4,0},{6,2},{8,4},{10,6},{12,8},{14,10},{1,13},{3,15... | collective-permute-start | bytes 491528 | tf_op jit(solution)/shard_map/ppermute | solution.py:295
  147.5 41.0 %copy-start.10 = (f32[256,2]{0,1:T(2,128)S(1)}, f32[256,2]{0,1:T(2,128)}, u32[]{:S(2)}) copy-start(f32[256,2]{0,1:T(2,128)} %param.20) | copy-start | bytes 6148
  147.5 13.0 %collective-permute-start.14 = (bf16[640,128]{1,0:T(8,128)(2,1)S(1)}, bf16[640,128]{1,0:T(8,128)(2,1)S(1)}, u32[]{:S(2)}, u32[]{:S(2)}) collective-permute-start(bf16[640,128]{1,0:T(8,128)(2,1)S(1)} %get-tuple-element.62), channel_id=1, source_target_pairs={{0,4},{2,6},{4,8},{6,10},{8,12},{10,14},{12,0},{14,2},{1,5},{3,7},... | collective-permute-start | bytes 491528 | tf_op jit(solution)/shard_map/ppermute | solution.py:295

commit v8 on v7

--- a/solution.py
+++ b/solution.py
@@ -136,7 +136,9 @@
         w = jnp.exp(ls[i] - m)
         total = total + w
         acc = acc + w * parts[i][0:HD, :].astype(f32)
-    out_ref[...] = (acc / total).astype(bf)
+    out = (acc / total).astype(bf)
+    for y in range(NY):
+        out_ref[y] = out
 
 
 def prepare(k_ref, v_ref, q_ref, w_ref, kv_ref, qs_ref, out_ref, kb_ref, vb_ref, qb_ref, wb_ref, sems):
@@ -178,12 +180,15 @@
     pick_ref[...] = jnp.where(hits, 1.0, 0.0).astype(bf)
 
 
-def project(at_ref, att_ref, w_ref, resid_ref, gain_ref, pick_ref, stream_ref, out_ref):
+def project(at_ref, own_ref, partner_ref, w_ref, resid_ref, gain_ref, pick_ref, stream_ref, out_ref):
     c0 = pl.multiple_of(at_ref[0], COLS)
     c1 = pl.multiple_of(at_ref[1], COLS)
-    weights = [jnp.concatenate([w_ref[t, q * HD : (q + 1) * HD, :] for t in range(NTP)], axis=0) for q in range(2)]
+    c = at_ref[3]
+    heads = [2 * y + c for y in range(NY)] + [2 * y + 1 - c for y in range(NY)]
+    weights = [jnp.concatenate([w_ref[t, q * HD : (q + 1) * HD, :] for t in heads], axis=0) for q in range(2)]
     w = jnp.concatenate(weights, axis=1)
-    mixed = lax.dot_general(att_ref[...], w, (((0,), (0,)), ((), ())), preferred_element_type=f32)
+    att = jnp.concatenate([ref[...].reshape(NY * HD, TOK) for ref in (own_ref, partner_ref)], axis=0)
+    mixed = lax.dot_general(att, w, (((0,), (0,)), ((), ())), preferred_element_type=f32)
     resid = jnp.concatenate([resid_ref[:, pl.ds(c0, COLS)], resid_ref[:, pl.ds(c1, COLS)]], axis=1)
     gain = jnp.concatenate([gain_ref[:, pl.ds(c0, COLS)], gain_ref[:, pl.ds(c1, COLS)]], axis=1)
     stream = resid.astype(f32) + mixed
@@ -317,7 +322,7 @@
     sds = jax.ShapeDtypeStruct
     half = NY // 2
     low = (lax.rem(y, half) * NC + c) * COLS
-    at_cols = jnp.stack([low, low + half * NC * COLS, y // half]).astype(jnp.int32)
+    at_cols = jnp.stack([low, low + half * NC * COLS, y // half, c]).astype(jnp.int32)
     at = jnp.stack([z, x]).astype(jnp.int32)
     small = pltpu.VMEM((HD, TOK), bf)
     kv_send, q_send, w_send = call(
@@ -325,7 +330,7 @@
         (sds((NZ, 2 * HD, TOK), bf), sds((NX, HD, TOK), bf), sds((NTP, 2 * HD, COLS), bf)),
         (keys.T, values.T, queries.T, out_weight),
         scratch=(small, small, small, pltpu.VMEM((HD, D), bf), pltpu.SemaphoreType.DMA((4,))),
-        space=pl.ANY,
+        space=pltpu.HBM,
     )
     kv_send, w_send, at, at_cols = lax.optimization_barrier((kv_send, w_send, at, at_cols))
     kv = exchange(kv_send, "z")
@@ -352,12 +357,14 @@
     pick, slots = call(
         route, (sds((NSP * SEND, TOK), bf), sds((8, TOK), jnp.int32)), (routes.T,)
     )
-    attended = call(merge, sds((HD, TOK), bf), tuple(parts))
-    attended = lax.all_gather(attended, TP, axis=0, tiled=True)
+    swap = [(0, 1), (1, 0)]
+    attended, w_cols = lax.optimization_barrier((call(merge, sds((NY, HD, TOK), bf), tuple(parts)), w_cols))
+    attended = exchange(attended, Y)
+    partner = lax.ppermute(attended, "c", swap)
     stream, outgoing = call(
         project,
         (sds((TOK, COLS), f32), sds((NSP, SEND, COLS), bf)),
-        (at_cols, attended, w_cols, resid, norm_gain.reshape(1, D), pick),
+        (at_cols, attended, partner, w_cols, resid, norm_gain.reshape(1, D), pick),
         smem=1,
     )
     arrived = exchange(outgoing, SP)
@@ -367,7 +374,6 @@
         (arrived,),
         scratch=(pltpu.VMEM((2 * ROWS, COLS), f32),),
     )
-    swap = [(0, 1), (1, 0)]
     owns = [every]
     for v, by in ((every, 1), (every, -1), (lower, 2), (higher, -2)):
         owns.append(shift(v, by))

time: 191 us -> 191 us (level)
  blocking collectives: 103 us -> 101 us
    all_gather x1 -> x0, blocking collectives: 17 us -> none  [layer(): attended = lax.all_gather(attended, TP, axis=0, tiled=True)]
    all_to_all x4 -> x5, blocking collectives: 86.4 us -> 101 us  [exchange(): return lax.all_to_all(v, axis, 0, 0, tiled=True)]
  transfers between devices with their start and end apart: 17 -> 18, of which waited for: 6 -> 9; matrix products, arithmetic and copies ran while one was open for 0% -> 0% of each run, Pallas kernels for 2% -> 2%
where the time goes in v8:
time: 191 us; the launch traced here: 190 us
  blocking collectives  101 us (53%)
  starting transfers between devices  56.8 us (30%)
  waiting for transfers between devices  17.8 us (9%)
  Pallas kernels  10.8 us (6%)
  local copies, waits for them, and re-layouts  3.27 us (2%)
    all_to_all x5, blocking collectives, exchange(): return lax.all_to_all(v, axis, 0, 0, tiled=True)  101 us
    ppermute x8, starting transfers between devices, shift(): return lax.ppermute(v, Y, [(i, (i + by) % NY) for i in range(NY)])  27.6 us
    ppermute x8, waiting for transfers between devices, shift(): return lax.ppermute(v, Y, [(i, (i + by) % NY) for i in range(NY)])  13.7 us
    pallas_call x10, Pallas kernels, call(): pl.pallas_call(body, out_shape=out_shape, in_specs=specs, out_specs=tuple...  10.8 us
    ppermute x3, starting transfers between devices, layer(): lax.ppermute(sent[n], 'x', [(i, (i + n) % NX) for i in range(NX)])  9.17 us
    all_to_all x1, starting transfers between devices, exchange(): return lax.all_to_all(v, axis, 0, 0, tiled=True)  7.56 us
    ppermute x3, starting transfers between devices, layer(): others.append(lax.ppermute(v, 'c', swap))  6.25 us
  transfers between devices with their start and end apart: 18, of which 9 were waited for; matrix products, arithmetic and copies ran while one was open for 0% of the time, Pallas kernels for 2%

profile of v8, /device:TPU:8, one launch (start us, length us, event | category | flops | bytes accessed | tf_op | source)
XLA Modules:
  0.0 190.2 jit_solution(6318762300410989749)
XLA Ops:
  4.5 27.6 %all_to_all.30.kv_ref = bf16[8,128,256]{2,1,0:T(8,128)(2,1)S(1)} all-to-all(bf16[8,128,256]{2,1,0:T(8,128)(2,1)S(1)} %get-tuple-element.39), channel_id=1, replica_groups=mesh['z'=8,'x'=4,'yh'=2,'yl'=4,'c'=2] {'z'}, dimensions={0} | all-to-all | bytes 1048576 | tf_op jit(solution)/shard_map/all_to_all | solution.py:304
  32.1 10.1 %all_to_all.31.q_ref = bf16[4,64,256]{2,1,0:T(8,128)(2,1)S(1)} all-to-all(bf16[4,64,256]{2,1,0:T(8,128)(2,1)S(1)} %get-tuple-element.40), channel_id=1, replica_groups=mesh['z'=8,'x'=4,'yh'=2,'yl'=4,'c'=2] {'x'}, dimensions={0} | all-to-all | bytes 262144 | tf_op jit(solution)/shard_map/all_to_all | solution.py:304
  42.1 7.6 %all-to-all-start.2 = ((bf16[16,128,128]{2,1,0:T(8,128)(2,1)}), bf16[16,128,128]{2,1,0:T(8,128)(2,1)S(1)}, u32[]{:S(2)}, u32[]{:S(2)}) async-start(bf16[16,128,128]{2,1,0:T(8,128)(2,1)} %get-tuple-element.46), calls=%async_computation.2 | async-start | bytes 1048576 | tf_op jit(solution)/shard_map/all_to_all | solution.py:304
  49.7 1.3 shard_map.119
  51.1 2.5 %collective-permute-start = (bf16[80,256]{1,0:T(8,128)(2,1)S(1)}, bf16[80,256]{1,0:T(8,128)(2,1)S(1)}, u32[]{:S(2)}, u32[]{:S(2)}) collective-permute-start(bf16[80,256]{1,0:T(8,128)(2,1)S(1)} %get-tuple-element.43), channel_id=1, source_target_pairs={{0,16},{16,32},{32,48},{48,0},{1,17},{17,33},{33,49},{49,1},{2,18}... | collective-permute-start | bytes 122888 | tf_op jit(solution)/shard_map/ppermute | solution.py:356
  53.6 4.0 %collective-permute-start.1 = (bf16[80,256]{1,0:T(8,128)(2,1)S(1)}, bf16[80,256]{1,0:T(8,128)(2,1)S(1)}, u32[]{:S(2)}, u32[]{:S(2)}) collective-permute-start(bf16[80,256]{1,0:T(8,128)(2,1)S(1)} %get-tuple-element.44), channel_id=1, source_target_pairs={{0,32},{16,48},{32,0},{48,16},{1,33},{17,49},{33,1},{49,17},{2,34}... | collective-permute-start | bytes 122888 | tf_op jit(solution)/shard_map/ppermute | solution.py:356
  57.6 2.7 %collective-permute-start.2 = (bf16[80,256]{1,0:T(8,128)(2,1)S(1)}, bf16[80,256]{1,0:T(8,128)(2,1)S(1)}, u32[]{:S(2)}, u32[]{:S(2)}) collective-permute-start(bf16[80,256]{1,0:T(8,128)(2,1)S(1)} %get-tuple-element.45), channel_id=1, source_target_pairs={{0,48},{16,0},{32,16},{48,32},{1,49},{17,1},{33,17},{49,33},{2,50}... | collective-permute-start | bytes 122888 | tf_op jit(solution)/shard_map/ppermute | solution.py:356
  61.0 2.5 %collective-permute-done.2.refs_3_ = bf16[80,256]{1,0:T(8,128)(2,1)S(1)} collective-permute-done((bf16[80,256]{1,0:T(8,128)(2,1)S(1)}, bf16[80,256]{1,0:T(8,128)(2,1)S(1)}, u32[]{:S(2)}, u32[]{:S(2)}) %collective-permute-start.2) | collective-permute-done | bytes 40992 | tf_op jit(solution)/shard_map/ppermute | solution.py:356
  63.9 16.7 %all_to_all.32.own_ref = bf16[8,64,256]{2,1,0:T(8,128)(2,1)S(1)} all-to-all(bf16[8,64,256]{2,1,0:T(8,128)(2,1)S(1)} %shard_map.120), channel_id=1, replica_groups=mesh['z'=8,'x'=4,'yh'=2,'yl'=4,'c'=2] {'yh','yl'}, dimensions={0} | all-to-all | bytes 524288 | tf_op jit(solution)/shard_map/all_to_all | solution.py:304
  80.7 1.9 %collective-permute-start.3 = (bf16[8,64,256]{2,1,0:T(8,128)(2,1)S(1)}, bf16[8,64,256]{2,1,0:T(8,128)(2,1)S(1)}, u32[]{:S(2)}, u32[]{:S(2)}) collective-permute-start(bf16[8,64,256]{2,1,0:T(8,128)(2,1)S(1)} %all_to_all.32.own_ref), channel_id=1, source_target_pairs={{0,1},{1,0},{2,3},{3,2},{4,5},{5,4},{6,7},{7,6},{8,9},{9,8},{10,11... | collective-permute-start | bytes 786440 | tf_op jit(solution)/shard_map/ppermute | solution.py:363
  84.1 1.4 shard_map.122
  85.5 19.6 %all_to_all.33.in_ref = bf16[32,40,128]{2,1,0:T(8,128)(2,1)S(1)} all-to-all(bf16[32,40,128]{2,1,0:T(8,128)(2,1)S(1)} %get-tuple-element.50), channel_id=1, replica_groups=mesh['z'=8,'x'=4,'yh'=2,'yl'=4,'c'=2] {'z','x'}, dimensions={0} | all-to-all | bytes 655360 | tf_op jit(solution)/shard_map/all_to_all | solution.py:304
  105.2 3.5 %collective-permute-start.8 = (bf16[1280,128]{1,0:T(8,128)(2,1)S(1)}, bf16[1280,128]{1,0:T(8,128)(2,1)S(1)}, u32[]{:S(2)}, u32[]{:S(2)}) collective-permute-start(bf16[1280,128]{1,0:T(8,128)(2,1)S(1)} %get-tuple-element.53.every_ref), channel_id=1, source_target_pairs={{0,14},{2,0},{4,2},{6,4},{8,6},{10,8},{12,10},{14,12},{1,15},{3,1}... | collective-permute-start | bytes 983048 | tf_op jit(solution)/shard_map/ppermute | solution.py:300
  108.7 2.5 %collective-permute-start.7 = (bf16[1280,128]{1,0:T(8,128)(2,1)S(1)}, bf16[1280,128]{1,0:T(8,128)(2,1)S(1)}, u32[]{:S(2)}, u32[]{:S(2)}) collective-permute-start(bf16[1280,128]{1,0:T(8,128)(2,1)S(1)} %get-tuple-element.53.every_ref), channel_id=1, source_target_pairs={{0,2},{2,4},{4,6},{6,8},{8,10},{10,12},{12,14},{14,0},{1,3},{3,5},... | collective-permute-start | bytes 983048 | tf_op jit(solution)/shard_map/ppermute | solution.py:300
  111.2 3.3 %collective-permute-start.4 = (bf16[640,128]{1,0:T(8,128)(2,1)S(1)}, bf16[640,128]{1,0:T(8,128)(2,1)S(1)}, u32[]{:S(2)}, u32[]{:S(2)}) collective-permute-start(bf16[640,128]{1,0:T(8,128)(2,1)S(1)} %get-tuple-element.51), channel_id=1, source_target_pairs={{0,4},{2,6},{4,8},{6,10},{8,12},{10,14},{12,0},{14,2},{1,5},{3,7},... | collective-permute-start | bytes 491528 | tf_op jit(solution)/shard_map/ppermute | solution.py:300
  114.5 4.6 %collective-permute-start.5 = (bf16[640,128]{1,0:T(8,128)(2,1)S(1)}, bf16[640,128]{1,0:T(8,128)(2,1)S(1)}, u32[]{:S(2)}, u32[]{:S(2)}) collective-permute-start(bf16[640,128]{1,0:T(8,128)(2,1)S(1)} %get-tuple-element.52), channel_id=1, source_target_pairs={{0,12},{2,14},{4,0},{6,2},{8,4},{10,6},{12,8},{14,10},{1,13},{3,15... | collective-permute-start | bytes 491528 | tf_op jit(solution)/shard_map/ppermute | solution.py:300
  119.2 2.5 %collective-permute-done.7.n0_ref = bf16[1280,128]{1,0:T(8,128)(2,1)S(1)} collective-permute-done((bf16[1280,128]{1,0:T(8,128)(2,1)S(1)}, bf16[1280,128]{1,0:T(8,128)(2,1)S(1)}, u32[]{:S(2)}, u32[]{:S(2)}) %collective-permute-start.7) | collective-permute-done | bytes 327712 | tf_op jit(solution)/shard_map/ppermute | solution.py:300
  121.7 1.9 %collective-permute-start.10 = (bf16[2560,128]{1,0:T(8,128)(2,1)S(1)}, bf16[2560,128]{1,0:T(8,128)(2,1)S(1)}, u32[]{:S(2)}, u32[]{:S(2)}) collective-permute-start(bf16[2560,128]{1,0:T(8,128)(2,1)S(1)} %pad_maximum_fusion), channel_id=1, source_target_pairs={{0,1},{1,0},{2,3},{3,2},{4,5},{5,4},{6,7},{7,6},{8,9},{9,8},{10,11... | collective-permute-start | bytes 1966088 | tf_op jit(solution)/shard_map/ppermute | solution.py:382
  123.6 2.4 %collective-permute-start.9 = (bf16[1280,128]{1,0:T(8,128)(2,1)S(1)}, bf16[1280,128]{1,0:T(8,128)(2,1)S(1)}, u32[]{:S(2)}, u32[]{:S(2)}) collective-permute-start(bf16[1280,128]{1,0:T(8,128)(2,1)S(1)} %get-tuple-element.53.every_ref), channel_id=1, source_target_pairs={{0,1},{1,0},{2,3},{3,2},{4,5},{5,4},{6,7},{7,6},{8,9},{9,8},{10,11... | collective-permute-start | bytes 983048 | tf_op jit(solution)/shard_map/ppermute | solution.py:382
  126.5 1.9 %collective-permute-start.6 = (bf16[1280,128]{1,0:T(8,128)(2,1)S(1)}, bf16[1280,128]{1,0:T(8,128)(2,1)S(1)}, u32[]{:S(2)}, u32[]{:S(2)}) collective-permute-start(bf16[1280,128]{1,0:T(8,128)(2,1)S(1)} %pad_maximum_fusion.1), channel_id=1, source_target_pairs={{0,1},{1,0},{2,3},{3,2},{4,5},{5,4},{6,7},{7,6},{8,9},{9,8},{10,11... | collective-permute-start | bytes 983048 | tf_op jit(solution)/shard_map/ppermute | solution.py:382
  128.5 1.7 shard_map.124
  130.3 1.9 %shard_map.125 = (bf16[1280,128]{1,0:T(8,128)(2,1)S(1)}, bf16[3840,128]{1,0:T(8,128)(2,1)S(1)}, bf16[1280,128]{1,0:T(8,128)(2,1)S(1)}, bf16[3840,128]{1,0:T(8,128)(2,1)S(1)}) custom-call(s32[2]{0:T(128)S(1)} %pad_add_fusion.at_ref, bf16[640,128]{1,0:T(8,128)(2,1)S(1)} %collective-permute-done.4.f0_ref, bf16[640,128]{1,0:T(8,128)(2,1)S(1)} %collective-permute-done.5.f1_ref, ...), custom_call_target="tpu_custom_call" | custom-call | tf_op jit(solution)/shard_map/pallas_call | solution.py:38
  132.2 2.4 %collective-permute-start.11 = (bf16[3840,128]{1,0:T(8,128)(2,1)S(1)}, bf16[3840,128]{1,0:T(8,128)(2,1)S(1)}, u32[]{:S(2)}, u32[]{:S(2)}) collective-permute-start(bf16[3840,128]{1,0:T(8,128)(2,1)S(1)} %get-tuple-element.58), channel_id=1, source_target_pairs={{0,1},{1,0},{2,3},{3,2},{4,5},{5,4},{6,7},{7,6},{8,9},{9,8},{10,11... | collective-permute-start | bytes 2949128 | tf_op jit(solution)/shard_map/ppermute | solution.py:396
  134.6 1.9 %collective-permute-start.14 = (bf16[1280,128]{1,0:T(8,128)(2,1)S(1)}, bf16[1280,128]{1,0:T(8,128)(2,1)S(1)}, u32[]{:S(2)}, u32[]{:S(2)}) collective-permute-start(bf16[1280,128]{1,0:T(8,128)(2,1)S(1)} %get-tuple-element.60), channel_id=1, source_target_pairs={{0,1},{1,0},{2,3},{3,2},{4,5},{5,4},{6,7},{7,6},{8,9},{9,8},{10,11... | collective-permute-start | bytes 983048 | tf_op jit(solution)/shard_map/ppermute | solution.py:395
  137.0 5.0 %collective-permute-start.13 = (bf16[1280,128]{1,0:T(8,128)(2,1)S(1)}, bf16[1280,128]{1,0:T(8,128)(2,1)S(1)}, u32[]{:S(2)}, u32[]{:S(2)}) collective-permute-start(bf16[1280,128]{1,0:T(8,128)(2,1)S(1)} %get-tuple-element.63), channel_id=1, source_target_pairs={{0,14},{2,0},{4,2},{6,4},{8,6},{10,8},{12,10},{14,12},{1,15},{3,1}... | collective-permute-start | bytes 983048 | tf_op jit(solution)/shard_map/ppermute | solution.py:300
  142.0 1.9 %collective-permute-start.12 = (bf16[1280,128]{1,0:T(8,128)(2,1)S(1)}, bf16[1280,128]{1,0:T(8,128)(2,1)S(1)}, u32[]{:S(2)}, u32[]{:S(2)}) collective-permute-start(bf16[1280,128]{1,0:T(8,128)(2,1)S(1)} %get-tuple-element.64), channel_id=1, source_target_pairs={{0,2},{2,4},{4,6},{6,8},{8,10},{10,12},{12,14},{14,0},{1,3},{3,5},... | collective-permute-start | bytes 983048 | tf_op jit(solution)/shard_map/ppermute | solution.py:300
  144.0 4.6 %collective-permute-start.16 = (bf16[640,128]{1,0:T(8,128)(2,1)S(1)}, bf16[640,128]{1,0:T(8,128)(2,1)S(1)}, u32[]{:S(2)}, u32[]{:S(2)}) collective-permute-start(bf16[640,128]{1,0:T(8,128)(2,1)S(1)} %get-tuple-element.65), channel_id=1, source_target_pairs={{0,12},{2,14},{4,0},{6,2},{8,4},{10,6},{12,8},{14,10},{1,13},{3,15... | collective-permute-start | bytes 491528 | tf_op jit(solution)/shard_map/ppermute | solution.py:300
  148.6 2.2 %collective-permute-start.15 = (bf16[640,128]{1,0:T(8,128)(2,1)S(1)}, bf16[640,128]{1,0:T(8,128)(2,1)S(1)}, u32[]{:S(2)}, u32[]{:S(2)}) collective-permute-start(bf16[640,128]{1,0:T(8,128)(2,1)S(1)} %get-tuple-element.66), channel_id=1, source_target_pairs={{0,4},{2,6},{4,8},{6,10},{8,12},{10,14},{12,0},{14,2},{1,5},{3,7},... | collective-permute-start | bytes 491528 | tf_op jit(solution)/shard_map/ppermute | solution.py:300
  150.8 5.7 %collective-permute-done.16.f1_ref = bf16[640,128]{1,0:T(8,128)(2,1)S(1)} collective-permute-done((bf16[640,128]{1,0:T(8,128)(2,1)S(1)}, bf16[640,128]{1,0:T(8,128)(2,1)S(1)}, u32[]{:S(2)}, u32[]{:S(2)}) %collective-permute-start.16) | collective-permute-done | bytes 163872 | tf_op jit(solution)/shard_map/ppermute | solution.py:300
  156.5 5.1 %collective-permute-done.15.f0_ref = bf16[640,128]{1,0:T(8,128)(2,1)S(1)} collective-permute-done((bf16[640,128]{1,0:T(8,128)(2,1)S(1)}, bf16[640,128]{1,0:T(8,128)(2,1)S(1)}, u32[]{:S(2)}, u32[]{:S(2)}) %collective-permute-start.15) | collective-permute-done | bytes 163872 | tf_op jit(solution)/shard_map/ppermute | solution.py:300
  161.9 26.6 %all_to_all.34 = bf16[64,24,128]{2,1,0:T(8,128)(2,1)S(1)} all-to-all(bf16[64,24,128]{2,1,0:T(8,128)(2,1)S(1)} %shard_map.126), channel_id=1, replica_groups=mesh['z'=8,'x'=4,'yh'=2,'yl'=4,'c'=2] {'z','x','yh'}, dimensions={0} | all-to-all | bytes 786432 | tf_op jit(solution)/shard_map/all_to_all | solution.py:304
  188.5 1.6 shard_map.127
  (50 shorter events, 8.6 us)
Async XLA Ops:
  0.2 1.0 copy-start.4
  1.1 0.8 copy-start.7
  1.9 0.8 copy-start.8
  2.6 0.8 copy-start.9
  4.4 45.2 %copy-start.6 = (f32[1,8192]{1,0:T(1,128)S(1)}, f32[1,8192]{1,0:T(1,128)}, u32[]{:S(2)}) copy-start(f32[1,8192]{1,0:T(1,128)} %gate_ref.1) | copy-start | bytes 98308
  42.1 21.8 %all-to-all-start.2 = ((bf16[16,128,128]{2,1,0:T(8,128)(2,1)}), bf16[16,128,128]{2,1,0:T(8,128)(2,1)S(1)}, u32[]{:S(2)}, u32[]{:S(2)}) async-start(bf16[16,128,128]{2,1,0:T(8,128)(2,1)} %get-tuple-element.46), calls=%async_computation.2 | async-start | bytes 1048576 | tf_op jit(solution)/shard_map/all_to_all | solution.py:304
  49.7 32.9 %copy-start.11 = (s32[256,2]{0,1:T(2,128)S(1)}, s32[256,2]{0,1:T(2,128)}, u32[]{:S(2)}) copy-start(s32[256,2]{0,1:T(2,128)} %param.19) | copy-start | bytes 6148
  49.7 34.4 %copy-start.2 = (bf16[256,2048]{1,0:T(8,128)(2,1)S(1)}, bf16[256,2048]{1,0:T(8,128)(2,1)}, u32[]{:S(2)}) copy-start(bf16[256,2048]{1,0:T(8,128)(2,1)} %resid_ref.1) | copy-start | bytes 3145732
  49.7 34.4 %copy-start.5 = (f32[2048]{0:T(1024)S(1)}, f32[2048]{0:T(1024)}, u32[]{:S(2)}) copy-start(f32[2048]{0:T(1024)} %param.18) | copy-start | bytes 24580
  51.1 9.2 %collective-permute-start = (bf16[80,256]{1,0:T(8,128)(2,1)S(1)}, bf16[80,256]{1,0:T(8,128)(2,1)S(1)}, u32[]{:S(2)}, u32[]{:S(2)}) collective-permute-start(bf16[80,256]{1,0:T(8,128)(2,1)S(1)} %get-tuple-element.43), channel_id=1, source_target_pairs={{0,16},{16,32},{32,48},{48,0},{1,17},{17,33},{33,49},{49,1},{2,18}... | collective-permute-start | bytes 122888 | tf_op jit(solution)/shard_map/ppermute | solution.py:356
  53.6 7.4 %collective-permute-start.1 = (bf16[80,256]{1,0:T(8,128)(2,1)S(1)}, bf16[80,256]{1,0:T(8,128)(2,1)S(1)}, u32[]{:S(2)}, u32[]{:S(2)}) collective-permute-start(bf16[80,256]{1,0:T(8,128)(2,1)S(1)} %get-tuple-element.44), channel_id=1, source_target_pairs={{0,32},{16,48},{32,0},{48,16},{1,33},{17,49},{33,1},{49,17},{2,34}... | collective-permute-start | bytes 122888 | tf_op jit(solution)/shard_map/ppermute | solution.py:356
  57.6 5.9 %collective-permute-start.2 = (bf16[80,256]{1,0:T(8,128)(2,1)S(1)}, bf16[80,256]{1,0:T(8,128)(2,1)S(1)}, u32[]{:S(2)}, u32[]{:S(2)}) collective-permute-start(bf16[80,256]{1,0:T(8,128)(2,1)S(1)} %get-tuple-element.45), channel_id=1, source_target_pairs={{0,48},{16,0},{32,16},{48,32},{1,49},{17,1},{33,17},{49,33},{2,50}... | collective-permute-start | bytes 122888 | tf_op jit(solution)/shard_map/ppermute | solution.py:356
  80.7 3.4 %collective-permute-start.3 = (bf16[8,64,256]{2,1,0:T(8,128)(2,1)S(1)}, bf16[8,64,256]{2,1,0:T(8,128)(2,1)S(1)}, u32[]{:S(2)}, u32[]{:S(2)}) collective-permute-start(bf16[8,64,256]{2,1,0:T(8,128)(2,1)S(1)} %all_to_all.32.own_ref), channel_id=1, source_target_pairs={{0,1},{1,0},{2,3},{3,2},{4,5},{5,4},{6,7},{7,6},{8,9},{9,8},{10,11... | collective-permute-start | bytes 786440 | tf_op jit(solution)/shard_map/ppermute | solution.py:363
  105.1 23.4 %copy-start.1 = (bf16[1,2048,256]{2,1,0:T(8,128)(2,1)S(1)}, bf16[1,2048,256]{2,1,0:T(8,128)(2,1)}, u32[]{:S(2)}) copy-start(bf16[1,2048,256]{2,1,0:T(8,128)(2,1)} %param.22) | copy-start | bytes 3145732
  105.2 23.3 %copy-start = (bf16[1,2048,256]{2,1,0:T(8,128)(2,1)S(1)}, bf16[1,2048,256]{2,1,0:T(8,128)(2,1)}, u32[]{:S(2)}) copy-start(bf16[1,2048,256]{2,1,0:T(8,128)(2,1)} %param.21) | copy-start | bytes 3145732
  105.2 14.0 %collective-permute-start.8 = (bf16[1280,128]{1,0:T(8,128)(2,1)S(1)}, bf16[1280,128]{1,0:T(8,128)(2,1)S(1)}, u32[]{:S(2)}, u32[]{:S(2)}) collective-permute-start(bf16[1280,128]{1,0:T(8,128)(2,1)S(1)} %get-tuple-element.53.every_ref), channel_id=1, source_target_pairs={{0,14},{2,0},{4,2},{6,4},{8,6},{10,8},{12,10},{14,12},{1,15},{3,1}... | collective-permute-start | bytes 983048 | tf_op jit(solution)/shard_map/ppermute | solution.py:300
  108.7 13.0 %collective-permute-start.7 = (bf16[1280,128]{1,0:T(8,128)(2,1)S(1)}, bf16[1280,128]{1,0:T(8,128)(2,1)S(1)}, u32[]{:S(2)}, u32[]{:S(2)}) collective-permute-start(bf16[1280,128]{1,0:T(8,128)(2,1)S(1)} %get-tuple-element.53.every_ref), channel_id=1, source_target_pairs={{0,2},{2,4},{4,6},{6,8},{8,10},{10,12},{12,14},{14,0},{1,3},{3,5},... | collective-permute-start | bytes 983048 | tf_op jit(solution)/shard_map/ppermute | solution.py:300
  111.2 15.2 %collective-permute-start.4 = (bf16[640,128]{1,0:T(8,128)(2,1)S(1)}, bf16[640,128]{1,0:T(8,128)(2,1)S(1)}, u32[]{:S(2)}, u32[]{:S(2)}) collective-permute-start(bf16[640,128]{1,0:T(8,128)(2,1)S(1)} %get-tuple-element.51), channel_id=1, source_target_pairs={{0,4},{2,6},{4,8},{6,10},{8,12},{10,14},{12,0},{14,2},{1,5},{3,7},... | collective-permute-start | bytes 491528 | tf_op jit(solution)/shard_map/ppermute | solution.py:300
  114.5 11.9 %collective-permute-start.5 = (bf16[640,128]{1,0:T(8,128)(2,1)S(1)}, bf16[640,128]{1,0:T(8,128)(2,1)S(1)}, u32[]{:S(2)}, u32[]{:S(2)}) collective-permute-start(bf16[640,128]{1,0:T(8,128)(2,1)S(1)} %get-tuple-element.52), channel_id=1, source_target_pairs={{0,12},{2,14},{4,0},{6,2},{8,4},{10,6},{12,8},{14,10},{1,13},{3,15... | collective-permute-start | bytes 491528 | tf_op jit(solution)/shard_map/ppermute | solution.py:300
  121.7 6.8 %collective-permute-start.10 = (bf16[2560,128]{1,0:T(8,128)(2,1)S(1)}, bf16[2560,128]{1,0:T(8,128)(2,1)S(1)}, u32[]{:S(2)}, u32[]{:S(2)}) collective-permute-start(bf16[2560,128]{1,0:T(8,128)(2,1)S(1)} %pad_maximum_fusion), channel_id=1, source_target_pairs={{0,1},{1,0},{2,3},{3,2},{4,5},{5,4},{6,7},{7,6},{8,9},{9,8},{10,11... | collective-permute-start | bytes 1966088 | tf_op jit(solution)/shard_map/ppermute | solution.py:382
  123.6 4.8 %collective-permute-start.9 = (bf16[1280,128]{1,0:T(8,128)(2,1)S(1)}, bf16[1280,128]{1,0:T(8,128)(2,1)S(1)}, u32[]{:S(2)}, u32[]{:S(2)}) collective-permute-start(bf16[1280,128]{1,0:T(8,128)(2,1)S(1)} %get-tuple-element.53.every_ref), channel_id=1, source_target_pairs={{0,1},{1,0},{2,3},{3,2},{4,5},{5,4},{6,7},{7,6},{8,9},{9,8},{10,11... | collective-permute-start | bytes 983048 | tf_op jit(solution)/shard_map/ppermute | solution.py:382
  126.5 3.8 %collective-permute-start.6 = (bf16[1280,128]{1,0:T(8,128)(2,1)S(1)}, bf16[1280,128]{1,0:T(8,128)(2,1)S(1)}, u32[]{:S(2)}, u32[]{:S(2)}) collective-permute-start(bf16[1280,128]{1,0:T(8,128)(2,1)S(1)} %pad_maximum_fusion.1), channel_id=1, source_target_pairs={{0,1},{1,0},{2,3},{3,2},{4,5},{5,4},{6,7},{7,6},{8,9},{9,8},{10,11... | collective-permute-start | bytes 983048 | tf_op jit(solution)/shard_map/ppermute | solution.py:382
  128.5 1.8 copy-start.3
  132.2 4.6 %collective-permute-start.11 = (bf16[3840,128]{1,0:T(8,128)(2,1)S(1)}, bf16[3840,128]{1,0:T(8,128)(2,1)S(1)}, u32[]{:S(2)}, u32[]{:S(2)}) collective-permute-start(bf16[3840,128]{1,0:T(8,128)(2,1)S(1)} %get-tuple-element.58), channel_id=1, source_target_pairs={{0,1},{1,0},{2,3},{3,2},{4,5},{5,4},{6,7},{7,6},{8,9},{9,8},{10,11... | collective-permute-start | bytes 2949128 | tf_op jit(solution)/shard_map/ppermute | solution.py:396
  134.6 9.3 %collective-permute-start.14 = (bf16[1280,128]{1,0:T(8,128)(2,1)S(1)}, bf16[1280,128]{1,0:T(8,128)(2,1)S(1)}, u32[]{:S(2)}, u32[]{:S(2)}) collective-permute-start(bf16[1280,128]{1,0:T(8,128)(2,1)S(1)} %get-tuple-element.60), channel_id=1, source_target_pairs={{0,1},{1,0},{2,3},{3,2},{4,5},{5,4},{6,7},{7,6},{8,9},{9,8},{10,11... | collective-permute-start | bytes 983048 | tf_op jit(solution)/shard_map/ppermute | solution.py:395
  137.0 24.6 %collective-permute-start.13 = (bf16[1280,128]{1,0:T(8,128)(2,1)S(1)}, bf16[1280,128]{1,0:T(8,128)(2,1)S(1)}, u32[]{:S(2)}, u32[]{:S(2)}) collective-permute-start(bf16[1280,128]{1,0:T(8,128)(2,1)S(1)} %get-tuple-element.63), channel_id=1, source_target_pairs={{0,14},{2,0},{4,2},{6,4},{8,6},{10,8},{12,10},{14,12},{1,15},{3,1}... | collective-permute-start | bytes 983048 | tf_op jit(solution)/shard_map/ppermute | solution.py:300
  142.0 19.6 %collective-permute-start.12 = (bf16[1280,128]{1,0:T(8,128)(2,1)S(1)}, bf16[1280,128]{1,0:T(8,128)(2,1)S(1)}, u32[]{:S(2)}, u32[]{:S(2)}) collective-permute-start(bf16[1280,128]{1,0:T(8,128)(2,1)S(1)} %get-tuple-element.64), channel_id=1, source_target_pairs={{0,2},{2,4},{4,6},{6,8},{8,10},{10,12},{12,14},{14,0},{1,3},{3,5},... | collective-permute-start | bytes 983048 | tf_op jit(solution)/shard_map/ppermute | solution.py:300
  144.0 12.5 %collective-permute-start.16 = (bf16[640,128]{1,0:T(8,128)(2,1)S(1)}, bf16[640,128]{1,0:T(8,128)(2,1)S(1)}, u32[]{:S(2)}, u32[]{:S(2)}) collective-permute-start(bf16[640,128]{1,0:T(8,128)(2,1)S(1)} %get-tuple-element.65), channel_id=1, source_target_pairs={{0,12},{2,14},{4,0},{6,2},{8,4},{10,6},{12,8},{14,10},{1,13},{3,15... | collective-permute-start | bytes 491528 | tf_op jit(solution)/shard_map/ppermute | solution.py:300
  148.6 39.9 %copy-start.10 = (f32[256,2]{0,1:T(2,128)S(1)}, f32[256,2]{0,1:T(2,128)}, u32[]{:S(2)}) copy-start(f32[256,2]{0,1:T(2,128)} %param.20) | copy-start | bytes 6148
  148.6 13.0 %collective-permute-start.15 = (bf16[640,128]{1,0:T(8,128)(2,1)S(1)}, bf16[640,128]{1,0:T(8,128)(2,1)S(1)}, u32[]{:S(2)}, u32[]{:S(2)}) collective-permute-start(bf16[640,128]{1,0:T(8,128)(2,1)S(1)} %get-tuple-element.66), channel_id=1, source_target_pairs={{0,4},{2,6},{4,8},{6,10},{8,12},{10,14},{12,0},{14,2},{1,5},{3,7},... | collective-permute-start | bytes 491528 | tf_op jit(solution)/shard_map/ppermute | solution.py:300

commit v9 on v7

--- a/solution.py
+++ b/solution.py
@@ -30,9 +30,9 @@
 INTERPRET = False
 
 
-def call(body, out_shape, inputs, smem=0, scratch=(), limit=12, space=pltpu.VMEM):
+def call(body, out_shape, inputs, smem=0, scratch=(), limit=12):
     specs = [pl.BlockSpec(memory_space=pltpu.SMEM)] * smem
-    specs += [pl.BlockSpec(memory_space=space)] * (len(inputs) - smem)
+    specs += [pl.BlockSpec(memory_space=pltpu.VMEM)] * (len(inputs) - smem)
     many = isinstance(out_shape, (tuple, list))
     vm = pl.BlockSpec(memory_space=pltpu.VMEM)
     return pl.pallas_call(
@@ -139,27 +139,19 @@
     out_ref[...] = (acc / total).astype(bf)
 
 
-def prepare(k_ref, v_ref, q_ref, w_ref, kv_ref, qs_ref, out_ref, kb_ref, vb_ref, qb_ref, wb_ref, sems):
-    pairs = ((k_ref, kb_ref), (v_ref, vb_ref), (q_ref, qb_ref), (w_ref, wb_ref))
-    copies = [pltpu.make_async_copy(a, b, sems.at[i]) for i, (a, b) in enumerate(pairs)]
-    for copy in copies:
-        copy.start()
-    for copy in copies[0:3]:
-        copy.wait()
+def prepare(kvq_ref, w_ref, kv_ref, qs_ref, out_ref):
     for z in range(NZ):
-        kv_ref[z, 0:HD, :] = kb_ref[...]
-        kv_ref[z, HD : 2 * HD, :] = vb_ref[...]
+        kv_ref[z] = kvq_ref[0 : 2 * HD, :]
     for x in range(NX):
-        qs_ref[x] = qb_ref[...]
-    copies[3].wait()
+        qs_ref[x] = kvq_ref[2 * HD :, :]
     for y in range(NY):
         for c in range(NC):
             for q in range(2):
                 block = (y % HALF + q * HALF) * NC + c
-                out_ref[y * NC + c, q * HD : (q + 1) * HD, :] = wb_ref[:, block * COLS : (block + 1) * COLS]
-
-
-def route(routes_ref, pick_ref, slots_ref):
+                out_ref[y * NC + c, q * HD : (q + 1) * HD, :] = w_ref[:, block * COLS : (block + 1) * COLS]
+
+
+def route(routes_ref, pick_ref, back_ref):
     e0, e1 = routes_ref[0:1, :], routes_ref[1:2, :]
     io = lax.broadcasted_iota(jnp.int32, (NSP, TOK), 0)
     h0, h1 = io == e0, io == e1
@@ -170,7 +162,12 @@
     before = jnp.dot(hit, upper, preferred_element_type=f32)
     r0 = jnp.sum(jnp.where(h0, before, 0.0), axis=0, keepdims=True).astype(jnp.int32)
     r1 = jnp.sum(jnp.where(h1, before, 0.0), axis=0, keepdims=True).astype(jnp.int32)
-    slots_ref[...] = jnp.concatenate([2 * SLOT * e0 + r0, 2 * SLOT * e1 + r1, jnp.zeros((6, TOK), jnp.int32)], axis=0)
+    slots = jnp.concatenate([2 * SLOT * e0 + r0, 2 * SLOT * e1 + r1, jnp.zeros((6, TOK), jnp.int32)], axis=0)
+    slots = slots.astype(f32).T
+    at = lax.broadcasted_iota(jnp.int32, (TOK, 2 * PADROWS), 1).astype(f32)
+    for k in range(2):
+        slot = slots[:, k : k + 1]
+        back_ref[k * TOK : (k + 1) * TOK, :] = jnp.where((at == slot) | (at == slot + SLOT), 1.0, 0.0).astype(bf)
     s0 = e0 * SEND + r0
     s1 = e1 * SEND + r1
     ir = lax.broadcasted_iota(jnp.int32, (NSP * SEND, TOK), 0)
@@ -278,16 +275,10 @@
             out_ref[2 * i + q] = jnp.concatenate([rows_ref[CAP * i : CAP * i + CAP, :], pad], axis=0).astype(bf)
 
 
-def finish(ret_ref, slots_ref, rw_ref, stream_ref, out_ref):
-    slots = slots_ref[...].astype(f32).T
+def finish(ret_ref, back_ref, rw_ref, stream_ref, out_ref):
     weight = jnp.concatenate([rw_ref[...], jnp.zeros((6, TOK), f32)], axis=0).T
-    lane = lax.broadcasted_iota(jnp.int32, (TOK, 2 * PADROWS), 1).astype(f32)
-    out = stream_ref[...]
-    for k in range(2):
-        slot = slots[:, k : k + 1]
-        pick = jnp.where((lane == slot) | (lane == slot + SLOT), 1.0, 0.0).astype(bf)
-        got = jnp.dot(pick, ret_ref[...], preferred_element_type=f32)
-        out = out + weight[:, k : k + 1] * got
+    got = jnp.dot(back_ref[...], ret_ref[...], preferred_element_type=f32)
+    out = stream_ref[...] + weight[:, 0:1] * got[0:TOK, :] + weight[:, 1:2] * got[TOK:, :]
     out_ref[...] = out.astype(bf)
 
 
@@ -319,18 +310,15 @@
     low = (lax.rem(y, half) * NC + c) * COLS
     at_cols = jnp.stack([low, low + half * NC * COLS, y // half]).astype(jnp.int32)
     at = jnp.stack([z, x]).astype(jnp.int32)
-    small = pltpu.VMEM((HD, TOK), bf)
     kv_send, q_send, w_send = call(
         prepare,
         (sds((NZ, 2 * HD, TOK), bf), sds((NX, HD, TOK), bf), sds((NTP, 2 * HD, COLS), bf)),
-        (keys.T, values.T, queries.T, out_weight),
-        scratch=(small, small, small, pltpu.VMEM((HD, D), bf), pltpu.SemaphoreType.DMA((4,))),
-        space=pl.ANY,
-    )
-    kv_send, w_send, at, at_cols = lax.optimization_barrier((kv_send, w_send, at, at_cols))
+        (jnp.concatenate([keys.T, values.T, queries.T], axis=0), out_weight),
+    )
+    q_send, w_send, at, at_cols = lax.optimization_barrier((q_send, w_send, at, at_cols))
+    q = exchange(q_send, "x")
+    kv_send, q = lax.optimization_barrier((kv_send, q))
     kv = exchange(kv_send, "z")
-    q_send, kv = lax.optimization_barrier((q_send, kv))
-    q = exchange(q_send, "x")
     w_cols = exchange(w_send, TP)
     sent = call(
         attend,
@@ -349,8 +337,8 @@
     parts = [sent[0]]
     for n in range(1, NX):
         parts.append(lax.ppermute(sent[n], "x", [(i, (i + n) % NX) for i in range(NX)]))
-    pick, slots = call(
-        route, (sds((NSP * SEND, TOK), bf), sds((8, TOK), jnp.int32)), (routes.T,)
+    pick, back_pick = call(
+        route, (sds((NSP * SEND, TOK), bf), sds((2 * TOK, 2 * PADROWS), bf)), (routes.T,)
     )
     attended = call(merge, sds((HD, TOK), bf), tuple(parts))
     attended = lax.all_gather(attended, TP, axis=0, tiled=True)
@@ -408,7 +396,7 @@
         scratch=(pltpu.VMEM((ROWS, COLS), f32),),
     )
     returned = exchange(back, ("z", "x", "yh")).reshape(2 * PADROWS, COLS)
-    return call(finish, sds((TOK, COLS), bf), (returned, slots, route_weight.T, stream))
+    return call(finish, sds((TOK, COLS), bf), (returned, back_pick, route_weight.T, stream))
 
 
 def solution(mesh):

time: 191 us -> 189 us (0.990)
  transfers between devices with their start and end apart: 17 -> 17, of which waited for: 6 -> 6; matrix products, arithmetic and copies ran while one was open for 0% -> 0% of each run, Pallas kernels for 2% -> 3%
where the time goes in v9:
time: 189 us; the launch traced here: 188 us
  blocking collectives  102 us (54%)
  starting transfers between devices  55.2 us (29%)
  waiting for transfers between devices  16.2 us (9%)
  Pallas kernels  10.6 us (6%)
  local copies, waits for them, and re-layouts  2.2 us (1%)
    all_to_all x4, blocking collectives, exchange(): return lax.all_to_all(v, axis, 0, 0, tiled=True)  85 us
    ppermute x8, starting transfers between devices, shift(): return lax.ppermute(v, Y, [(i, (i + by) % NY) for i in range(NY)])  27.7 us
    all_gather x1, blocking collectives, layer(): attended = lax.all_gather(attended, TP, axis=0, tiled=True)  17 us
    ppermute x8, waiting for transfers between devices, shift(): return lax.ppermute(v, Y, [(i, (i + by) % NY) for i in range(NY)])  14.5 us
    pallas_call x10, Pallas kernels, call(): pl.pallas_call(body, out_shape=out_shape, in_specs=specs, out_specs=tuple...  10.6 us
    ppermute x3, starting transfers between devices, layer(): lax.ppermute(sent[n], 'x', [(i, (i + n) % NX) for i in range(NX)])  9.18 us
    all_to_all x1, starting transfers between devices, exchange(): return lax.all_to_all(v, axis, 0, 0, tiled=True)  7.69 us
    ppermute x3, starting transfers between devices, layer(): others.append(lax.ppermute(v, 'c', swap))  6.25 us
  transfers between devices with their start and end apart: 17, of which 6 were waited for; matrix products, arithmetic and copies ran while one was open for 0% of the time, Pallas kernels for 3%

profile of v9, /device:TPU:8, one launch (start us, length us, event | category | flops | bytes accessed | tf_op | source)
XLA Modules:
  0.0 187.9 jit_solution(2077280381313271035)
XLA Ops:
  2.8 10.1 %all_to_all.25.q_ref = bf16[4,64,256]{2,1,0:T(8,128)(2,1)S(1)} all-to-all(bf16[4,64,256]{2,1,0:T(8,128)(2,1)S(1)} %get-tuple-element.37), channel_id=1, replica_groups=mesh['z'=8,'x'=4,'yh'=2,'yl'=4,'c'=2] {'x'}, dimensions={0} | all-to-all | bytes 262144 | tf_op jit(solution)/shard_map/all_to_all | solution.py:290
  12.9 26.3 %all_to_all.26.kv_ref = bf16[8,128,256]{2,1,0:T(8,128)(2,1)S(1)} all-to-all(bf16[8,128,256]{2,1,0:T(8,128)(2,1)S(1)} %get-tuple-element.39), channel_id=1, replica_groups=mesh['z'=8,'x'=4,'yh'=2,'yl'=4,'c'=2] {'z'}, dimensions={0} | all-to-all | bytes 1048576 | tf_op jit(solution)/shard_map/all_to_all | solution.py:290
  39.2 7.7 %all-to-all-start.2 = ((bf16[16,128,128]{2,1,0:T(8,128)(2,1)}), bf16[16,128,128]{2,1,0:T(8,128)(2,1)S(1)}, u32[]{:S(2)}, u32[]{:S(2)}) async-start(bf16[16,128,128]{2,1,0:T(8,128)(2,1)} %get-tuple-element.44), calls=%async_computation.2 | async-start | bytes 1048576 | tf_op jit(solution)/shard_map/all_to_all | solution.py:290
  46.9 1.3 shard_map.119
  48.2 2.5 %collective-permute-start = (bf16[80,256]{1,0:T(8,128)(2,1)S(1)}, bf16[80,256]{1,0:T(8,128)(2,1)S(1)}, u32[]{:S(2)}, u32[]{:S(2)}) collective-permute-start(bf16[80,256]{1,0:T(8,128)(2,1)S(1)} %get-tuple-element.41), channel_id=1, source_target_pairs={{0,16},{16,32},{32,48},{48,0},{1,17},{17,33},{33,49},{49,1},{2,18}... | collective-permute-start | bytes 122888 | tf_op jit(solution)/shard_map/ppermute | solution.py:339
  50.7 4.0 %collective-permute-start.1 = (bf16[80,256]{1,0:T(8,128)(2,1)S(1)}, bf16[80,256]{1,0:T(8,128)(2,1)S(1)}, u32[]{:S(2)}, u32[]{:S(2)}) collective-permute-start(bf16[80,256]{1,0:T(8,128)(2,1)S(1)} %get-tuple-element.42), channel_id=1, source_target_pairs={{0,32},{16,48},{32,0},{48,16},{1,33},{17,49},{33,1},{49,17},{2,34}... | collective-permute-start | bytes 122888 | tf_op jit(solution)/shard_map/ppermute | solution.py:339
  54.7 2.7 %collective-permute-start.2 = (bf16[80,256]{1,0:T(8,128)(2,1)S(1)}, bf16[80,256]{1,0:T(8,128)(2,1)S(1)}, u32[]{:S(2)}, u32[]{:S(2)}) collective-permute-start(bf16[80,256]{1,0:T(8,128)(2,1)S(1)} %get-tuple-element.43), channel_id=1, source_target_pairs={{0,48},{16,0},{32,16},{48,32},{1,49},{17,1},{33,17},{49,33},{2,50}... | collective-permute-start | bytes 122888 | tf_op jit(solution)/shard_map/ppermute | solution.py:339
  57.4 1.7 shard_map.121
  59.1 1.4 collective-permute-done.2.refs_3_
  60.6 17.0 %all_gather.3.att_ref = bf16[1024,256]{1,0:T(8,128)(2,1)S(1)} all-gather(bf16[64,256]{1,0:T(8,128)(2,1)S(1)} %shard_map.120), channel_id=1, replica_groups=mesh['z'=8,'x'=4,'yh'=2,'yl'=4,'c'=2] {'yh','yl','c'}, dimensions={0}, use_global_device_ids=true | all-gather | bytes 557056 | tf_op jit(solution)/shard_map/all_gather | solution.py:344
  78.9 1.4 shard_map.122
  80.3 20.9 %all_to_all.27.in_ref = bf16[32,40,128]{2,1,0:T(8,128)(2,1)S(1)} all-to-all(bf16[32,40,128]{2,1,0:T(8,128)(2,1)S(1)} %get-tuple-element.46), channel_id=1, replica_groups=mesh['z'=8,'x'=4,'yh'=2,'yl'=4,'c'=2] {'z','x'}, dimensions={0} | all-to-all | bytes 655360 | tf_op jit(solution)/shard_map/all_to_all | solution.py:290
  101.3 3.8 %collective-permute-start.7 = (bf16[1280,128]{1,0:T(8,128)(2,1)S(1)}, bf16[1280,128]{1,0:T(8,128)(2,1)S(1)}, u32[]{:S(2)}, u32[]{:S(2)}) collective-permute-start(bf16[1280,128]{1,0:T(8,128)(2,1)S(1)} %get-tuple-element.49.every_ref), channel_id=1, source_target_pairs={{0,14},{2,0},{4,2},{6,4},{8,6},{10,8},{12,10},{14,12},{1,15},{3,1}... | collective-permute-start | bytes 983048 | tf_op jit(solution)/shard_map/ppermute | solution.py:286
  105.1 2.2 %collective-permute-start.6 = (bf16[1280,128]{1,0:T(8,128)(2,1)S(1)}, bf16[1280,128]{1,0:T(8,128)(2,1)S(1)}, u32[]{:S(2)}, u32[]{:S(2)}) collective-permute-start(bf16[1280,128]{1,0:T(8,128)(2,1)S(1)} %get-tuple-element.49.every_ref), channel_id=1, source_target_pairs={{0,2},{2,4},{4,6},{6,8},{8,10},{10,12},{12,14},{14,0},{1,3},{3,5},... | collective-permute-start | bytes 983048 | tf_op jit(solution)/shard_map/ppermute | solution.py:286
  107.2 5.5 %collective-permute-start.3 = (bf16[640,128]{1,0:T(8,128)(2,1)S(1)}, bf16[640,128]{1,0:T(8,128)(2,1)S(1)}, u32[]{:S(2)}, u32[]{:S(2)}) collective-permute-start(bf16[640,128]{1,0:T(8,128)(2,1)S(1)} %get-tuple-element.47), channel_id=1, source_target_pairs={{0,4},{2,6},{4,8},{6,10},{8,12},{10,14},{12,0},{14,2},{1,5},{3,7},... | collective-permute-start | bytes 491528 | tf_op jit(solution)/shard_map/ppermute | solution.py:286
  112.7 2.5 %collective-permute-start.4 = (bf16[640,128]{1,0:T(8,128)(2,1)S(1)}, bf16[640,128]{1,0:T(8,128)(2,1)S(1)}, u32[]{:S(2)}, u32[]{:S(2)}) collective-permute-start(bf16[640,128]{1,0:T(8,128)(2,1)S(1)} %get-tuple-element.48), channel_id=1, source_target_pairs={{0,12},{2,14},{4,0},{6,2},{8,4},{10,6},{12,8},{14,10},{1,13},{3,15... | collective-permute-start | bytes 491528 | tf_op jit(solution)/shard_map/ppermute | solution.py:286
  115.2 2.4 %collective-permute-done.6.n0_ref = bf16[1280,128]{1,0:T(8,128)(2,1)S(1)} collective-permute-done((bf16[1280,128]{1,0:T(8,128)(2,1)S(1)}, bf16[1280,128]{1,0:T(8,128)(2,1)S(1)}, u32[]{:S(2)}, u32[]{:S(2)}) %collective-permute-start.6) | collective-permute-done | bytes 327712 | tf_op jit(solution)/shard_map/ppermute | solution.py:286
  117.6 1.9 %collective-permute-start.9 = (bf16[2560,128]{1,0:T(8,128)(2,1)S(1)}, bf16[2560,128]{1,0:T(8,128)(2,1)S(1)}, u32[]{:S(2)}, u32[]{:S(2)}) collective-permute-start(bf16[2560,128]{1,0:T(8,128)(2,1)S(1)} %pad_maximum_fusion), channel_id=1, source_target_pairs={{0,1},{1,0},{2,3},{3,2},{4,5},{5,4},{6,7},{7,6},{8,9},{9,8},{10,11... | collective-permute-start | bytes 1966088 | tf_op jit(solution)/shard_map/ppermute | solution.py:364
  119.6 2.4 %collective-permute-start.8 = (bf16[1280,128]{1,0:T(8,128)(2,1)S(1)}, bf16[1280,128]{1,0:T(8,128)(2,1)S(1)}, u32[]{:S(2)}, u32[]{:S(2)}) collective-permute-start(bf16[1280,128]{1,0:T(8,128)(2,1)S(1)} %get-tuple-element.49.every_ref), channel_id=1, source_target_pairs={{0,1},{1,0},{2,3},{3,2},{4,5},{5,4},{6,7},{7,6},{8,9},{9,8},{10,11... | collective-permute-start | bytes 983048 | tf_op jit(solution)/shard_map/ppermute | solution.py:364
  122.0 1.4 collective-permute-done.3.f0_ref
  123.4 1.9 %collective-permute-start.5 = (bf16[1280,128]{1,0:T(8,128)(2,1)S(1)}, bf16[1280,128]{1,0:T(8,128)(2,1)S(1)}, u32[]{:S(2)}, u32[]{:S(2)}) collective-permute-start(bf16[1280,128]{1,0:T(8,128)(2,1)S(1)} %pad_maximum_fusion.1), channel_id=1, source_target_pairs={{0,1},{1,0},{2,3},{3,2},{4,5},{5,4},{6,7},{7,6},{8,9},{9,8},{10,11... | collective-permute-start | bytes 983048 | tf_op jit(solution)/shard_map/ppermute | solution.py:364
  125.4 1.7 shard_map.124
  127.2 1.9 %shard_map.125 = (bf16[1280,128]{1,0:T(8,128)(2,1)S(1)}, bf16[3840,128]{1,0:T(8,128)(2,1)S(1)}, bf16[1280,128]{1,0:T(8,128)(2,1)S(1)}, bf16[3840,128]{1,0:T(8,128)(2,1)S(1)}) custom-call(s32[2]{0:T(128)S(1)} %pad_add_fusion.at_ref, bf16[640,128]{1,0:T(8,128)(2,1)S(1)} %collective-permute-done.3.f0_ref, bf16[640,128]{1,0:T(8,128)(2,1)S(1)} %collective-permute-done.4.f1_ref, ...), custom_call_target="tpu_custom_call" | custom-call | tf_op jit(solution)/shard_map/pallas_call | solution.py:38
  129.1 2.4 %collective-permute-start.10 = (bf16[3840,128]{1,0:T(8,128)(2,1)S(1)}, bf16[3840,128]{1,0:T(8,128)(2,1)S(1)}, u32[]{:S(2)}, u32[]{:S(2)}) collective-permute-start(bf16[3840,128]{1,0:T(8,128)(2,1)S(1)} %get-tuple-element.54), channel_id=1, source_target_pairs={{0,1},{1,0},{2,3},{3,2},{4,5},{5,4},{6,7},{7,6},{8,9},{9,8},{10,11... | collective-permute-start | bytes 2949128 | tf_op jit(solution)/shard_map/ppermute | solution.py:378
  131.5 1.9 %collective-permute-start.13 = (bf16[1280,128]{1,0:T(8,128)(2,1)S(1)}, bf16[1280,128]{1,0:T(8,128)(2,1)S(1)}, u32[]{:S(2)}, u32[]{:S(2)}) collective-permute-start(bf16[1280,128]{1,0:T(8,128)(2,1)S(1)} %get-tuple-element.56), channel_id=1, source_target_pairs={{0,1},{1,0},{2,3},{3,2},{4,5},{5,4},{6,7},{7,6},{8,9},{9,8},{10,11... | collective-permute-start | bytes 983048 | tf_op jit(solution)/shard_map/ppermute | solution.py:377
  133.9 5.1 %collective-permute-start.12 = (bf16[1280,128]{1,0:T(8,128)(2,1)S(1)}, bf16[1280,128]{1,0:T(8,128)(2,1)S(1)}, u32[]{:S(2)}, u32[]{:S(2)}) collective-permute-start(bf16[1280,128]{1,0:T(8,128)(2,1)S(1)} %get-tuple-element.59), channel_id=1, source_target_pairs={{0,14},{2,0},{4,2},{6,4},{8,6},{10,8},{12,10},{14,12},{1,15},{3,1}... | collective-permute-start | bytes 983048 | tf_op jit(solution)/shard_map/ppermute | solution.py:286
  139.0 1.9 %collective-permute-start.11 = (bf16[1280,128]{1,0:T(8,128)(2,1)S(1)}, bf16[1280,128]{1,0:T(8,128)(2,1)S(1)}, u32[]{:S(2)}, u32[]{:S(2)}) collective-permute-start(bf16[1280,128]{1,0:T(8,128)(2,1)S(1)} %get-tuple-element.60), channel_id=1, source_target_pairs={{0,2},{2,4},{4,6},{6,8},{8,10},{10,12},{12,14},{14,0},{1,3},{3,5},... | collective-permute-start | bytes 983048 | tf_op jit(solution)/shard_map/ppermute | solution.py:286
  141.0 4.6 %collective-permute-start.15 = (bf16[640,128]{1,0:T(8,128)(2,1)S(1)}, bf16[640,128]{1,0:T(8,128)(2,1)S(1)}, u32[]{:S(2)}, u32[]{:S(2)}) collective-permute-start(bf16[640,128]{1,0:T(8,128)(2,1)S(1)} %get-tuple-element.61), channel_id=1, source_target_pairs={{0,12},{2,14},{4,0},{6,2},{8,4},{10,6},{12,8},{14,10},{1,13},{3,15... | collective-permute-start | bytes 491528 | tf_op jit(solution)/shard_map/ppermute | solution.py:286
  145.6 2.2 %collective-permute-start.14 = (bf16[640,128]{1,0:T(8,128)(2,1)S(1)}, bf16[640,128]{1,0:T(8,128)(2,1)S(1)}, u32[]{:S(2)}, u32[]{:S(2)}) collective-permute-start(bf16[640,128]{1,0:T(8,128)(2,1)S(1)} %get-tuple-element.62), channel_id=1, source_target_pairs={{0,4},{2,6},{4,8},{6,10},{8,12},{10,14},{12,0},{14,2},{1,5},{3,7},... | collective-permute-start | bytes 491528 | tf_op jit(solution)/shard_map/ppermute | solution.py:286
  147.8 5.7 %collective-permute-done.15.f1_ref = bf16[640,128]{1,0:T(8,128)(2,1)S(1)} collective-permute-done((bf16[640,128]{1,0:T(8,128)(2,1)S(1)}, bf16[640,128]{1,0:T(8,128)(2,1)S(1)}, u32[]{:S(2)}, u32[]{:S(2)}) %collective-permute-start.15) | collective-permute-done | bytes 163872 | tf_op jit(solution)/shard_map/ppermute | solution.py:286
  153.5 5.1 %collective-permute-done.14.f0_ref = bf16[640,128]{1,0:T(8,128)(2,1)S(1)} collective-permute-done((bf16[640,128]{1,0:T(8,128)(2,1)S(1)}, bf16[640,128]{1,0:T(8,128)(2,1)S(1)}, u32[]{:S(2)}, u32[]{:S(2)}) %collective-permute-start.14) | collective-permute-done | bytes 163872 | tf_op jit(solution)/shard_map/ppermute | solution.py:286
  158.9 27.7 %all_to_all.28 = bf16[64,24,128]{2,1,0:T(8,128)(2,1)S(1)} all-to-all(bf16[64,24,128]{2,1,0:T(8,128)(2,1)S(1)} %shard_map.126), channel_id=1, replica_groups=mesh['z'=8,'x'=4,'yh'=2,'yl'=4,'c'=2] {'z','x','yh'}, dimensions={0} | all-to-all | bytes 786432 | tf_op jit(solution)/shard_map/all_to_all | solution.py:290
  (43 shorter events, 6.4 us)
Async XLA Ops:
  0.9 0.9 copy-start.4
  1.8 45.0 %copy-start.6 = (f32[1,8192]{1,0:T(1,128)S(1)}, f32[1,8192]{1,0:T(1,128)}, u32[]{:S(2)}) copy-start(f32[1,8192]{1,0:T(1,128)} %gate_ref.1) | copy-start | bytes 98308
  12.9 44.6 %copy-start.8 = (s32[256,2]{0,1:T(2,128)S(1)}, s32[256,2]{0,1:T(2,128)}, u32[]{:S(2)}) copy-start(s32[256,2]{0,1:T(2,128)} %param.19) | copy-start | bytes 6148
  39.2 38.5 %copy-start.5 = (f32[2048]{0:T(1024)S(1)}, f32[2048]{0:T(1024)}, u32[]{:S(2)}) copy-start(f32[2048]{0:T(1024)} %param.18) | copy-start | bytes 24580
  39.2 38.5 %all-to-all-start.2 = ((bf16[16,128,128]{2,1,0:T(8,128)(2,1)}), bf16[16,128,128]{2,1,0:T(8,128)(2,1)S(1)}, u32[]{:S(2)}, u32[]{:S(2)}) async-start(bf16[16,128,128]{2,1,0:T(8,128)(2,1)} %get-tuple-element.44), calls=%async_computation.2 | async-start | bytes 1048576 | tf_op jit(solution)/shard_map/all_to_all | solution.py:290
  48.2 10.9 %collective-permute-start = (bf16[80,256]{1,0:T(8,128)(2,1)S(1)}, bf16[80,256]{1,0:T(8,128)(2,1)S(1)}, u32[]{:S(2)}, u32[]{:S(2)}) collective-permute-start(bf16[80,256]{1,0:T(8,128)(2,1)S(1)} %get-tuple-element.41), channel_id=1, source_target_pairs={{0,16},{16,32},{32,48},{48,0},{1,17},{17,33},{33,49},{49,1},{2,18}... | collective-permute-start | bytes 122888 | tf_op jit(solution)/shard_map/ppermute | solution.py:339
  50.7 8.4 %collective-permute-start.1 = (bf16[80,256]{1,0:T(8,128)(2,1)S(1)}, bf16[80,256]{1,0:T(8,128)(2,1)S(1)}, u32[]{:S(2)}, u32[]{:S(2)}) collective-permute-start(bf16[80,256]{1,0:T(8,128)(2,1)S(1)} %get-tuple-element.42), channel_id=1, source_target_pairs={{0,32},{16,48},{32,0},{48,16},{1,33},{17,49},{33,1},{49,17},{2,34}... | collective-permute-start | bytes 122888 | tf_op jit(solution)/shard_map/ppermute | solution.py:339
  54.7 5.9 %collective-permute-start.2 = (bf16[80,256]{1,0:T(8,128)(2,1)S(1)}, bf16[80,256]{1,0:T(8,128)(2,1)S(1)}, u32[]{:S(2)}, u32[]{:S(2)}) collective-permute-start(bf16[80,256]{1,0:T(8,128)(2,1)S(1)} %get-tuple-element.43), channel_id=1, source_target_pairs={{0,48},{16,0},{32,16},{48,32},{1,49},{17,1},{33,17},{49,33},{2,50}... | collective-permute-start | bytes 122888 | tf_op jit(solution)/shard_map/ppermute | solution.py:339
  77.7 1.2 copy-start.2
  101.2 24.2 %copy-start = (bf16[1,2048,256]{2,1,0:T(8,128)(2,1)S(1)}, bf16[1,2048,256]{2,1,0:T(8,128)(2,1)}, u32[]{:S(2)}) copy-start(bf16[1,2048,256]{2,1,0:T(8,128)(2,1)} %param.21) | copy-start | bytes 3145732
  101.2 24.2 %copy-start.1 = (bf16[1,2048,256]{2,1,0:T(8,128)(2,1)S(1)}, bf16[1,2048,256]{2,1,0:T(8,128)(2,1)}, u32[]{:S(2)}) copy-start(bf16[1,2048,256]{2,1,0:T(8,128)(2,1)} %param.22) | copy-start | bytes 3145732
  101.3 14.0 %collective-permute-start.7 = (bf16[1280,128]{1,0:T(8,128)(2,1)S(1)}, bf16[1280,128]{1,0:T(8,128)(2,1)S(1)}, u32[]{:S(2)}, u32[]{:S(2)}) collective-permute-start(bf16[1280,128]{1,0:T(8,128)(2,1)S(1)} %get-tuple-element.49.every_ref), channel_id=1, source_target_pairs={{0,14},{2,0},{4,2},{6,4},{8,6},{10,8},{12,10},{14,12},{1,15},{3,1}... | collective-permute-start | bytes 983048 | tf_op jit(solution)/shard_map/ppermute | solution.py:286
  105.1 12.5 %collective-permute-start.6 = (bf16[1280,128]{1,0:T(8,128)(2,1)S(1)}, bf16[1280,128]{1,0:T(8,128)(2,1)S(1)}, u32[]{:S(2)}, u32[]{:S(2)}) collective-permute-start(bf16[1280,128]{1,0:T(8,128)(2,1)S(1)} %get-tuple-element.49.every_ref), channel_id=1, source_target_pairs={{0,2},{2,4},{4,6},{6,8},{8,10},{10,12},{12,14},{14,0},{1,3},{3,5},... | collective-permute-start | bytes 983048 | tf_op jit(solution)/shard_map/ppermute | solution.py:286
  107.2 16.1 %collective-permute-start.3 = (bf16[640,128]{1,0:T(8,128)(2,1)S(1)}, bf16[640,128]{1,0:T(8,128)(2,1)S(1)}, u32[]{:S(2)}, u32[]{:S(2)}) collective-permute-start(bf16[640,128]{1,0:T(8,128)(2,1)S(1)} %get-tuple-element.47), channel_id=1, source_target_pairs={{0,4},{2,6},{4,8},{6,10},{8,12},{10,14},{12,0},{14,2},{1,5},{3,7},... | collective-permute-start | bytes 491528 | tf_op jit(solution)/shard_map/ppermute | solution.py:286
  112.7 10.6 %collective-permute-start.4 = (bf16[640,128]{1,0:T(8,128)(2,1)S(1)}, bf16[640,128]{1,0:T(8,128)(2,1)S(1)}, u32[]{:S(2)}, u32[]{:S(2)}) collective-permute-start(bf16[640,128]{1,0:T(8,128)(2,1)S(1)} %get-tuple-element.48), channel_id=1, source_target_pairs={{0,12},{2,14},{4,0},{6,2},{8,4},{10,6},{12,8},{14,10},{1,13},{3,15... | collective-permute-start | bytes 491528 | tf_op jit(solution)/shard_map/ppermute | solution.py:286
  117.6 7.8 %collective-permute-start.9 = (bf16[2560,128]{1,0:T(8,128)(2,1)S(1)}, bf16[2560,128]{1,0:T(8,128)(2,1)S(1)}, u32[]{:S(2)}, u32[]{:S(2)}) collective-permute-start(bf16[2560,128]{1,0:T(8,128)(2,1)S(1)} %pad_maximum_fusion), channel_id=1, source_target_pairs={{0,1},{1,0},{2,3},{3,2},{4,5},{5,4},{6,7},{7,6},{8,9},{9,8},{10,11... | collective-permute-start | bytes 1966088 | tf_op jit(solution)/shard_map/ppermute | solution.py:364
  119.6 5.8 %collective-permute-start.8 = (bf16[1280,128]{1,0:T(8,128)(2,1)S(1)}, bf16[1280,128]{1,0:T(8,128)(2,1)S(1)}, u32[]{:S(2)}, u32[]{:S(2)}) collective-permute-start(bf16[1280,128]{1,0:T(8,128)(2,1)S(1)} %get-tuple-element.49.every_ref), channel_id=1, source_target_pairs={{0,1},{1,0},{2,3},{3,2},{4,5},{5,4},{6,7},{7,6},{8,9},{9,8},{10,11... | collective-permute-start | bytes 983048 | tf_op jit(solution)/shard_map/ppermute | solution.py:364
  123.4 3.8 %collective-permute-start.5 = (bf16[1280,128]{1,0:T(8,128)(2,1)S(1)}, bf16[1280,128]{1,0:T(8,128)(2,1)S(1)}, u32[]{:S(2)}, u32[]{:S(2)}) collective-permute-start(bf16[1280,128]{1,0:T(8,128)(2,1)S(1)} %pad_maximum_fusion.1), channel_id=1, source_target_pairs={{0,1},{1,0},{2,3},{3,2},{4,5},{5,4},{6,7},{7,6},{8,9},{9,8},{10,11... | collective-permute-start | bytes 983048 | tf_op jit(solution)/shard_map/ppermute | solution.py:364
  125.4 1.8 copy-start.3
  129.1 4.6 %collective-permute-start.10 = (bf16[3840,128]{1,0:T(8,128)(2,1)S(1)}, bf16[3840,128]{1,0:T(8,128)(2,1)S(1)}, u32[]{:S(2)}, u32[]{:S(2)}) collective-permute-start(bf16[3840,128]{1,0:T(8,128)(2,1)S(1)} %get-tuple-element.54), channel_id=1, source_target_pairs={{0,1},{1,0},{2,3},{3,2},{4,5},{5,4},{6,7},{7,6},{8,9},{9,8},{10,11... | collective-permute-start | bytes 2949128 | tf_op jit(solution)/shard_map/ppermute | solution.py:378
  131.5 9.4 %collective-permute-start.13 = (bf16[1280,128]{1,0:T(8,128)(2,1)S(1)}, bf16[1280,128]{1,0:T(8,128)(2,1)S(1)}, u32[]{:S(2)}, u32[]{:S(2)}) collective-permute-start(bf16[1280,128]{1,0:T(8,128)(2,1)S(1)} %get-tuple-element.56), channel_id=1, source_target_pairs={{0,1},{1,0},{2,3},{3,2},{4,5},{5,4},{6,7},{7,6},{8,9},{9,8},{10,11... | collective-permute-start | bytes 983048 | tf_op jit(solution)/shard_map/ppermute | solution.py:377
  133.9 24.8 %collective-permute-start.12 = (bf16[1280,128]{1,0:T(8,128)(2,1)S(1)}, bf16[1280,128]{1,0:T(8,128)(2,1)S(1)}, u32[]{:S(2)}, u32[]{:S(2)}) collective-permute-start(bf16[1280,128]{1,0:T(8,128)(2,1)S(1)} %get-tuple-element.59), channel_id=1, source_target_pairs={{0,14},{2,0},{4,2},{6,4},{8,6},{10,8},{12,10},{14,12},{1,15},{3,1}... | collective-permute-start | bytes 983048 | tf_op jit(solution)/shard_map/ppermute | solution.py:286
  139.0 19.6 %collective-permute-start.11 = (bf16[1280,128]{1,0:T(8,128)(2,1)S(1)}, bf16[1280,128]{1,0:T(8,128)(2,1)S(1)}, u32[]{:S(2)}, u32[]{:S(2)}) collective-permute-start(bf16[1280,128]{1,0:T(8,128)(2,1)S(1)} %get-tuple-element.60), channel_id=1, source_target_pairs={{0,2},{2,4},{4,6},{6,8},{8,10},{10,12},{12,14},{14,0},{1,3},{3,5},... | collective-permute-start | bytes 983048 | tf_op jit(solution)/shard_map/ppermute | solution.py:286
  141.0 12.5 %collective-permute-start.15 = (bf16[640,128]{1,0:T(8,128)(2,1)S(1)}, bf16[640,128]{1,0:T(8,128)(2,1)S(1)}, u32[]{:S(2)}, u32[]{:S(2)}) collective-permute-start(bf16[640,128]{1,0:T(8,128)(2,1)S(1)} %get-tuple-element.61), channel_id=1, source_target_pairs={{0,12},{2,14},{4,0},{6,2},{8,4},{10,6},{12,8},{14,10},{1,13},{3,15... | collective-permute-start | bytes 491528 | tf_op jit(solution)/shard_map/ppermute | solution.py:286
  145.6 41.1 %copy-start.7 = (f32[256,2]{0,1:T(2,128)S(1)}, f32[256,2]{0,1:T(2,128)}, u32[]{:S(2)}) copy-start(f32[256,2]{0,1:T(2,128)} %param.20) | copy-start | bytes 6148
  145.6 13.0 %collective-permute-start.14 = (bf16[640,128]{1,0:T(8,128)(2,1)S(1)}, bf16[640,128]{1,0:T(8,128)(2,1)S(1)}, u32[]{:S(2)}, u32[]{:S(2)}) collective-permute-start(bf16[640,128]{1,0:T(8,128)(2,1)S(1)} %get-tuple-element.62), channel_id=1, source_target_pairs={{0,4},{2,6},{4,8},{6,10},{8,12},{10,14},{12,0},{14,2},{1,5},{3,7},... | collective-permute-start | bytes 491528 | tf_op jit(solution)/shard_map/ppermute | solution.py:286

commit v10 on v9

--- a/solution.py
+++ b/solution.py
@@ -139,11 +139,14 @@
     out_ref[...] = (acc / total).astype(bf)
 
 
-def prepare(kvq_ref, w_ref, kv_ref, qs_ref, out_ref):
+def prepare(kvq_ref, kv_ref, qs_ref):
     for z in range(NZ):
         kv_ref[z] = kvq_ref[0 : 2 * HD, :]
     for x in range(NX):
         qs_ref[x] = kvq_ref[2 * HD :, :]
+
+
+def spread_weight(w_ref, out_ref):
     for y in range(NY):
         for c in range(NC):
             for q in range(2):
@@ -151,7 +154,9 @@
                 out_ref[y * NC + c, q * HD : (q + 1) * HD, :] = w_ref[:, block * COLS : (block + 1) * COLS]
 
 
-def route(routes_ref, pick_ref, back_ref):
+def route(at_ref, routes_ref, resid_ref, pick_ref, back_ref, cols_ref):
+    for q in range(2):
+        cols_ref[:, q * COLS : (q + 1) * COLS] = resid_ref[:, pl.ds(pl.multiple_of(at_ref[q], COLS), COLS)]
     e0, e1 = routes_ref[0:1, :], routes_ref[1:2, :]
     io = lax.broadcasted_iota(jnp.int32, (NSP, TOK), 0)
     h0, h1 = io == e0, io == e1
@@ -181,9 +186,8 @@
     weights = [jnp.concatenate([w_ref[t, q * HD : (q + 1) * HD, :] for t in range(NTP)], axis=0) for q in range(2)]
     w = jnp.concatenate(weights, axis=1)
     mixed = lax.dot_general(att_ref[...], w, (((0,), (0,)), ((), ())), preferred_element_type=f32)
-    resid = jnp.concatenate([resid_ref[:, pl.ds(c0, COLS)], resid_ref[:, pl.ds(c1, COLS)]], axis=1)
     gain = jnp.concatenate([gain_ref[:, pl.ds(c0, COLS)], gain_ref[:, pl.ds(c1, COLS)]], axis=1)
-    stream = resid.astype(f32) + mixed
+    stream = resid_ref[...].astype(f32) + mixed
     stream_ref[...] = jnp.where(at_ref[2] == 0, stream[:, 0:COLS], stream[:, COLS:])
     scaled = (stream * gain).astype(bf)
     sent = jnp.dot(pick_ref[...], scaled, preferred_element_type=f32).reshape(NSP, SEND, 2 * COLS)
@@ -310,15 +314,17 @@
     low = (lax.rem(y, half) * NC + c) * COLS
     at_cols = jnp.stack([low, low + half * NC * COLS, y // half]).astype(jnp.int32)
     at = jnp.stack([z, x]).astype(jnp.int32)
-    kv_send, q_send, w_send = call(
+    kv_send, q_send = call(
         prepare,
-        (sds((NZ, 2 * HD, TOK), bf), sds((NX, HD, TOK), bf), sds((NTP, 2 * HD, COLS), bf)),
-        (jnp.concatenate([keys.T, values.T, queries.T], axis=0), out_weight),
-    )
-    q_send, w_send, at, at_cols = lax.optimization_barrier((q_send, w_send, at, at_cols))
+        (sds((NZ, 2 * HD, TOK), bf), sds((NX, HD, TOK), bf)),
+        (jnp.concatenate([keys.T, values.T, queries.T], axis=0),),
+    )
+    q_send, at, at_cols = lax.optimization_barrier((q_send, at, at_cols))
     q = exchange(q_send, "x")
     kv_send, q = lax.optimization_barrier((kv_send, q))
     kv = exchange(kv_send, "z")
+    w_raw, kv = lax.optimization_barrier((out_weight, kv))
+    w_send = call(spread_weight, sds((NTP, 2 * HD, COLS), bf), (w_raw,))
     w_cols = exchange(w_send, TP)
     sent = call(
         attend,
@@ -332,20 +338,23 @@
             pltpu.VMEM((HD + 16, ROW), f32),
             pltpu.VMEM((HD + 16, ROW), bf),
         ),
-        limit=24,
+        limit=14,
     )
     parts = [sent[0]]
     for n in range(1, NX):
         parts.append(lax.ppermute(sent[n], "x", [(i, (i + n) % NX) for i in range(NX)]))
-    pick, back_pick = call(
-        route, (sds((NSP * SEND, TOK), bf), sds((2 * TOK, 2 * PADROWS), bf)), (routes.T,)
+    pick, back_pick, resid_cols = call(
+        route,
+        (sds((NSP * SEND, TOK), bf), sds((2 * TOK, 2 * PADROWS), bf), sds((TOK, 2 * COLS), bf)),
+        (at_cols, routes.T, resid),
+        smem=1,
     )
     attended = call(merge, sds((HD, TOK), bf), tuple(parts))
     attended = lax.all_gather(attended, TP, axis=0, tiled=True)
     stream, outgoing = call(
         project,
         (sds((TOK, COLS), f32), sds((NSP, SEND, COLS), bf)),
-        (at_cols, attended, w_cols, resid, norm_gain.reshape(1, D), pick),
+        (at_cols, attended, w_cols, resid_cols, norm_gain.reshape(1, D), pick),
         smem=1,
     )
     arrived = exchange(outgoing, SP)

time: 189 us -> 188 us (level)
    pallas_call x10 -> x11, Pallas kernels: 10.6 us -> 11.2 us  [call(): pl.pallas_call(body, out_shape=out_shape, in_specs=specs, out_specs=tuple...]
  transfers between devices with their start and end apart: 17 -> 17, of which waited for: 6 -> 5; matrix products, arithmetic and copies ran while one was open for 0% -> 0% of each run, Pallas kernels for 3% -> 3%
where the time goes in v10:
time: 188 us; the launch traced here: 187 us
  blocking collectives  103 us (55%)
  starting transfers between devices  55 us (29%)
  waiting for transfers between devices  14.8 us (8%)
  Pallas kernels  11.2 us (6%)
    all_to_all x4, blocking collectives, exchange(): return lax.all_to_all(v, axis, 0, 0, tiled=True)  85.6 us
    ppermute x8, starting transfers between devices, shift(): return lax.ppermute(v, Y, [(i, (i + by) % NY) for i in range(NY)])  27.7 us
    all_gather x1, blocking collectives, layer(): attended = lax.all_gather(attended, TP, axis=0, tiled=True)  17 us
    ppermute x8, waiting for transfers between devices, shift(): return lax.ppermute(v, Y, [(i, (i + by) % NY) for i in range(NY)])  14.5 us
    pallas_call x11, Pallas kernels, call(): pl.pallas_call(body, out_shape=out_shape, in_specs=specs, out_specs=tuple...  11.2 us
    ppermute x3, starting transfers between devices, layer(): lax.ppermute(sent[n], 'x', [(i, (i + n) % NX) for i in range(NX)])  9.18 us
    all_to_all x1, starting transfers between devices, exchange(): return lax.all_to_all(v, axis, 0, 0, tiled=True)  7.56 us
    ppermute x3, starting transfers between devices, layer(): others.append(lax.ppermute(v, 'c', swap))  6.25 us
  transfers between devices with their start and end apart: 17, of which 5 were waited for; matrix products, arithmetic and copies ran while one was open for 0% of the time, Pallas kernels for 3%

profile of v10, /device:TPU:8, one launch (start us, length us, event | category | flops | bytes accessed | tf_op | source)
XLA Modules:
  0.0 186.7 jit_solution(14417617352241289120)
XLA Ops:
  1.1 10.1 %all_to_all.25.q_ref = bf16[4,64,256]{2,1,0:T(8,128)(2,1)S(1)} all-to-all(bf16[4,64,256]{2,1,0:T(8,128)(2,1)S(1)} %get-tuple-element.37), channel_id=1, replica_groups=mesh['z'=8,'x'=4,'yh'=2,'yl'=4,'c'=2] {'x'}, dimensions={0} | all-to-all | bytes 262144 | tf_op jit(solution)/shard_map/all_to_all | solution.py:294
  11.1 26.3 %all_to_all.26.kv_ref = bf16[8,128,256]{2,1,0:T(8,128)(2,1)S(1)} all-to-all(bf16[8,128,256]{2,1,0:T(8,128)(2,1)S(1)} %get-tuple-element.39), channel_id=1, replica_groups=mesh['z'=8,'x'=4,'yh'=2,'yl'=4,'c'=2] {'z'}, dimensions={0} | all-to-all | bytes 1048576 | tf_op jit(solution)/shard_map/all_to_all | solution.py:294
  38.3 7.6 %all-to-all-start.2 = ((bf16[16,128,128]{2,1,0:T(8,128)(2,1)}), bf16[16,128,128]{2,1,0:T(8,128)(2,1)S(1)}, u32[]{:S(2)}, u32[]{:S(2)}) async-start(bf16[16,128,128]{2,1,0:T(8,128)(2,1)} %shard_map.121), calls=%async_computation.2 | async-start | bytes 1048576 | tf_op jit(solution)/shard_map/all_to_all | solution.py:294
  45.9 1.3 shard_map.119
  47.2 2.5 %collective-permute-start = (bf16[80,256]{1,0:T(8,128)(2,1)S(1)}, bf16[80,256]{1,0:T(8,128)(2,1)S(1)}, u32[]{:S(2)}, u32[]{:S(2)}) collective-permute-start(bf16[80,256]{1,0:T(8,128)(2,1)S(1)} %get-tuple-element.42), channel_id=1, source_target_pairs={{0,16},{16,32},{32,48},{48,0},{1,17},{17,33},{33,49},{49,1},{2,18}... | collective-permute-start | bytes 122888 | tf_op jit(solution)/shard_map/ppermute | solution.py:345
  49.7 4.0 %collective-permute-start.1 = (bf16[80,256]{1,0:T(8,128)(2,1)S(1)}, bf16[80,256]{1,0:T(8,128)(2,1)S(1)}, u32[]{:S(2)}, u32[]{:S(2)}) collective-permute-start(bf16[80,256]{1,0:T(8,128)(2,1)S(1)} %get-tuple-element.43), channel_id=1, source_target_pairs={{0,32},{16,48},{32,0},{48,16},{1,33},{17,49},{33,1},{49,17},{2,34}... | collective-permute-start | bytes 122888 | tf_op jit(solution)/shard_map/ppermute | solution.py:345
  53.7 2.7 %collective-permute-start.2 = (bf16[80,256]{1,0:T(8,128)(2,1)S(1)}, bf16[80,256]{1,0:T(8,128)(2,1)S(1)}, u32[]{:S(2)}, u32[]{:S(2)}) collective-permute-start(bf16[80,256]{1,0:T(8,128)(2,1)S(1)} %get-tuple-element.44), channel_id=1, source_target_pairs={{0,48},{16,0},{32,16},{48,32},{1,49},{17,1},{33,17},{49,33},{2,50}... | collective-permute-start | bytes 122888 | tf_op jit(solution)/shard_map/ppermute | solution.py:345
  56.4 1.2 copy-done.2
  57.7 2.2 %shard_map.122 = (bf16[1280,256]{1,0:T(8,128)(2,1)S(1)}, bf16[512,1536]{1,0:T(8,128)(2,1)S(1)}, bf16[256,256]{1,0:T(8,128)(2,1)S(1)}) custom-call(s32[3]{0:T(128)S(1)} %pad_add_fusion.2.at_ref, s32[2,256]{1,0:T(2,128)S(1)} %bitcast.26, bf16[256,2048]{1,0:T(8,128)(2,1)S(1)} %copy-done.2), custom_call_target="tpu_custom_call" | custom-call | tf_op jit(solution)/shard_map/pallas_call | solution.py:38
  60.0 17.0 %all_gather.3.att_ref = bf16[1024,256]{1,0:T(8,128)(2,1)S(1)} all-gather(bf16[64,256]{1,0:T(8,128)(2,1)S(1)} %shard_map.120), channel_id=1, replica_groups=mesh['z'=8,'x'=4,'yh'=2,'yl'=4,'c'=2] {'yh','yl','c'}, dimensions={0}, use_global_device_ids=true | all-gather | bytes 557056 | tf_op jit(solution)/shard_map/all_gather | solution.py:353
  77.0 1.4 shard_map.123
  78.4 21.5 %all_to_all.27.in_ref = bf16[32,40,128]{2,1,0:T(8,128)(2,1)S(1)} all-to-all(bf16[32,40,128]{2,1,0:T(8,128)(2,1)S(1)} %get-tuple-element.48), channel_id=1, replica_groups=mesh['z'=8,'x'=4,'yh'=2,'yl'=4,'c'=2] {'z','x'}, dimensions={0} | all-to-all | bytes 655360 | tf_op jit(solution)/shard_map/all_to_all | solution.py:294
  100.1 3.8 %collective-permute-start.7 = (bf16[1280,128]{1,0:T(8,128)(2,1)S(1)}, bf16[1280,128]{1,0:T(8,128)(2,1)S(1)}, u32[]{:S(2)}, u32[]{:S(2)}) collective-permute-start(bf16[1280,128]{1,0:T(8,128)(2,1)S(1)} %get-tuple-element.51.every_ref), channel_id=1, source_target_pairs={{0,14},{2,0},{4,2},{6,4},{8,6},{10,8},{12,10},{14,12},{1,15},{3,1}... | collective-permute-start | bytes 983048 | tf_op jit(solution)/shard_map/ppermute | solution.py:290
  103.9 2.2 %collective-permute-start.6 = (bf16[1280,128]{1,0:T(8,128)(2,1)S(1)}, bf16[1280,128]{1,0:T(8,128)(2,1)S(1)}, u32[]{:S(2)}, u32[]{:S(2)}) collective-permute-start(bf16[1280,128]{1,0:T(8,128)(2,1)S(1)} %get-tuple-element.51.every_ref), channel_id=1, source_target_pairs={{0,2},{2,4},{4,6},{6,8},{8,10},{10,12},{12,14},{14,0},{1,3},{3,5},... | collective-permute-start | bytes 983048 | tf_op jit(solution)/shard_map/ppermute | solution.py:290
  106.1 5.5 %collective-permute-start.3 = (bf16[640,128]{1,0:T(8,128)(2,1)S(1)}, bf16[640,128]{1,0:T(8,128)(2,1)S(1)}, u32[]{:S(2)}, u32[]{:S(2)}) collective-permute-start(bf16[640,128]{1,0:T(8,128)(2,1)S(1)} %get-tuple-element.49), channel_id=1, source_target_pairs={{0,4},{2,6},{4,8},{6,10},{8,12},{10,14},{12,0},{14,2},{1,5},{3,7},... | collective-permute-start | bytes 491528 | tf_op jit(solution)/shard_map/ppermute | solution.py:290
  111.6 2.5 %collective-permute-start.4 = (bf16[640,128]{1,0:T(8,128)(2,1)S(1)}, bf16[640,128]{1,0:T(8,128)(2,1)S(1)}, u32[]{:S(2)}, u32[]{:S(2)}) collective-permute-start(bf16[640,128]{1,0:T(8,128)(2,1)S(1)} %get-tuple-element.50), channel_id=1, source_target_pairs={{0,12},{2,14},{4,0},{6,2},{8,4},{10,6},{12,8},{14,10},{1,13},{3,15... | collective-permute-start | bytes 491528 | tf_op jit(solution)/shard_map/ppermute | solution.py:290
  114.0 2.3 %collective-permute-done.6.n0_ref = bf16[1280,128]{1,0:T(8,128)(2,1)S(1)} collective-permute-done((bf16[1280,128]{1,0:T(8,128)(2,1)S(1)}, bf16[1280,128]{1,0:T(8,128)(2,1)S(1)}, u32[]{:S(2)}, u32[]{:S(2)}) %collective-permute-start.6) | collective-permute-done | bytes 327712 | tf_op jit(solution)/shard_map/ppermute | solution.py:290
  116.4 1.9 %collective-permute-start.9 = (bf16[2560,128]{1,0:T(8,128)(2,1)S(1)}, bf16[2560,128]{1,0:T(8,128)(2,1)S(1)}, u32[]{:S(2)}, u32[]{:S(2)}) collective-permute-start(bf16[2560,128]{1,0:T(8,128)(2,1)S(1)} %pad_maximum_fusion), channel_id=1, source_target_pairs={{0,1},{1,0},{2,3},{3,2},{4,5},{5,4},{6,7},{7,6},{8,9},{9,8},{10,11... | collective-permute-start | bytes 1966088 | tf_op jit(solution)/shard_map/ppermute | solution.py:373
  118.4 2.4 %collective-permute-start.8 = (bf16[1280,128]{1,0:T(8,128)(2,1)S(1)}, bf16[1280,128]{1,0:T(8,128)(2,1)S(1)}, u32[]{:S(2)}, u32[]{:S(2)}) collective-permute-start(bf16[1280,128]{1,0:T(8,128)(2,1)S(1)} %get-tuple-element.51.every_ref), channel_id=1, source_target_pairs={{0,1},{1,0},{2,3},{3,2},{4,5},{5,4},{6,7},{7,6},{8,9},{9,8},{10,11... | collective-permute-start | bytes 983048 | tf_op jit(solution)/shard_map/ppermute | solution.py:373
  120.8 1.4 collective-permute-done.3.f0_ref
  122.2 1.9 %collective-permute-start.5 = (bf16[1280,128]{1,0:T(8,128)(2,1)S(1)}, bf16[1280,128]{1,0:T(8,128)(2,1)S(1)}, u32[]{:S(2)}, u32[]{:S(2)}) collective-permute-start(bf16[1280,128]{1,0:T(8,128)(2,1)S(1)} %pad_maximum_fusion.1), channel_id=1, source_target_pairs={{0,1},{1,0},{2,3},{3,2},{4,5},{5,4},{6,7},{7,6},{8,9},{9,8},{10,11... | collective-permute-start | bytes 983048 | tf_op jit(solution)/shard_map/ppermute | solution.py:373
  124.2 1.7 shard_map.125
  126.0 1.9 %shard_map.126 = (bf16[1280,128]{1,0:T(8,128)(2,1)S(1)}, bf16[3840,128]{1,0:T(8,128)(2,1)S(1)}, bf16[1280,128]{1,0:T(8,128)(2,1)S(1)}, bf16[3840,128]{1,0:T(8,128)(2,1)S(1)}) custom-call(s32[2]{0:T(128)S(1)} %pad_add_fusion.at_ref, bf16[640,128]{1,0:T(8,128)(2,1)S(1)} %collective-permute-done.3.f0_ref, bf16[640,128]{1,0:T(8,128)(2,1)S(1)} %collective-permute-done.4.f1_ref, ...), custom_call_target="tpu_custom_call" | custom-call | tf_op jit(solution)/shard_map/pallas_call | solution.py:38
  127.9 2.4 %collective-permute-start.10 = (bf16[3840,128]{1,0:T(8,128)(2,1)S(1)}, bf16[3840,128]{1,0:T(8,128)(2,1)S(1)}, u32[]{:S(2)}, u32[]{:S(2)}) collective-permute-start(bf16[3840,128]{1,0:T(8,128)(2,1)S(1)} %get-tuple-element.56), channel_id=1, source_target_pairs={{0,1},{1,0},{2,3},{3,2},{4,5},{5,4},{6,7},{7,6},{8,9},{9,8},{10,11... | collective-permute-start | bytes 2949128 | tf_op jit(solution)/shard_map/ppermute | solution.py:387
  130.4 1.9 %collective-permute-start.13 = (bf16[1280,128]{1,0:T(8,128)(2,1)S(1)}, bf16[1280,128]{1,0:T(8,128)(2,1)S(1)}, u32[]{:S(2)}, u32[]{:S(2)}) collective-permute-start(bf16[1280,128]{1,0:T(8,128)(2,1)S(1)} %get-tuple-element.58), channel_id=1, source_target_pairs={{0,1},{1,0},{2,3},{3,2},{4,5},{5,4},{6,7},{7,6},{8,9},{9,8},{10,11... | collective-permute-start | bytes 983048 | tf_op jit(solution)/shard_map/ppermute | solution.py:386
  132.7 5.1 %collective-permute-start.12 = (bf16[1280,128]{1,0:T(8,128)(2,1)S(1)}, bf16[1280,128]{1,0:T(8,128)(2,1)S(1)}, u32[]{:S(2)}, u32[]{:S(2)}) collective-permute-start(bf16[1280,128]{1,0:T(8,128)(2,1)S(1)} %get-tuple-element.61), channel_id=1, source_target_pairs={{0,14},{2,0},{4,2},{6,4},{8,6},{10,8},{12,10},{14,12},{1,15},{3,1}... | collective-permute-start | bytes 983048 | tf_op jit(solution)/shard_map/ppermute | solution.py:290
  137.8 1.9 %collective-permute-start.11 = (bf16[1280,128]{1,0:T(8,128)(2,1)S(1)}, bf16[1280,128]{1,0:T(8,128)(2,1)S(1)}, u32[]{:S(2)}, u32[]{:S(2)}) collective-permute-start(bf16[1280,128]{1,0:T(8,128)(2,1)S(1)} %get-tuple-element.62), channel_id=1, source_target_pairs={{0,2},{2,4},{4,6},{6,8},{8,10},{10,12},{12,14},{14,0},{1,3},{3,5},... | collective-permute-start | bytes 983048 | tf_op jit(solution)/shard_map/ppermute | solution.py:290
  139.9 4.6 %collective-permute-start.15 = (bf16[640,128]{1,0:T(8,128)(2,1)S(1)}, bf16[640,128]{1,0:T(8,128)(2,1)S(1)}, u32[]{:S(2)}, u32[]{:S(2)}) collective-permute-start(bf16[640,128]{1,0:T(8,128)(2,1)S(1)} %get-tuple-element.63), channel_id=1, source_target_pairs={{0,12},{2,14},{4,0},{6,2},{8,4},{10,6},{12,8},{14,10},{1,13},{3,15... | collective-permute-start | bytes 491528 | tf_op jit(solution)/shard_map/ppermute | solution.py:290
  144.5 2.2 %collective-permute-start.14 = (bf16[640,128]{1,0:T(8,128)(2,1)S(1)}, bf16[640,128]{1,0:T(8,128)(2,1)S(1)}, u32[]{:S(2)}, u32[]{:S(2)}) collective-permute-start(bf16[640,128]{1,0:T(8,128)(2,1)S(1)} %get-tuple-element.64), channel_id=1, source_target_pairs={{0,4},{2,6},{4,8},{6,10},{8,12},{10,14},{12,0},{14,2},{1,5},{3,7},... | collective-permute-start | bytes 491528 | tf_op jit(solution)/shard_map/ppermute | solution.py:290
  146.6 5.7 %collective-permute-done.15.f1_ref = bf16[640,128]{1,0:T(8,128)(2,1)S(1)} collective-permute-done((bf16[640,128]{1,0:T(8,128)(2,1)S(1)}, bf16[640,128]{1,0:T(8,128)(2,1)S(1)}, u32[]{:S(2)}, u32[]{:S(2)}) %collective-permute-start.15) | collective-permute-done | bytes 163872 | tf_op jit(solution)/shard_map/ppermute | solution.py:290
  152.3 5.1 %collective-permute-done.14.f0_ref = bf16[640,128]{1,0:T(8,128)(2,1)S(1)} collective-permute-done((bf16[640,128]{1,0:T(8,128)(2,1)S(1)}, bf16[640,128]{1,0:T(8,128)(2,1)S(1)}, u32[]{:S(2)}, u32[]{:S(2)}) %collective-permute-start.14) | collective-permute-done | bytes 163872 | tf_op jit(solution)/shard_map/ppermute | solution.py:290
  157.8 27.7 %all_to_all.28 = bf16[64,24,128]{2,1,0:T(8,128)(2,1)S(1)} all-to-all(bf16[64,24,128]{2,1,0:T(8,128)(2,1)S(1)} %shard_map.127), channel_id=1, replica_groups=mesh['z'=8,'x'=4,'yh'=2,'yl'=4,'c'=2] {'z','x','yh'}, dimensions={0} | all-to-all | bytes 786432 | tf_op jit(solution)/shard_map/all_to_all | solution.py:294
  (44 shorter events, 4.3 us)
Async XLA Ops:
  0.0 37.4 %copy-start.4 = (bf16[64,2048]{1,0:T(8,128)(2,1)S(1)}, bf16[64,2048]{1,0:T(8,128)(2,1)}, u32[]{:S(2)}) copy-start(bf16[64,2048]{1,0:T(8,128)(2,1)} %w_ref) | copy-start | bytes 786436
  11.1 34.7 %copy-start.6 = (f32[1,8192]{1,0:T(1,128)S(1)}, f32[1,8192]{1,0:T(1,128)}, u32[]{:S(2)}) copy-start(f32[1,8192]{1,0:T(1,128)} %gate_ref.1) | copy-start | bytes 98308
  37.4 19.0 %copy-start.7 = (s32[256,2]{0,1:T(2,128)S(1)}, s32[256,2]{0,1:T(2,128)}, u32[]{:S(2)}) copy-start(s32[256,2]{0,1:T(2,128)} %param.19) | copy-start | bytes 6148
  38.3 38.7 %all-to-all-start.2 = ((bf16[16,128,128]{2,1,0:T(8,128)(2,1)}), bf16[16,128,128]{2,1,0:T(8,128)(2,1)S(1)}, u32[]{:S(2)}, u32[]{:S(2)}) async-start(bf16[16,128,128]{2,1,0:T(8,128)(2,1)} %shard_map.121), calls=%async_computation.2 | async-start | bytes 1048576 | tf_op jit(solution)/shard_map/all_to_all | solution.py:294
  45.9 31.2 %copy-start.5 = (f32[2048]{0:T(1024)S(1)}, f32[2048]{0:T(1024)}, u32[]{:S(2)}) copy-start(f32[2048]{0:T(1024)} %param.18) | copy-start | bytes 24580
  47.2 12.7 %collective-permute-start = (bf16[80,256]{1,0:T(8,128)(2,1)S(1)}, bf16[80,256]{1,0:T(8,128)(2,1)S(1)}, u32[]{:S(2)}, u32[]{:S(2)}) collective-permute-start(bf16[80,256]{1,0:T(8,128)(2,1)S(1)} %get-tuple-element.42), channel_id=1, source_target_pairs={{0,16},{16,32},{32,48},{48,0},{1,17},{17,33},{33,49},{49,1},{2,18}... | collective-permute-start | bytes 122888 | tf_op jit(solution)/shard_map/ppermute | solution.py:345
  49.7 10.2 %collective-permute-start.1 = (bf16[80,256]{1,0:T(8,128)(2,1)S(1)}, bf16[80,256]{1,0:T(8,128)(2,1)S(1)}, u32[]{:S(2)}, u32[]{:S(2)}) collective-permute-start(bf16[80,256]{1,0:T(8,128)(2,1)S(1)} %get-tuple-element.43), channel_id=1, source_target_pairs={{0,32},{16,48},{32,0},{48,16},{1,33},{17,49},{33,1},{49,17},{2,34}... | collective-permute-start | bytes 122888 | tf_op jit(solution)/shard_map/ppermute | solution.py:345
  53.7 6.2 %collective-permute-start.2 = (bf16[80,256]{1,0:T(8,128)(2,1)S(1)}, bf16[80,256]{1,0:T(8,128)(2,1)S(1)}, u32[]{:S(2)}, u32[]{:S(2)}) collective-permute-start(bf16[80,256]{1,0:T(8,128)(2,1)S(1)} %get-tuple-element.44), channel_id=1, source_target_pairs={{0,48},{16,0},{32,16},{48,32},{1,49},{17,1},{33,17},{49,33},{2,50}... | collective-permute-start | bytes 122888 | tf_op jit(solution)/shard_map/ppermute | solution.py:345
  56.4 1.2 copy-start.2
  100.0 24.2 %copy-start = (bf16[1,2048,256]{2,1,0:T(8,128)(2,1)S(1)}, bf16[1,2048,256]{2,1,0:T(8,128)(2,1)}, u32[]{:S(2)}) copy-start(bf16[1,2048,256]{2,1,0:T(8,128)(2,1)} %param.21) | copy-start | bytes 3145732
  100.0 24.2 %copy-start.1 = (bf16[1,2048,256]{2,1,0:T(8,128)(2,1)S(1)}, bf16[1,2048,256]{2,1,0:T(8,128)(2,1)}, u32[]{:S(2)}) copy-start(bf16[1,2048,256]{2,1,0:T(8,128)(2,1)} %param.22) | copy-start | bytes 3145732
  100.1 14.0 %collective-permute-start.7 = (bf16[1280,128]{1,0:T(8,128)(2,1)S(1)}, bf16[1280,128]{1,0:T(8,128)(2,1)S(1)}, u32[]{:S(2)}, u32[]{:S(2)}) collective-permute-start(bf16[1280,128]{1,0:T(8,128)(2,1)S(1)} %get-tuple-element.51.every_ref), channel_id=1, source_target_pairs={{0,14},{2,0},{4,2},{6,4},{8,6},{10,8},{12,10},{14,12},{1,15},{3,1}... | collective-permute-start | bytes 983048 | tf_op jit(solution)/shard_map/ppermute | solution.py:290
  103.9 12.5 %collective-permute-start.6 = (bf16[1280,128]{1,0:T(8,128)(2,1)S(1)}, bf16[1280,128]{1,0:T(8,128)(2,1)S(1)}, u32[]{:S(2)}, u32[]{:S(2)}) collective-permute-start(bf16[1280,128]{1,0:T(8,128)(2,1)S(1)} %get-tuple-element.51.every_ref), channel_id=1, source_target_pairs={{0,2},{2,4},{4,6},{6,8},{8,10},{10,12},{12,14},{14,0},{1,3},{3,5},... | collective-permute-start | bytes 983048 | tf_op jit(solution)/shard_map/ppermute | solution.py:290
  106.1 16.1 %collective-permute-start.3 = (bf16[640,128]{1,0:T(8,128)(2,1)S(1)}, bf16[640,128]{1,0:T(8,128)(2,1)S(1)}, u32[]{:S(2)}, u32[]{:S(2)}) collective-permute-start(bf16[640,128]{1,0:T(8,128)(2,1)S(1)} %get-tuple-element.49), channel_id=1, source_target_pairs={{0,4},{2,6},{4,8},{6,10},{8,12},{10,14},{12,0},{14,2},{1,5},{3,7},... | collective-permute-start | bytes 491528 | tf_op jit(solution)/shard_map/ppermute | solution.py:290
  111.6 10.6 %collective-permute-start.4 = (bf16[640,128]{1,0:T(8,128)(2,1)S(1)}, bf16[640,128]{1,0:T(8,128)(2,1)S(1)}, u32[]{:S(2)}, u32[]{:S(2)}) collective-permute-start(bf16[640,128]{1,0:T(8,128)(2,1)S(1)} %get-tuple-element.50), channel_id=1, source_target_pairs={{0,12},{2,14},{4,0},{6,2},{8,4},{10,6},{12,8},{14,10},{1,13},{3,15... | collective-permute-start | bytes 491528 | tf_op jit(solution)/shard_map/ppermute | solution.py:290
  116.4 7.8 %collective-permute-start.9 = (bf16[2560,128]{1,0:T(8,128)(2,1)S(1)}, bf16[2560,128]{1,0:T(8,128)(2,1)S(1)}, u32[]{:S(2)}, u32[]{:S(2)}) collective-permute-start(bf16[2560,128]{1,0:T(8,128)(2,1)S(1)} %pad_maximum_fusion), channel_id=1, source_target_pairs={{0,1},{1,0},{2,3},{3,2},{4,5},{5,4},{6,7},{7,6},{8,9},{9,8},{10,11... | collective-permute-start | bytes 1966088 | tf_op jit(solution)/shard_map/ppermute | solution.py:373
  118.4 5.9 %collective-permute-start.8 = (bf16[1280,128]{1,0:T(8,128)(2,1)S(1)}, bf16[1280,128]{1,0:T(8,128)(2,1)S(1)}, u32[]{:S(2)}, u32[]{:S(2)}) collective-permute-start(bf16[1280,128]{1,0:T(8,128)(2,1)S(1)} %get-tuple-element.51.every_ref), channel_id=1, source_target_pairs={{0,1},{1,0},{2,3},{3,2},{4,5},{5,4},{6,7},{7,6},{8,9},{9,8},{10,11... | collective-permute-start | bytes 983048 | tf_op jit(solution)/shard_map/ppermute | solution.py:373
  122.2 3.8 %collective-permute-start.5 = (bf16[1280,128]{1,0:T(8,128)(2,1)S(1)}, bf16[1280,128]{1,0:T(8,128)(2,1)S(1)}, u32[]{:S(2)}, u32[]{:S(2)}) collective-permute-start(bf16[1280,128]{1,0:T(8,128)(2,1)S(1)} %pad_maximum_fusion.1), channel_id=1, source_target_pairs={{0,1},{1,0},{2,3},{3,2},{4,5},{5,4},{6,7},{7,6},{8,9},{9,8},{10,11... | collective-permute-start | bytes 983048 | tf_op jit(solution)/shard_map/ppermute | solution.py:373
  124.2 1.8 copy-start.3
  127.9 4.6 %collective-permute-start.10 = (bf16[3840,128]{1,0:T(8,128)(2,1)S(1)}, bf16[3840,128]{1,0:T(8,128)(2,1)S(1)}, u32[]{:S(2)}, u32[]{:S(2)}) collective-permute-start(bf16[3840,128]{1,0:T(8,128)(2,1)S(1)} %get-tuple-element.56), channel_id=1, source_target_pairs={{0,1},{1,0},{2,3},{3,2},{4,5},{5,4},{6,7},{7,6},{8,9},{9,8},{10,11... | collective-permute-start | bytes 2949128 | tf_op jit(solution)/shard_map/ppermute | solution.py:387
  130.4 9.4 %collective-permute-start.13 = (bf16[1280,128]{1,0:T(8,128)(2,1)S(1)}, bf16[1280,128]{1,0:T(8,128)(2,1)S(1)}, u32[]{:S(2)}, u32[]{:S(2)}) collective-permute-start(bf16[1280,128]{1,0:T(8,128)(2,1)S(1)} %get-tuple-element.58), channel_id=1, source_target_pairs={{0,1},{1,0},{2,3},{3,2},{4,5},{5,4},{6,7},{7,6},{8,9},{9,8},{10,11... | collective-permute-start | bytes 983048 | tf_op jit(solution)/shard_map/ppermute | solution.py:386
  132.7 24.7 %collective-permute-start.12 = (bf16[1280,128]{1,0:T(8,128)(2,1)S(1)}, bf16[1280,128]{1,0:T(8,128)(2,1)S(1)}, u32[]{:S(2)}, u32[]{:S(2)}) collective-permute-start(bf16[1280,128]{1,0:T(8,128)(2,1)S(1)} %get-tuple-element.61), channel_id=1, source_target_pairs={{0,14},{2,0},{4,2},{6,4},{8,6},{10,8},{12,10},{14,12},{1,15},{3,1}... | collective-permute-start | bytes 983048 | tf_op jit(solution)/shard_map/ppermute | solution.py:290
  137.8 19.6 %collective-permute-start.11 = (bf16[1280,128]{1,0:T(8,128)(2,1)S(1)}, bf16[1280,128]{1,0:T(8,128)(2,1)S(1)}, u32[]{:S(2)}, u32[]{:S(2)}) collective-permute-start(bf16[1280,128]{1,0:T(8,128)(2,1)S(1)} %get-tuple-element.62), channel_id=1, source_target_pairs={{0,2},{2,4},{4,6},{6,8},{8,10},{10,12},{12,14},{14,0},{1,3},{3,5},... | collective-permute-start | bytes 983048 | tf_op jit(solution)/shard_map/ppermute | solution.py:290
  139.9 12.5 %collective-permute-start.15 = (bf16[640,128]{1,0:T(8,128)(2,1)S(1)}, bf16[640,128]{1,0:T(8,128)(2,1)S(1)}, u32[]{:S(2)}, u32[]{:S(2)}) collective-permute-start(bf16[640,128]{1,0:T(8,128)(2,1)S(1)} %get-tuple-element.63), channel_id=1, source_target_pairs={{0,12},{2,14},{4,0},{6,2},{8,4},{10,6},{12,8},{14,10},{1,13},{3,15... | collective-permute-start | bytes 491528 | tf_op jit(solution)/shard_map/ppermute | solution.py:290
  144.5 41.0 %copy-start.8 = (f32[256,2]{0,1:T(2,128)S(1)}, f32[256,2]{0,1:T(2,128)}, u32[]{:S(2)}) copy-start(f32[256,2]{0,1:T(2,128)} %param.20) | copy-start | bytes 6148
  144.5 13.0 %collective-permute-start.14 = (bf16[640,128]{1,0:T(8,128)(2,1)S(1)}, bf16[640,128]{1,0:T(8,128)(2,1)S(1)}, u32[]{:S(2)}, u32[]{:S(2)}) collective-permute-start(bf16[640,128]{1,0:T(8,128)(2,1)S(1)} %get-tuple-element.64), channel_id=1, source_target_pairs={{0,4},{2,6},{4,8},{6,10},{8,12},{10,14},{12,0},{14,2},{1,5},{3,7},... | collective-permute-start | bytes 491528 | tf_op jit(solution)/shard_map/ppermute | solution.py:290

commit v11 on v10

--- a/solution.py
+++ b/solution.py
@@ -154,7 +154,7 @@
                 out_ref[y * NC + c, q * HD : (q + 1) * HD, :] = w_ref[:, block * COLS : (block + 1) * COLS]
 
 
-def route(at_ref, routes_ref, resid_ref, pick_ref, back_ref, cols_ref):
+def route(at_ref, routes_ref, resid_ref, pick_ref, slots_ref, cols_ref):
     for q in range(2):
         cols_ref[:, q * COLS : (q + 1) * COLS] = resid_ref[:, pl.ds(pl.multiple_of(at_ref[q], COLS), COLS)]
     e0, e1 = routes_ref[0:1, :], routes_ref[1:2, :]
@@ -167,12 +167,7 @@
     before = jnp.dot(hit, upper, preferred_element_type=f32)
     r0 = jnp.sum(jnp.where(h0, before, 0.0), axis=0, keepdims=True).astype(jnp.int32)
     r1 = jnp.sum(jnp.where(h1, before, 0.0), axis=0, keepdims=True).astype(jnp.int32)
-    slots = jnp.concatenate([2 * SLOT * e0 + r0, 2 * SLOT * e1 + r1, jnp.zeros((6, TOK), jnp.int32)], axis=0)
-    slots = slots.astype(f32).T
-    at = lax.broadcasted_iota(jnp.int32, (TOK, 2 * PADROWS), 1).astype(f32)
-    for k in range(2):
-        slot = slots[:, k : k + 1]
-        back_ref[k * TOK : (k + 1) * TOK, :] = jnp.where((at == slot) | (at == slot + SLOT), 1.0, 0.0).astype(bf)
+    slots_ref[...] = jnp.concatenate([2 * SLOT * e0 + r0, 2 * SLOT * e1 + r1, jnp.zeros((6, TOK), jnp.int32)], axis=0)
     s0 = e0 * SEND + r0
     s1 = e1 * SEND + r1
     ir = lax.broadcasted_iota(jnp.int32, (NSP * SEND, TOK), 0)
@@ -277,6 +272,14 @@
         rows_ref[...] = acc + far_ref[...].astype(f32)
         for i in range(NSP):
             out_ref[2 * i + q] = jnp.concatenate([rows_ref[CAP * i : CAP * i + CAP, :], pad], axis=0).astype(bf)
+
+
+def route_back(slots_ref, back_ref):
+    slots = slots_ref[...].astype(f32).T
+    at = lax.broadcasted_iota(jnp.int32, (TOK, 2 * PADROWS), 1).astype(f32)
+    for k in range(2):
+        slot = slots[:, k : k + 1]
+        back_ref[k * TOK : (k + 1) * TOK, :] = jnp.where((at == slot) | (at == slot + SLOT), 1.0, 0.0).astype(bf)
 
 
 def finish(ret_ref, back_ref, rw_ref, stream_ref, out_ref):
@@ -343,9 +346,9 @@
     parts = [sent[0]]
     for n in range(1, NX):
         parts.append(lax.ppermute(sent[n], "x", [(i, (i + n) % NX) for i in range(NX)]))
-    pick, back_pick, resid_cols = call(
+    pick, slots, resid_cols = call(
         route,
-        (sds((NSP * SEND, TOK), bf), sds((2 * TOK, 2 * PADROWS), bf), sds((TOK, 2 * COLS), bf)),
+        (sds((NSP * SEND, TOK), bf), sds((8, TOK), jnp.int32), sds((TOK, 2 * COLS), bf)),
         (at_cols, routes.T, resid),
         smem=1,
     )
@@ -398,6 +401,7 @@
         (near_mine, near_theirs, 2, 2, -1),
     ):
         got.append(shift(pair(a, b, first, count), by))
+    back_pick = call(route_back, sds((2 * TOK, 2 * PADROWS), bf), (slots,))
     back = call(
         gather_sum,
         sds((2 * NSP, SLOT, COLS), bf),

time: 188 us -> 188 us (level)
  blocking collectives: 103 us -> 74.3 us
  waiting for transfers between devices: 14.8 us -> 35.2 us
  starting transfers between devices: 55 us -> 63.4 us
    all_to_all x4 -> x3, blocking collectives: 85.6 us -> 57.2 us  [exchange(): return lax.all_to_all(v, axis, 0, 0, tiled=True)]
    all_to_all x1 -> x2, waiting for transfers between devices: 0.01 us -> 19.1 us  [exchange(): return lax.all_to_all(v, axis, 0, 0, tiled=True)]
    all_to_all x1 -> x2, starting transfers between devices: 7.56 us -> 15.9 us  [exchange(): return lax.all_to_all(v, axis, 0, 0, tiled=True)]
    pallas_call x11 -> x12, Pallas kernels: 11.2 us -> 12.1 us  [call(): pl.pallas_call(body, out_shape=out_shape, in_specs=specs, out_specs=tuple...]
  transfers between devices with their start and end apart: 17 -> 18, of which waited for: 5 -> 7; matrix products, arithmetic and copies ran while one was open for 0% -> 0% of each run, Pallas kernels for 3% -> 3%
where the time goes in v11:
time: 188 us; the launch traced here: 187 us
  blocking collectives  74.3 us (40%)
  starting transfers between devices  63.4 us (34%)
  waiting for transfers between devices  35.2 us (19%)
  Pallas kernels  12.1 us (6%)
    all_to_all x3, blocking collectives, exchange(): return lax.all_to_all(v, axis, 0, 0, tiled=True)  57.2 us
    ppermute x8, starting transfers between devices, shift(): return lax.ppermute(v, Y, [(i, (i + by) % NY) for i in range(NY)])  27.7 us
    all_to_all x2, waiting for transfers between devices, exchange(): return lax.all_to_all(v, axis, 0, 0, tiled=True)  19.1 us
    all_gather x1, blocking collectives, layer(): attended = lax.all_gather(attended, TP, axis=0, tiled=True)  17 us
    all_to_all x2, starting transfers between devices, exchange(): return lax.all_to_all(v, axis, 0, 0, tiled=True)  15.9 us
    ppermute x8, waiting for transfers between devices, shift(): return lax.ppermute(v, Y, [(i, (i + by) % NY) for i in range(NY)])  14.5 us
    pallas_call x12, Pallas kernels, call(): pl.pallas_call(body, out_shape=out_shape, in_specs=specs, out_specs=tuple...  12.1 us
    ppermute x3, starting transfers between devices, layer(): lax.ppermute(sent[n], 'x', [(i, (i + n) % NX) for i in range(NX)])  9.18 us
  transfers between devices with their start and end apart: 18, of which 7 were waited for; matrix products, arithmetic and copies ran while one was open for 0% of the time, Pallas kernels for 3%

profile of v11, /device:TPU:8, one launch (start us, length us, event | category | flops | bytes accessed | tf_op | source)
XLA Modules:
  0.0 186.8 jit_solution(6319302527813306567)
XLA Ops:
  1.1 10.1 %all_to_all.25.q_ref = bf16[4,64,256]{2,1,0:T(8,128)(2,1)S(1)} all-to-all(bf16[4,64,256]{2,1,0:T(8,128)(2,1)S(1)} %get-tuple-element.37), channel_id=1, replica_groups=mesh['z'=8,'x'=4,'yh'=2,'yl'=4,'c'=2] {'x'}, dimensions={0} | all-to-all | bytes 262144 | tf_op jit(solution)/shard_map/all_to_all | solution.py:297
  11.1 26.3 %all_to_all.26.kv_ref = bf16[8,128,256]{2,1,0:T(8,128)(2,1)S(1)} all-to-all(bf16[8,128,256]{2,1,0:T(8,128)(2,1)S(1)} %get-tuple-element.39), channel_id=1, replica_groups=mesh['z'=8,'x'=4,'yh'=2,'yl'=4,'c'=2] {'z'}, dimensions={0} | all-to-all | bytes 1048576 | tf_op jit(solution)/shard_map/all_to_all | solution.py:297
  38.3 7.6 %all-to-all-start.2 = ((bf16[16,128,128]{2,1,0:T(8,128)(2,1)}), bf16[16,128,128]{2,1,0:T(8,128)(2,1)S(1)}, u32[]{:S(2)}, u32[]{:S(2)}) async-start(bf16[16,128,128]{2,1,0:T(8,128)(2,1)} %shard_map.121), calls=%async_computation.2 | async-start | bytes 1048576 | tf_op jit(solution)/shard_map/all_to_all | solution.py:297
  45.9 1.3 shard_map.119
  47.2 2.5 %collective-permute-start = (bf16[80,256]{1,0:T(8,128)(2,1)S(1)}, bf16[80,256]{1,0:T(8,128)(2,1)S(1)}, u32[]{:S(2)}, u32[]{:S(2)}) collective-permute-start(bf16[80,256]{1,0:T(8,128)(2,1)S(1)} %get-tuple-element.42), channel_id=1, source_target_pairs={{0,16},{16,32},{32,48},{48,0},{1,17},{17,33},{33,49},{49,1},{2,18}... | collective-permute-start | bytes 122888 | tf_op jit(solution)/shard_map/ppermute | solution.py:348
  49.7 4.0 %collective-permute-start.1 = (bf16[80,256]{1,0:T(8,128)(2,1)S(1)}, bf16[80,256]{1,0:T(8,128)(2,1)S(1)}, u32[]{:S(2)}, u32[]{:S(2)}) collective-permute-start(bf16[80,256]{1,0:T(8,128)(2,1)S(1)} %get-tuple-element.43), channel_id=1, source_target_pairs={{0,32},{16,48},{32,0},{48,16},{1,33},{17,49},{33,1},{49,17},{2,34}... | collective-permute-start | bytes 122888 | tf_op jit(solution)/shard_map/ppermute | solution.py:348
  53.7 2.7 %collective-permute-start.2 = (bf16[80,256]{1,0:T(8,128)(2,1)S(1)}, bf16[80,256]{1,0:T(8,128)(2,1)S(1)}, u32[]{:S(2)}, u32[]{:S(2)}) collective-permute-start(bf16[80,256]{1,0:T(8,128)(2,1)S(1)} %get-tuple-element.44), channel_id=1, source_target_pairs={{0,48},{16,0},{32,16},{48,32},{1,49},{17,1},{33,17},{49,33},{2,50}... | collective-permute-start | bytes 122888 | tf_op jit(solution)/shard_map/ppermute | solution.py:348
  56.5 1.8 shard_map.122
  59.6 17.0 %all_gather.3.att_ref = bf16[1024,256]{1,0:T(8,128)(2,1)S(1)} all-gather(bf16[64,256]{1,0:T(8,128)(2,1)S(1)} %shard_map.120), channel_id=1, replica_groups=mesh['z'=8,'x'=4,'yh'=2,'yl'=4,'c'=2] {'yh','yl','c'}, dimensions={0}, use_global_device_ids=true | all-gather | bytes 557056 | tf_op jit(solution)/shard_map/all_gather | solution.py:356
  76.7 1.4 shard_map.123
  78.1 20.9 %all_to_all.27.in_ref = bf16[32,40,128]{2,1,0:T(8,128)(2,1)S(1)} all-to-all(bf16[32,40,128]{2,1,0:T(8,128)(2,1)S(1)} %get-tuple-element.48), channel_id=1, replica_groups=mesh['z'=8,'x'=4,'yh'=2,'yl'=4,'c'=2] {'z','x'}, dimensions={0} | all-to-all | bytes 655360 | tf_op jit(solution)/shard_map/all_to_all | solution.py:297
  99.1 3.8 %collective-permute-start.7 = (bf16[1280,128]{1,0:T(8,128)(2,1)S(1)}, bf16[1280,128]{1,0:T(8,128)(2,1)S(1)}, u32[]{:S(2)}, u32[]{:S(2)}) collective-permute-start(bf16[1280,128]{1,0:T(8,128)(2,1)S(1)} %get-tuple-element.51.every_ref), channel_id=1, source_target_pairs={{0,14},{2,0},{4,2},{6,4},{8,6},{10,8},{12,10},{14,12},{1,15},{3,1}... | collective-permute-start | bytes 983048 | tf_op jit(solution)/shard_map/ppermute | solution.py:293
  102.9 2.2 %collective-permute-start.6 = (bf16[1280,128]{1,0:T(8,128)(2,1)S(1)}, bf16[1280,128]{1,0:T(8,128)(2,1)S(1)}, u32[]{:S(2)}, u32[]{:S(2)}) collective-permute-start(bf16[1280,128]{1,0:T(8,128)(2,1)S(1)} %get-tuple-element.51.every_ref), channel_id=1, source_target_pairs={{0,2},{2,4},{4,6},{6,8},{8,10},{10,12},{12,14},{14,0},{1,3},{3,5},... | collective-permute-start | bytes 983048 | tf_op jit(solution)/shard_map/ppermute | solution.py:293
  105.0 5.5 %collective-permute-start.3 = (bf16[640,128]{1,0:T(8,128)(2,1)S(1)}, bf16[640,128]{1,0:T(8,128)(2,1)S(1)}, u32[]{:S(2)}, u32[]{:S(2)}) collective-permute-start(bf16[640,128]{1,0:T(8,128)(2,1)S(1)} %get-tuple-element.49), channel_id=1, source_target_pairs={{0,4},{2,6},{4,8},{6,10},{8,12},{10,14},{12,0},{14,2},{1,5},{3,7},... | collective-permute-start | bytes 491528 | tf_op jit(solution)/shard_map/ppermute | solution.py:293
  110.5 2.5 %collective-permute-start.4 = (bf16[640,128]{1,0:T(8,128)(2,1)S(1)}, bf16[640,128]{1,0:T(8,128)(2,1)S(1)}, u32[]{:S(2)}, u32[]{:S(2)}) collective-permute-start(bf16[640,128]{1,0:T(8,128)(2,1)S(1)} %get-tuple-element.50), channel_id=1, source_target_pairs={{0,12},{2,14},{4,0},{6,2},{8,4},{10,6},{12,8},{14,10},{1,13},{3,15... | collective-permute-start | bytes 491528 | tf_op jit(solution)/shard_map/ppermute | solution.py:293
  113.0 2.4 %collective-permute-done.6.n0_ref = bf16[1280,128]{1,0:T(8,128)(2,1)S(1)} collective-permute-done((bf16[1280,128]{1,0:T(8,128)(2,1)S(1)}, bf16[1280,128]{1,0:T(8,128)(2,1)S(1)}, u32[]{:S(2)}, u32[]{:S(2)}) %collective-permute-start.6) | collective-permute-done | bytes 327712 | tf_op jit(solution)/shard_map/ppermute | solution.py:293
  115.4 1.9 %collective-permute-start.9 = (bf16[2560,128]{1,0:T(8,128)(2,1)S(1)}, bf16[2560,128]{1,0:T(8,128)(2,1)S(1)}, u32[]{:S(2)}, u32[]{:S(2)}) collective-permute-start(bf16[2560,128]{1,0:T(8,128)(2,1)S(1)} %pad_maximum_fusion), channel_id=1, source_target_pairs={{0,1},{1,0},{2,3},{3,2},{4,5},{5,4},{6,7},{7,6},{8,9},{9,8},{10,11... | collective-permute-start | bytes 1966088 | tf_op jit(solution)/shard_map/ppermute | solution.py:376
  117.4 2.4 %collective-permute-start.8 = (bf16[1280,128]{1,0:T(8,128)(2,1)S(1)}, bf16[1280,128]{1,0:T(8,128)(2,1)S(1)}, u32[]{:S(2)}, u32[]{:S(2)}) collective-permute-start(bf16[1280,128]{1,0:T(8,128)(2,1)S(1)} %get-tuple-element.51.every_ref), channel_id=1, source_target_pairs={{0,1},{1,0},{2,3},{3,2},{4,5},{5,4},{6,7},{7,6},{8,9},{9,8},{10,11... | collective-permute-start | bytes 983048 | tf_op jit(solution)/shard_map/ppermute | solution.py:376
  119.8 1.4 collective-permute-done.3.f0_ref
  121.2 1.9 %collective-permute-start.5 = (bf16[1280,128]{1,0:T(8,128)(2,1)S(1)}, bf16[1280,128]{1,0:T(8,128)(2,1)S(1)}, u32[]{:S(2)}, u32[]{:S(2)}) collective-permute-start(bf16[1280,128]{1,0:T(8,128)(2,1)S(1)} %pad_maximum_fusion.1), channel_id=1, source_target_pairs={{0,1},{1,0},{2,3},{3,2},{4,5},{5,4},{6,7},{7,6},{8,9},{9,8},{10,11... | collective-permute-start | bytes 983048 | tf_op jit(solution)/shard_map/ppermute | solution.py:376
  123.2 1.7 shard_map.125
  125.0 1.9 %shard_map.126 = (bf16[1280,128]{1,0:T(8,128)(2,1)S(1)}, bf16[3840,128]{1,0:T(8,128)(2,1)S(1)}, bf16[1280,128]{1,0:T(8,128)(2,1)S(1)}, bf16[3840,128]{1,0:T(8,128)(2,1)S(1)}) custom-call(s32[2]{0:T(128)S(1)} %pad_add_fusion.at_ref, bf16[640,128]{1,0:T(8,128)(2,1)S(1)} %collective-permute-done.3.f0_ref, bf16[640,128]{1,0:T(8,128)(2,1)S(1)} %collective-permute-done.4.f1_ref, ...), custom_call_target="tpu_custom_call" | custom-call | tf_op jit(solution)/shard_map/pallas_call | solution.py:38
  126.9 2.4 %collective-permute-start.10 = (bf16[3840,128]{1,0:T(8,128)(2,1)S(1)}, bf16[3840,128]{1,0:T(8,128)(2,1)S(1)}, u32[]{:S(2)}, u32[]{:S(2)}) collective-permute-start(bf16[3840,128]{1,0:T(8,128)(2,1)S(1)} %get-tuple-element.56), channel_id=1, source_target_pairs={{0,1},{1,0},{2,3},{3,2},{4,5},{5,4},{6,7},{7,6},{8,9},{9,8},{10,11... | collective-permute-start | bytes 2949128 | tf_op jit(solution)/shard_map/ppermute | solution.py:390
  129.3 1.9 %collective-permute-start.13 = (bf16[1280,128]{1,0:T(8,128)(2,1)S(1)}, bf16[1280,128]{1,0:T(8,128)(2,1)S(1)}, u32[]{:S(2)}, u32[]{:S(2)}) collective-permute-start(bf16[1280,128]{1,0:T(8,128)(2,1)S(1)} %get-tuple-element.58), channel_id=1, source_target_pairs={{0,1},{1,0},{2,3},{3,2},{4,5},{5,4},{6,7},{7,6},{8,9},{9,8},{10,11... | collective-permute-start | bytes 983048 | tf_op jit(solution)/shard_map/ppermute | solution.py:389
  131.7 5.1 %collective-permute-start.12 = (bf16[1280,128]{1,0:T(8,128)(2,1)S(1)}, bf16[1280,128]{1,0:T(8,128)(2,1)S(1)}, u32[]{:S(2)}, u32[]{:S(2)}) collective-permute-start(bf16[1280,128]{1,0:T(8,128)(2,1)S(1)} %get-tuple-element.61), channel_id=1, source_target_pairs={{0,14},{2,0},{4,2},{6,4},{8,6},{10,8},{12,10},{14,12},{1,15},{3,1}... | collective-permute-start | bytes 983048 | tf_op jit(solution)/shard_map/ppermute | solution.py:293
  136.8 1.9 %collective-permute-start.11 = (bf16[1280,128]{1,0:T(8,128)(2,1)S(1)}, bf16[1280,128]{1,0:T(8,128)(2,1)S(1)}, u32[]{:S(2)}, u32[]{:S(2)}) collective-permute-start(bf16[1280,128]{1,0:T(8,128)(2,1)S(1)} %get-tuple-element.62), channel_id=1, source_target_pairs={{0,2},{2,4},{4,6},{6,8},{8,10},{10,12},{12,14},{14,0},{1,3},{3,5},... | collective-permute-start | bytes 983048 | tf_op jit(solution)/shard_map/ppermute | solution.py:293
  138.8 4.6 %collective-permute-start.15 = (bf16[640,128]{1,0:T(8,128)(2,1)S(1)}, bf16[640,128]{1,0:T(8,128)(2,1)S(1)}, u32[]{:S(2)}, u32[]{:S(2)}) collective-permute-start(bf16[640,128]{1,0:T(8,128)(2,1)S(1)} %get-tuple-element.63), channel_id=1, source_target_pairs={{0,12},{2,14},{4,0},{6,2},{8,4},{10,6},{12,8},{14,10},{1,13},{3,15... | collective-permute-start | bytes 491528 | tf_op jit(solution)/shard_map/ppermute | solution.py:293
  143.4 2.2 %collective-permute-start.14 = (bf16[640,128]{1,0:T(8,128)(2,1)S(1)}, bf16[640,128]{1,0:T(8,128)(2,1)S(1)}, u32[]{:S(2)}, u32[]{:S(2)}) collective-permute-start(bf16[640,128]{1,0:T(8,128)(2,1)S(1)} %get-tuple-element.64), channel_id=1, source_target_pairs={{0,4},{2,6},{4,8},{6,10},{8,12},{10,14},{12,0},{14,2},{1,5},{3,7},... | collective-permute-start | bytes 491528 | tf_op jit(solution)/shard_map/ppermute | solution.py:293
  145.6 5.7 %collective-permute-done.15.f1_ref = bf16[640,128]{1,0:T(8,128)(2,1)S(1)} collective-permute-done((bf16[640,128]{1,0:T(8,128)(2,1)S(1)}, bf16[640,128]{1,0:T(8,128)(2,1)S(1)}, u32[]{:S(2)}, u32[]{:S(2)}) %collective-permute-start.15) | collective-permute-done | bytes 163872 | tf_op jit(solution)/shard_map/ppermute | solution.py:293
  151.3 5.1 %collective-permute-done.14.f0_ref = bf16[640,128]{1,0:T(8,128)(2,1)S(1)} collective-permute-done((bf16[640,128]{1,0:T(8,128)(2,1)S(1)}, bf16[640,128]{1,0:T(8,128)(2,1)S(1)}, u32[]{:S(2)}, u32[]{:S(2)}) %collective-permute-start.14) | collective-permute-done | bytes 163872 | tf_op jit(solution)/shard_map/ppermute | solution.py:293
  157.5 8.4 %all-to-all-start.4 = ((bf16[64,24,128]{2,1,0:T(8,128)(2,1)}), bf16[64,24,128]{2,1,0:T(8,128)(2,1)S(1)}, u32[]{:S(2)}, u32[]{:S(2)}) async-start(bf16[64,24,128]{2,1,0:T(8,128)(2,1)} %shard_map.127), calls=%async_computation.4 | async-start | bytes 786432 | tf_op jit(solution)/shard_map/all_to_all | solution.py:297
  166.4 19.1 %all-to-all-done.4 = bf16[64,24,128]{2,1,0:T(8,128)(2,1)S(1)} async-done(((bf16[64,24,128]{2,1,0:T(8,128)(2,1)}), bf16[64,24,128]{2,1,0:T(8,128)(2,1)S(1)}, u32[]{:S(2)}, u32[]{:S(2)}) %all-to-all-start.4) | async-done | bytes 393248 | tf_op jit(solution)/shard_map/all_to_all | solution.py:297
  (46 shorter events, 7.0 us)
Async XLA Ops:
  0.0 37.4 %copy-start.4 = (bf16[64,2048]{1,0:T(8,128)(2,1)S(1)}, bf16[64,2048]{1,0:T(8,128)(2,1)}, u32[]{:S(2)}) copy-start(bf16[64,2048]{1,0:T(8,128)(2,1)} %w_ref) | copy-start | bytes 786436
  11.1 34.7 %copy-start.6 = (f32[1,8192]{1,0:T(1,128)S(1)}, f32[1,8192]{1,0:T(1,128)}, u32[]{:S(2)}) copy-start(f32[1,8192]{1,0:T(1,128)} %gate_ref.1) | copy-start | bytes 98308
  37.4 19.0 %copy-start.2 = (bf16[256,2048]{1,0:T(8,128)(2,1)S(1)}, bf16[256,2048]{1,0:T(8,128)(2,1)}, u32[]{:S(2)}) copy-start(bf16[256,2048]{1,0:T(8,128)(2,1)} %resid_ref.1) | copy-start | bytes 3145732
  37.4 19.0 %copy-start.7 = (s32[256,2]{0,1:T(2,128)S(1)}, s32[256,2]{0,1:T(2,128)}, u32[]{:S(2)}) copy-start(s32[256,2]{0,1:T(2,128)} %param.19) | copy-start | bytes 6148
  38.3 38.4 %all-to-all-start.2 = ((bf16[16,128,128]{2,1,0:T(8,128)(2,1)}), bf16[16,128,128]{2,1,0:T(8,128)(2,1)S(1)}, u32[]{:S(2)}, u32[]{:S(2)}) async-start(bf16[16,128,128]{2,1,0:T(8,128)(2,1)} %shard_map.121), calls=%async_computation.2 | async-start | bytes 1048576 | tf_op jit(solution)/shard_map/all_to_all | solution.py:297
  45.9 30.8 %copy-start.5 = (f32[2048]{0:T(1024)S(1)}, f32[2048]{0:T(1024)}, u32[]{:S(2)}) copy-start(f32[2048]{0:T(1024)} %param.18) | copy-start | bytes 24580
  47.2 11.0 %collective-permute-start = (bf16[80,256]{1,0:T(8,128)(2,1)S(1)}, bf16[80,256]{1,0:T(8,128)(2,1)S(1)}, u32[]{:S(2)}, u32[]{:S(2)}) collective-permute-start(bf16[80,256]{1,0:T(8,128)(2,1)S(1)} %get-tuple-element.42), channel_id=1, source_target_pairs={{0,16},{16,32},{32,48},{48,0},{1,17},{17,33},{33,49},{49,1},{2,18}... | collective-permute-start | bytes 122888 | tf_op jit(solution)/shard_map/ppermute | solution.py:348
  49.7 8.5 %collective-permute-start.1 = (bf16[80,256]{1,0:T(8,128)(2,1)S(1)}, bf16[80,256]{1,0:T(8,128)(2,1)S(1)}, u32[]{:S(2)}, u32[]{:S(2)}) collective-permute-start(bf16[80,256]{1,0:T(8,128)(2,1)S(1)} %get-tuple-element.43), channel_id=1, source_target_pairs={{0,32},{16,48},{32,0},{48,16},{1,33},{17,49},{33,1},{49,17},{2,34}... | collective-permute-start | bytes 122888 | tf_op jit(solution)/shard_map/ppermute | solution.py:348
  53.7 5.9 %collective-permute-start.2 = (bf16[80,256]{1,0:T(8,128)(2,1)S(1)}, bf16[80,256]{1,0:T(8,128)(2,1)S(1)}, u32[]{:S(2)}, u32[]{:S(2)}) collective-permute-start(bf16[80,256]{1,0:T(8,128)(2,1)S(1)} %get-tuple-element.44), channel_id=1, source_target_pairs={{0,48},{16,0},{32,16},{48,32},{1,49},{17,1},{33,17},{49,33},{2,50}... | collective-permute-start | bytes 122888 | tf_op jit(solution)/shard_map/ppermute | solution.py:348
  99.0 24.2 %copy-start = (bf16[1,2048,256]{2,1,0:T(8,128)(2,1)S(1)}, bf16[1,2048,256]{2,1,0:T(8,128)(2,1)}, u32[]{:S(2)}) copy-start(bf16[1,2048,256]{2,1,0:T(8,128)(2,1)} %param.21) | copy-start | bytes 3145732
  99.0 24.2 %copy-start.1 = (bf16[1,2048,256]{2,1,0:T(8,128)(2,1)S(1)}, bf16[1,2048,256]{2,1,0:T(8,128)(2,1)}, u32[]{:S(2)}) copy-start(bf16[1,2048,256]{2,1,0:T(8,128)(2,1)} %param.22) | copy-start | bytes 3145732
  99.1 14.0 %collective-permute-start.7 = (bf16[1280,128]{1,0:T(8,128)(2,1)S(1)}, bf16[1280,128]{1,0:T(8,128)(2,1)S(1)}, u32[]{:S(2)}, u32[]{:S(2)}) collective-permute-start(bf16[1280,128]{1,0:T(8,128)(2,1)S(1)} %get-tuple-element.51.every_ref), channel_id=1, source_target_pairs={{0,14},{2,0},{4,2},{6,4},{8,6},{10,8},{12,10},{14,12},{1,15},{3,1}... | collective-permute-start | bytes 983048 | tf_op jit(solution)/shard_map/ppermute | solution.py:293
  102.9 12.5 %collective-permute-start.6 = (bf16[1280,128]{1,0:T(8,128)(2,1)S(1)}, bf16[1280,128]{1,0:T(8,128)(2,1)S(1)}, u32[]{:S(2)}, u32[]{:S(2)}) collective-permute-start(bf16[1280,128]{1,0:T(8,128)(2,1)S(1)} %get-tuple-element.51.every_ref), channel_id=1, source_target_pairs={{0,2},{2,4},{4,6},{6,8},{8,10},{10,12},{12,14},{14,0},{1,3},{3,5},... | collective-permute-start | bytes 983048 | tf_op jit(solution)/shard_map/ppermute | solution.py:293
  105.0 16.1 %collective-permute-start.3 = (bf16[640,128]{1,0:T(8,128)(2,1)S(1)}, bf16[640,128]{1,0:T(8,128)(2,1)S(1)}, u32[]{:S(2)}, u32[]{:S(2)}) collective-permute-start(bf16[640,128]{1,0:T(8,128)(2,1)S(1)} %get-tuple-element.49), channel_id=1, source_target_pairs={{0,4},{2,6},{4,8},{6,10},{8,12},{10,14},{12,0},{14,2},{1,5},{3,7},... | collective-permute-start | bytes 491528 | tf_op jit(solution)/shard_map/ppermute | solution.py:293
  110.5 10.6 %collective-permute-start.4 = (bf16[640,128]{1,0:T(8,128)(2,1)S(1)}, bf16[640,128]{1,0:T(8,128)(2,1)S(1)}, u32[]{:S(2)}, u32[]{:S(2)}) collective-permute-start(bf16[640,128]{1,0:T(8,128)(2,1)S(1)} %get-tuple-element.50), channel_id=1, source_target_pairs={{0,12},{2,14},{4,0},{6,2},{8,4},{10,6},{12,8},{14,10},{1,13},{3,15... | collective-permute-start | bytes 491528 | tf_op jit(solution)/shard_map/ppermute | solution.py:293
  115.4 7.7 %collective-permute-start.9 = (bf16[2560,128]{1,0:T(8,128)(2,1)S(1)}, bf16[2560,128]{1,0:T(8,128)(2,1)S(1)}, u32[]{:S(2)}, u32[]{:S(2)}) collective-permute-start(bf16[2560,128]{1,0:T(8,128)(2,1)S(1)} %pad_maximum_fusion), channel_id=1, source_target_pairs={{0,1},{1,0},{2,3},{3,2},{4,5},{5,4},{6,7},{7,6},{8,9},{9,8},{10,11... | collective-permute-start | bytes 1966088 | tf_op jit(solution)/shard_map/ppermute | solution.py:376
  117.4 5.8 %collective-permute-start.8 = (bf16[1280,128]{1,0:T(8,128)(2,1)S(1)}, bf16[1280,128]{1,0:T(8,128)(2,1)S(1)}, u32[]{:S(2)}, u32[]{:S(2)}) collective-permute-start(bf16[1280,128]{1,0:T(8,128)(2,1)S(1)} %get-tuple-element.51.every_ref), channel_id=1, source_target_pairs={{0,1},{1,0},{2,3},{3,2},{4,5},{5,4},{6,7},{7,6},{8,9},{9,8},{10,11... | collective-permute-start | bytes 983048 | tf_op jit(solution)/shard_map/ppermute | solution.py:376
  121.2 3.8 %collective-permute-start.5 = (bf16[1280,128]{1,0:T(8,128)(2,1)S(1)}, bf16[1280,128]{1,0:T(8,128)(2,1)S(1)}, u32[]{:S(2)}, u32[]{:S(2)}) collective-permute-start(bf16[1280,128]{1,0:T(8,128)(2,1)S(1)} %pad_maximum_fusion.1), channel_id=1, source_target_pairs={{0,1},{1,0},{2,3},{3,2},{4,5},{5,4},{6,7},{7,6},{8,9},{9,8},{10,11... | collective-permute-start | bytes 983048 | tf_op jit(solution)/shard_map/ppermute | solution.py:376
  123.2 1.8 copy-start.3
  126.9 4.6 %collective-permute-start.10 = (bf16[3840,128]{1,0:T(8,128)(2,1)S(1)}, bf16[3840,128]{1,0:T(8,128)(2,1)S(1)}, u32[]{:S(2)}, u32[]{:S(2)}) collective-permute-start(bf16[3840,128]{1,0:T(8,128)(2,1)S(1)} %get-tuple-element.56), channel_id=1, source_target_pairs={{0,1},{1,0},{2,3},{3,2},{4,5},{5,4},{6,7},{7,6},{8,9},{9,8},{10,11... | collective-permute-start | bytes 2949128 | tf_op jit(solution)/shard_map/ppermute | solution.py:390
  129.3 9.4 %collective-permute-start.13 = (bf16[1280,128]{1,0:T(8,128)(2,1)S(1)}, bf16[1280,128]{1,0:T(8,128)(2,1)S(1)}, u32[]{:S(2)}, u32[]{:S(2)}) collective-permute-start(bf16[1280,128]{1,0:T(8,128)(2,1)S(1)} %get-tuple-element.58), channel_id=1, source_target_pairs={{0,1},{1,0},{2,3},{3,2},{4,5},{5,4},{6,7},{7,6},{8,9},{9,8},{10,11... | collective-permute-start | bytes 983048 | tf_op jit(solution)/shard_map/ppermute | solution.py:389
  131.7 24.7 %collective-permute-start.12 = (bf16[1280,128]{1,0:T(8,128)(2,1)S(1)}, bf16[1280,128]{1,0:T(8,128)(2,1)S(1)}, u32[]{:S(2)}, u32[]{:S(2)}) collective-permute-start(bf16[1280,128]{1,0:T(8,128)(2,1)S(1)} %get-tuple-element.61), channel_id=1, source_target_pairs={{0,14},{2,0},{4,2},{6,4},{8,6},{10,8},{12,10},{14,12},{1,15},{3,1}... | collective-permute-start | bytes 983048 | tf_op jit(solution)/shard_map/ppermute | solution.py:293
  136.8 19.6 %collective-permute-start.11 = (bf16[1280,128]{1,0:T(8,128)(2,1)S(1)}, bf16[1280,128]{1,0:T(8,128)(2,1)S(1)}, u32[]{:S(2)}, u32[]{:S(2)}) collective-permute-start(bf16[1280,128]{1,0:T(8,128)(2,1)S(1)} %get-tuple-element.62), channel_id=1, source_target_pairs={{0,2},{2,4},{4,6},{6,8},{8,10},{10,12},{12,14},{14,0},{1,3},{3,5},... | collective-permute-start | bytes 983048 | tf_op jit(solution)/shard_map/ppermute | solution.py:293
  138.8 12.5 %collective-permute-start.15 = (bf16[640,128]{1,0:T(8,128)(2,1)S(1)}, bf16[640,128]{1,0:T(8,128)(2,1)S(1)}, u32[]{:S(2)}, u32[]{:S(2)}) collective-permute-start(bf16[640,128]{1,0:T(8,128)(2,1)S(1)} %get-tuple-element.63), channel_id=1, source_target_pairs={{0,12},{2,14},{4,0},{6,2},{8,4},{10,6},{12,8},{14,10},{1,13},{3,15... | collective-permute-start | bytes 491528 | tf_op jit(solution)/shard_map/ppermute | solution.py:293
  143.4 13.0 %collective-permute-start.14 = (bf16[640,128]{1,0:T(8,128)(2,1)S(1)}, bf16[640,128]{1,0:T(8,128)(2,1)S(1)}, u32[]{:S(2)}, u32[]{:S(2)}) collective-permute-start(bf16[640,128]{1,0:T(8,128)(2,1)S(1)} %get-tuple-element.64), channel_id=1, source_target_pairs={{0,4},{2,6},{4,8},{6,10},{8,12},{10,14},{12,0},{14,2},{1,5},{3,7},... | collective-permute-start | bytes 491528 | tf_op jit(solution)/shard_map/ppermute | solution.py:293
  157.5 28.1 %copy-start.8 = (f32[256,2]{0,1:T(2,128)S(1)}, f32[256,2]{0,1:T(2,128)}, u32[]{:S(2)}) copy-start(f32[256,2]{0,1:T(2,128)} %param.20) | copy-start | bytes 6148
  157.5 28.1 %all-to-all-start.4 = ((bf16[64,24,128]{2,1,0:T(8,128)(2,1)}), bf16[64,24,128]{2,1,0:T(8,128)(2,1)S(1)}, u32[]{:S(2)}, u32[]{:S(2)}) async-start(bf16[64,24,128]{2,1,0:T(8,128)(2,1)} %shard_map.127), calls=%async_computation.4 | async-start | bytes 786432 | tf_op jit(solution)/shard_map/all_to_all | solution.py:297

commit v12 on v11

--- a/solution.py
+++ b/solution.py
@@ -167,7 +167,7 @@
     before = jnp.dot(hit, upper, preferred_element_type=f32)
     r0 = jnp.sum(jnp.where(h0, before, 0.0), axis=0, keepdims=True).astype(jnp.int32)
     r1 = jnp.sum(jnp.where(h1, before, 0.0), axis=0, keepdims=True).astype(jnp.int32)
-    slots_ref[...] = jnp.concatenate([2 * SLOT * e0 + r0, 2 * SLOT * e1 + r1, jnp.zeros((6, TOK), jnp.int32)], axis=0)
+    slots_ref[...] = jnp.concatenate([SLOT * e0 + r0, SLOT * e1 + r1, jnp.zeros((6, TOK), jnp.int32)], axis=0)
     s0 = e0 * SEND + r0
     s1 = e1 * SEND + r1
     ir = lax.broadcasted_iota(jnp.int32, (NSP * SEND, TOK), 0)
@@ -214,28 +214,28 @@
 )
 
 
-def accumulate(y, c, pieces, owns, others, wg_ref, wu_ref, gain_ref, g_ref, u_ref, sq_ref, fresh):
+def accumulate(y, c, pieces, owns, others, wg_ref, wu_ref, gain_ref, g_ref, u_ref, sq_ref, before):
     for off, upper, n, at in pieces:
         mine, theirs = owns[n][at : at + ROWS, :], others[n][at : at + ROWS, :]
         block = lax.rem(y + off, HALF) + upper * HALF
         first = pl.multiple_of((2 * block + c) * COLS, COLS)
         second = pl.multiple_of((2 * block + 1 - c) * COLS, COLS)
         xx = jnp.concatenate([mine, theirs], axis=1)
-        for w_ref, acc_ref in ((wg_ref, g_ref), (wu_ref, u_ref)):
+        for i, (w_ref, acc_ref) in enumerate(((wg_ref, g_ref), (wu_ref, u_ref))):
             w = jnp.concatenate([w_ref[pl.ds(first, COLS), :], w_ref[pl.ds(second, COLS), :]], axis=0)
             part = jnp.dot(xx, w, preferred_element_type=f32)
-            acc_ref[...] = part if fresh else acc_ref[...] + part
+            acc_ref[...] = part if before is None else before[i][...] + part
         a = mine.astype(f32) * (1.0 / gain_ref[:, pl.ds(first, COLS)])
         b = theirs.astype(f32) * (1.0 / gain_ref[:, pl.ds(second, COLS)])
         part = a * a + b * b
-        sq_ref[...] = part if fresh else sq_ref[...] + part
-        fresh = False
+        sq_ref[...] = part if before is None else before[2][...] + part
+        before = (g_ref, u_ref, sq_ref)
 
 
 def experts_near(at_ref, every_ref, n0_ref, n1_ref, swap_ref, near_ref, wg_ref, wu_ref, gain_ref, g_ref, u_ref, sq_ref):
     owns = (every_ref, n0_ref, n1_ref)
     others = (swap_ref, near_ref.at[0 : 2 * ROWS], near_ref.at[2 * ROWS :])
-    accumulate(at_ref[0], at_ref[1], NEAR, owns, others, wg_ref, wu_ref, gain_ref, g_ref, u_ref, sq_ref, True)
+    accumulate(at_ref[0], at_ref[1], NEAR, owns, others, wg_ref, wu_ref, gain_ref, g_ref, u_ref, sq_ref, None)
 
 
 def experts(at_ref, f0_ref, f1_ref, far_ref, g_in, u_in, sq_in, wg_ref, wu_ref, wd_ref, gain_ref, *refs):
@@ -243,10 +243,8 @@
     g_ref, u_ref, sq_ref, h_ref = refs[4:]
     y, c = at_ref[0], at_ref[1]
     others = (far_ref.at[0:ROWS], far_ref.at[ROWS:])
-    g_ref[...] = g_in[...]
-    u_ref[...] = u_in[...]
-    sq_ref[...] = sq_in[...]
-    accumulate(y, c, FAR, (f0_ref, f1_ref), others, wg_ref, wu_ref, gain_ref, g_ref, u_ref, sq_ref, False)
+    before = (g_in, u_in, sq_in)
+    accumulate(y, c, FAR, (f0_ref, f1_ref), others, wg_ref, wu_ref, gain_ref, g_ref, u_ref, sq_ref, before)
     scale = lax.rsqrt(jnp.sum(sq_ref[...], axis=1, keepdims=True) / D + EPS)
     gate = g_ref[...] * scale
     up = u_ref[...] * scale
@@ -271,7 +269,7 @@
         acc = acc + n0_ref[at, :].astype(f32) + n1_ref[at, :].astype(f32)
         rows_ref[...] = acc + far_ref[...].astype(f32)
         for i in range(NSP):
-            out_ref[2 * i + q] = jnp.concatenate([rows_ref[CAP * i : CAP * i + CAP, :], pad], axis=0).astype(bf)
+            out_ref[q * NSP + i] = jnp.concatenate([rows_ref[CAP * i : CAP * i + CAP, :], pad], axis=0).astype(bf)
 
 
 def route_back(slots_ref, back_ref):
@@ -279,7 +277,7 @@
     at = lax.broadcasted_iota(jnp.int32, (TOK, 2 * PADROWS), 1).astype(f32)
     for k in range(2):
         slot = slots[:, k : k + 1]
-        back_ref[k * TOK : (k + 1) * TOK, :] = jnp.where((at == slot) | (at == slot + SLOT), 1.0, 0.0).astype(bf)
+        back_ref[k * TOK : (k + 1) * TOK, :] = jnp.where((at == slot) | (at == slot + PADROWS), 1.0, 0.0).astype(bf)
 
 
 def finish(ret_ref, back_ref, rw_ref, stream_ref, out_ref):
@@ -408,7 +406,7 @@
         (near_mine, near_theirs, got[2], got[3], got[0], got[1]),
         scratch=(pltpu.VMEM((ROWS, COLS), f32),),
     )
-    returned = exchange(back, ("z", "x", "yh")).reshape(2 * PADROWS, COLS)
+    returned = exchange(back, ("yh", "z", "x")).reshape(2 * PADROWS, COLS)
     return call(finish, sds((TOK, COLS), bf), (returned, back_pick, route_weight.T, stream))
 
 

time: 188 us -> 187 us (level)
  the two profiles are of different devices: /device:TPU:8 before, /device:TPU:14 now
where the time goes in v12:
time: 187 us; the launch traced here: 186 us
  blocking collectives  72 us (39%)
  starting transfers between devices  63.9 us (34%)
  waiting for transfers between devices  36.1 us (19%)
  Pallas kernels  12.1 us (6%)
    all_to_all x3, blocking collectives, exchange(): return lax.all_to_all(v, axis, 0, 0, tiled=True)  54.9 us
    ppermute x8, starting transfers between devices, shift(): return lax.ppermute(v, Y, [(i, (i + by) % NY) for i in range(NY)])  27.7 us
    all_to_all x2, waiting for transfers between devices, exchange(): return lax.all_to_all(v, axis, 0, 0, tiled=True)  18.2 us
    all_gather x1, blocking collectives, layer(): attended = lax.all_gather(attended, TP, axis=0, tiled=True)  17 us
    all_to_all x2, starting transfers between devices, exchange(): return lax.all_to_all(v, axis, 0, 0, tiled=True)  16.4 us
    ppermute x8, waiting for transfers between devices, shift(): return lax.ppermute(v, Y, [(i, (i + by) % NY) for i in range(NY)])  15.5 us
    pallas_call x12, Pallas kernels, call(): pl.pallas_call(body, out_shape=out_shape, in_specs=specs, out_specs=tuple...  12.1 us
    ppermute x3, starting transfers between devices, layer(): lax.ppermute(sent[n], 'x', [(i, (i + n) % NX) for i in range(NX)])  9.22 us
  transfers between devices with their start and end apart: 18, of which 8 were waited for; matrix products, arithmetic and copies ran while one was open for 0% of the time, Pallas kernels for 3%

profile of v12, /device:TPU:14, one launch (start us, length us, event | category | flops | bytes accessed | tf_op | source)
XLA Modules:
  0.0 185.9 jit_solution(9724551570627603681)
XLA Ops:
  1.1 8.5 %all_to_all.25.q_ref = bf16[4,64,256]{2,1,0:T(8,128)(2,1)S(1)} all-to-all(bf16[4,64,256]{2,1,0:T(8,128)(2,1)S(1)} %get-tuple-element.37), channel_id=1, replica_groups=mesh['z'=8,'x'=4,'yh'=2,'yl'=4,'c'=2] {'x'}, dimensions={0} | all-to-all | bytes 262144 | tf_op jit(solution)/shard_map/all_to_all | solution.py:295
  9.5 26.3 %all_to_all.26.kv_ref = bf16[8,128,256]{2,1,0:T(8,128)(2,1)S(1)} all-to-all(bf16[8,128,256]{2,1,0:T(8,128)(2,1)S(1)} %get-tuple-element.39), channel_id=1, replica_groups=mesh['z'=8,'x'=4,'yh'=2,'yl'=4,'c'=2] {'z'}, dimensions={0} | all-to-all | bytes 1048576 | tf_op jit(solution)/shard_map/all_to_all | solution.py:295
  36.7 7.6 %all-to-all-start.2 = ((bf16[16,128,128]{2,1,0:T(8,128)(2,1)}), bf16[16,128,128]{2,1,0:T(8,128)(2,1)S(1)}, u32[]{:S(2)}, u32[]{:S(2)}) async-start(bf16[16,128,128]{2,1,0:T(8,128)(2,1)} %shard_map.121), calls=%async_computation.2 | async-start | bytes 1048576 | tf_op jit(solution)/shard_map/all_to_all | solution.py:295
  45.6 4.0 %collective-permute-start = (bf16[80,256]{1,0:T(8,128)(2,1)S(1)}, bf16[80,256]{1,0:T(8,128)(2,1)S(1)}, u32[]{:S(2)}, u32[]{:S(2)}) collective-permute-start(bf16[80,256]{1,0:T(8,128)(2,1)S(1)} %get-tuple-element.42), channel_id=1, source_target_pairs={{0,16},{16,32},{32,48},{48,0},{1,17},{17,33},{33,49},{49,1},{2,18}... | collective-permute-start | bytes 122888 | tf_op jit(solution)/shard_map/ppermute | solution.py:346
  49.6 2.1 %collective-permute-start.1 = (bf16[80,256]{1,0:T(8,128)(2,1)S(1)}, bf16[80,256]{1,0:T(8,128)(2,1)S(1)}, u32[]{:S(2)}, u32[]{:S(2)}) collective-permute-start(bf16[80,256]{1,0:T(8,128)(2,1)S(1)} %get-tuple-element.43), channel_id=1, source_target_pairs={{0,32},{16,48},{32,0},{48,16},{1,33},{17,49},{33,1},{49,17},{2,34}... | collective-permute-start | bytes 122888 | tf_op jit(solution)/shard_map/ppermute | solution.py:346
  51.8 3.1 %collective-permute-start.2 = (bf16[80,256]{1,0:T(8,128)(2,1)S(1)}, bf16[80,256]{1,0:T(8,128)(2,1)S(1)}, u32[]{:S(2)}, u32[]{:S(2)}) collective-permute-start(bf16[80,256]{1,0:T(8,128)(2,1)S(1)} %get-tuple-element.44), channel_id=1, source_target_pairs={{0,48},{16,0},{32,16},{48,32},{1,49},{17,1},{33,17},{49,33},{2,50}... | collective-permute-start | bytes 122888 | tf_op jit(solution)/shard_map/ppermute | solution.py:346
  54.9 1.8 shard_map.122
  57.0 1.8 collective-permute-done.2.refs_3_
  58.9 17.0 %all_gather.3.att_ref = bf16[1024,256]{1,0:T(8,128)(2,1)S(1)} all-gather(bf16[64,256]{1,0:T(8,128)(2,1)S(1)} %shard_map.120), channel_id=1, replica_groups=mesh['z'=8,'x'=4,'yh'=2,'yl'=4,'c'=2] {'yh','yl','c'}, dimensions={0}, use_global_device_ids=true | all-gather | bytes 557056 | tf_op jit(solution)/shard_map/all_gather | solution.py:354
  75.9 1.4 shard_map.123
  77.4 20.2 %all_to_all.27.in_ref = bf16[32,40,128]{2,1,0:T(8,128)(2,1)S(1)} all-to-all(bf16[32,40,128]{2,1,0:T(8,128)(2,1)S(1)} %get-tuple-element.48), channel_id=1, replica_groups=mesh['z'=8,'x'=4,'yh'=2,'yl'=4,'c'=2] {'z','x'}, dimensions={0} | all-to-all | bytes 655360 | tf_op jit(solution)/shard_map/all_to_all | solution.py:295
  97.6 3.8 %collective-permute-start.7 = (bf16[1280,128]{1,0:T(8,128)(2,1)S(1)}, bf16[1280,128]{1,0:T(8,128)(2,1)S(1)}, u32[]{:S(2)}, u32[]{:S(2)}) collective-permute-start(bf16[1280,128]{1,0:T(8,128)(2,1)S(1)} %get-tuple-element.51.every_ref), channel_id=1, source_target_pairs={{0,14},{2,0},{4,2},{6,4},{8,6},{10,8},{12,10},{14,12},{1,15},{3,1}... | collective-permute-start | bytes 983048 | tf_op jit(solution)/shard_map/ppermute | solution.py:291
  101.5 2.2 %collective-permute-start.6 = (bf16[1280,128]{1,0:T(8,128)(2,1)S(1)}, bf16[1280,128]{1,0:T(8,128)(2,1)S(1)}, u32[]{:S(2)}, u32[]{:S(2)}) collective-permute-start(bf16[1280,128]{1,0:T(8,128)(2,1)S(1)} %get-tuple-element.51.every_ref), channel_id=1, source_target_pairs={{0,2},{2,4},{4,6},{6,8},{8,10},{10,12},{12,14},{14,0},{1,3},{3,5},... | collective-permute-start | bytes 983048 | tf_op jit(solution)/shard_map/ppermute | solution.py:291
  103.6 5.5 %collective-permute-start.3 = (bf16[640,128]{1,0:T(8,128)(2,1)S(1)}, bf16[640,128]{1,0:T(8,128)(2,1)S(1)}, u32[]{:S(2)}, u32[]{:S(2)}) collective-permute-start(bf16[640,128]{1,0:T(8,128)(2,1)S(1)} %get-tuple-element.49), channel_id=1, source_target_pairs={{0,4},{2,6},{4,8},{6,10},{8,12},{10,14},{12,0},{14,2},{1,5},{3,7},... | collective-permute-start | bytes 491528 | tf_op jit(solution)/shard_map/ppermute | solution.py:291
  109.1 2.5 %collective-permute-start.4 = (bf16[640,128]{1,0:T(8,128)(2,1)S(1)}, bf16[640,128]{1,0:T(8,128)(2,1)S(1)}, u32[]{:S(2)}, u32[]{:S(2)}) collective-permute-start(bf16[640,128]{1,0:T(8,128)(2,1)S(1)} %get-tuple-element.50), channel_id=1, source_target_pairs={{0,12},{2,14},{4,0},{6,2},{8,4},{10,6},{12,8},{14,10},{1,13},{3,15... | collective-permute-start | bytes 491528 | tf_op jit(solution)/shard_map/ppermute | solution.py:291
  111.6 2.6 %collective-permute-done.6.n0_ref = bf16[1280,128]{1,0:T(8,128)(2,1)S(1)} collective-permute-done((bf16[1280,128]{1,0:T(8,128)(2,1)S(1)}, bf16[1280,128]{1,0:T(8,128)(2,1)S(1)}, u32[]{:S(2)}, u32[]{:S(2)}) %collective-permute-start.6) | collective-permute-done | bytes 327712 | tf_op jit(solution)/shard_map/ppermute | solution.py:291
  114.3 1.9 %collective-permute-start.9 = (bf16[2560,128]{1,0:T(8,128)(2,1)S(1)}, bf16[2560,128]{1,0:T(8,128)(2,1)S(1)}, u32[]{:S(2)}, u32[]{:S(2)}) collective-permute-start(bf16[2560,128]{1,0:T(8,128)(2,1)S(1)} %pad_maximum_fusion), channel_id=1, source_target_pairs={{0,1},{1,0},{2,3},{3,2},{4,5},{5,4},{6,7},{7,6},{8,9},{9,8},{10,11... | collective-permute-start | bytes 1966088 | tf_op jit(solution)/shard_map/ppermute | solution.py:374
  116.2 2.4 %collective-permute-start.8 = (bf16[1280,128]{1,0:T(8,128)(2,1)S(1)}, bf16[1280,128]{1,0:T(8,128)(2,1)S(1)}, u32[]{:S(2)}, u32[]{:S(2)}) collective-permute-start(bf16[1280,128]{1,0:T(8,128)(2,1)S(1)} %get-tuple-element.51.every_ref), channel_id=1, source_target_pairs={{0,1},{1,0},{2,3},{3,2},{4,5},{5,4},{6,7},{7,6},{8,9},{9,8},{10,11... | collective-permute-start | bytes 983048 | tf_op jit(solution)/shard_map/ppermute | solution.py:374
  118.6 1.6 collective-permute-done.3.f0_ref
  120.3 1.9 %collective-permute-start.5 = (bf16[1280,128]{1,0:T(8,128)(2,1)S(1)}, bf16[1280,128]{1,0:T(8,128)(2,1)S(1)}, u32[]{:S(2)}, u32[]{:S(2)}) collective-permute-start(bf16[1280,128]{1,0:T(8,128)(2,1)S(1)} %pad_maximum_fusion.1), channel_id=1, source_target_pairs={{0,1},{1,0},{2,3},{3,2},{4,5},{5,4},{6,7},{7,6},{8,9},{9,8},{10,11... | collective-permute-start | bytes 983048 | tf_op jit(solution)/shard_map/ppermute | solution.py:374
  122.3 1.7 shard_map.125
  124.1 1.9 %shard_map.126 = (bf16[1280,128]{1,0:T(8,128)(2,1)S(1)}, bf16[3840,128]{1,0:T(8,128)(2,1)S(1)}, bf16[1280,128]{1,0:T(8,128)(2,1)S(1)}, bf16[3840,128]{1,0:T(8,128)(2,1)S(1)}) custom-call(s32[2]{0:T(128)S(1)} %pad_add_fusion.at_ref, bf16[640,128]{1,0:T(8,128)(2,1)S(1)} %collective-permute-done.3.f0_ref, bf16[640,128]{1,0:T(8,128)(2,1)S(1)} %collective-permute-done.4.f1_ref, ...), custom_call_target="tpu_custom_call" | custom-call | tf_op jit(solution)/shard_map/pallas_call | solution.py:38
  126.0 2.4 %collective-permute-start.10 = (bf16[3840,128]{1,0:T(8,128)(2,1)S(1)}, bf16[3840,128]{1,0:T(8,128)(2,1)S(1)}, u32[]{:S(2)}, u32[]{:S(2)}) collective-permute-start(bf16[3840,128]{1,0:T(8,128)(2,1)S(1)} %get-tuple-element.56), channel_id=1, source_target_pairs={{0,1},{1,0},{2,3},{3,2},{4,5},{5,4},{6,7},{7,6},{8,9},{9,8},{10,11... | collective-permute-start | bytes 2949128 | tf_op jit(solution)/shard_map/ppermute | solution.py:388
  128.4 1.9 %collective-permute-start.13 = (bf16[1280,128]{1,0:T(8,128)(2,1)S(1)}, bf16[1280,128]{1,0:T(8,128)(2,1)S(1)}, u32[]{:S(2)}, u32[]{:S(2)}) collective-permute-start(bf16[1280,128]{1,0:T(8,128)(2,1)S(1)} %get-tuple-element.58), channel_id=1, source_target_pairs={{0,1},{1,0},{2,3},{3,2},{4,5},{5,4},{6,7},{7,6},{8,9},{9,8},{10,11... | collective-permute-start | bytes 983048 | tf_op jit(solution)/shard_map/ppermute | solution.py:387
  130.8 5.1 %collective-permute-start.12 = (bf16[1280,128]{1,0:T(8,128)(2,1)S(1)}, bf16[1280,128]{1,0:T(8,128)(2,1)S(1)}, u32[]{:S(2)}, u32[]{:S(2)}) collective-permute-start(bf16[1280,128]{1,0:T(8,128)(2,1)S(1)} %get-tuple-element.61), channel_id=1, source_target_pairs={{0,14},{2,0},{4,2},{6,4},{8,6},{10,8},{12,10},{14,12},{1,15},{3,1}... | collective-permute-start | bytes 983048 | tf_op jit(solution)/shard_map/ppermute | solution.py:291
  135.9 1.9 %collective-permute-start.11 = (bf16[1280,128]{1,0:T(8,128)(2,1)S(1)}, bf16[1280,128]{1,0:T(8,128)(2,1)S(1)}, u32[]{:S(2)}, u32[]{:S(2)}) collective-permute-start(bf16[1280,128]{1,0:T(8,128)(2,1)S(1)} %get-tuple-element.62), channel_id=1, source_target_pairs={{0,2},{2,4},{4,6},{6,8},{8,10},{10,12},{12,14},{14,0},{1,3},{3,5},... | collective-permute-start | bytes 983048 | tf_op jit(solution)/shard_map/ppermute | solution.py:291
  138.0 4.6 %collective-permute-start.15 = (bf16[640,128]{1,0:T(8,128)(2,1)S(1)}, bf16[640,128]{1,0:T(8,128)(2,1)S(1)}, u32[]{:S(2)}, u32[]{:S(2)}) collective-permute-start(bf16[640,128]{1,0:T(8,128)(2,1)S(1)} %get-tuple-element.63), channel_id=1, source_target_pairs={{0,12},{2,14},{4,0},{6,2},{8,4},{10,6},{12,8},{14,10},{1,13},{3,15... | collective-permute-start | bytes 491528 | tf_op jit(solution)/shard_map/ppermute | solution.py:291
  142.5 2.2 %collective-permute-start.14 = (bf16[640,128]{1,0:T(8,128)(2,1)S(1)}, bf16[640,128]{1,0:T(8,128)(2,1)S(1)}, u32[]{:S(2)}, u32[]{:S(2)}) collective-permute-start(bf16[640,128]{1,0:T(8,128)(2,1)S(1)} %get-tuple-element.64), channel_id=1, source_target_pairs={{0,4},{2,6},{4,8},{6,10},{8,12},{10,14},{12,0},{14,2},{1,5},{3,7},... | collective-permute-start | bytes 491528 | tf_op jit(solution)/shard_map/ppermute | solution.py:291
  144.7 5.7 %collective-permute-done.15.f1_ref = bf16[640,128]{1,0:T(8,128)(2,1)S(1)} collective-permute-done((bf16[640,128]{1,0:T(8,128)(2,1)S(1)}, bf16[640,128]{1,0:T(8,128)(2,1)S(1)}, u32[]{:S(2)}, u32[]{:S(2)}) %collective-permute-start.15) | collective-permute-done | bytes 163872 | tf_op jit(solution)/shard_map/ppermute | solution.py:291
  150.4 5.5 %collective-permute-done.14.f0_ref = bf16[640,128]{1,0:T(8,128)(2,1)S(1)} collective-permute-done((bf16[640,128]{1,0:T(8,128)(2,1)S(1)}, bf16[640,128]{1,0:T(8,128)(2,1)S(1)}, u32[]{:S(2)}, u32[]{:S(2)}) %collective-permute-start.14) | collective-permute-done | bytes 163872 | tf_op jit(solution)/shard_map/ppermute | solution.py:291
  157.0 8.8 %all-to-all-start.4 = ((bf16[64,24,128]{2,1,0:T(8,128)(2,1)}), bf16[64,24,128]{2,1,0:T(8,128)(2,1)S(1)}, u32[]{:S(2)}, u32[]{:S(2)}) async-start(bf16[64,24,128]{2,1,0:T(8,128)(2,1)} %shard_map.127), calls=%async_computation.4 | async-start | bytes 786432 | tf_op jit(solution)/shard_map/all_to_all | solution.py:295
  166.5 18.2 %all-to-all-done.4 = bf16[64,24,128]{2,1,0:T(8,128)(2,1)S(1)} async-done(((bf16[64,24,128]{2,1,0:T(8,128)(2,1)}), bf16[64,24,128]{2,1,0:T(8,128)(2,1)S(1)}, u32[]{:S(2)}, u32[]{:S(2)}) %all-to-all-start.4) | async-done | bytes 393248 | tf_op jit(solution)/shard_map/all_to_all | solution.py:295
  (46 shorter events, 7.3 us)
Async XLA Ops:
  0.0 35.8 %copy-start.4 = (bf16[64,2048]{1,0:T(8,128)(2,1)S(1)}, bf16[64,2048]{1,0:T(8,128)(2,1)}, u32[]{:S(2)}) copy-start(bf16[64,2048]{1,0:T(8,128)(2,1)} %w_ref) | copy-start | bytes 786436
  9.5 34.7 %copy-start.6 = (f32[1,8192]{1,0:T(1,128)S(1)}, f32[1,8192]{1,0:T(1,128)}, u32[]{:S(2)}) copy-start(f32[1,8192]{1,0:T(1,128)} %gate_ref.1) | copy-start | bytes 98308
  35.8 19.0 %copy-start.2 = (bf16[256,2048]{1,0:T(8,128)(2,1)S(1)}, bf16[256,2048]{1,0:T(8,128)(2,1)}, u32[]{:S(2)}) copy-start(bf16[256,2048]{1,0:T(8,128)(2,1)} %resid_ref.1) | copy-start | bytes 3145732
  35.8 19.1 %copy-start.7 = (s32[256,2]{0,1:T(2,128)S(1)}, s32[256,2]{0,1:T(2,128)}, u32[]{:S(2)}) copy-start(s32[256,2]{0,1:T(2,128)} %param.19) | copy-start | bytes 6148
  36.7 39.2 %all-to-all-start.2 = ((bf16[16,128,128]{2,1,0:T(8,128)(2,1)}), bf16[16,128,128]{2,1,0:T(8,128)(2,1)S(1)}, u32[]{:S(2)}, u32[]{:S(2)}) async-start(bf16[16,128,128]{2,1,0:T(8,128)(2,1)} %shard_map.121), calls=%async_computation.2 | async-start | bytes 1048576 | tf_op jit(solution)/shard_map/all_to_all | solution.py:295
  44.3 31.7 %copy-start.5 = (f32[2048]{0:T(1024)S(1)}, f32[2048]{0:T(1024)}, u32[]{:S(2)}) copy-start(f32[2048]{0:T(1024)} %param.18) | copy-start | bytes 24580
  45.6 11.0 %collective-permute-start = (bf16[80,256]{1,0:T(8,128)(2,1)S(1)}, bf16[80,256]{1,0:T(8,128)(2,1)S(1)}, u32[]{:S(2)}, u32[]{:S(2)}) collective-permute-start(bf16[80,256]{1,0:T(8,128)(2,1)S(1)} %get-tuple-element.42), channel_id=1, source_target_pairs={{0,16},{16,32},{32,48},{48,0},{1,17},{17,33},{33,49},{49,1},{2,18}... | collective-permute-start | bytes 122888 | tf_op jit(solution)/shard_map/ppermute | solution.py:346
  49.6 7.4 %collective-permute-start.1 = (bf16[80,256]{1,0:T(8,128)(2,1)S(1)}, bf16[80,256]{1,0:T(8,128)(2,1)S(1)}, u32[]{:S(2)}, u32[]{:S(2)}) collective-permute-start(bf16[80,256]{1,0:T(8,128)(2,1)S(1)} %get-tuple-element.43), channel_id=1, source_target_pairs={{0,32},{16,48},{32,0},{48,16},{1,33},{17,49},{33,1},{49,17},{2,34}... | collective-permute-start | bytes 122888 | tf_op jit(solution)/shard_map/ppermute | solution.py:346
  51.8 7.1 %collective-permute-start.2 = (bf16[80,256]{1,0:T(8,128)(2,1)S(1)}, bf16[80,256]{1,0:T(8,128)(2,1)S(1)}, u32[]{:S(2)}, u32[]{:S(2)}) collective-permute-start(bf16[80,256]{1,0:T(8,128)(2,1)S(1)} %get-tuple-element.44), channel_id=1, source_target_pairs={{0,48},{16,0},{32,16},{48,32},{1,49},{17,1},{33,17},{49,33},{2,50}... | collective-permute-start | bytes 122888 | tf_op jit(solution)/shard_map/ppermute | solution.py:346
  97.5 24.8 %copy-start = (bf16[1,2048,256]{2,1,0:T(8,128)(2,1)S(1)}, bf16[1,2048,256]{2,1,0:T(8,128)(2,1)}, u32[]{:S(2)}) copy-start(bf16[1,2048,256]{2,1,0:T(8,128)(2,1)} %param.21) | copy-start | bytes 3145732
  97.5 24.8 %copy-start.1 = (bf16[1,2048,256]{2,1,0:T(8,128)(2,1)S(1)}, bf16[1,2048,256]{2,1,0:T(8,128)(2,1)}, u32[]{:S(2)}) copy-start(bf16[1,2048,256]{2,1,0:T(8,128)(2,1)} %param.22) | copy-start | bytes 3145732
  97.6 14.0 %collective-permute-start.7 = (bf16[1280,128]{1,0:T(8,128)(2,1)S(1)}, bf16[1280,128]{1,0:T(8,128)(2,1)S(1)}, u32[]{:S(2)}, u32[]{:S(2)}) collective-permute-start(bf16[1280,128]{1,0:T(8,128)(2,1)S(1)} %get-tuple-element.51.every_ref), channel_id=1, source_target_pairs={{0,14},{2,0},{4,2},{6,4},{8,6},{10,8},{12,10},{14,12},{1,15},{3,1}... | collective-permute-start | bytes 983048 | tf_op jit(solution)/shard_map/ppermute | solution.py:291
  101.5 12.8 %collective-permute-start.6 = (bf16[1280,128]{1,0:T(8,128)(2,1)S(1)}, bf16[1280,128]{1,0:T(8,128)(2,1)S(1)}, u32[]{:S(2)}, u32[]{:S(2)}) collective-permute-start(bf16[1280,128]{1,0:T(8,128)(2,1)S(1)} %get-tuple-element.51.every_ref), channel_id=1, source_target_pairs={{0,2},{2,4},{4,6},{6,8},{8,10},{10,12},{12,14},{14,0},{1,3},{3,5},... | collective-permute-start | bytes 983048 | tf_op jit(solution)/shard_map/ppermute | solution.py:291
  103.6 16.6 %collective-permute-start.3 = (bf16[640,128]{1,0:T(8,128)(2,1)S(1)}, bf16[640,128]{1,0:T(8,128)(2,1)S(1)}, u32[]{:S(2)}, u32[]{:S(2)}) collective-permute-start(bf16[640,128]{1,0:T(8,128)(2,1)S(1)} %get-tuple-element.49), channel_id=1, source_target_pairs={{0,4},{2,6},{4,8},{6,10},{8,12},{10,14},{12,0},{14,2},{1,5},{3,7},... | collective-permute-start | bytes 491528 | tf_op jit(solution)/shard_map/ppermute | solution.py:291
  109.1 11.1 %collective-permute-start.4 = (bf16[640,128]{1,0:T(8,128)(2,1)S(1)}, bf16[640,128]{1,0:T(8,128)(2,1)S(1)}, u32[]{:S(2)}, u32[]{:S(2)}) collective-permute-start(bf16[640,128]{1,0:T(8,128)(2,1)S(1)} %get-tuple-element.50), channel_id=1, source_target_pairs={{0,12},{2,14},{4,0},{6,2},{8,4},{10,6},{12,8},{14,10},{1,13},{3,15... | collective-permute-start | bytes 491528 | tf_op jit(solution)/shard_map/ppermute | solution.py:291
  114.3 8.0 %collective-permute-start.9 = (bf16[2560,128]{1,0:T(8,128)(2,1)S(1)}, bf16[2560,128]{1,0:T(8,128)(2,1)S(1)}, u32[]{:S(2)}, u32[]{:S(2)}) collective-permute-start(bf16[2560,128]{1,0:T(8,128)(2,1)S(1)} %pad_maximum_fusion), channel_id=1, source_target_pairs={{0,1},{1,0},{2,3},{3,2},{4,5},{5,4},{6,7},{7,6},{8,9},{9,8},{10,11... | collective-permute-start | bytes 1966088 | tf_op jit(solution)/shard_map/ppermute | solution.py:374
  116.2 6.1 %collective-permute-start.8 = (bf16[1280,128]{1,0:T(8,128)(2,1)S(1)}, bf16[1280,128]{1,0:T(8,128)(2,1)S(1)}, u32[]{:S(2)}, u32[]{:S(2)}) collective-permute-start(bf16[1280,128]{1,0:T(8,128)(2,1)S(1)} %get-tuple-element.51.every_ref), channel_id=1, source_target_pairs={{0,1},{1,0},{2,3},{3,2},{4,5},{5,4},{6,7},{7,6},{8,9},{9,8},{10,11... | collective-permute-start | bytes 983048 | tf_op jit(solution)/shard_map/ppermute | solution.py:374
  120.3 3.8 %collective-permute-start.5 = (bf16[1280,128]{1,0:T(8,128)(2,1)S(1)}, bf16[1280,128]{1,0:T(8,128)(2,1)S(1)}, u32[]{:S(2)}, u32[]{:S(2)}) collective-permute-start(bf16[1280,128]{1,0:T(8,128)(2,1)S(1)} %pad_maximum_fusion.1), channel_id=1, source_target_pairs={{0,1},{1,0},{2,3},{3,2},{4,5},{5,4},{6,7},{7,6},{8,9},{9,8},{10,11... | collective-permute-start | bytes 983048 | tf_op jit(solution)/shard_map/ppermute | solution.py:374
  122.3 1.8 copy-start.3
  126.0 4.6 %collective-permute-start.10 = (bf16[3840,128]{1,0:T(8,128)(2,1)S(1)}, bf16[3840,128]{1,0:T(8,128)(2,1)S(1)}, u32[]{:S(2)}, u32[]{:S(2)}) collective-permute-start(bf16[3840,128]{1,0:T(8,128)(2,1)S(1)} %get-tuple-element.56), channel_id=1, source_target_pairs={{0,1},{1,0},{2,3},{3,2},{4,5},{5,4},{6,7},{7,6},{8,9},{9,8},{10,11... | collective-permute-start | bytes 2949128 | tf_op jit(solution)/shard_map/ppermute | solution.py:388
  128.4 9.4 %collective-permute-start.13 = (bf16[1280,128]{1,0:T(8,128)(2,1)S(1)}, bf16[1280,128]{1,0:T(8,128)(2,1)S(1)}, u32[]{:S(2)}, u32[]{:S(2)}) collective-permute-start(bf16[1280,128]{1,0:T(8,128)(2,1)S(1)} %get-tuple-element.58), channel_id=1, source_target_pairs={{0,1},{1,0},{2,3},{3,2},{4,5},{5,4},{6,7},{7,6},{8,9},{9,8},{10,11... | collective-permute-start | bytes 983048 | tf_op jit(solution)/shard_map/ppermute | solution.py:387
  130.8 25.2 %collective-permute-start.12 = (bf16[1280,128]{1,0:T(8,128)(2,1)S(1)}, bf16[1280,128]{1,0:T(8,128)(2,1)S(1)}, u32[]{:S(2)}, u32[]{:S(2)}) collective-permute-start(bf16[1280,128]{1,0:T(8,128)(2,1)S(1)} %get-tuple-element.61), channel_id=1, source_target_pairs={{0,14},{2,0},{4,2},{6,4},{8,6},{10,8},{12,10},{14,12},{1,15},{3,1}... | collective-permute-start | bytes 983048 | tf_op jit(solution)/shard_map/ppermute | solution.py:291
  135.9 20.0 %collective-permute-start.11 = (bf16[1280,128]{1,0:T(8,128)(2,1)S(1)}, bf16[1280,128]{1,0:T(8,128)(2,1)S(1)}, u32[]{:S(2)}, u32[]{:S(2)}) collective-permute-start(bf16[1280,128]{1,0:T(8,128)(2,1)S(1)} %get-tuple-element.62), channel_id=1, source_target_pairs={{0,2},{2,4},{4,6},{6,8},{8,10},{10,12},{12,14},{14,0},{1,3},{3,5},... | collective-permute-start | bytes 983048 | tf_op jit(solution)/shard_map/ppermute | solution.py:291
  138.0 12.5 %collective-permute-start.15 = (bf16[640,128]{1,0:T(8,128)(2,1)S(1)}, bf16[640,128]{1,0:T(8,128)(2,1)S(1)}, u32[]{:S(2)}, u32[]{:S(2)}) collective-permute-start(bf16[640,128]{1,0:T(8,128)(2,1)S(1)} %get-tuple-element.63), channel_id=1, source_target_pairs={{0,12},{2,14},{4,0},{6,2},{8,4},{10,6},{12,8},{14,10},{1,13},{3,15... | collective-permute-start | bytes 491528 | tf_op jit(solution)/shard_map/ppermute | solution.py:291
  142.5 13.4 %collective-permute-start.14 = (bf16[640,128]{1,0:T(8,128)(2,1)S(1)}, bf16[640,128]{1,0:T(8,128)(2,1)S(1)}, u32[]{:S(2)}, u32[]{:S(2)}) collective-permute-start(bf16[640,128]{1,0:T(8,128)(2,1)S(1)} %get-tuple-element.64), channel_id=1, source_target_pairs={{0,4},{2,6},{4,8},{6,10},{8,12},{10,14},{12,0},{14,2},{1,5},{3,7},... | collective-permute-start | bytes 491528 | tf_op jit(solution)/shard_map/ppermute | solution.py:291
  157.0 27.6 %copy-start.8 = (f32[256,2]{0,1:T(2,128)S(1)}, f32[256,2]{0,1:T(2,128)}, u32[]{:S(2)}) copy-start(f32[256,2]{0,1:T(2,128)} %param.20) | copy-start | bytes 6148
  157.0 27.6 %all-to-all-start.4 = ((bf16[64,24,128]{2,1,0:T(8,128)(2,1)}), bf16[64,24,128]{2,1,0:T(8,128)(2,1)S(1)}, u32[]{:S(2)}, u32[]{:S(2)}) async-start(bf16[64,24,128]{2,1,0:T(8,128)(2,1)} %shard_map.127), calls=%async_computation.4 | async-start | bytes 786432 | tf_op jit(solution)/shard_map/all_to_all | solution.py:295
